TPU v7x, 128 devices: a whole 4x4x4 slice. The times are simulated.
128 devices in a mesh: kv: 32 (over z, y, core), tp: 4 (over x).
Axes of the slice: x: 4, y: 4, z: 4, core: 2. Of those that a mesh axis runs over, the one named last changes fastest.
Arguments:
- tokens: bfloat16 [128, 4, 4096], P(None, None, ('kv', 'tp')), may hold values from -6 to 6
- input_norm_gain: float32 [4096], replicated, may hold values from 0.1 to 1.9
- w_query: bfloat16 [4096, 4096], P(None, 'kv'), may hold values from -0.09375 to 0.09375
- w_forget: bfloat16 [4096, 4096], P(None, 'kv'), may hold values from -0.09375 to 0.09375
- w_input: bfloat16 [32, 128, 4096], P('kv', 'tp'), may hold values from -0.09375 to 0.09375
- w_gate: bfloat16 [32, 128, 4096], P('kv', 'tp'), may hold values from -0.09375 to 0.09375
- forget_floor: float32 [4096], P('kv'), may hold values from 0 to 0.95
- head_gain: float32 [128], P('tp'), may hold values from 0.1 to 1.9
- w_out: bfloat16 [4096, 4096], P('kv'), may hold values from -0.09375 to 0.09375
- state: float32 [128, 32, 128, 128], P(None, 'kv', 'tp'), may hold values from -12 to 12
- prev_forget: float32 [128, 4, 4096], P(None, None, 'kv'), may hold values from 0.2 to 1
- prev_input: bfloat16 [128, 4, 32, 128], P(None, None, 'kv', 'tp'), may hold values from -6 to 6
- accepted: int32 [128], replicated, may hold values from 0 to 4
Outputs:
- mixed: bfloat16 [128, 4, 4096], P(None, None, ('kv', 'tp'))
- new_state: float32 [128, 32, 128, 128], P(None, 'kv', 'tp')
All inputs are finite; a program needn't handle non-finite values.
Results may differ from a plain program's by a relative error of at most 0.019.
Values may be sent and summed in bfloat16 or wider, within the bound.
No kernel may reach another device: no remote copies, remote signals or barrier semaphores. Data moves between devices by JAX's collectives and lax.ppermute only.
A program may use at most 64 MiB of HBM per device.

v0:
```python
import functools

import jax
import jax.numpy as jnp
from jax import lax
from jax.experimental import pallas as pl
from jax.experimental.pallas import tpu as pltpu
from jax.sharding import Mesh, PartitionSpec as P


NORM_EPSILON = 1e-06


def whole():
    return pl.BlockSpec(memory_space=pltpu.VMEM)


def shaped(shape, dtype):
    return jax.ShapeDtypeStruct(shape, dtype)


def call(kernel, out_shape, scratch, cost, limit, in_specs, out_specs):
    return pl.pallas_call(
        kernel,
        out_shape=out_shape,
        in_specs=in_specs,
        out_specs=out_specs,
        scratch_shapes=scratch,
        cost_estimate=pl.CostEstimate(flops=cost[0], bytes_accessed=cost[1], transcendentals=0),
        compiler_params=pltpu.CompilerParams(vmem_limit_bytes=limit),
    )


def advance_kernel(accepted, prev_forget, prev_input, state, new_state, rounded, live):
    block = pl.program_id(0)
    count, proposals, size = prev_forget.shape
    lanes = prev_input.shape[2]

    @pl.when(block == 0)
    def _():
        live[...] = jnp.broadcast_to(accepted[...].astype(jnp.float32), (size, lanes)).T

    shift = lax.rem(lanes - block * count, lanes)
    values = [
        pltpu.roll(prev_input[p].astype(jnp.float32), shift, 1) for p in range(proposals)
    ]
    taken = live[pl.ds(pl.multiple_of(block * count, count), count), :]
    rest = jnp.ones((count, size), jnp.float32)
    terms = [None] * proposals
    for p in reversed(range(proposals)):
        gate = jnp.where(taken > p, prev_forget[:, p, :], 1.0)
        terms[p] = rest * (1.0 - gate)
        rest = rest * gate
    for s in range(count):
        fresh = rest[s : s + 1] * state[s]
        for p in range(proposals):
            fresh = fresh + terms[p][s : s + 1] * values[p][:, s : s + 1]
        new_state[s] = fresh
        rounded[s] = fresh.astype(jnp.bfloat16)


def advance(accepted, prev_forget, prev_input, state):
    seqs, values, keys = state.shape
    proposals = prev_forget.shape[1]
    count = 32
    span = pl.BlockSpec((count, values, keys), lambda i: (i, 0, 0))
    return pl.pallas_call(
        advance_kernel,
        grid=(seqs // count,),
        in_specs=[
            pl.BlockSpec((1, seqs), lambda i: (0, 0)),
            pl.BlockSpec((count, proposals, keys), lambda i: (i, 0, 0)),
            pl.BlockSpec((proposals, values, seqs), lambda i: (0, 0, 0)),
            span,
        ],
        out_specs=[span, span],
        out_shape=[shaped(state.shape, jnp.float32), shaped(state.shape, jnp.bfloat16)],
        scratch_shapes=[pltpu.VMEM((keys, seqs), jnp.float32)],
        name="advance",
        cost_estimate=pl.CostEstimate(
            flops=1_000_000_000, bytes_accessed=5 << 20, transcendentals=0
        ),
        compiler_params=pltpu.CompilerParams(vmem_limit_bytes=60 << 20),
    )(accepted[None], prev_forget, prev_input, state)


def split_in_three(value):
    high = value.astype(jnp.bfloat16).astype(jnp.float32)
    middle = (value - high).astype(jnp.bfloat16).astype(jnp.float32)
    return high, middle, value - high - middle


def three_rows(parts, width):
    rest = jnp.zeros((16 - 3 * parts[0].shape[0], width), jnp.float32)
    return jnp.concatenate([*parts, rest], axis=0).astype(jnp.bfloat16)


def source_kernel(tokens, gain, out, columns):
    steps, features, seqs = tokens.shape
    size = gain.shape[1]
    row = 2 * lax.axis_index("zy") + lax.axis_index("core")
    columns[...] = jnp.broadcast_to(gain[pl.ds(row, 1), :], (size, size)).T
    at = pl.multiple_of(lax.axis_index("tp") * features, features)
    scale = columns[pl.ds(at, features), :]
    squares = []
    for t in range(steps):
        wide = tokens[t].astype(jnp.float32)
        squares.append(jnp.sum(wide * wide, axis=0, keepdims=True))
        scaled = (wide * scale).astype(jnp.bfloat16)
        for z in range(out.shape[0]):
            out[z, pl.ds(t * features, features), :] = scaled
    tail = three_rows(split_in_three(jnp.concatenate(squares, axis=0)), seqs)
    for z in range(out.shape[0]):
        out[z, pl.ds(steps * features, 16), :] = tail


def source(tokens, gain, planes):
    steps, features, seqs = tokens.shape
    size = gain.shape[1]
    return call(
        source_kernel,
        shaped((planes, steps * features + 16, seqs), jnp.bfloat16),
        [pltpu.VMEM((size, seqs), jnp.float32)],
        (1_000_000, 1 << 20),
        60 << 20,
        [whole()] * 2,
        whole(),
    )(tokens, gain)


def turn_kernel(w_query, w_forget, w_input, w_gate, keyed, m0, m1, m2, m3, rows, mixed, sems):
    mine = lax.axis_index("tp")
    group, part, size = 4, rows.shape[2], w_query.shape[2]
    at = pl.multiple_of(mine * part, part)
    copies = [
        pltpu.make_async_copy(w_input.at[0], mixed.at[0], sems.at[0]),
        pltpu.make_async_copy(w_gate.at[0], mixed.at[1], sems.at[1]),
        pltpu.make_async_copy(w_query.at[:, pl.ds(at, part), :], rows.at[0], sems.at[2]),
        pltpu.make_async_copy(w_forget.at[:, pl.ds(at, part), :], rows.at[1], sems.at[3]),
    ]
    for copy in copies:
        copy.start()
    copies[0].wait()
    copies[1].wait()
    lane = lax.broadcasted_iota(jnp.int32, (2 * part, size), 1) // part
    for q in range(rows.shape[1] // group):
        to = pl.ds(q * size, size)
        blocks = []
        for k in range(group):
            cut = pl.ds((q * group + k) * size, size)
            both = [mixed[i, :, cut].astype(jnp.float32) for i in range(2)]
            blocks.append(jnp.concatenate(both, axis=0))
        for d, out in enumerate((m0, m1, m2, m3)):
            theirs = (mine ^ d)
            total = None
            for k in range(group):
                turned = pltpu.roll(blocks[k], lax.rem(group + k - theirs, group) * part, 1)
                total = turned if total is None else jnp.where(lane == k, turned, total)
            out[:, to] = total.astype(jnp.bfloat16)
    copies[2].wait()
    copies[3].wait()
    for q in range(rows.shape[1] // group):
        for i in range(2):
            block = rows[i, pl.ds(q * group, group)].astype(jnp.float32).reshape(size, size)
            keyed[pl.ds(i * size, size), pl.ds(q * size, size)] = block.T.astype(jnp.bfloat16)


def turn(w_query, w_forget, w_input, w_gate):
    width, size = w_query.shape
    values = w_input.shape[1]
    far = pl.BlockSpec(memory_space=pltpu.HBM)
    outs = call(
        turn_kernel,
        [shaped((2 * size, width // 4), jnp.bfloat16)]
        + [shaped((2 * values, width // 4), jnp.bfloat16)] * 4,
        [
            pltpu.VMEM((2, width // size, size // 4, size), jnp.bfloat16),
            pltpu.VMEM((2, values, width), jnp.bfloat16),
            pltpu.SemaphoreType.DMA((4,)),
        ],
        (1_000_000_000, 2 << 20),
        16 << 20,
        [far] * 4,
        [whole()] * 5,
    )(
        w_query.reshape(width // size, size, size),
        w_forget.reshape(width // size, size, size),
        w_input,
        w_gate,
    )
    return outs[0], outs[1:]


def outward_kernel(w_out, outward, held, sems):
    cuts, size, span = held.shape
    copies = [
        pltpu.make_async_copy(w_out.at[:, pl.ds(c * span, span)], held.at[c], sems.at[c])
        for c in range(cuts)
    ]
    for copy in copies:
        copy.start()
    for c in range(cuts):
        copies[c].wait()
        for b in range(span // size):
            block = held[c, :, pl.ds(b * size, size)].astype(jnp.float32)
            outward[c * (span // size) + b] = block.T.astype(jnp.bfloat16)


def turn_outward(w_out):
    size, width = w_out.shape
    return call(
        outward_kernel,
        shaped((width // size, size, size), jnp.bfloat16),
        [pltpu.VMEM((4, size, width // 4), jnp.bfloat16), pltpu.SemaphoreType.DMA((4,))],
        (1_000_000_000, 2 << 20),
        16 << 20,
        [pl.BlockSpec(memory_space=pltpu.HBM)],
        whole(),
    )(w_out)


def project_kernel(own, other, keyed, w0, w1, w2, w3, o0, o1, o2, o3, held, ready):
    core, mine = lax.axis_index("core"), lax.axis_index("tp")
    blocks, _, seqs = own.shape
    group, keys = 4, keyed.shape[0]
    part = held.shape[0] // (2 * blocks)
    squares = jnp.zeros((16, seqs), jnp.float32)
    for half, ref in ((core, own), (1 - core, other)):
        for b in range(blocks):
            at = pl.multiple_of((2 * b + half) * part, part)
            for t in range(group):
                held[pl.ds(at, part), pl.ds(t * seqs, seqs)] = ref[b, pl.ds(t * part, part), :]
            squares = squares + ref[b, pl.ds(group * part, 16), :].astype(jnp.float32)
    totals = squares[0:4] + squares[4:8] + squares[8:12]
    rows = held[...]
    first = jnp.dot(keyed[...], rows, preferred_element_type=jnp.float32).astype(jnp.bfloat16)
    for t in range(group):
        ready[t, pl.ds(0, keys), :] = first[:, t * seqs : (t + 1) * seqs]
        tail = three_rows(split_in_three(totals[t : t + 1]), seqs)
        ready[t, pl.ds(ready.shape[1] - 16, 16), :] = tail
    for d, weight in enumerate((w0, w1, w2, w3)):
        more = weight.shape[0]
        at = pl.multiple_of(keys + (mine ^ d) * more, more)
        second = jnp.dot(weight[...], rows, preferred_element_type=jnp.float32).astype(jnp.bfloat16)
        for t in range(group):
            ready[t, pl.ds(at, more), :] = second[:, t * seqs : (t + 1) * seqs]
    for d, out in enumerate((o0, o1, o2, o3)):
        out[...] = ready[(mine ^ d)]


def project(own, other, keyed, weights):
    _, _, seqs = own.shape
    keys, width = keyed.shape
    rows = keys + 4 * weights[0].shape[0] + 16
    return call(
        project_kernel,
        [shaped((rows, seqs), jnp.bfloat16)] * 4,
        [pltpu.VMEM((width, 4 * seqs), jnp.bfloat16), pltpu.VMEM((4, rows, seqs), jnp.bfloat16)],
        (1_000_000_000, 3 << 20),
        16 << 20,
        [whole()] * 7,
        [whole()] * 4,
    )(own, other, keyed, *weights)


def finish_kernel(width, p0, p1, p2, p3, o0, o1, o2, o3, held):
    mine = lax.axis_index("tp")
    group = 4
    rows, keys = held.shape[0], o0.shape[0] * 4 // 5
    total = sum(ref[pl.ds(rows, 16), :].astype(jnp.float32) for ref in (p0, p1, p2, p3))
    factor = lax.rsqrt(jnp.sum(total, axis=0, keepdims=True) / width + NORM_EPSILON)
    value = sum(ref[pl.ds(0, rows), :].astype(jnp.float32) for ref in (p0, p1, p2, p3))
    held[...] = (value * factor).astype(jnp.bfloat16)
    more = (rows - keys) // group
    for d, out in enumerate((o0, o1, o2, o3)):
        at = pl.multiple_of(keys + (mine ^ d) * more, more)
        out[pl.ds(0, keys), :] = held[pl.ds(0, keys), :]
        out[pl.ds(keys, more), :] = held[pl.ds(at, more), :]


def finish(parts, keys, width):
    rows, seqs = parts[0].shape
    rows = rows - 16
    return call(
        functools.partial(finish_kernel, width),
        [shaped((keys + (rows - keys) // 4, seqs), jnp.bfloat16)] * 4,
        [pltpu.VMEM((rows, seqs), jnp.bfloat16)],
        (100_000_000, 1 << 20),
        16 << 20,
        [whole()] * 4,
        [whole()] * 4,
    )(*parts)


def recur_kernel(r0, r1, r2, r3, before, floor, head_gain, o0, o1, o2, o3, seen, ready):
    mine = lax.axis_index("tp")
    size = floor.shape[1]
    values = head_gain.shape[1]
    count = before.shape[0] // values
    steps = 4
    for d, ref in enumerate((r0, r1, r2, r3)):
        seen[mine ^ d] = ref[...]
    low = jnp.broadcast_to(floor[...], (count, size)).T
    scale = jnp.broadcast_to(head_gain[...], (count, values)).T
    forget, keys, fresh, sums, asked = [], [], [], [], []
    for t in range(steps):
        gate = low + (1.0 - low) * jax.nn.sigmoid(seen[t, pl.ds(size, size), :].astype(jnp.float32))
        forget.append(gate)
        keys.append(1.0 - gate)
        fresh.append(seen[t, pl.ds(2 * size, values), :].astype(jnp.float32))
    for t in range(steps):
        moved = seen[t, pl.ds(0, size), :].astype(jnp.float32)
        out = None
        for u in reversed(range(t + 1)):
            score = jnp.sum(moved * keys[u], axis=0, keepdims=True)
            term = score * fresh[u]
            out = term if out is None else out + term
            moved = moved * forget[u]
        sums.append(out)
        asked.append(moved.astype(jnp.bfloat16))
    lane = lax.broadcasted_iota(jnp.int32, (values, count), 1)
    asked = jnp.concatenate(asked, axis=1)
    group = 8
    for b in range(count // group):
        read = jnp.dot(
            before[pl.ds(b * group * values, group * values), :],
            asked,
            preferred_element_type=jnp.float32,
        )
        for s in range(group):
            hit = lane == b * group + s
            for t in range(steps):
                part = read[s * values : (s + 1) * values, t * count : (t + 1) * count]
                sums[t] = sums[t] + jnp.where(hit, part, 0.0)
    for t in range(steps):
        out = sums[t]
        square = jnp.sum(out * out, axis=0, keepdims=True)
        gate = seen[t, pl.ds(2 * size + values, values), :].astype(jnp.float32)
        shown = out * scale * (gate * jax.nn.sigmoid(gate))
        ready[t, pl.ds(0, values), :] = shown.astype(jnp.bfloat16)
        ready[t, pl.ds(values, 16), :] = three_rows(split_in_three(square), count)
    for d, ref in enumerate((o0, o1, o2, o3)):
        ref[...] = ready[mine ^ d]


def recur(received, before, floor, head_gain):
    rows, count = received[0].shape
    values = head_gain.shape[1]
    return call(
        recur_kernel,
        [shaped((values + 16, count), jnp.bfloat16)] * 4,
        [
            pltpu.VMEM((4, rows, count), jnp.bfloat16),
            pltpu.VMEM((4, values + 16, count), jnp.bfloat16),
        ],
        (1_000_000_000, 2 << 20),
        16 << 20,
        [whole()] * 7,
        [whole()] * 4,
    )(*received, before, floor, head_gain)


def gathered(parts, joined):
    mine = lax.axis_index("tp")
    values = joined.shape[0] // 4
    total = None
    for d, ref in enumerate(parts):
        at = pl.multiple_of((mine ^ d) * values, values)
        joined[pl.ds(at, values), :] = ref[pl.ds(0, values), :]
        square = jnp.sum(ref[pl.ds(values, 16), :].astype(jnp.float32), axis=0, keepdims=True)
        total = square if total is None else total + square
    return lax.rsqrt(total / joined.shape[0] + NORM_EPSILON)


def away_kernel(p0, p1, p2, p3, outward, sent, joined):
    core = lax.axis_index("core")
    factor = gathered((p0, p1, p2, p3), joined)
    for b in range(sent.shape[0]):
        part = jnp.dot(outward[2 * b + 1 - core], joined[...], preferred_element_type=jnp.float32)
        sent[b] = (part * factor).astype(jnp.bfloat16)


def keep_kernel(p0, p1, p2, p3, outward, came, kept, joined):
    core = lax.axis_index("core")
    factor = gathered((p0, p1, p2, p3), joined)
    for b in range(kept.shape[0]):
        part = jnp.dot(outward[2 * b + core], joined[...], preferred_element_type=jnp.float32)
        kept[b] = (part * factor + came[b].astype(jnp.float32)).astype(jnp.bfloat16)


def outward_half(kernel, parts, outward, *more):
    blocks, size, _ = outward.shape
    return call(
        kernel,
        shaped((blocks // 2, size, parts[0].shape[1]), jnp.bfloat16),
        [pltpu.VMEM((size, parts[0].shape[1]), jnp.bfloat16)],
        (100_000_000, 2 << 20),
        16 << 20,
        [whole()] * (5 + len(more)),
        whole(),
    )(*parts, outward, *more)


def sum_kernel(parts, out):
    total = parts[0].astype(jnp.float32)
    for b in range(1, parts.shape[0]):
        total = total + parts[b].astype(jnp.float32)
    out[...] = total.astype(out.dtype)


def sums(parts):
    return call(
        sum_kernel,
        shaped(parts.shape[1:], jnp.bfloat16),
        [],
        (1_000_000, 1 << 20),
        8 << 20,
        [whole()],
        whole(),
    )(parts)


def body(
    tokens,
    input_norm_gain,
    w_query,
    w_forget,
    w_input,
    w_gate,
    forget_floor,
    head_gain,
    w_out,
    state,
    prev_forget,
    prev_input,
    accepted,
):
    planes, group = lax.axis_size("zy"), lax.axis_size("tp")
    seqs, proposals, features = tokens.shape
    width, size = w_query.shape
    swap = [(0, 1), (1, 0)]
    hops = [[(i, i ^ d) for i in range(group)] for d in range(group)]

    def passed(parts):
        return [parts[0]] + [lax.ppermute(parts[d], "tp", hops[d]) for d in (1, 2, 3)]

    spread = source(tokens.transpose(1, 2, 0), input_norm_gain.reshape(-1, size), planes)
    own = lax.all_to_all(spread, "zy", 0, 0, tiled=True)
    other = lax.ppermute(own, "core", swap)
    keyed, mixing = turn(w_query, w_forget, w_input, w_gate)
    weights = passed(mixing)
    new_state, rounded = advance(
        accepted,
        prev_forget,
        prev_input.reshape(seqs, proposals, -1).transpose(1, 2, 0),
        state[:, 0],
    )

    partial = passed(project(own, other, keyed, weights))
    received = passed(finish(partial, 2 * size, width))
    shown = recur(received, rounded.reshape(-1, size), forget_floor[None], head_gain[None])
    parts = passed(shown)
    parts[0], w_out = lax.optimization_barrier((parts[0], w_out))
    outward = turn_outward(w_out)
    sent = outward_half(away_kernel, parts, outward)
    came = lax.ppermute(sent, "core", swap)
    kept = outward_half(keep_kernel, parts, outward, came)
    terms = lax.all_to_all(
        kept.reshape(planes * group, features, seqs), ("zy", "tp"), 0, 0, tiled=True
    )
    mixed = sums(terms.reshape(planes, group, features, seqs))
    return mixed.transpose(2, 0, 1), new_state[:, None]


def solution(mesh):
    kv, tp = mesh.shape["kv"], mesh.shape["tp"]
    finer = Mesh(mesh.devices.reshape(kv // 2, 2, tp), ("zy", "core", "tp"))
    rows = ("zy", "core")
    placed = (
        P(None, None, (*rows, "tp")),
        P(),
        P(None, rows),
        P(None, rows),
        P(rows, "tp", None),
        P(rows, "tp", None),
        P(rows),
        P("tp"),
        P(rows, None),
        P(None, rows, "tp", None),
        P(None, None, rows),
        P(None, None, rows, "tp"),
        P(),
    )

    return jax.shard_map(
        body,
        mesh=finer,
        in_specs=placed,
        out_specs=(P(None, None, (*rows, "tp")), P(None, rows, "tp", None)),
        check_vma=False,
    )
```

profile of v0, /device:TPU:0, one launch (start us, length us, event | category | flops | bytes accessed | tf_op | source)
XLA Modules:
  0.0 96.2 jit_solution(2748783469752348228)
XLA Ops:
  0.6 1.7 %shard_map.140 = bf16[16,144,128]{2,1,0:T(8,128)(2,1)} custom-call(bf16[4,32,128]{2,1,0:T(8,128)(2,1)} %bitcast.25, f32[32,128]{1,0:T(8,128)} %bitcast.27), custom_call_target="tpu_custom_call" | custom-call | flops 1000000 | bytes 1048576 | tf_op jit(solution)/shard_map/pallas_call | solution.py:120
  2.4 20.4 %all_to_all.10.own = bf16[16,144,128]{2,1,0:T(8,128)(2,1)S(1)} all-to-all(bf16[16,144,128]{2,1,0:T(8,128)(2,1)} %shard_map.140), channel_id=1, replica_groups=mesh['zy'=16,'core'=2,'tp'=4] {'zy'}, dimensions={0} | all-to-all | bytes 1179648 | tf_op jit(solution)/shard_map/all_to_all | solution.py:448
  22.8 1.2 %copy-done = bf16[4096,128]{1,0:T(8,128)(2,1)S(1)} copy-done((bf16[4096,128]{1,0:T(8,128)(2,1)S(1)}, bf16[4096,128]{1,0:T(8,128)(2,1)}, u32[]{:S(2)}) %copy-start) | copy-done | bytes 1048600
  24.0 1.2 %copy-done.1 = bf16[4096,128]{1,0:T(8,128)(2,1)S(1)} copy-done((bf16[4096,128]{1,0:T(8,128)(2,1)S(1)}, bf16[4096,128]{1,0:T(8,128)(2,1)}, u32[]{:S(2)}) %copy-start.1) | copy-done | bytes 1048600
  25.2 0.9 copy-done.3
  26.2 0.9 copy-done.4
  27.1 0.9 shard_map.141
  28.1 1.6 %collective-permute-start.1 = (bf16[64,1024]{1,0:T(8,128)(2,1)S(1)}, bf16[64,1024]{1,0:T(8,128)(2,1)S(1)}, u32[]{:S(2)}, u32[]{:S(2)}) collective-permute-start(bf16[64,1024]{1,0:T(8,128)(2,1)S(1)} %get-tuple-element.25), channel_id=1, source_target_pairs={{0,1},{1,0},{2,3},{3,2},{4,5},{5,4},{6,7},{7,6},{8,9},{9,8},{10,11... | collective-permute-start | bytes 393224 | tf_op jit(solution)/shard_map/ppermute | solution.py:445
  29.6 2.7 %collective-permute-start.2 = (bf16[64,1024]{1,0:T(8,128)(2,1)S(1)}, bf16[64,1024]{1,0:T(8,128)(2,1)S(1)}, u32[]{:S(2)}, u32[]{:S(2)}) collective-permute-start(bf16[64,1024]{1,0:T(8,128)(2,1)S(1)} %get-tuple-element.26), channel_id=1, source_target_pairs={{0,2},{1,3},{2,0},{3,1},{4,6},{5,7},{6,4},{7,5},{8,10},{9,11},{10,... | collective-permute-start | bytes 393224 | tf_op jit(solution)/shard_map/ppermute | solution.py:445
  32.4 0.5 collective-permute-start.3
  32.9 1.7 %collective-permute-done.1.w1 = bf16[64,1024]{1,0:T(8,128)(2,1)S(1)} collective-permute-done((bf16[64,1024]{1,0:T(8,128)(2,1)S(1)}, bf16[64,1024]{1,0:T(8,128)(2,1)S(1)}, u32[]{:S(2)}, u32[]{:S(2)}) %collective-permute-start.1) | collective-permute-done | bytes 131104 | tf_op jit(solution)/shard_map/ppermute | solution.py:445
  34.5 4.6 %collective-permute-done.2.w2 = bf16[64,1024]{1,0:T(8,128)(2,1)S(1)} collective-permute-done((bf16[64,1024]{1,0:T(8,128)(2,1)S(1)}, bf16[64,1024]{1,0:T(8,128)(2,1)S(1)}, u32[]{:S(2)}, u32[]{:S(2)}) %collective-permute-start.2) | collective-permute-done | bytes 131104 | tf_op jit(solution)/shard_map/ppermute | solution.py:445
  39.2 2.4 %collective-permute-done.3.w3 = bf16[64,1024]{1,0:T(8,128)(2,1)S(1)} collective-permute-done((bf16[64,1024]{1,0:T(8,128)(2,1)S(1)}, bf16[64,1024]{1,0:T(8,128)(2,1)S(1)}, u32[]{:S(2)}, u32[]{:S(2)}) %collective-permute-start.3) | collective-permute-done | bytes 131104 | tf_op jit(solution)/shard_map/ppermute | solution.py:445
  41.6 1.3 %shard_map.142 = (bf16[528,128]{1,0:T(8,128)(2,1)S(1)}, bf16[528,128]{1,0:T(8,128)(2,1)S(1)}, bf16[528,128]{1,0:T(8,128)(2,1)S(1)}, bf16[528,128]{1,0:T(8,128)(2,1)S(1)}) custom-call(bf16[16,144,128]{2,1,0:T(8,128)(2,1)S(1)} %all_to_all.10.own, bf16[16,144,128]{2,1,0:T(8,128)(2,1)S(1)} %collective-permute-done.other, ...), custom_call_target="tpu_custom_call" | custom-call | flops 1000000000 | bytes 3145728 | tf_op jit(solution)/shard_map/pallas_call | solution.py:255
  43.0 1.9 %collective-permute-start.5 = (bf16[528,128]{1,0:T(8,128)(2,1)S(1)}, bf16[528,128]{1,0:T(8,128)(2,1)S(1)}, u32[]{:S(2)}, u32[]{:S(2)}) collective-permute-start(bf16[528,128]{1,0:T(8,128)(2,1)S(1)} %get-tuple-element.30), channel_id=1, source_target_pairs={{0,2},{1,3},{2,0},{3,1},{4,6},{5,7},{6,4},{7,5},{8,10},{9,11},{10,... | collective-permute-start | bytes 405512 | tf_op jit(solution)/shard_map/ppermute | solution.py:445
  44.9 2.7 %collective-permute-start.6 = (bf16[528,128]{1,0:T(8,128)(2,1)S(1)}, bf16[528,128]{1,0:T(8,128)(2,1)S(1)}, u32[]{:S(2)}, u32[]{:S(2)}) collective-permute-start(bf16[528,128]{1,0:T(8,128)(2,1)S(1)} %get-tuple-element.31), channel_id=1, source_target_pairs={{0,3},{1,2},{2,1},{3,0},{4,7},{5,6},{6,5},{7,4},{8,11},{9,10},{10,... | collective-permute-start | bytes 405512 | tf_op jit(solution)/shard_map/ppermute | solution.py:445
  47.7 1.8 %collective-permute-done.4.p1 = bf16[528,128]{1,0:T(8,128)(2,1)S(1)} collective-permute-done((bf16[528,128]{1,0:T(8,128)(2,1)S(1)}, bf16[528,128]{1,0:T(8,128)(2,1)S(1)}, u32[]{:S(2)}, u32[]{:S(2)}) %collective-permute-start.4) | collective-permute-done | bytes 135200 | tf_op jit(solution)/shard_map/ppermute | solution.py:445
  49.4 1.7 %collective-permute-done.5.p2 = bf16[528,128]{1,0:T(8,128)(2,1)S(1)} collective-permute-done((bf16[528,128]{1,0:T(8,128)(2,1)S(1)}, bf16[528,128]{1,0:T(8,128)(2,1)S(1)}, u32[]{:S(2)}, u32[]{:S(2)}) %collective-permute-start.5) | collective-permute-done | bytes 135200 | tf_op jit(solution)/shard_map/ppermute | solution.py:445
  51.1 2.1 %collective-permute-done.6.p3 = bf16[528,128]{1,0:T(8,128)(2,1)S(1)} collective-permute-done((bf16[528,128]{1,0:T(8,128)(2,1)S(1)}, bf16[528,128]{1,0:T(8,128)(2,1)S(1)}, u32[]{:S(2)}, u32[]{:S(2)}) %collective-permute-start.6) | collective-permute-done | bytes 135200 | tf_op jit(solution)/shard_map/ppermute | solution.py:445
  53.5 4.2 %collective-permute-start.8 = (bf16[320,128]{1,0:T(8,128)(2,1)S(1)}, bf16[320,128]{1,0:T(8,128)(2,1)S(1)}, u32[]{:S(2)}, u32[]{:S(2)}) collective-permute-start(bf16[320,128]{1,0:T(8,128)(2,1)S(1)} %get-tuple-element.34), channel_id=1, source_target_pairs={{0,2},{1,3},{2,0},{3,1},{4,6},{5,7},{6,4},{7,5},{8,10},{9,11},{10,... | collective-permute-start | bytes 245768 | tf_op jit(solution)/shard_map/ppermute | solution.py:445
  57.7 0.5 collective-permute-start.9
  58.1 5.0 %advance.1 = (f32[128,32,128]{2,1,0:T(8,128)}, bf16[128,32,128]{2,1,0:T(8,128)(2,1)}) custom-call(s32[1,128]{1,0:T(1,128)} %bitcast.30, f32[128,4,128]{2,1,0:T(4,128)} %prev_forget.1, bf16[4,32,128]{2,1,0:T(8,128)(2,1)} %bitcast.29, f32[128,32,128]{2,1,0:T(8,128)} %bitcast.28), custom_call_target="tpu_custom_call" | custom-call | flops 1000000000 | bytes 5242880 | tf_op jit(solution)/shard_map/advance/pallas_call | solution.py:67
  63.3 1.3 %copy-done.7 = bf16[128,32,128]{2,1,0:T(8,128)(2,1)S(1)} copy-done((bf16[128,32,128]{2,1,0:T(8,128)(2,1)S(1)}, bf16[128,32,128]{2,1,0:T(8,128)(2,1)}, u32[]{:S(2)}) %copy-start.7) | copy-done | bytes 1048600
  64.6 1.4 %shard_map.144 = (bf16[48,128]{1,0:T(8,128)(2,1)S(1)}, bf16[48,128]{1,0:T(8,128)(2,1)S(1)}, bf16[48,128]{1,0:T(8,128)(2,1)S(1)}, bf16[48,128]{1,0:T(8,128)(2,1)S(1)}) custom-call(bf16[320,128]{1,0:T(8,128)(2,1)S(1)} %get-tuple-element.32.r0, bf16[320,128]{1,0:T(8,128)(2,1)S(1)} %collective-permute-done.7.r1, bf16[320,128]{1,0:T(8,128)(2,1)S(1)} %collective-permute-done.8.r2, ...), custom_call_target="tpu_custom_call" | custom-call | flops 1000000000 | bytes 2097152 | tf_op jit(solution)/shard_map/pallas_call | solution.py:349
  66.2 4.0 %collective-permute-start.11 = (bf16[48,128]{1,0:T(8,128)(2,1)S(1)}, bf16[48,128]{1,0:T(8,128)(2,1)S(1)}, u32[]{:S(2)}, u32[]{:S(2)}) collective-permute-start(bf16[48,128]{1,0:T(8,128)(2,1)S(1)} %get-tuple-element.40), channel_id=1, source_target_pairs={{0,2},{1,3},{2,0},{3,1},{4,6},{5,7},{6,4},{7,5},{8,10},{9,11},{10,... | collective-permute-start | bytes 36872 | tf_op jit(solution)/shard_map/ppermute | solution.py:445
  70.2 0.6 collective-permute-start.12
  70.9 0.7 shard_map.145.outward
  71.5 0.5 collective-permute-done.11.p2
  72.0 3.1 %collective-permute-done.12.p3 = bf16[48,128]{1,0:T(8,128)(2,1)S(1)} collective-permute-done((bf16[48,128]{1,0:T(8,128)(2,1)S(1)}, bf16[48,128]{1,0:T(8,128)(2,1)S(1)}, u32[]{:S(2)}, u32[]{:S(2)}) %collective-permute-start.12) | collective-permute-done | bytes 12320 | tf_op jit(solution)/shard_map/ppermute | solution.py:445
  75.5 1.9 %collective-permute-done.13.came = bf16[16,128,128]{2,1,0:T(8,128)(2,1)S(1)} collective-permute-done((bf16[16,128,128]{2,1,0:T(8,128)(2,1)S(1)}, bf16[16,128,128]{2,1,0:T(8,128)(2,1)S(1)}, u32[]{:S(2)}, u32[]{:S(2)}) %collective-permute-start.13) | collective-permute-done | bytes 524320 | tf_op jit(solution)/shard_map/ppermute | solution.py:466
  77.7 17.8 %all_to_all.11 = bf16[64,32,128]{2,1,0:T(8,128)(2,1)S(1)} all-to-all(bf16[64,32,128]{2,1,0:T(8,128)(2,1)S(1)} %bitcast.19), channel_id=1, replica_groups=mesh['zy'=16,'core'=2,'tp'=4] {'zy','tp'}, dimensions={0} | all-to-all | bytes 1048576 | tf_op jit(solution)/shard_map/all_to_all | solution.py:468
  95.5 0.7 shard_map.148
  (24 shorter events, 1.3 us)
Async XLA Ops:
  22.8 18.8 %collective-permute-start = (bf16[16,144,128]{2,1,0:T(8,128)(2,1)S(1)}, bf16[16,144,128]{2,1,0:T(8,128)(2,1)S(1)}, u32[]{:S(2)}, u32[]{:S(2)}) collective-permute-start(bf16[16,144,128]{2,1,0:T(8,128)(2,1)S(1)} %all_to_all.10.own), channel_id=1, source_target_pairs={{0,4},{4,0},{1,5},{5,1},{2,6},{6,2},{3,7},{7,3},{8,12},{12,8},{9,1... | collective-permute-start | bytes 1769480 | tf_op jit(solution)/shard_map/ppermute | solution.py:449
  22.8 1.2 %copy-start = (bf16[4096,128]{1,0:T(8,128)(2,1)S(1)}, bf16[4096,128]{1,0:T(8,128)(2,1)}, u32[]{:S(2)}) copy-start(bf16[4096,128]{1,0:T(8,128)(2,1)} %param.15) | copy-start | bytes 3145732
  24.0 1.2 %copy-start.1 = (bf16[4096,128]{1,0:T(8,128)(2,1)S(1)}, bf16[4096,128]{1,0:T(8,128)(2,1)}, u32[]{:S(2)}) copy-start(bf16[4096,128]{1,0:T(8,128)(2,1)} %param.16) | copy-start | bytes 3145732
  25.2 0.9 copy-start.3
  26.2 0.9 copy-start.4
  28.1 6.4 %collective-permute-start.1 = (bf16[64,1024]{1,0:T(8,128)(2,1)S(1)}, bf16[64,1024]{1,0:T(8,128)(2,1)S(1)}, u32[]{:S(2)}, u32[]{:S(2)}) collective-permute-start(bf16[64,1024]{1,0:T(8,128)(2,1)S(1)} %get-tuple-element.25), channel_id=1, source_target_pairs={{0,1},{1,0},{2,3},{3,2},{4,5},{5,4},{6,7},{7,6},{8,9},{9,8},{10,11... | collective-permute-start | bytes 393224 | tf_op jit(solution)/shard_map/ppermute | solution.py:445
  29.6 9.5 %collective-permute-start.2 = (bf16[64,1024]{1,0:T(8,128)(2,1)S(1)}, bf16[64,1024]{1,0:T(8,128)(2,1)S(1)}, u32[]{:S(2)}, u32[]{:S(2)}) collective-permute-start(bf16[64,1024]{1,0:T(8,128)(2,1)S(1)} %get-tuple-element.26), channel_id=1, source_target_pairs={{0,2},{1,3},{2,0},{3,1},{4,6},{5,7},{6,4},{7,5},{8,10},{9,11},{10,... | collective-permute-start | bytes 393224 | tf_op jit(solution)/shard_map/ppermute | solution.py:445
  32.4 9.2 %collective-permute-start.3 = (bf16[64,1024]{1,0:T(8,128)(2,1)S(1)}, bf16[64,1024]{1,0:T(8,128)(2,1)S(1)}, u32[]{:S(2)}, u32[]{:S(2)}) collective-permute-start(bf16[64,1024]{1,0:T(8,128)(2,1)S(1)} %get-tuple-element.27), channel_id=1, source_target_pairs={{0,3},{1,2},{2,1},{3,0},{4,7},{5,6},{6,5},{7,4},{8,11},{9,10},{10,... | collective-permute-start | bytes 393224 | tf_op jit(solution)/shard_map/ppermute | solution.py:445
  42.9 6.5 %collective-permute-start.4 = (bf16[528,128]{1,0:T(8,128)(2,1)S(1)}, bf16[528,128]{1,0:T(8,128)(2,1)S(1)}, u32[]{:S(2)}, u32[]{:S(2)}) collective-permute-start(bf16[528,128]{1,0:T(8,128)(2,1)S(1)} %get-tuple-element.29), channel_id=1, source_target_pairs={{0,1},{1,0},{2,3},{3,2},{4,5},{5,4},{6,7},{7,6},{8,9},{9,8},{10,11... | collective-permute-start | bytes 405512 | tf_op jit(solution)/shard_map/ppermute | solution.py:445
  43.0 8.1 %collective-permute-start.5 = (bf16[528,128]{1,0:T(8,128)(2,1)S(1)}, bf16[528,128]{1,0:T(8,128)(2,1)S(1)}, u32[]{:S(2)}, u32[]{:S(2)}) collective-permute-start(bf16[528,128]{1,0:T(8,128)(2,1)S(1)} %get-tuple-element.30), channel_id=1, source_target_pairs={{0,2},{1,3},{2,0},{3,1},{4,6},{5,7},{6,4},{7,5},{8,10},{9,11},{10,... | collective-permute-start | bytes 405512 | tf_op jit(solution)/shard_map/ppermute | solution.py:445
  44.9 8.3 %collective-permute-start.6 = (bf16[528,128]{1,0:T(8,128)(2,1)S(1)}, bf16[528,128]{1,0:T(8,128)(2,1)S(1)}, u32[]{:S(2)}, u32[]{:S(2)}) collective-permute-start(bf16[528,128]{1,0:T(8,128)(2,1)S(1)} %get-tuple-element.31), channel_id=1, source_target_pairs={{0,3},{1,2},{2,1},{3,0},{4,7},{5,6},{6,5},{7,4},{8,11},{9,10},{10,... | collective-permute-start | bytes 405512 | tf_op jit(solution)/shard_map/ppermute | solution.py:445
  53.2 10.1 %copy-start.5 = (f32[128]{0:T(128)S(1)}, f32[128]{0:T(128)}, u32[]{:S(2)}) copy-start(f32[128]{0:T(128)} %param.19) | copy-start | bytes 1540
  53.2 10.1 %copy-start.6 = (f32[32]{0:T(128)S(1)}, f32[32]{0:T(128)}, u32[]{:S(2)}) copy-start(f32[32]{0:T(128)} %param.20) | copy-start | bytes 388
  53.4 9.8 %collective-permute-start.7 = (bf16[320,128]{1,0:T(8,128)(2,1)S(1)}, bf16[320,128]{1,0:T(8,128)(2,1)S(1)}, u32[]{:S(2)}, u32[]{:S(2)}) collective-permute-start(bf16[320,128]{1,0:T(8,128)(2,1)S(1)} %get-tuple-element.33), channel_id=1, source_target_pairs={{0,1},{1,0},{2,3},{3,2},{4,5},{5,4},{6,7},{7,6},{8,9},{9,8},{10,11... | collective-permute-start | bytes 245768 | tf_op jit(solution)/shard_map/ppermute | solution.py:445
  53.5 9.7 %collective-permute-start.8 = (bf16[320,128]{1,0:T(8,128)(2,1)S(1)}, bf16[320,128]{1,0:T(8,128)(2,1)S(1)}, u32[]{:S(2)}, u32[]{:S(2)}) collective-permute-start(bf16[320,128]{1,0:T(8,128)(2,1)S(1)} %get-tuple-element.34), channel_id=1, source_target_pairs={{0,2},{1,3},{2,0},{3,1},{4,6},{5,7},{6,4},{7,5},{8,10},{9,11},{10,... | collective-permute-start | bytes 245768 | tf_op jit(solution)/shard_map/ppermute | solution.py:445
  57.7 5.7 %collective-permute-start.9 = (bf16[320,128]{1,0:T(8,128)(2,1)S(1)}, bf16[320,128]{1,0:T(8,128)(2,1)S(1)}, u32[]{:S(2)}, u32[]{:S(2)}) collective-permute-start(bf16[320,128]{1,0:T(8,128)(2,1)S(1)} %get-tuple-element.35), channel_id=1, source_target_pairs={{0,3},{1,2},{2,1},{3,0},{4,7},{5,6},{6,5},{7,4},{8,11},{9,10},{10,... | collective-permute-start | bytes 245768 | tf_op jit(solution)/shard_map/ppermute | solution.py:445
  63.1 7.7 %copy-start.2 = (bf16[128,4096]{1,0:T(8,128)(2,1)S(1)}, bf16[128,4096]{1,0:T(8,128)(2,1)}, u32[]{:S(2)}) copy-start(bf16[128,4096]{1,0:T(8,128)(2,1)} %w_out) | copy-start | bytes 3145732
  63.3 1.3 %copy-start.7 = (bf16[128,32,128]{2,1,0:T(8,128)(2,1)S(1)}, bf16[128,32,128]{2,1,0:T(8,128)(2,1)}, u32[]{:S(2)}) copy-start(bf16[128,32,128]{2,1,0:T(8,128)(2,1)} %get-tuple-element.36) | copy-start | bytes 3145732
  66.1 5.5 %collective-permute-start.10 = (bf16[48,128]{1,0:T(8,128)(2,1)S(1)}, bf16[48,128]{1,0:T(8,128)(2,1)S(1)}, u32[]{:S(2)}, u32[]{:S(2)}) collective-permute-start(bf16[48,128]{1,0:T(8,128)(2,1)S(1)} %get-tuple-element.39), channel_id=1, source_target_pairs={{0,1},{1,0},{2,3},{3,2},{4,5},{5,4},{6,7},{7,6},{8,9},{9,8},{10,11... | collective-permute-start | bytes 36872 | tf_op jit(solution)/shard_map/ppermute | solution.py:445
  66.2 5.8 %collective-permute-start.11 = (bf16[48,128]{1,0:T(8,128)(2,1)S(1)}, bf16[48,128]{1,0:T(8,128)(2,1)S(1)}, u32[]{:S(2)}, u32[]{:S(2)}) collective-permute-start(bf16[48,128]{1,0:T(8,128)(2,1)S(1)} %get-tuple-element.40), channel_id=1, source_target_pairs={{0,2},{1,3},{2,0},{3,1},{4,6},{5,7},{6,4},{7,5},{8,10},{9,11},{10,... | collective-permute-start | bytes 36872 | tf_op jit(solution)/shard_map/ppermute | solution.py:445
  70.2 4.9 %collective-permute-start.12 = (bf16[48,128]{1,0:T(8,128)(2,1)S(1)}, bf16[48,128]{1,0:T(8,128)(2,1)S(1)}, u32[]{:S(2)}, u32[]{:S(2)}) collective-permute-start(bf16[48,128]{1,0:T(8,128)(2,1)S(1)} %get-tuple-element.41), channel_id=1, source_target_pairs={{0,3},{1,2},{2,1},{3,0},{4,7},{5,6},{6,5},{7,4},{8,11},{9,10},{10,... | collective-permute-start | bytes 36872 | tf_op jit(solution)/shard_map/ppermute | solution.py:445
  75.4 2.0 %collective-permute-start.13 = (bf16[16,128,128]{2,1,0:T(8,128)(2,1)S(1)}, bf16[16,128,128]{2,1,0:T(8,128)(2,1)S(1)}, u32[]{:S(2)}, u32[]{:S(2)}) collective-permute-start(bf16[16,128,128]{2,1,0:T(8,128)(2,1)S(1)} %shard_map.146), channel_id=1, source_target_pairs={{0,4},{4,0},{1,5},{5,1},{2,6},{6,2},{3,7},{7,3},{8,12},{12,8},{9,1... | collective-permute-start | bytes 1572872 | tf_op jit(solution)/shard_map/ppermute | solution.py:466
where the time goes:
time: 96.8 us; the launch traced here: 96.2 us
  blocking collectives  38.2 us (39%)
  waiting for transfers between devices  19.9 us (21%)
  starting transfers between devices  19.2 us (20%)
  Pallas kernels  12.5 us (13%)
  local copies, waits for them, and re-layouts  5.69 us (6%)
    all_to_all x1, blocking collectives, body(): own = lax.all_to_all(spread, 'zy', 0, 0, tiled=True)  20.4 us
    ppermute x12, starting transfers between devices, passed(): lax.ppermute(parts[d], 'tp', hops[d])  19.1 us
    ppermute x12, waiting for transfers between devices, passed(): lax.ppermute(parts[d], 'tp', hops[d])  18 us
    all_to_all x1, blocking collectives, body(): lax.all_to_all(kept.reshape(planes * group, features, seqs), ('zy', 'tp')...  17.8 us
    unnamed x16, local copies, waits for them, and re-layouts  5.69 us
    pallas_call x1, Pallas kernels, advance(): pl.pallas_call(advance_kernel, grid=(seqs // count,), in_specs=[pl.BlockS...  4.98 us
  transfers between devices with their start and end apart: 14, of which 10 were waited for; matrix products, arithmetic and copies ran while one was open for 0% of the time, Pallas kernels for 7%

commit v1 on v0

v1 whole, which is shorter than its diff:
```python
import jax
import jax.numpy as jnp
from jax import lax
from jax.experimental import pallas as pl
from jax.experimental.pallas import tpu as pltpu
from jax.sharding import Mesh, PartitionSpec as P


NORM_EPSILON = 1e-06


def whole():
    return pl.BlockSpec(memory_space=pltpu.VMEM)


def shaped(shape, dtype):
    return jax.ShapeDtypeStruct(shape, dtype)


def call(kernel, out_shape, scratch, cost, limit, in_specs, out_specs):
    return pl.pallas_call(
        kernel,
        out_shape=out_shape,
        in_specs=in_specs,
        out_specs=out_specs,
        scratch_shapes=scratch,
        cost_estimate=pl.CostEstimate(flops=cost[0], bytes_accessed=cost[1], transcendentals=0),
        compiler_params=pltpu.CompilerParams(vmem_limit_bytes=limit),
    )


def advance_kernel(accepted, prev_forget, prev_input, state, new_state, rounded, live):
    block = pl.program_id(0)
    count, proposals, size = prev_forget.shape
    lanes = prev_input.shape[2]

    @pl.when(block == 0)
    def _():
        live[...] = jnp.broadcast_to(accepted[...].astype(jnp.float32), (size, lanes)).T

    shift = lax.rem(lanes - block * count, lanes)
    values = [
        pltpu.roll(prev_input[p].astype(jnp.float32), shift, 1) for p in range(proposals)
    ]
    taken = live[pl.ds(pl.multiple_of(block * count, count), count), :]
    rest = jnp.ones((count, size), jnp.float32)
    terms = [None] * proposals
    for p in reversed(range(proposals)):
        gate = jnp.where(taken > p, prev_forget[:, p, :], 1.0)
        terms[p] = rest * (1.0 - gate)
        rest = rest * gate
    for s in range(count):
        fresh = rest[s : s + 1] * state[s]
        for p in range(proposals):
            fresh = fresh + terms[p][s : s + 1] * values[p][:, s : s + 1]
        new_state[s] = fresh
        rounded[s] = fresh.astype(jnp.bfloat16)


def advance(accepted, prev_forget, prev_input, state):
    seqs, values, keys = state.shape
    proposals = prev_forget.shape[1]
    count = 32
    span = pl.BlockSpec((count, values, keys), lambda i: (i, 0, 0))
    return pl.pallas_call(
        advance_kernel,
        grid=(seqs // count,),
        in_specs=[
            pl.BlockSpec((1, seqs), lambda i: (0, 0)),
            pl.BlockSpec((count, proposals, keys), lambda i: (i, 0, 0)),
            pl.BlockSpec((proposals, values, seqs), lambda i: (0, 0, 0)),
            span,
        ],
        out_specs=[span, span],
        out_shape=[shaped(state.shape, jnp.float32), shaped(state.shape, jnp.bfloat16)],
        scratch_shapes=[pltpu.VMEM((keys, seqs), jnp.float32)],
        name="advance",
        cost_estimate=pl.CostEstimate(
            flops=1_000_000_000, bytes_accessed=5 << 20, transcendentals=0
        ),
        compiler_params=pltpu.CompilerParams(vmem_limit_bytes=16 << 20),
    )(accepted[None], prev_forget, prev_input, state)


def split_in_three(value):
    high = value.astype(jnp.bfloat16).astype(jnp.float32)
    middle = (value - high).astype(jnp.bfloat16).astype(jnp.float32)
    return high, middle, value - high - middle


def three_rows(parts, width):
    rest = jnp.zeros((16 - 3 * parts[0].shape[0], width), jnp.float32)
    return jnp.concatenate([*parts, rest], axis=0).astype(jnp.bfloat16)


def source_kernel(tokens, out):
    steps = tokens.shape[0]
    for z in range(out.shape[0] // steps):
        out[pl.ds(z * steps, steps)] = tokens[...]


def source(tokens, planes):
    steps, features, seqs = tokens.shape
    return call(
        source_kernel,
        shaped((planes * steps, features, seqs), jnp.bfloat16),
        [],
        (1_000_000, 1 << 20),
        60 << 20,
        [whole()],
        whole(),
    )(tokens)


def turn_kernel(gain, w_query, w_forget, keyed):
    size = gain.shape[1]
    for b in range(w_query.shape[0] // size):
        at = pl.ds(b * size, size)
        row = gain[pl.ds(b, 1), :]
        for i, weight in enumerate((w_query, w_forget)):
            block = weight[at, :].astype(jnp.float32).T
            keyed[pl.ds(i * size, size), at] = (block * row).astype(jnp.bfloat16)


def turn(gain, w_query, w_forget):
    width, size = w_query.shape
    return call(
        turn_kernel,
        shaped((2 * size, width), jnp.bfloat16),
        [],
        (1_000_000_000, 4 << 20),
        16 << 20,
        [whole()] * 3,
        whole(),
    )(gain, w_query, w_forget)


def fold_kernel(gain, w0, w1, w2, w3, out):
    values, size = w0.shape[1], gain.shape[1]
    for b in range(gain.shape[0]):
        at = pl.ds(b * size, size)
        for d, weight in enumerate((w0, w1, w2, w3)):
            value = weight[0, :, at].astype(jnp.float32) * gain[pl.ds(b, 1), :]
            out[pl.ds(d * values, values), at] = value.astype(jnp.bfloat16)


def fold(gain, weights):
    _, values, width = weights[0].shape
    return call(
        fold_kernel,
        shaped((4 * values, width), jnp.bfloat16),
        [],
        (1_000_000_000, 2 << 20),
        16 << 20,
        [whole()] * 5,
        whole(),
    )(gain, *weights)


def project_kernel(own, other, keyed, mixing, o0, o1, o2, o3, held, scale):
    core = lax.axis_index("core")
    blocks, size, seqs = own.shape
    squares = jnp.zeros((8, seqs), jnp.float32)
    for half, ref in ((core, own), (1 - core, other)):
        for b in range(blocks):
            part = ref[b]
            held[pl.ds(pl.multiple_of((2 * b + half) * size, size), size), :] = part
            wide = part.astype(jnp.float32)
            squares = squares + jnp.sum((wide * wide).reshape(size // 8, 8, seqs), axis=0)
    total = jnp.sum(squares, axis=0, keepdims=True)
    factor = lax.rsqrt(total / (2 * blocks * size) + NORM_EPSILON)
    scale[...] = jnp.broadcast_to(factor, scale.shape)
    rows = held[...]
    first = jnp.dot(keyed[...], rows, preferred_element_type=jnp.float32) * factor
    first = first.astype(jnp.bfloat16)
    second = jnp.dot(mixing[...], rows, preferred_element_type=jnp.float32) * factor
    second = second.astype(jnp.bfloat16)
    keys, values = first.shape[0], second.shape[0] // 4
    for d, out in enumerate((o0, o1, o2, o3)):
        out[pl.ds(0, keys), :] = first
        out[pl.ds(keys, values), :] = second[d * values : (d + 1) * values]


def project(own, other, keyed, mixing):
    blocks, size, seqs = own.shape
    rows = keyed.shape[0] + mixing.shape[0] // 4
    outs = call(
        project_kernel,
        [shaped((rows, seqs), jnp.bfloat16)] * 4
        + [shaped((2 * blocks * size, seqs), jnp.bfloat16), shaped((8, seqs), jnp.float32)],
        [],
        (1_000_000_000, 3 << 20),
        16 << 20,
        [whole()] * 4,
        [whole()] * 6,
    )(own, other, keyed, mixing)
    return outs[:4], outs[4], outs[5]


def gate_kernel(gain, w0, w1, w2, w3, rows, scale, out, held):
    values, size = w0.shape[1], gain.shape[1]
    for b in range(gain.shape[0]):
        at = pl.ds(b * size, size)
        for d, weight in enumerate((w0, w1, w2, w3)):
            value = weight[0, :, at].astype(jnp.float32) * gain[pl.ds(b, 1), :]
            held[pl.ds(d * values, values), at] = value.astype(jnp.bfloat16)
    raw = jnp.dot(held[...], rows[...], preferred_element_type=jnp.float32) * scale[0:1]
    raw = raw.astype(jnp.bfloat16).astype(jnp.float32)
    out[...] = raw * jax.nn.sigmoid(raw)


def gate(gain, weights, rows, scale):
    _, values, width = weights[0].shape
    return call(
        gate_kernel,
        shaped((4 * values, rows.shape[1]), jnp.float32),
        [pltpu.VMEM((4 * values, width), jnp.bfloat16)],
        (1_000_000_000, 3 << 20),
        16 << 20,
        [whole()] * 7,
        whole(),
    )(gain, *weights, rows, scale)


def outward_kernel(w_out, outward, held, sems):
    cuts, size, span = held.shape
    copies = [
        pltpu.make_async_copy(w_out.at[:, pl.ds(c * span, span)], held.at[c], sems.at[c])
        for c in range(cuts)
    ]
    for copy in copies:
        copy.start()
    for c in range(cuts):
        copies[c].wait()
        for b in range(span // size):
            block = held[c, :, pl.ds(b * size, size)].astype(jnp.float32)
            outward[c * (span // size) + b] = block.T.astype(jnp.bfloat16)


def turn_outward(w_out):
    size, width = w_out.shape
    return call(
        outward_kernel,
        shaped((width // size, size, size), jnp.bfloat16),
        [pltpu.VMEM((4, size, width // 4), jnp.bfloat16), pltpu.SemaphoreType.DMA((4,))],
        (1_000_000_000, 2 << 20),
        16 << 20,
        [pl.BlockSpec(memory_space=pltpu.HBM)],
        whole(),
    )(w_out)


def recur_kernel(r0, r1, r2, r3, before, floor, head_gain, o0, o1, o2, o3, seen, ready):
    mine = lax.axis_index("tp")
    size = floor.shape[1]
    values = head_gain.shape[1]
    count = before.shape[0] // values
    steps = 4
    for d, ref in enumerate((r0, r1, r2, r3)):
        seen[mine ^ d] = ref[...]
    low = jnp.broadcast_to(floor[...], (count, size)).T
    scale = jnp.broadcast_to(head_gain[...], (count, values)).T
    forget, keys, fresh, sums, asked = [], [], [], [], []
    for t in range(steps):
        gate = low + (1.0 - low) * jax.nn.sigmoid(seen[t, pl.ds(size, size), :].astype(jnp.float32))
        forget.append(gate)
        keys.append(1.0 - gate)
        fresh.append(seen[t, pl.ds(2 * size, values), :].astype(jnp.float32))
    for t in range(steps):
        moved = seen[t, pl.ds(0, size), :].astype(jnp.float32)
        out = None
        for u in reversed(range(t + 1)):
            score = jnp.sum(moved * keys[u], axis=0, keepdims=True)
            term = score * fresh[u]
            out = term if out is None else out + term
            moved = moved * forget[u]
        sums.append(out)
        asked.append(moved.astype(jnp.bfloat16))
    lane = lax.broadcasted_iota(jnp.int32, (values, count), 1)
    asked = jnp.concatenate(asked, axis=1)
    group = 8
    for b in range(count // group):
        read = jnp.dot(
            before[pl.ds(b * group * values, group * values), :],
            asked,
            preferred_element_type=jnp.float32,
        )
        for s in range(group):
            hit = lane == b * group + s
            for t in range(steps):
                part = read[s * values : (s + 1) * values, t * count : (t + 1) * count]
                sums[t] = sums[t] + jnp.where(hit, part, 0.0)
    for t in range(steps):
        out = sums[t]
        square = jnp.sum(out * out, axis=0, keepdims=True)
        ready[t, pl.ds(0, values), :] = (out * scale).astype(jnp.bfloat16)
        ready[t, pl.ds(values, 16), :] = three_rows(split_in_three(square), count)
    for d, ref in enumerate((o0, o1, o2, o3)):
        ref[...] = ready[mine ^ d]


def recur(received, before, floor, head_gain):
    rows, count = received[0].shape
    values = head_gain.shape[1]
    return call(
        recur_kernel,
        [shaped((values + 16, count), jnp.bfloat16)] * 4,
        [
            pltpu.VMEM((4, rows, count), jnp.bfloat16),
            pltpu.VMEM((4, values + 16, count), jnp.bfloat16),
        ],
        (1_000_000_000, 2 << 20),
        16 << 20,
        [whole()] * 7,
        [whole()] * 4,
    )(*received, before, floor, head_gain)


def gathered(parts, gates, joined):
    mine = lax.axis_index("tp")
    values = joined.shape[0] // 4
    total = None
    for d, ref in enumerate(parts):
        at = pl.multiple_of((mine ^ d) * values, values)
        value = ref[pl.ds(0, values), :].astype(jnp.float32) * gates[pl.ds(d * values, values), :]
        joined[pl.ds(at, values), :] = value.astype(jnp.bfloat16)
        square = jnp.sum(ref[pl.ds(values, 16), :].astype(jnp.float32), axis=0, keepdims=True)
        total = square if total is None else total + square
    return lax.rsqrt(total / joined.shape[0] + NORM_EPSILON)


def away_kernel(p0, p1, p2, p3, gates, outward, sent, joined):
    core = lax.axis_index("core")
    factor = gathered((p0, p1, p2, p3), gates, joined)
    for b in range(sent.shape[0]):
        part = jnp.dot(outward[2 * b + 1 - core], joined[...], preferred_element_type=jnp.float32)
        sent[b] = (part * factor).astype(jnp.bfloat16)


def keep_kernel(p0, p1, p2, p3, gates, outward, came, kept, joined):
    core = lax.axis_index("core")
    factor = gathered((p0, p1, p2, p3), gates, joined)
    for b in range(kept.shape[0]):
        part = jnp.dot(outward[2 * b + core], joined[...], preferred_element_type=jnp.float32)
        kept[b] = (part * factor + came[b].astype(jnp.float32)).astype(jnp.bfloat16)


def outward_half(kernel, parts, gates, outward, *more):
    blocks, size, _ = outward.shape
    return call(
        kernel,
        shaped((blocks // 2, size, parts[0].shape[1]), jnp.bfloat16),
        [pltpu.VMEM((size, parts[0].shape[1]), jnp.bfloat16)],
        (100_000_000, 2 << 20),
        16 << 20,
        [whole()] * (6 + len(more)),
        whole(),
    )(*parts, gates, outward, *more)


def sum_kernel(parts, out):
    total = parts[0].astype(jnp.float32)
    for b in range(1, parts.shape[0]):
        total = total + parts[b].astype(jnp.float32)
    out[...] = total.astype(out.dtype)


def sums(parts):
    return call(
        sum_kernel,
        shaped(parts.shape[1:], jnp.bfloat16),
        [],
        (1_000_000, 1 << 20),
        8 << 20,
        [whole()],
        whole(),
    )(parts)


def body(
    tokens,
    input_norm_gain,
    w_query,
    w_forget,
    w_input,
    w_gate,
    forget_floor,
    head_gain,
    w_out,
    state,
    prev_forget,
    prev_input,
    accepted,
):
    planes, group = lax.axis_size("zy"), lax.axis_size("tp")
    seqs, proposals, features = tokens.shape
    _, size = w_query.shape
    swap = [(0, 1), (1, 0)]
    hops = [[(i, i ^ d) for i in range(group)] for d in range(group)]

    def passed(parts):
        return [parts[0]] + [lax.ppermute(parts[d], "tp", hops[d]) for d in (1, 2, 3)]

    gain = input_norm_gain.reshape(-1, size)
    inputs = passed([w_input] * group)
    own = lax.all_to_all(source(tokens.transpose(1, 2, 0), planes), ("zy", "tp"), 0, 0, tiled=True)
    own = own.reshape(planes, group * features, seqs)
    other = lax.ppermute(own, "core", swap)
    gates = passed([w_gate] * group)
    keyed = turn(gain, w_query, w_forget)
    mixing = fold(gain, inputs)
    new_state, rounded = advance(
        accepted,
        prev_forget,
        prev_input.reshape(seqs, proposals, -1).transpose(1, 2, 0),
        state[:, 0],
    )

    sends, rows, scale = project(own, other, keyed, mixing)
    received = passed(sends)
    shown = recur(received, rounded.reshape(-1, size), forget_floor[None], head_gain[None])
    parts = passed(shown)
    outward = turn_outward(w_out)
    opened = gate(gain, gates, rows, scale)
    sent = outward_half(away_kernel, parts, opened, outward)
    came = lax.ppermute(sent, "core", swap)
    kept = outward_half(keep_kernel, parts, opened, outward, came)
    terms = lax.all_to_all(
        kept.reshape(planes * group, features, seqs), ("zy", "tp"), 0, 0, tiled=True
    )
    mixed = sums(terms.reshape(planes, group, features, seqs))
    return mixed.transpose(2, 0, 1), new_state[:, None]


def solution(mesh):
    kv, tp = mesh.shape["kv"], mesh.shape["tp"]
    finer = Mesh(mesh.devices.reshape(kv // 2, 2, tp), ("zy", "core", "tp"))
    rows = ("zy", "core")
    placed = (
        P(None, None, (*rows, "tp")),
        P(),
        P(None, rows),
        P(None, rows),
        P(rows, "tp", None),
        P(rows, "tp", None),
        P(rows),
        P("tp"),
        P(rows, None),
        P(None, rows, "tp", None),
        P(None, None, rows),
        P(None, None, rows, "tp"),
        P(),
    )

    return jax.shard_map(
        body,
        mesh=finer,
        in_specs=placed,
        out_specs=(P(None, None, (*rows, "tp")), P(None, rows, "tp", None)),
        check_vma=False,
    )
```

time: 96.8 us -> 92.3 us (0.954)
  blocking collectives: 38.2 us -> 43.3 us
  local copies, waits for them, and re-layouts: 5.69 us -> 2 us
  waiting for transfers between devices: 19.9 us -> 17.2 us
  Pallas kernels: 12.5 us -> 10.9 us
  starting transfers between devices: 19.2 us -> 17.8 us
    all_to_all x1, blocking collectives: 20.4 us -> 24.9 us  [body(): lax.all_to_all(source(tokens.transpose(1, 2, 0), planes), ('zy', 'tp'), 0...]
    unnamed x16 -> x26, local copies, waits for them, and re-layouts: 5.69 us -> 2 us
    ppermute x12, waiting for transfers between devices: 18 us -> 15.3 us  [passed(): lax.ppermute(parts[d], 'tp', hops[d])]
    pallas_call x1, Pallas kernels: 4.98 us -> 3.12 us  [advance(): pl.pallas_call(advance_kernel, grid=(seqs // count,), in_specs=[pl.BlockS...]
    ppermute x12, starting transfers between devices: 19.1 us -> 17.7 us  [passed(): lax.ppermute(parts[d], 'tp', hops[d])]
    pallas_call x4 -> x5, Pallas kernels: 4.11 us -> 4.36 us  [the longest x1 1.71 us: source(): call(source_kernel, shaped((planes * steps, features, seqs), jnp.bfloat16...]
  transfers between devices with their start and end apart: 14 -> 14, of which waited for: 10 -> 6; matrix products, arithmetic and copies ran while one was open for 0% -> 0% of each run, Pallas kernels for 7% -> 9%
where the time goes in v1:
time: 92.3 us; the launch traced here: 92 us
  blocking collectives  43.3 us (47%)
  starting transfers between devices  17.8 us (19%)
  waiting for transfers between devices  17.2 us (19%)
  Pallas kernels  10.9 us (12%)
  local copies, waits for them, and re-layouts  2 us (2%)
    all_to_all x1, blocking collectives, body(): lax.all_to_all(source(tokens.transpose(1, 2, 0), planes), ('zy', 'tp'), 0...  24.9 us
    all_to_all x1, blocking collectives, body(): lax.all_to_all(kept.reshape(planes * group, features, seqs), ('zy', 'tp')...  18.5 us
    ppermute x12, starting transfers between devices, passed(): lax.ppermute(parts[d], 'tp', hops[d])  17.7 us
    ppermute x12, waiting for transfers between devices, passed(): lax.ppermute(parts[d], 'tp', hops[d])  15.3 us
    pallas_call x1, Pallas kernels, advance(): pl.pallas_call(advance_kernel, grid=(seqs // count,), in_specs=[pl.BlockS...  3.12 us
    unnamed x26, local copies, waits for them, and re-layouts  2 us
    ppermute x1, waiting for transfers between devices, body(): came = lax.ppermute(sent, 'core', swap)  1.9 us
  transfers between devices with their start and end apart: 14, of which 6 were waited for; matrix products, arithmetic and copies ran while one was open for 0% of the time, Pallas kernels for 9%

profile of v1, /device:TPU:0, one launch (start us, length us, event | category | flops | bytes accessed | tf_op | source)
XLA Modules:
  0.0 92.0 jit_solution(3725216651220662916)
XLA Ops:
  0.6 1.7 %shard_map.140 = bf16[64,32,128]{2,1,0:T(8,128)(2,1)} custom-call(bf16[4,32,128]{2,1,0:T(8,128)(2,1)} %bitcast.30), custom_call_target="tpu_custom_call" | custom-call | flops 1000000 | bytes 1048576 | tf_op jit(solution)/shard_map/pallas_call | solution.py:104
  2.3 24.9 %all_to_all.10 = bf16[64,32,128]{2,1,0:T(8,128)(2,1)S(1)} all-to-all(bf16[64,32,128]{2,1,0:T(8,128)(2,1)} %shard_map.140), channel_id=1, replica_groups=mesh['zy'=16,'core'=2,'tp'=4] {'zy','tp'}, dimensions={0} | all-to-all | bytes 1048576 | tf_op jit(solution)/shard_map/all_to_all | solution.py:406
  27.2 0.6 collective-permute-start.1
  27.8 1.8 %collective-permute-start.2 = (bf16[1,32,4096]{2,1,0:T(8,128)(2,1)}, bf16[1,32,4096]{2,1,0:T(8,128)(2,1)S(1)}, u32[]{:S(2)}, u32[]{:S(2)}) collective-permute-start(bf16[1,32,4096]{2,1,0:T(8,128)(2,1)} %w0.2), channel_id=1, source_target_pairs={{0,2},{1,3},{2,0},{3,1},{4,6},{5,7},{6,4},{7,5},{8,10},{9,11},{10,... | collective-permute-start | bytes 786440 | tf_op jit(solution)/shard_map/ppermute | solution.py:402
  29.6 2.3 %collective-permute-start.3 = (bf16[1,32,4096]{2,1,0:T(8,128)(2,1)}, bf16[1,32,4096]{2,1,0:T(8,128)(2,1)S(1)}, u32[]{:S(2)}, u32[]{:S(2)}) collective-permute-start(bf16[1,32,4096]{2,1,0:T(8,128)(2,1)} %w0.2), channel_id=1, source_target_pairs={{0,3},{1,2},{2,1},{3,0},{4,7},{5,6},{6,5},{7,4},{8,11},{9,10},{10,... | collective-permute-start | bytes 786440 | tf_op jit(solution)/shard_map/ppermute | solution.py:402
  31.9 1.2 %copy-done.1 = bf16[4096,128]{1,0:T(8,128)(2,1)S(1)} copy-done((bf16[4096,128]{1,0:T(8,128)(2,1)S(1)}, bf16[4096,128]{1,0:T(8,128)(2,1)}, u32[]{:S(2)}) %copy-start.1) | copy-done | bytes 1048600
  33.2 0.7 copy-done.2
  33.9 0.7 shard_map.141.keyed
  34.6 2.1 %collective-permute-done.1.w1 = bf16[1,32,4096]{2,1,0:T(8,128)(2,1)S(1)} collective-permute-done((bf16[1,32,4096]{2,1,0:T(8,128)(2,1)}, bf16[1,32,4096]{2,1,0:T(8,128)(2,1)S(1)}, u32[]{:S(2)}, u32[]{:S(2)}) %collective-permute-start.1) | collective-permute-done | bytes 262176 | tf_op jit(solution)/shard_map/ppermute | solution.py:402
  36.6 1.2 %collective-permute-start.11 = (bf16[1,32,4096]{2,1,0:T(8,128)(2,1)S(1)}, bf16[1,32,4096]{2,1,0:T(8,128)(2,1)S(1)}, u32[]{:S(2)}, u32[]{:S(2)}) collective-permute-start(bf16[1,32,4096]{2,1,0:T(8,128)(2,1)S(1)} %copy-done.8), channel_id=1, source_target_pairs={{0,2},{1,3},{2,0},{3,1},{4,6},{5,7},{6,4},{7,5},{8,10},{9,11},{10,... | collective-permute-start | bytes 786440 | tf_op jit(solution)/shard_map/ppermute | solution.py:402
  37.8 4.8 %collective-permute-done.2.w2 = bf16[1,32,4096]{2,1,0:T(8,128)(2,1)S(1)} collective-permute-done((bf16[1,32,4096]{2,1,0:T(8,128)(2,1)}, bf16[1,32,4096]{2,1,0:T(8,128)(2,1)S(1)}, u32[]{:S(2)}, u32[]{:S(2)}) %collective-permute-start.2) | collective-permute-done | bytes 262176 | tf_op jit(solution)/shard_map/ppermute | solution.py:402
  42.6 2.3 %collective-permute-start.12 = (bf16[1,32,4096]{2,1,0:T(8,128)(2,1)S(1)}, bf16[1,32,4096]{2,1,0:T(8,128)(2,1)S(1)}, u32[]{:S(2)}, u32[]{:S(2)}) collective-permute-start(bf16[1,32,4096]{2,1,0:T(8,128)(2,1)S(1)} %copy-done.8), channel_id=1, source_target_pairs={{0,3},{1,2},{2,1},{3,0},{4,7},{5,6},{6,5},{7,4},{8,11},{9,10},{10,... | collective-permute-start | bytes 786440 | tf_op jit(solution)/shard_map/ppermute | solution.py:402
  45.0 0.3 shard_map.142.mixing
  45.3 1.2 %shard_map.143 = (bf16[288,128]{1,0:T(8,128)(2,1)S(1)}, bf16[288,128]{1,0:T(8,128)(2,1)S(1)}, bf16[288,128]{1,0:T(8,128)(2,1)S(1)}, bf16[288,128]{1,0:T(8,128)(2...) custom-call(bf16[16,128,128]{2,1,0:T(8,128)(2,1)S(1)} %bitcast.20, ...), custom_call_target="tpu_custom_call" | custom-call | flops 1000000000 | bytes 3145728 | tf_op jit(solution)/shard_map/pallas_call | solution.py:187
  46.5 0.1 collective-permute-start.4
  46.6 0.7 shard_map.146.outward
  47.3 3.7 %collective-permute-start.5 = (bf16[288,128]{1,0:T(8,128)(2,1)S(1)}, bf16[288,128]{1,0:T(8,128)(2,1)S(1)}, u32[]{:S(2)}, u32[]{:S(2)}) collective-permute-start(bf16[288,128]{1,0:T(8,128)(2,1)S(1)} %get-tuple-element.16), channel_id=1, source_target_pairs={{0,2},{1,3},{2,0},{3,1},{4,6},{5,7},{6,4},{7,5},{8,10},{9,11},{10,... | collective-permute-start | bytes 221192 | tf_op jit(solution)/shard_map/ppermute | solution.py:402
  51.0 4.2 %collective-permute-done.4.r1 = bf16[288,128]{1,0:T(8,128)(2,1)S(1)} collective-permute-done((bf16[288,128]{1,0:T(8,128)(2,1)S(1)}, bf16[288,128]{1,0:T(8,128)(2,1)S(1)}, u32[]{:S(2)}, u32[]{:S(2)}) %collective-permute-start.4) | collective-permute-done | bytes 73760 | tf_op jit(solution)/shard_map/ppermute | solution.py:402
  55.2 0.9 collective-permute-start.6
  56.1 3.1 %advance.1 = (f32[128,32,128]{2,1,0:T(8,128)}, bf16[128,32,128]{2,1,0:T(8,128)(2,1)S(1)}) custom-call(s32[1,128]{1,0:T(1,128)S(1)} %bitcast.26, f32[128,4,128]{2,1,0:T(4,128)S(1)} %copy-done.7, bf16[4,32,128]{2,1,0:T(8,128)(2,1)S(1)} %bitcast.25, f32[128,32,128]{2,1,0:T(8,128)S(1)} %bitcast.24), custom_call_target="tpu_custom_call" | custom-call | flops 1000000000 | bytes 5242880 | tf_op jit(solution)/shard_map/advance/pallas_call | solution.py:65
  59.2 1.5 %collective-permute-done.6.r3 = bf16[288,128]{1,0:T(8,128)(2,1)S(1)} collective-permute-done((bf16[288,128]{1,0:T(8,128)(2,1)S(1)}, bf16[288,128]{1,0:T(8,128)(2,1)S(1)}, u32[]{:S(2)}, u32[]{:S(2)}) %collective-permute-start.6) | collective-permute-done | bytes 73760 | tf_op jit(solution)/shard_map/ppermute | solution.py:402
  60.7 1.4 %shard_map.144 = (bf16[48,128]{1,0:T(8,128)(2,1)S(1)}, bf16[48,128]{1,0:T(8,128)(2,1)S(1)}, bf16[48,128]{1,0:T(8,128)(2,1)S(1)}, bf16[48,128]{1,0:T(8,128)(2,1)S(1)}) custom-call(bf16[288,128]{1,0:T(8,128)(2,1)S(1)} %get-tuple-element.14.r0, bf16[288,128]{1,0:T(8,128)(2,1)S(1)} %collective-permute-done.4.r1, bf16[288,128]{1,0:T(8,128)(2,1)S(1)} %collective-permute-done.5.r2, ...), custom_call_target="tpu_custom_call" | custom-call | flops 1000000000 | bytes 2097152 | tf_op jit(solution)/shard_map/pallas_call | solution.py:305
  62.2 0.1 collective-permute-start.7
  62.2 3.1 %collective-permute-start.8 = (bf16[48,128]{1,0:T(8,128)(2,1)S(1)}, bf16[48,128]{1,0:T(8,128)(2,1)S(1)}, u32[]{:S(2)}, u32[]{:S(2)}) collective-permute-start(bf16[48,128]{1,0:T(8,128)(2,1)S(1)} %get-tuple-element.21), channel_id=1, source_target_pairs={{0,2},{1,3},{2,0},{3,1},{4,6},{5,7},{6,4},{7,5},{8,10},{9,11},{10,... | collective-permute-start | bytes 36872 | tf_op jit(solution)/shard_map/ppermute | solution.py:402
  65.3 1.6 %collective-permute-start.9 = (bf16[48,128]{1,0:T(8,128)(2,1)S(1)}, bf16[48,128]{1,0:T(8,128)(2,1)S(1)}, u32[]{:S(2)}, u32[]{:S(2)}) collective-permute-start(bf16[48,128]{1,0:T(8,128)(2,1)S(1)} %get-tuple-element.22), channel_id=1, source_target_pairs={{0,3},{1,2},{2,1},{3,0},{4,7},{5,6},{6,5},{7,4},{8,11},{9,10},{10,... | collective-permute-start | bytes 36872 | tf_op jit(solution)/shard_map/ppermute | solution.py:402
  66.9 0.6 shard_map.145.gates
  67.5 2.7 %collective-permute-done.9.p3 = bf16[48,128]{1,0:T(8,128)(2,1)S(1)} collective-permute-done((bf16[48,128]{1,0:T(8,128)(2,1)S(1)}, bf16[48,128]{1,0:T(8,128)(2,1)S(1)}, u32[]{:S(2)}, u32[]{:S(2)}) %collective-permute-start.9) | collective-permute-done | bytes 12320 | tf_op jit(solution)/shard_map/ppermute | solution.py:402
  70.2 0.3 shard_map.147
  70.7 1.9 %collective-permute-done.13.came = bf16[16,128,128]{2,1,0:T(8,128)(2,1)S(1)} collective-permute-done((bf16[16,128,128]{2,1,0:T(8,128)(2,1)S(1)}, bf16[16,128,128]{2,1,0:T(8,128)(2,1)S(1)}, u32[]{:S(2)}, u32[]{:S(2)}) %collective-permute-start.13) | collective-permute-done | bytes 524320 | tf_op jit(solution)/shard_map/ppermute | solution.py:426
  72.5 0.3 shard_map.148
  72.9 18.5 %all_to_all.11 = bf16[64,32,128]{2,1,0:T(8,128)(2,1)S(1)} all-to-all(bf16[64,32,128]{2,1,0:T(8,128)(2,1)S(1)} %bitcast.18), channel_id=1, replica_groups=mesh['zy'=16,'core'=2,'tp'=4] {'zy','tp'}, dimensions={0} | all-to-all | bytes 1048576 | tf_op jit(solution)/shard_map/all_to_all | solution.py:428
  91.3 0.7 shard_map.149
  (35 shorter events, 0.2 us)
Async XLA Ops:
  0.6 31.3 %copy-start = (bf16[4096,128]{1,0:T(8,128)(2,1)S(1)}, bf16[4096,128]{1,0:T(8,128)(2,1)}, u32[]{:S(2)}) copy-start(bf16[4096,128]{1,0:T(8,128)(2,1)} %w_query.1) | copy-start | bytes 3145732
  27.2 18.0 %collective-permute-start = (bf16[16,128,128]{2,1,0:T(8,128)(2,1)S(1)}, bf16[16,128,128]{2,1,0:T(8,128)(2,1)S(1)}, u32[]{:S(2)}, u32[]{:S(2)}) collective-permute-start(bf16[16,128,128]{2,1,0:T(8,128)(2,1)S(1)} %bitcast.19), channel_id=1, source_target_pairs={{0,4},{4,0},{1,5},{5,1},{2,6},{6,2},{3,7},{7,3},{8,12},{12,8},{9,1... | collective-permute-start | bytes 1572872 | tf_op jit(solution)/shard_map/ppermute | solution.py:408
  27.2 9.4 %collective-permute-start.1 = (bf16[1,32,4096]{2,1,0:T(8,128)(2,1)}, bf16[1,32,4096]{2,1,0:T(8,128)(2,1)S(1)}, u32[]{:S(2)}, u32[]{:S(2)}) collective-permute-start(bf16[1,32,4096]{2,1,0:T(8,128)(2,1)} %w0.2), channel_id=1, source_target_pairs={{0,1},{1,0},{2,3},{3,2},{4,5},{5,4},{6,7},{7,6},{8,9},{9,8},{10,11... | collective-permute-start | bytes 786440 | tf_op jit(solution)/shard_map/ppermute | solution.py:402
  27.8 14.8 %collective-permute-start.2 = (bf16[1,32,4096]{2,1,0:T(8,128)(2,1)}, bf16[1,32,4096]{2,1,0:T(8,128)(2,1)S(1)}, u32[]{:S(2)}, u32[]{:S(2)}) collective-permute-start(bf16[1,32,4096]{2,1,0:T(8,128)(2,1)} %w0.2), channel_id=1, source_target_pairs={{0,2},{1,3},{2,0},{3,1},{4,6},{5,7},{6,4},{7,5},{8,10},{9,11},{10,... | collective-permute-start | bytes 786440 | tf_op jit(solution)/shard_map/ppermute | solution.py:402
  29.6 15.4 %collective-permute-start.3 = (bf16[1,32,4096]{2,1,0:T(8,128)(2,1)}, bf16[1,32,4096]{2,1,0:T(8,128)(2,1)S(1)}, u32[]{:S(2)}, u32[]{:S(2)}) collective-permute-start(bf16[1,32,4096]{2,1,0:T(8,128)(2,1)} %w0.2), channel_id=1, source_target_pairs={{0,3},{1,2},{2,1},{3,0},{4,7},{5,6},{6,5},{7,4},{8,11},{9,10},{10,... | collective-permute-start | bytes 786440 | tf_op jit(solution)/shard_map/ppermute | solution.py:402
  31.9 33.4 %collective-permute-start.10 = (bf16[1,32,4096]{2,1,0:T(8,128)(2,1)}, bf16[1,32,4096]{2,1,0:T(8,128)(2,1)S(1)}, u32[]{:S(2)}, u32[]{:S(2)}) collective-permute-start(bf16[1,32,4096]{2,1,0:T(8,128)(2,1)} %w0.3), channel_id=1, source_target_pairs={{0,1},{1,0},{2,3},{3,2},{4,5},{5,4},{6,7},{7,6},{8,9},{9,8},{10,11... | collective-permute-start | bytes 786440 | tf_op jit(solution)/shard_map/ppermute | solution.py:402
  31.9 1.2 %copy-start.1 = (bf16[4096,128]{1,0:T(8,128)(2,1)S(1)}, bf16[4096,128]{1,0:T(8,128)(2,1)}, u32[]{:S(2)}) copy-start(bf16[4096,128]{1,0:T(8,128)(2,1)} %w_forget.1) | copy-start | bytes 3145732
  33.2 0.7 copy-start.2
  33.9 2.7 %copy-start.8 = (bf16[1,32,4096]{2,1,0:T(8,128)(2,1)S(1)}, bf16[1,32,4096]{2,1,0:T(8,128)(2,1)}, u32[]{:S(2)}) copy-start(bf16[1,32,4096]{2,1,0:T(8,128)(2,1)} %w0.3) | copy-start | bytes 786436
  33.9 11.1 %copy-start.6 = (bf16[1,32,4096]{2,1,0:T(8,128)(2,1)S(1)}, bf16[1,32,4096]{2,1,0:T(8,128)(2,1)}, u32[]{:S(2)}) copy-start(bf16[1,32,4096]{2,1,0:T(8,128)(2,1)} %w0.2) | copy-start | bytes 786436
  36.6 30.3 %collective-permute-start.11 = (bf16[1,32,4096]{2,1,0:T(8,128)(2,1)S(1)}, bf16[1,32,4096]{2,1,0:T(8,128)(2,1)S(1)}, u32[]{:S(2)}, u32[]{:S(2)}) collective-permute-start(bf16[1,32,4096]{2,1,0:T(8,128)(2,1)S(1)} %copy-done.8), channel_id=1, source_target_pairs={{0,2},{1,3},{2,0},{3,1},{4,6},{5,7},{6,4},{7,5},{8,10},{9,11},{10,... | collective-permute-start | bytes 786440 | tf_op jit(solution)/shard_map/ppermute | solution.py:402
  42.6 24.3 %collective-permute-start.12 = (bf16[1,32,4096]{2,1,0:T(8,128)(2,1)S(1)}, bf16[1,32,4096]{2,1,0:T(8,128)(2,1)S(1)}, u32[]{:S(2)}, u32[]{:S(2)}) collective-permute-start(bf16[1,32,4096]{2,1,0:T(8,128)(2,1)S(1)} %copy-done.8), channel_id=1, source_target_pairs={{0,3},{1,2},{2,1},{3,0},{4,7},{5,6},{6,5},{7,4},{8,11},{9,10},{10,... | collective-permute-start | bytes 786440 | tf_op jit(solution)/shard_map/ppermute | solution.py:402
  45.3 1.3 %copy-start.5 = (bf16[128,4096]{1,0:T(8,128)(2,1)S(1)}, bf16[128,4096]{1,0:T(8,128)(2,1)}, u32[]{:S(2)}) copy-start(bf16[128,4096]{1,0:T(8,128)(2,1)} %w_out.1) | copy-start | bytes 3145732
  46.4 9.6 %copy-start.4 = (f32[128,1,32,128]{3,2,1,0:T(8,128)S(1)}, f32[128,1,32,128]{3,2,1,0:T(8,128)}, u32[]{:S(2)}) copy-start(f32[128,1,32,128]{3,2,1,0:T(8,128)} %param.22) | copy-start | bytes 6291460
  46.5 9.6 %copy-start.7 = (f32[128,4,128]{2,1,0:T(4,128)S(1)}, f32[128,4,128]{2,1,0:T(4,128)}, u32[]{:S(2)}) copy-start(f32[128,4,128]{2,1,0:T(4,128)} %prev_forget.1) | copy-start | bytes 786436
  46.5 9.6 %copy-start.9 = (bf16[128,4,1,32]{0,3,2,1:T(8,128)(2,1)S(1)}, bf16[128,4,1,32]{0,3,2,1:T(8,128)(2,1)}, u32[]{:S(2)}) copy-start(bf16[128,4,1,32]{0,3,2,1:T(8,128)(2,1)} %param.24) | copy-start | bytes 98308
  46.5 9.6 %copy-start.10 = (s32[128]{0:T(128)S(1)}, s32[128]{0:T(128)}, u32[]{:S(2)}) copy-start(s32[128]{0:T(128)} %param.25) | copy-start | bytes 1540
  46.5 8.7 %collective-permute-start.4 = (bf16[288,128]{1,0:T(8,128)(2,1)S(1)}, bf16[288,128]{1,0:T(8,128)(2,1)S(1)}, u32[]{:S(2)}, u32[]{:S(2)}) collective-permute-start(bf16[288,128]{1,0:T(8,128)(2,1)S(1)} %get-tuple-element.15), channel_id=1, source_target_pairs={{0,1},{1,0},{2,3},{3,2},{4,5},{5,4},{6,7},{7,6},{8,9},{9,8},{10,11... | collective-permute-start | bytes 221192 | tf_op jit(solution)/shard_map/ppermute | solution.py:402
  47.3 13.4 %copy-start.11 = (f32[128]{0:T(128)S(1)}, f32[128]{0:T(128)}, u32[]{:S(2)}) copy-start(f32[128]{0:T(128)} %param.19) | copy-start | bytes 1540
  47.3 13.4 %copy-start.12 = (f32[32]{0:T(128)S(1)}, f32[32]{0:T(128)}, u32[]{:S(2)}) copy-start(f32[32]{0:T(128)} %param.20) | copy-start | bytes 388
  47.3 11.9 %collective-permute-start.5 = (bf16[288,128]{1,0:T(8,128)(2,1)S(1)}, bf16[288,128]{1,0:T(8,128)(2,1)S(1)}, u32[]{:S(2)}, u32[]{:S(2)}) collective-permute-start(bf16[288,128]{1,0:T(8,128)(2,1)S(1)} %get-tuple-element.16), channel_id=1, source_target_pairs={{0,2},{1,3},{2,0},{3,1},{4,6},{5,7},{6,4},{7,5},{8,10},{9,11},{10,... | collective-permute-start | bytes 221192 | tf_op jit(solution)/shard_map/ppermute | solution.py:402
  55.2 5.6 %collective-permute-start.6 = (bf16[288,128]{1,0:T(8,128)(2,1)S(1)}, bf16[288,128]{1,0:T(8,128)(2,1)S(1)}, u32[]{:S(2)}, u32[]{:S(2)}) collective-permute-start(bf16[288,128]{1,0:T(8,128)(2,1)S(1)} %get-tuple-element.17), channel_id=1, source_target_pairs={{0,3},{1,2},{2,1},{3,0},{4,7},{5,6},{6,5},{7,4},{8,11},{9,10},{10,... | collective-permute-start | bytes 221192 | tf_op jit(solution)/shard_map/ppermute | solution.py:402
  59.2 7.8 %copy-start.3 = (f32[4096]{0:T(1024)S(1)}, f32[4096]{0:T(1024)}, u32[]{:S(2)}) copy-start(f32[4096]{0:T(1024)} %param.14) | copy-start | bytes 49156
  62.2 5.4 %collective-permute-start.7 = (bf16[48,128]{1,0:T(8,128)(2,1)S(1)}, bf16[48,128]{1,0:T(8,128)(2,1)S(1)}, u32[]{:S(2)}, u32[]{:S(2)}) collective-permute-start(bf16[48,128]{1,0:T(8,128)(2,1)S(1)} %get-tuple-element.20), channel_id=1, source_target_pairs={{0,1},{1,0},{2,3},{3,2},{4,5},{5,4},{6,7},{7,6},{8,9},{9,8},{10,11... | collective-permute-start | bytes 36872 | tf_op jit(solution)/shard_map/ppermute | solution.py:402
  62.2 5.3 %collective-permute-start.8 = (bf16[48,128]{1,0:T(8,128)(2,1)S(1)}, bf16[48,128]{1,0:T(8,128)(2,1)S(1)}, u32[]{:S(2)}, u32[]{:S(2)}) collective-permute-start(bf16[48,128]{1,0:T(8,128)(2,1)S(1)} %get-tuple-element.21), channel_id=1, source_target_pairs={{0,2},{1,3},{2,0},{3,1},{4,6},{5,7},{6,4},{7,5},{8,10},{9,11},{10,... | collective-permute-start | bytes 36872 | tf_op jit(solution)/shard_map/ppermute | solution.py:402
  65.3 4.9 %collective-permute-start.9 = (bf16[48,128]{1,0:T(8,128)(2,1)S(1)}, bf16[48,128]{1,0:T(8,128)(2,1)S(1)}, u32[]{:S(2)}, u32[]{:S(2)}) collective-permute-start(bf16[48,128]{1,0:T(8,128)(2,1)S(1)} %get-tuple-element.22), channel_id=1, source_target_pairs={{0,3},{1,2},{2,1},{3,0},{4,7},{5,6},{6,5},{7,4},{8,11},{9,10},{10,... | collective-permute-start | bytes 36872 | tf_op jit(solution)/shard_map/ppermute | solution.py:402
  70.6 2.0 %collective-permute-start.13 = (bf16[16,128,128]{2,1,0:T(8,128)(2,1)S(1)}, bf16[16,128,128]{2,1,0:T(8,128)(2,1)S(1)}, u32[]{:S(2)}, u32[]{:S(2)}) collective-permute-start(bf16[16,128,128]{2,1,0:T(8,128)(2,1)S(1)} %shard_map.147), channel_id=1, source_target_pairs={{0,4},{4,0},{1,5},{5,1},{2,6},{6,2},{3,7},{7,3},{8,12},{12,8},{9,1... | collective-permute-start | bytes 1572872 | tf_op jit(solution)/shard_map/ppermute | solution.py:426

commit v2 on v1

--- a/solution.py
+++ b/solution.py
@@ -112,114 +112,91 @@
     )(tokens)
 
 
-def turn_kernel(gain, w_query, w_forget, keyed):
-    size = gain.shape[1]
-    for b in range(w_query.shape[0] // size):
-        at = pl.ds(b * size, size)
-        row = gain[pl.ds(b, 1), :]
-        for i, weight in enumerate((w_query, w_forget)):
-            block = weight[at, :].astype(jnp.float32).T
-            keyed[pl.ds(i * size, size), at] = (block * row).astype(jnp.bfloat16)
-
-
-def turn(gain, w_query, w_forget):
+def join_kernel(w_query, w_forget, joined):
+    size = w_query.shape[1]
+    joined[:, pl.ds(0, size)] = w_query[...]
+    joined[:, pl.ds(size, size)] = w_forget[...]
+
+
+def join(w_query, w_forget):
     width, size = w_query.shape
     return call(
-        turn_kernel,
-        shaped((2 * size, width), jnp.bfloat16),
+        join_kernel,
+        shaped((width, 2 * size), jnp.bfloat16),
         [],
         (1_000_000_000, 4 << 20),
         16 << 20,
-        [whole()] * 3,
-        whole(),
-    )(gain, w_query, w_forget)
-
-
-def fold_kernel(gain, w0, w1, w2, w3, out):
-    values, size = w0.shape[1], gain.shape[1]
-    for b in range(gain.shape[0]):
-        at = pl.ds(b * size, size)
-        for d, weight in enumerate((w0, w1, w2, w3)):
-            value = weight[0, :, at].astype(jnp.float32) * gain[pl.ds(b, 1), :]
-            out[pl.ds(d * values, values), at] = value.astype(jnp.bfloat16)
-
-
-def fold(gain, weights):
-    _, values, width = weights[0].shape
-    return call(
-        fold_kernel,
-        shaped((4 * values, width), jnp.bfloat16),
-        [],
-        (1_000_000_000, 2 << 20),
-        16 << 20,
-        [whole()] * 5,
-        whole(),
-    )(gain, *weights)
-
-
-def project_kernel(own, other, keyed, mixing, o0, o1, o2, o3, held, scale):
+        [whole()] * 2,
+        whole(),
+    )(w_query, w_forget)
+
+
+def across(left, right):
+    return lax.dot_general(
+        left, right, (((1,), (1,)), ((), ())), preferred_element_type=jnp.float32
+    )
+
+
+def project_kernel(own, other, gain, joined, w0, w1, w2, w3, o0, o1, o2, o3, rows, scale):
     core = lax.axis_index("core")
     blocks, size, seqs = own.shape
     squares = jnp.zeros((8, seqs), jnp.float32)
     for half, ref in ((core, own), (1 - core, other)):
         for b in range(blocks):
-            part = ref[b]
-            held[pl.ds(pl.multiple_of((2 * b + half) * size, size), size), :] = part
-            wide = part.astype(jnp.float32)
+            wide = ref[b].astype(jnp.float32)
             squares = squares + jnp.sum((wide * wide).reshape(size // 8, 8, seqs), axis=0)
+            row = 2 * b + half
+            at = pl.ds(pl.multiple_of(row * size, size), size)
+            rows[:, at] = (wide.T * gain[pl.ds(row, 1), :]).astype(jnp.bfloat16)
     total = jnp.sum(squares, axis=0, keepdims=True)
     factor = lax.rsqrt(total / (2 * blocks * size) + NORM_EPSILON)
     scale[...] = jnp.broadcast_to(factor, scale.shape)
-    rows = held[...]
-    first = jnp.dot(keyed[...], rows, preferred_element_type=jnp.float32) * factor
-    first = first.astype(jnp.bfloat16)
-    second = jnp.dot(mixing[...], rows, preferred_element_type=jnp.float32) * factor
-    second = second.astype(jnp.bfloat16)
-    keys, values = first.shape[0], second.shape[0] // 4
-    for d, out in enumerate((o0, o1, o2, o3)):
-        out[pl.ds(0, keys), :] = first
-        out[pl.ds(keys, values), :] = second[d * values : (d + 1) * values]
-
-
-def project(own, other, keyed, mixing):
+    first = jnp.dot(rows[...], joined[...], preferred_element_type=jnp.float32)
+    keys, values = first.shape[1], w0.shape[1]
+    for i in range(keys // size):
+        part = (first[:, i * size : (i + 1) * size].T * factor).astype(jnp.bfloat16)
+        for out in (o0, o1, o2, o3):
+            out[pl.ds(i * size, size), :] = part
+    for weight, out in ((w0, o0), (w1, o1), (w2, o2), (w3, o3)):
+        second = across(weight[0], rows[...]) * factor
+        out[pl.ds(keys, values), :] = second.astype(jnp.bfloat16)
+
+
+def project(own, other, gain, joined, weights):
     blocks, size, seqs = own.shape
-    rows = keyed.shape[0] + mixing.shape[0] // 4
+    height = joined.shape[1] + weights[0].shape[1]
     outs = call(
         project_kernel,
-        [shaped((rows, seqs), jnp.bfloat16)] * 4
-        + [shaped((2 * blocks * size, seqs), jnp.bfloat16), shaped((8, seqs), jnp.float32)],
+        [shaped((height, seqs), jnp.bfloat16)] * 4
+        + [shaped((seqs, 2 * blocks * size), jnp.bfloat16), shaped((8, seqs), jnp.float32)],
         [],
         (1_000_000_000, 3 << 20),
         16 << 20,
-        [whole()] * 4,
+        [whole()] * 8,
         [whole()] * 6,
-    )(own, other, keyed, mixing)
+    )(own, other, gain, joined, *weights)
     return outs[:4], outs[4], outs[5]
 
 
-def gate_kernel(gain, w0, w1, w2, w3, rows, scale, out, held):
-    values, size = w0.shape[1], gain.shape[1]
-    for b in range(gain.shape[0]):
-        at = pl.ds(b * size, size)
-        for d, weight in enumerate((w0, w1, w2, w3)):
-            value = weight[0, :, at].astype(jnp.float32) * gain[pl.ds(b, 1), :]
-            held[pl.ds(d * values, values), at] = value.astype(jnp.bfloat16)
-    raw = jnp.dot(held[...], rows[...], preferred_element_type=jnp.float32) * scale[0:1]
-    raw = raw.astype(jnp.bfloat16).astype(jnp.float32)
-    out[...] = raw * jax.nn.sigmoid(raw)
-
-
-def gate(gain, weights, rows, scale):
-    _, values, width = weights[0].shape
+def gate_kernel(w0, w1, w2, w3, rows, scale, out):
+    values = w0.shape[1]
+    for d, weight in enumerate((w0, w1, w2, w3)):
+        raw = across(weight[0], rows[...]) * scale[0:1]
+        raw = raw.astype(jnp.bfloat16).astype(jnp.float32)
+        out[pl.ds(d * values, values), :] = raw * jax.nn.sigmoid(raw)
+
+
+def gate(weights, rows, scale):
+    values = weights[0].shape[1]
     return call(
         gate_kernel,
-        shaped((4 * values, rows.shape[1]), jnp.float32),
-        [pltpu.VMEM((4 * values, width), jnp.bfloat16)],
+        shaped((4 * values, rows.shape[0]), jnp.float32),
+        [],
         (1_000_000_000, 3 << 20),
         16 << 20,
-        [whole()] * 7,
-        whole(),
-    )(gain, *weights, rows, scale)
+        [whole()] * 6,
+        whole(),
+    )(*weights, rows, scale)
 
 
 def outward_kernel(w_out, outward, held, sems):
@@ -402,13 +379,12 @@
         return [parts[0]] + [lax.ppermute(parts[d], "tp", hops[d]) for d in (1, 2, 3)]
 
     gain = input_norm_gain.reshape(-1, size)
-    inputs = passed([w_input] * group)
     own = lax.all_to_all(source(tokens.transpose(1, 2, 0), planes), ("zy", "tp"), 0, 0, tiled=True)
     own = own.reshape(planes, group * features, seqs)
     other = lax.ppermute(own, "core", swap)
+    inputs = passed([w_input] * group)
     gates = passed([w_gate] * group)
-    keyed = turn(gain, w_query, w_forget)
-    mixing = fold(gain, inputs)
+    joined = join(w_query, w_forget)
     new_state, rounded = advance(
         accepted,
         prev_forget,
@@ -416,12 +392,12 @@
         state[:, 0],
     )
 
-    sends, rows, scale = project(own, other, keyed, mixing)
+    sends, rows, scale = project(own, other, gain, joined, inputs)
     received = passed(sends)
     shown = recur(received, rounded.reshape(-1, size), forget_floor[None], head_gain[None])
     parts = passed(shown)
     outward = turn_outward(w_out)
-    opened = gate(gain, gates, rows, scale)
+    opened = gate(gates, rows, scale)
     sent = outward_half(away_kernel, parts, opened, outward)
     came = lax.ppermute(sent, "core", swap)
     kept = outward_half(keep_kernel, parts, opened, outward, came)

time: 92.3 us -> 92.4 us (level)
  Pallas kernels: 10.9 us -> 12.3 us
    pallas_call x4 -> x3, Pallas kernels: 2.65 us -> 4.06 us  [the longest x1 2.26 us: project(): call(project_kernel, [shaped((height, seqs), jnp.bfloat16)] * 4 + [shaped...]
    unnamed x26 -> x24, local copies, waits for them, and re-layouts: 2 us -> 1.29 us
  transfers between devices with their start and end apart: 14 -> 14, of which waited for: 6 -> 6; matrix products, arithmetic and copies ran while one was open for 0% -> 0% of each run, Pallas kernels for 9% -> 10%
where the time goes in v2:
time: 92.4 us; the launch traced here: 92.1 us
  blocking collectives  43.5 us (47%)
  starting transfers between devices  17.7 us (19%)
  waiting for transfers between devices  16.5 us (18%)
  Pallas kernels  12.3 us (13%)
  local copies, waits for them, and re-layouts  1.29 us (1%)
    all_to_all x1, blocking collectives, body(): lax.all_to_all(source(tokens.transpose(1, 2, 0), planes), ('zy', 'tp'), 0...  25 us
    all_to_all x1, blocking collectives, body(): lax.all_to_all(kept.reshape(planes * group, features, seqs), ('zy', 'tp')...  18.4 us
    ppermute x12, starting transfers between devices, passed(): lax.ppermute(parts[d], 'tp', hops[d])  17.7 us
    ppermute x12, waiting for transfers between devices, passed(): lax.ppermute(parts[d], 'tp', hops[d])  14.6 us
    pallas_call x1, Pallas kernels, advance(): pl.pallas_call(advance_kernel, grid=(seqs // count,), in_specs=[pl.BlockS...  3.12 us
    pallas_call x1, Pallas kernels, project(): call(project_kernel, [shaped((height, seqs), jnp.bfloat16)] * 4 + [shaped...  2.26 us
    ppermute x1, waiting for transfers between devices, body(): came = lax.ppermute(sent, 'core', swap)  1.9 us
  transfers between devices with their start and end apart: 14, of which 6 were waited for; matrix products, arithmetic and copies ran while one was open for 0% of the time, Pallas kernels for 10%

profile of v2, /device:TPU:0, one launch (start us, length us, event | category | flops | bytes accessed | tf_op | source)
XLA Modules:
  0.0 92.1 jit_solution(14479978975378355270)
XLA Ops:
  0.6 1.7 %shard_map.140 = bf16[64,32,128]{2,1,0:T(8,128)(2,1)} custom-call(bf16[4,32,128]{2,1,0:T(8,128)(2,1)} %bitcast.28), custom_call_target="tpu_custom_call" | custom-call | flops 1000000 | bytes 1048576 | tf_op jit(solution)/shard_map/pallas_call | solution.py:104
  2.4 25.0 %all_to_all.10 = bf16[64,32,128]{2,1,0:T(8,128)(2,1)S(1)} all-to-all(bf16[64,32,128]{2,1,0:T(8,128)(2,1)} %shard_map.140), channel_id=1, replica_groups=mesh['zy'=16,'core'=2,'tp'=4] {'zy','tp'}, dimensions={0} | all-to-all | bytes 1048576 | tf_op jit(solution)/shard_map/all_to_all | solution.py:382
  27.4 0.6 collective-permute-start.1
  27.9 1.8 %collective-permute-start.2 = (bf16[1,32,4096]{2,1,0:T(8,128)(2,1)}, bf16[1,32,4096]{2,1,0:T(8,128)(2,1)S(1)}, u32[]{:S(2)}, u32[]{:S(2)}) collective-permute-start(bf16[1,32,4096]{2,1,0:T(8,128)(2,1)} %w0.2), channel_id=1, source_target_pairs={{0,2},{1,3},{2,0},{3,1},{4,6},{5,7},{6,4},{7,5},{8,10},{9,11},{10,... | collective-permute-start | bytes 786440 | tf_op jit(solution)/shard_map/ppermute | solution.py:379
  29.7 2.3 %collective-permute-start.3 = (bf16[1,32,4096]{2,1,0:T(8,128)(2,1)}, bf16[1,32,4096]{2,1,0:T(8,128)(2,1)S(1)}, u32[]{:S(2)}, u32[]{:S(2)}) collective-permute-start(bf16[1,32,4096]{2,1,0:T(8,128)(2,1)} %w0.2), channel_id=1, source_target_pairs={{0,3},{1,2},{2,1},{3,0},{4,7},{5,6},{6,5},{7,4},{8,11},{9,10},{10,... | collective-permute-start | bytes 786440 | tf_op jit(solution)/shard_map/ppermute | solution.py:379
  32.1 1.2 %copy-done.1 = bf16[4096,128]{1,0:T(8,128)(2,1)S(1)} copy-done((bf16[4096,128]{1,0:T(8,128)(2,1)S(1)}, bf16[4096,128]{1,0:T(8,128)(2,1)}, u32[]{:S(2)}) %copy-start.1) | copy-done | bytes 1048600
  33.3 0.4 shard_map.141.joined
  33.7 3.1 %collective-permute-done.1.w1 = bf16[1,32,4096]{2,1,0:T(8,128)(2,1)S(1)} collective-permute-done((bf16[1,32,4096]{2,1,0:T(8,128)(2,1)}, bf16[1,32,4096]{2,1,0:T(8,128)(2,1)S(1)}, u32[]{:S(2)}, u32[]{:S(2)}) %collective-permute-start.1) | collective-permute-done | bytes 262176 | tf_op jit(solution)/shard_map/ppermute | solution.py:379
  36.8 1.2 %collective-permute-start.11 = (bf16[1,32,4096]{2,1,0:T(8,128)(2,1)S(1)}, bf16[1,32,4096]{2,1,0:T(8,128)(2,1)S(1)}, u32[]{:S(2)}, u32[]{:S(2)}) collective-permute-start(bf16[1,32,4096]{2,1,0:T(8,128)(2,1)S(1)} %copy-done.7), channel_id=1, source_target_pairs={{0,2},{1,3},{2,0},{3,1},{4,6},{5,7},{6,4},{7,5},{8,10},{9,11},{10,... | collective-permute-start | bytes 786440 | tf_op jit(solution)/shard_map/ppermute | solution.py:379
  38.0 4.8 %collective-permute-done.2.w2 = bf16[1,32,4096]{2,1,0:T(8,128)(2,1)S(1)} collective-permute-done((bf16[1,32,4096]{2,1,0:T(8,128)(2,1)}, bf16[1,32,4096]{2,1,0:T(8,128)(2,1)S(1)}, u32[]{:S(2)}, u32[]{:S(2)}) %collective-permute-start.2) | collective-permute-done | bytes 262176 | tf_op jit(solution)/shard_map/ppermute | solution.py:379
  42.8 2.3 %collective-permute-start.12 = (bf16[1,32,4096]{2,1,0:T(8,128)(2,1)S(1)}, bf16[1,32,4096]{2,1,0:T(8,128)(2,1)S(1)}, u32[]{:S(2)}, u32[]{:S(2)}) collective-permute-start(bf16[1,32,4096]{2,1,0:T(8,128)(2,1)S(1)} %copy-done.7), channel_id=1, source_target_pairs={{0,3},{1,2},{2,1},{3,0},{4,7},{5,6},{6,5},{7,4},{8,11},{9,10},{10,... | collective-permute-start | bytes 786440 | tf_op jit(solution)/shard_map/ppermute | solution.py:379
  45.1 2.3 %shard_map.142 = (bf16[288,128]{1,0:T(8,128)(2,1)S(1)}, bf16[288,128]{1,0:T(8,128)(2,1)S(1)}, bf16[288,128]{1,0:T(8,128)(2,1)S(1)}, bf16[288,128]{1,0:T(8,128)(2...) custom-call(bf16[16,128,128]{2,1,0:T(8,128)(2,1)S(1)} %bitcast.20, ...), custom_call_target="tpu_custom_call" | custom-call | flops 1000000000 | bytes 3145728 | tf_op jit(solution)/shard_map/pallas_call | solution.py:168
  47.4 0.0 copy-start.6
  47.4 0.1 collective-permute-start.4
  47.5 0.7 shard_map.145.outward
  48.2 3.7 %collective-permute-start.5 = (bf16[288,128]{1,0:T(8,128)(2,1)S(1)}, bf16[288,128]{1,0:T(8,128)(2,1)S(1)}, u32[]{:S(2)}, u32[]{:S(2)}) collective-permute-start(bf16[288,128]{1,0:T(8,128)(2,1)S(1)} %get-tuple-element.16), channel_id=1, source_target_pairs={{0,2},{1,3},{2,0},{3,1},{4,6},{5,7},{6,4},{7,5},{8,10},{9,11},{10,... | collective-permute-start | bytes 221192 | tf_op jit(solution)/shard_map/ppermute | solution.py:379
  51.9 3.4 %collective-permute-done.4.r1 = bf16[288,128]{1,0:T(8,128)(2,1)S(1)} collective-permute-done((bf16[288,128]{1,0:T(8,128)(2,1)S(1)}, bf16[288,128]{1,0:T(8,128)(2,1)S(1)}, u32[]{:S(2)}, u32[]{:S(2)}) %collective-permute-start.4) | collective-permute-done | bytes 73760 | tf_op jit(solution)/shard_map/ppermute | solution.py:379
  55.3 0.9 collective-permute-start.6
  56.2 3.1 %advance.1 = (f32[128,32,128]{2,1,0:T(8,128)}, bf16[128,32,128]{2,1,0:T(8,128)(2,1)S(1)}) custom-call(s32[1,128]{1,0:T(1,128)S(1)} %bitcast.24, f32[128,4,128]{2,1,0:T(4,128)S(1)} %copy-done.6, bf16[4,32,128]{2,1,0:T(8,128)(2,1)S(1)} %bitcast.23, f32[128,32,128]{2,1,0:T(8,128)S(1)} %bitcast.22), custom_call_target="tpu_custom_call" | custom-call | flops 1000000000 | bytes 5242880 | tf_op jit(solution)/shard_map/advance/pallas_call | solution.py:65
  59.3 1.5 %collective-permute-done.6.r3 = bf16[288,128]{1,0:T(8,128)(2,1)S(1)} collective-permute-done((bf16[288,128]{1,0:T(8,128)(2,1)S(1)}, bf16[288,128]{1,0:T(8,128)(2,1)S(1)}, u32[]{:S(2)}, u32[]{:S(2)}) %collective-permute-start.6) | collective-permute-done | bytes 73760 | tf_op jit(solution)/shard_map/ppermute | solution.py:379
  60.9 1.4 %shard_map.143 = (bf16[48,128]{1,0:T(8,128)(2,1)S(1)}, bf16[48,128]{1,0:T(8,128)(2,1)S(1)}, bf16[48,128]{1,0:T(8,128)(2,1)S(1)}, bf16[48,128]{1,0:T(8,128)(2,1)S(1)}) custom-call(bf16[288,128]{1,0:T(8,128)(2,1)S(1)} %get-tuple-element.14.r0, bf16[288,128]{1,0:T(8,128)(2,1)S(1)} %collective-permute-done.4.r1, bf16[288,128]{1,0:T(8,128)(2,1)S(1)} %collective-permute-done.5.r2, ...), custom_call_target="tpu_custom_call" | custom-call | flops 1000000000 | bytes 2097152 | tf_op jit(solution)/shard_map/pallas_call | solution.py:282
  62.3 0.1 collective-permute-start.7
  62.4 3.1 %collective-permute-start.8 = (bf16[48,128]{1,0:T(8,128)(2,1)S(1)}, bf16[48,128]{1,0:T(8,128)(2,1)S(1)}, u32[]{:S(2)}, u32[]{:S(2)}) collective-permute-start(bf16[48,128]{1,0:T(8,128)(2,1)S(1)} %get-tuple-element.21), channel_id=1, source_target_pairs={{0,2},{1,3},{2,0},{3,1},{4,6},{5,7},{6,4},{7,5},{8,10},{9,11},{10,... | collective-permute-start | bytes 36872 | tf_op jit(solution)/shard_map/ppermute | solution.py:379
  65.5 1.6 %collective-permute-start.9 = (bf16[48,128]{1,0:T(8,128)(2,1)S(1)}, bf16[48,128]{1,0:T(8,128)(2,1)S(1)}, u32[]{:S(2)}, u32[]{:S(2)}) collective-permute-start(bf16[48,128]{1,0:T(8,128)(2,1)S(1)} %get-tuple-element.22), channel_id=1, source_target_pairs={{0,3},{1,2},{2,1},{3,0},{4,7},{5,6},{6,5},{7,4},{8,11},{9,10},{10,... | collective-permute-start | bytes 36872 | tf_op jit(solution)/shard_map/ppermute | solution.py:379
  67.1 1.4 %shard_map.144.gates = f32[128,128]{1,0:T(8,128)S(1)} custom-call(bf16[1,32,4096]{2,1,0:T(8,128)(2,1)S(1)} %copy-done.7, bf16[1,32,4096]{2,1,0:T(8,128)(2,1)S(1)} %collective-permute-done.10.w1, bf16[1,32,4096]{2,1,0:T(8,128)(2,1)S(1)} %collective-permute-done.11.w2, bf16[1,32,4096]{2,1,0:T(8,128)(2,1)S(1)} %collective-permute-done.12.w3, ...), custom_call_target="tpu_custom_call" | custom-call | flops 1000000000 | bytes 3145728 | tf_op jit(solution)/shard_map/pallas_call | solution.py:191
  68.5 1.8 %collective-permute-done.9.p3 = bf16[48,128]{1,0:T(8,128)(2,1)S(1)} collective-permute-done((bf16[48,128]{1,0:T(8,128)(2,1)S(1)}, bf16[48,128]{1,0:T(8,128)(2,1)S(1)}, u32[]{:S(2)}, u32[]{:S(2)}) %collective-permute-start.9) | collective-permute-done | bytes 12320 | tf_op jit(solution)/shard_map/ppermute | solution.py:379
  70.4 0.3 shard_map.146
  70.7 0.1 collective-permute-start.13
  70.8 1.9 %collective-permute-done.13.came = bf16[16,128,128]{2,1,0:T(8,128)(2,1)S(1)} collective-permute-done((bf16[16,128,128]{2,1,0:T(8,128)(2,1)S(1)}, bf16[16,128,128]{2,1,0:T(8,128)(2,1)S(1)}, u32[]{:S(2)}, u32[]{:S(2)}) %collective-permute-start.13) | collective-permute-done | bytes 524320 | tf_op jit(solution)/shard_map/ppermute | solution.py:402
  72.7 0.3 shard_map.147
  73.0 18.4 %all_to_all.11 = bf16[64,32,128]{2,1,0:T(8,128)(2,1)S(1)} all-to-all(bf16[64,32,128]{2,1,0:T(8,128)(2,1)S(1)} %bitcast.18), channel_id=1, replica_groups=mesh['zy'=16,'core'=2,'tp'=4] {'zy','tp'}, dimensions={0} | all-to-all | bytes 1048576 | tf_op jit(solution)/shard_map/all_to_all | solution.py:404
  91.4 0.7 shard_map.148
  (32 shorter events, 0.1 us)
Async XLA Ops:
  0.6 31.5 %copy-start = (bf16[4096,128]{1,0:T(8,128)(2,1)S(1)}, bf16[4096,128]{1,0:T(8,128)(2,1)}, u32[]{:S(2)}) copy-start(bf16[4096,128]{1,0:T(8,128)(2,1)} %w_query.1) | copy-start | bytes 3145732
  2.3 34.4 %copy-start.7 = (bf16[1,32,4096]{2,1,0:T(8,128)(2,1)S(1)}, bf16[1,32,4096]{2,1,0:T(8,128)(2,1)}, u32[]{:S(2)}) copy-start(bf16[1,32,4096]{2,1,0:T(8,128)(2,1)} %w0.3) | copy-start | bytes 786436
  2.4 42.8 %copy-start.2 = (bf16[1,32,4096]{2,1,0:T(8,128)(2,1)S(1)}, bf16[1,32,4096]{2,1,0:T(8,128)(2,1)}, u32[]{:S(2)}) copy-start(bf16[1,32,4096]{2,1,0:T(8,128)(2,1)} %w0.2) | copy-start | bytes 786436
  2.4 42.8 %copy-start.3 = (f32[4096]{0:T(1024)S(1)}, f32[4096]{0:T(1024)}, u32[]{:S(2)}) copy-start(f32[4096]{0:T(1024)} %param.14) | copy-start | bytes 49156
  27.4 17.7 %collective-permute-start = (bf16[16,128,128]{2,1,0:T(8,128)(2,1)S(1)}, bf16[16,128,128]{2,1,0:T(8,128)(2,1)S(1)}, u32[]{:S(2)}, u32[]{:S(2)}) collective-permute-start(bf16[16,128,128]{2,1,0:T(8,128)(2,1)S(1)} %bitcast.19), channel_id=1, source_target_pairs={{0,4},{4,0},{1,5},{5,1},{2,6},{6,2},{3,7},{7,3},{8,12},{12,8},{9,1... | collective-permute-start | bytes 1572872 | tf_op jit(solution)/shard_map/ppermute | solution.py:384
  27.4 9.4 %collective-permute-start.1 = (bf16[1,32,4096]{2,1,0:T(8,128)(2,1)}, bf16[1,32,4096]{2,1,0:T(8,128)(2,1)S(1)}, u32[]{:S(2)}, u32[]{:S(2)}) collective-permute-start(bf16[1,32,4096]{2,1,0:T(8,128)(2,1)} %w0.2), channel_id=1, source_target_pairs={{0,1},{1,0},{2,3},{3,2},{4,5},{5,4},{6,7},{7,6},{8,9},{9,8},{10,11... | collective-permute-start | bytes 786440 | tf_op jit(solution)/shard_map/ppermute | solution.py:379
  27.9 14.8 %collective-permute-start.2 = (bf16[1,32,4096]{2,1,0:T(8,128)(2,1)}, bf16[1,32,4096]{2,1,0:T(8,128)(2,1)S(1)}, u32[]{:S(2)}, u32[]{:S(2)}) collective-permute-start(bf16[1,32,4096]{2,1,0:T(8,128)(2,1)} %w0.2), channel_id=1, source_target_pairs={{0,2},{1,3},{2,0},{3,1},{4,6},{5,7},{6,4},{7,5},{8,10},{9,11},{10,... | collective-permute-start | bytes 786440 | tf_op jit(solution)/shard_map/ppermute | solution.py:379
  29.7 15.4 %collective-permute-start.3 = (bf16[1,32,4096]{2,1,0:T(8,128)(2,1)}, bf16[1,32,4096]{2,1,0:T(8,128)(2,1)S(1)}, u32[]{:S(2)}, u32[]{:S(2)}) collective-permute-start(bf16[1,32,4096]{2,1,0:T(8,128)(2,1)} %w0.2), channel_id=1, source_target_pairs={{0,3},{1,2},{2,1},{3,0},{4,7},{5,6},{6,5},{7,4},{8,11},{9,10},{10,... | collective-permute-start | bytes 786440 | tf_op jit(solution)/shard_map/ppermute | solution.py:379
  32.1 33.4 %collective-permute-start.10 = (bf16[1,32,4096]{2,1,0:T(8,128)(2,1)}, bf16[1,32,4096]{2,1,0:T(8,128)(2,1)S(1)}, u32[]{:S(2)}, u32[]{:S(2)}) collective-permute-start(bf16[1,32,4096]{2,1,0:T(8,128)(2,1)} %w0.3), channel_id=1, source_target_pairs={{0,1},{1,0},{2,3},{3,2},{4,5},{5,4},{6,7},{7,6},{8,9},{9,8},{10,11... | collective-permute-start | bytes 786440 | tf_op jit(solution)/shard_map/ppermute | solution.py:379
  32.1 1.2 %copy-start.1 = (bf16[4096,128]{1,0:T(8,128)(2,1)S(1)}, bf16[4096,128]{1,0:T(8,128)(2,1)}, u32[]{:S(2)}) copy-start(bf16[4096,128]{1,0:T(8,128)(2,1)} %w_forget.1) | copy-start | bytes 3145732
  36.8 30.3 %collective-permute-start.11 = (bf16[1,32,4096]{2,1,0:T(8,128)(2,1)S(1)}, bf16[1,32,4096]{2,1,0:T(8,128)(2,1)S(1)}, u32[]{:S(2)}, u32[]{:S(2)}) collective-permute-start(bf16[1,32,4096]{2,1,0:T(8,128)(2,1)S(1)} %copy-done.7), channel_id=1, source_target_pairs={{0,2},{1,3},{2,0},{3,1},{4,6},{5,7},{6,4},{7,5},{8,10},{9,11},{10,... | collective-permute-start | bytes 786440 | tf_op jit(solution)/shard_map/ppermute | solution.py:379
  42.8 24.3 %collective-permute-start.12 = (bf16[1,32,4096]{2,1,0:T(8,128)(2,1)S(1)}, bf16[1,32,4096]{2,1,0:T(8,128)(2,1)S(1)}, u32[]{:S(2)}, u32[]{:S(2)}) collective-permute-start(bf16[1,32,4096]{2,1,0:T(8,128)(2,1)S(1)} %copy-done.7), channel_id=1, source_target_pairs={{0,3},{1,2},{2,1},{3,0},{4,7},{5,6},{6,5},{7,4},{8,11},{9,10},{10,... | collective-permute-start | bytes 786440 | tf_op jit(solution)/shard_map/ppermute | solution.py:379
  45.1 2.4 %copy-start.5 = (bf16[128,4096]{1,0:T(8,128)(2,1)S(1)}, bf16[128,4096]{1,0:T(8,128)(2,1)}, u32[]{:S(2)}) copy-start(bf16[128,4096]{1,0:T(8,128)(2,1)} %w_out.1) | copy-start | bytes 3145732
  47.4 8.8 %copy-start.4 = (f32[128,1,32,128]{3,2,1,0:T(8,128)S(1)}, f32[128,1,32,128]{3,2,1,0:T(8,128)}, u32[]{:S(2)}) copy-start(f32[128,1,32,128]{3,2,1,0:T(8,128)} %param.22) | copy-start | bytes 6291460
  47.4 8.8 %copy-start.6 = (f32[128,4,128]{2,1,0:T(4,128)S(1)}, f32[128,4,128]{2,1,0:T(4,128)}, u32[]{:S(2)}) copy-start(f32[128,4,128]{2,1,0:T(4,128)} %prev_forget.1) | copy-start | bytes 786436
  47.4 8.8 %copy-start.8 = (bf16[128,4,1,32]{0,3,2,1:T(8,128)(2,1)S(1)}, bf16[128,4,1,32]{0,3,2,1:T(8,128)(2,1)}, u32[]{:S(2)}) copy-start(bf16[128,4,1,32]{0,3,2,1:T(8,128)(2,1)} %param.24) | copy-start | bytes 98308
  47.4 8.8 %copy-start.9 = (s32[128]{0:T(128)S(1)}, s32[128]{0:T(128)}, u32[]{:S(2)}) copy-start(s32[128]{0:T(128)} %param.25) | copy-start | bytes 1540
  47.4 7.8 %collective-permute-start.4 = (bf16[288,128]{1,0:T(8,128)(2,1)S(1)}, bf16[288,128]{1,0:T(8,128)(2,1)S(1)}, u32[]{:S(2)}, u32[]{:S(2)}) collective-permute-start(bf16[288,128]{1,0:T(8,128)(2,1)S(1)} %get-tuple-element.15), channel_id=1, source_target_pairs={{0,1},{1,0},{2,3},{3,2},{4,5},{5,4},{6,7},{7,6},{8,9},{9,8},{10,11... | collective-permute-start | bytes 221192 | tf_op jit(solution)/shard_map/ppermute | solution.py:379
  48.2 12.6 %copy-start.10 = (f32[128]{0:T(128)S(1)}, f32[128]{0:T(128)}, u32[]{:S(2)}) copy-start(f32[128]{0:T(128)} %param.19) | copy-start | bytes 1540
  48.2 12.6 %copy-start.11 = (f32[32]{0:T(128)S(1)}, f32[32]{0:T(128)}, u32[]{:S(2)}) copy-start(f32[32]{0:T(128)} %param.20) | copy-start | bytes 388
  48.2 11.1 %collective-permute-start.5 = (bf16[288,128]{1,0:T(8,128)(2,1)S(1)}, bf16[288,128]{1,0:T(8,128)(2,1)S(1)}, u32[]{:S(2)}, u32[]{:S(2)}) collective-permute-start(bf16[288,128]{1,0:T(8,128)(2,1)S(1)} %get-tuple-element.16), channel_id=1, source_target_pairs={{0,2},{1,3},{2,0},{3,1},{4,6},{5,7},{6,4},{7,5},{8,10},{9,11},{10,... | collective-permute-start | bytes 221192 | tf_op jit(solution)/shard_map/ppermute | solution.py:379
  55.3 5.6 %collective-permute-start.6 = (bf16[288,128]{1,0:T(8,128)(2,1)S(1)}, bf16[288,128]{1,0:T(8,128)(2,1)S(1)}, u32[]{:S(2)}, u32[]{:S(2)}) collective-permute-start(bf16[288,128]{1,0:T(8,128)(2,1)S(1)} %get-tuple-element.17), channel_id=1, source_target_pairs={{0,3},{1,2},{2,1},{3,0},{4,7},{5,6},{6,5},{7,4},{8,11},{9,10},{10,... | collective-permute-start | bytes 221192 | tf_op jit(solution)/shard_map/ppermute | solution.py:379
  62.3 6.2 %collective-permute-start.7 = (bf16[48,128]{1,0:T(8,128)(2,1)S(1)}, bf16[48,128]{1,0:T(8,128)(2,1)S(1)}, u32[]{:S(2)}, u32[]{:S(2)}) collective-permute-start(bf16[48,128]{1,0:T(8,128)(2,1)S(1)} %get-tuple-element.20), channel_id=1, source_target_pairs={{0,1},{1,0},{2,3},{3,2},{4,5},{5,4},{6,7},{7,6},{8,9},{9,8},{10,11... | collective-permute-start | bytes 36872 | tf_op jit(solution)/shard_map/ppermute | solution.py:379
  62.4 6.2 %collective-permute-start.8 = (bf16[48,128]{1,0:T(8,128)(2,1)S(1)}, bf16[48,128]{1,0:T(8,128)(2,1)S(1)}, u32[]{:S(2)}, u32[]{:S(2)}) collective-permute-start(bf16[48,128]{1,0:T(8,128)(2,1)S(1)} %get-tuple-element.21), channel_id=1, source_target_pairs={{0,2},{1,3},{2,0},{3,1},{4,6},{5,7},{6,4},{7,5},{8,10},{9,11},{10,... | collective-permute-start | bytes 36872 | tf_op jit(solution)/shard_map/ppermute | solution.py:379
  65.5 4.9 %collective-permute-start.9 = (bf16[48,128]{1,0:T(8,128)(2,1)S(1)}, bf16[48,128]{1,0:T(8,128)(2,1)S(1)}, u32[]{:S(2)}, u32[]{:S(2)}) collective-permute-start(bf16[48,128]{1,0:T(8,128)(2,1)S(1)} %get-tuple-element.22), channel_id=1, source_target_pairs={{0,3},{1,2},{2,1},{3,0},{4,7},{5,6},{6,5},{7,4},{8,11},{9,10},{10,... | collective-permute-start | bytes 36872 | tf_op jit(solution)/shard_map/ppermute | solution.py:379
  70.7 2.0 %collective-permute-start.13 = (bf16[16,128,128]{2,1,0:T(8,128)(2,1)S(1)}, bf16[16,128,128]{2,1,0:T(8,128)(2,1)S(1)}, u32[]{:S(2)}, u32[]{:S(2)}) collective-permute-start(bf16[16,128,128]{2,1,0:T(8,128)(2,1)S(1)} %shard_map.146), channel_id=1, source_target_pairs={{0,4},{4,0},{1,5},{5,1},{2,6},{6,2},{3,7},{7,3},{8,12},{12,8},{9,1... | collective-permute-start | bytes 1572872 | tf_op jit(solution)/shard_map/ppermute | solution.py:402

commit v3 on v1

--- a/solution.py
+++ b/solution.py
@@ -222,7 +222,8 @@
     )(gain, *weights, rows, scale)
 
 
-def outward_kernel(w_out, outward, held, sems):
+def outward_kernel(w_out, mine, theirs, held, sems):
+    core = lax.axis_index("core")
     cuts, size, span = held.shape
     copies = [
         pltpu.make_async_copy(w_out.at[:, pl.ds(c * span, span)], held.at[c], sems.at[c])
@@ -230,23 +231,26 @@
     ]
     for copy in copies:
         copy.start()
+    pairs = span // size // 2
     for c in range(cuts):
         copies[c].wait()
-        for b in range(span // size):
-            block = held[c, :, pl.ds(b * size, size)].astype(jnp.float32)
-            outward[c * (span // size) + b] = block.T.astype(jnp.bfloat16)
+        for b in range(pairs):
+            for half, out in ((core, mine), (1 - core, theirs)):
+                at = pl.multiple_of((2 * b + half) * size, size)
+                block = held[c, :, pl.ds(at, size)].astype(jnp.float32)
+                out[c * pairs + b] = block.T.astype(jnp.bfloat16)
 
 
 def turn_outward(w_out):
     size, width = w_out.shape
     return call(
         outward_kernel,
-        shaped((width // size, size, size), jnp.bfloat16),
+        [shaped((width // size // 2, size, size), jnp.bfloat16)] * 2,
         [pltpu.VMEM((4, size, width // 4), jnp.bfloat16), pltpu.SemaphoreType.DMA((4,))],
         (1_000_000_000, 2 << 20),
         16 << 20,
         [pl.BlockSpec(memory_space=pltpu.HBM)],
-        whole(),
+        [whole()] * 2,
     )(w_out)
 
 
@@ -316,46 +320,52 @@
     )(*received, before, floor, head_gain)
 
 
-def gathered(parts, gates, joined):
+def hide_kernel(p0, p1, p2, p3, gates, hidden):
     mine = lax.axis_index("tp")
-    values = joined.shape[0] // 4
+    values = hidden.shape[0] // 4
+    parts = (p0, p1, p2, p3)
     total = None
+    for ref in parts:
+        square = jnp.sum(ref[pl.ds(values, 16), :].astype(jnp.float32), axis=0, keepdims=True)
+        total = square if total is None else total + square
+    factor = lax.rsqrt(total / hidden.shape[0] + NORM_EPSILON)
     for d, ref in enumerate(parts):
         at = pl.multiple_of((mine ^ d) * values, values)
-        value = ref[pl.ds(0, values), :].astype(jnp.float32) * gates[pl.ds(d * values, values), :]
-        joined[pl.ds(at, values), :] = value.astype(jnp.bfloat16)
-        square = jnp.sum(ref[pl.ds(values, 16), :].astype(jnp.float32), axis=0, keepdims=True)
-        total = square if total is None else total + square
-    return lax.rsqrt(total / joined.shape[0] + NORM_EPSILON)
-
-
-def away_kernel(p0, p1, p2, p3, gates, outward, sent, joined):
-    core = lax.axis_index("core")
-    factor = gathered((p0, p1, p2, p3), gates, joined)
-    for b in range(sent.shape[0]):
-        part = jnp.dot(outward[2 * b + 1 - core], joined[...], preferred_element_type=jnp.float32)
-        sent[b] = (part * factor).astype(jnp.bfloat16)
-
-
-def keep_kernel(p0, p1, p2, p3, gates, outward, came, kept, joined):
-    core = lax.axis_index("core")
-    factor = gathered((p0, p1, p2, p3), gates, joined)
-    for b in range(kept.shape[0]):
-        part = jnp.dot(outward[2 * b + core], joined[...], preferred_element_type=jnp.float32)
-        kept[b] = (part * factor + came[b].astype(jnp.float32)).astype(jnp.bfloat16)
-
-
-def outward_half(kernel, parts, gates, outward, *more):
-    blocks, size, _ = outward.shape
-    return call(
-        kernel,
-        shaped((blocks // 2, size, parts[0].shape[1]), jnp.bfloat16),
-        [pltpu.VMEM((size, parts[0].shape[1]), jnp.bfloat16)],
+        value = ref[pl.ds(0, values), :].astype(jnp.float32) * factor
+        value = value * gates[pl.ds(d * values, values), :]
+        hidden[pl.ds(at, values), :] = value.astype(jnp.bfloat16)
+
+
+def hide(parts, gates):
+    return call(
+        hide_kernel,
+        shaped(gates.shape, jnp.bfloat16),
+        [],
+        (1_000_000, 1 << 18),
+        16 << 20,
+        [whole()] * 5,
+        whole(),
+    )(*parts, gates)
+
+
+def emit_kernel(hidden, other, ours, theirs, out):
+    for b in range(out.shape[0]):
+        part = jnp.dot(ours[b], hidden[...], preferred_element_type=jnp.float32)
+        part = part + jnp.dot(theirs[b], other[...], preferred_element_type=jnp.float32)
+        out[b] = part.astype(jnp.bfloat16)
+
+
+def emit(hidden, other, ours, theirs):
+    blocks, size, _ = ours.shape
+    return call(
+        emit_kernel,
+        shaped((blocks, size, hidden.shape[1]), jnp.bfloat16),
+        [],
         (100_000_000, 2 << 20),
         16 << 20,
-        [whole()] * (6 + len(more)),
-        whole(),
-    )(*parts, gates, outward, *more)
+        [whole()] * 4,
+        whole(),
+    )(hidden, other, ours, theirs)
 
 
 def sum_kernel(parts, out):
@@ -402,10 +412,12 @@
         return [parts[0]] + [lax.ppermute(parts[d], "tp", hops[d]) for d in (1, 2, 3)]
 
     gain = input_norm_gain.reshape(-1, size)
-    inputs = passed([w_input] * group)
-    own = lax.all_to_all(source(tokens.transpose(1, 2, 0), planes), ("zy", "tp"), 0, 0, tiled=True)
+    own = lax.all_to_all(
+        source(tokens.transpose(1, 2, 0), planes), ("zy", "tp"), 0, 0, tiled=True
+    )
     own = own.reshape(planes, group * features, seqs)
     other = lax.ppermute(own, "core", swap)
+    inputs = passed([w_input] * group)
     gates = passed([w_gate] * group)
     keyed = turn(gain, w_query, w_forget)
     mixing = fold(gain, inputs)
@@ -418,13 +430,13 @@
 
     sends, rows, scale = project(own, other, keyed, mixing)
     received = passed(sends)
+    ours, theirs = turn_outward(w_out)
+    theirs = lax.ppermute(theirs, "core", swap)
     shown = recur(received, rounded.reshape(-1, size), forget_floor[None], head_gain[None])
     parts = passed(shown)
-    outward = turn_outward(w_out)
     opened = gate(gain, gates, rows, scale)
-    sent = outward_half(away_kernel, parts, opened, outward)
-    came = lax.ppermute(sent, "core", swap)
-    kept = outward_half(keep_kernel, parts, opened, outward, came)
+    hidden = hide(parts, opened)
+    kept = emit(hidden, lax.ppermute(hidden, "core", swap), ours, theirs)
     terms = lax.all_to_all(
         kept.reshape(planes * group, features, seqs), ("zy", "tp"), 0, 0, tiled=True
     )

time: 92.3 us -> 98 us (1.062)
  waiting for transfers between devices: 17.2 us -> 22.8 us
  starting transfers between devices: 17.8 us -> 19.2 us
    ppermute x12, waiting for transfers between devices: 15.3 us -> 21.6 us  [passed(): lax.ppermute(parts[d], 'tp', hops[d])]
    ppermute x12, starting transfers between devices: 17.7 us -> 19 us  [passed(): lax.ppermute(parts[d], 'tp', hops[d])]
    unnamed x26 -> x24, local copies, waits for them, and re-layouts: 2 us -> 1.29 us
  transfers between devices with their start and end apart: 14 -> 15, of which waited for: 6 -> 6; matrix products, arithmetic and copies ran while one was open for 0% -> 0% of each run, Pallas kernels for 9% -> 8%
where the time goes in v3:
time: 98 us; the launch traced here: 97.6 us
  blocking collectives  42.9 us (44%)
  waiting for transfers between devices  22.8 us (23%)
  starting transfers between devices  19.2 us (20%)
  Pallas kernels  10.6 us (11%)
  local copies, waits for them, and re-layouts  1.29 us (1%)
    all_to_all x1, blocking collectives, body(): lax.all_to_all(source(tokens.transpose(1, 2, 0), planes), ('zy', 'tp'), 0...  24.9 us
    ppermute x12, waiting for transfers between devices, passed(): lax.ppermute(parts[d], 'tp', hops[d])  21.6 us
    ppermute x12, starting transfers between devices, passed(): lax.ppermute(parts[d], 'tp', hops[d])  19 us
    all_to_all x1, blocking collectives, body(): lax.all_to_all(kept.reshape(planes * group, features, seqs), ('zy', 'tp')...  18 us
    pallas_call x1, Pallas kernels, advance(): pl.pallas_call(advance_kernel, grid=(seqs // count,), in_specs=[pl.BlockS...  3.12 us
  transfers between devices with their start and end apart: 15, of which 6 were waited for; matrix products, arithmetic and copies ran while one was open for 0% of the time, Pallas kernels for 8%

profile of v3, /device:TPU:0, one launch (start us, length us, event | category | flops | bytes accessed | tf_op | source)
XLA Modules:
  0.0 97.6 jit_solution(14841214727526736505)
XLA Ops:
  0.6 1.6 %shard_map.140 = bf16[64,32,128]{2,1,0:T(8,128)(2,1)} custom-call(bf16[4,32,128]{2,1,0:T(8,128)(2,1)} %bitcast.30), custom_call_target="tpu_custom_call" | custom-call | flops 1000000 | bytes 1048576 | tf_op jit(solution)/shard_map/pallas_call | solution.py:104
  2.3 24.9 %all_to_all.10 = bf16[64,32,128]{2,1,0:T(8,128)(2,1)S(1)} all-to-all(bf16[64,32,128]{2,1,0:T(8,128)(2,1)} %shard_map.140), channel_id=1, replica_groups=mesh['zy'=16,'core'=2,'tp'=4] {'zy','tp'}, dimensions={0} | all-to-all | bytes 1048576 | tf_op jit(solution)/shard_map/all_to_all | solution.py:415
  27.2 0.6 collective-permute-start.1
  27.8 1.8 %collective-permute-start.2 = (bf16[1,32,4096]{2,1,0:T(8,128)(2,1)}, bf16[1,32,4096]{2,1,0:T(8,128)(2,1)S(1)}, u32[]{:S(2)}, u32[]{:S(2)}) collective-permute-start(bf16[1,32,4096]{2,1,0:T(8,128)(2,1)} %w0.2), channel_id=1, source_target_pairs={{0,2},{1,3},{2,0},{3,1},{4,6},{5,7},{6,4},{7,5},{8,10},{9,11},{10,... | collective-permute-start | bytes 786440 | tf_op jit(solution)/shard_map/ppermute | solution.py:412
  29.6 2.3 %collective-permute-start.3 = (bf16[1,32,4096]{2,1,0:T(8,128)(2,1)}, bf16[1,32,4096]{2,1,0:T(8,128)(2,1)S(1)}, u32[]{:S(2)}, u32[]{:S(2)}) collective-permute-start(bf16[1,32,4096]{2,1,0:T(8,128)(2,1)} %w0.2), channel_id=1, source_target_pairs={{0,3},{1,2},{2,1},{3,0},{4,7},{5,6},{6,5},{7,4},{8,11},{9,10},{10,... | collective-permute-start | bytes 786440 | tf_op jit(solution)/shard_map/ppermute | solution.py:412
  31.9 1.2 %copy-done.4 = bf16[128,4096]{1,0:T(8,128)(2,1)S(1)} copy-done((bf16[128,4096]{1,0:T(8,128)(2,1)S(1)}, bf16[128,4096]{1,0:T(8,128)(2,1)}, u32[]{:S(2)}) %copy-start.4) | copy-done | bytes 1048600
  33.2 0.7 shard_map.147
  33.8 0.1 collective-permute-start.14
  34.0 0.7 shard_map.141.keyed
  34.6 2.0 %collective-permute-done.1.w1 = bf16[1,32,4096]{2,1,0:T(8,128)(2,1)S(1)} collective-permute-done((bf16[1,32,4096]{2,1,0:T(8,128)(2,1)}, bf16[1,32,4096]{2,1,0:T(8,128)(2,1)S(1)}, u32[]{:S(2)}, u32[]{:S(2)}) %collective-permute-start.1) | collective-permute-done | bytes 262176 | tf_op jit(solution)/shard_map/ppermute | solution.py:412
  36.6 5.5 %collective-permute-done.2.w2 = bf16[1,32,4096]{2,1,0:T(8,128)(2,1)S(1)} collective-permute-done((bf16[1,32,4096]{2,1,0:T(8,128)(2,1)}, bf16[1,32,4096]{2,1,0:T(8,128)(2,1)S(1)}, u32[]{:S(2)}, u32[]{:S(2)}) %collective-permute-start.2) | collective-permute-done | bytes 262176 | tf_op jit(solution)/shard_map/ppermute | solution.py:412
  42.1 2.6 %collective-permute-done.3.w3 = bf16[1,32,4096]{2,1,0:T(8,128)(2,1)S(1)} collective-permute-done((bf16[1,32,4096]{2,1,0:T(8,128)(2,1)}, bf16[1,32,4096]{2,1,0:T(8,128)(2,1)S(1)}, u32[]{:S(2)}, u32[]{:S(2)}) %collective-permute-start.3) | collective-permute-done | bytes 262176 | tf_op jit(solution)/shard_map/ppermute | solution.py:412
  44.7 0.3 shard_map.142.mixing
  45.1 1.2 %shard_map.143 = (bf16[288,128]{1,0:T(8,128)(2,1)S(1)}, bf16[288,128]{1,0:T(8,128)(2,1)S(1)}, bf16[288,128]{1,0:T(8,128)(2,1)S(1)}, bf16[288,128]{1,0:T(8,128)(2...) custom-call(bf16[16,128,128]{2,1,0:T(8,128)(2,1)S(1)} %bitcast.20, ...), custom_call_target="tpu_custom_call" | custom-call | flops 1000000000 | bytes 3145728 | tf_op jit(solution)/shard_map/pallas_call | solution.py:187
  46.2 0.1 collective-permute-start.4
  46.3 3.8 %collective-permute-start.5 = (bf16[288,128]{1,0:T(8,128)(2,1)S(1)}, bf16[288,128]{1,0:T(8,128)(2,1)S(1)}, u32[]{:S(2)}, u32[]{:S(2)}) collective-permute-start(bf16[288,128]{1,0:T(8,128)(2,1)S(1)} %get-tuple-element.18), channel_id=1, source_target_pairs={{0,2},{1,3},{2,0},{3,1},{4,6},{5,7},{6,4},{7,5},{8,10},{9,11},{10,... | collective-permute-start | bytes 221192 | tf_op jit(solution)/shard_map/ppermute | solution.py:412
  50.1 2.4 %collective-permute-start.11 = (bf16[1,32,4096]{2,1,0:T(8,128)(2,1)S(1)}, bf16[1,32,4096]{2,1,0:T(8,128)(2,1)S(1)}, u32[]{:S(2)}, u32[]{:S(2)}) collective-permute-start(bf16[1,32,4096]{2,1,0:T(8,128)(2,1)S(1)} %copy-done.7), channel_id=1, source_target_pairs={{0,2},{1,3},{2,0},{3,1},{4,6},{5,7},{6,4},{7,5},{8,10},{9,11},{10,... | collective-permute-start | bytes 786440 | tf_op jit(solution)/shard_map/ppermute | solution.py:412
  52.5 2.3 %collective-permute-start.12 = (bf16[1,32,4096]{2,1,0:T(8,128)(2,1)S(1)}, bf16[1,32,4096]{2,1,0:T(8,128)(2,1)S(1)}, u32[]{:S(2)}, u32[]{:S(2)}) collective-permute-start(bf16[1,32,4096]{2,1,0:T(8,128)(2,1)S(1)} %copy-done.7), channel_id=1, source_target_pairs={{0,3},{1,2},{2,1},{3,0},{4,7},{5,6},{6,5},{7,4},{8,11},{9,10},{10,... | collective-permute-start | bytes 786440 | tf_op jit(solution)/shard_map/ppermute | solution.py:412
  54.8 0.9 collective-permute-start.6
  55.8 3.1 %advance.1 = (f32[128,32,128]{2,1,0:T(8,128)}, bf16[128,32,128]{2,1,0:T(8,128)(2,1)S(1)}) custom-call(s32[1,128]{1,0:T(1,128)S(1)} %bitcast.26, f32[128,4,128]{2,1,0:T(4,128)S(1)} %copy-done.6, bf16[4,32,128]{2,1,0:T(8,128)(2,1)S(1)} %bitcast.25, f32[128,32,128]{2,1,0:T(8,128)S(1)} %bitcast.24), custom_call_target="tpu_custom_call" | custom-call | flops 1000000000 | bytes 5242880 | tf_op jit(solution)/shard_map/advance/pallas_call | solution.py:65
  58.9 8.4 %collective-permute-done.6.r3 = bf16[288,128]{1,0:T(8,128)(2,1)S(1)} collective-permute-done((bf16[288,128]{1,0:T(8,128)(2,1)S(1)}, bf16[288,128]{1,0:T(8,128)(2,1)S(1)}, u32[]{:S(2)}, u32[]{:S(2)}) %collective-permute-start.6) | collective-permute-done | bytes 73760 | tf_op jit(solution)/shard_map/ppermute | solution.py:412
  67.3 1.4 %shard_map.144 = (bf16[48,128]{1,0:T(8,128)(2,1)S(1)}, bf16[48,128]{1,0:T(8,128)(2,1)S(1)}, bf16[48,128]{1,0:T(8,128)(2,1)S(1)}, bf16[48,128]{1,0:T(8,128)(2,1)S(1)}) custom-call(bf16[288,128]{1,0:T(8,128)(2,1)S(1)} %get-tuple-element.16.r0, bf16[288,128]{1,0:T(8,128)(2,1)S(1)} %collective-permute-done.4.r1, bf16[288,128]{1,0:T(8,128)(2,1)S(1)} %collective-permute-done.5.r2, ...), custom_call_target="tpu_custom_call" | custom-call | flops 1000000000 | bytes 2097152 | tf_op jit(solution)/shard_map/pallas_call | solution.py:309
  68.8 0.1 collective-permute-start.7
  68.9 3.5 %collective-permute-start.8 = (bf16[48,128]{1,0:T(8,128)(2,1)S(1)}, bf16[48,128]{1,0:T(8,128)(2,1)S(1)}, u32[]{:S(2)}, u32[]{:S(2)}) collective-permute-start(bf16[48,128]{1,0:T(8,128)(2,1)S(1)} %get-tuple-element.23), channel_id=1, source_target_pairs={{0,2},{1,3},{2,0},{3,1},{4,6},{5,7},{6,4},{7,5},{8,10},{9,11},{10,... | collective-permute-start | bytes 36872 | tf_op jit(solution)/shard_map/ppermute | solution.py:412
  72.3 1.2 %collective-permute-start.9 = (bf16[48,128]{1,0:T(8,128)(2,1)S(1)}, bf16[48,128]{1,0:T(8,128)(2,1)S(1)}, u32[]{:S(2)}, u32[]{:S(2)}) collective-permute-start(bf16[48,128]{1,0:T(8,128)(2,1)S(1)} %get-tuple-element.24), channel_id=1, source_target_pairs={{0,3},{1,2},{2,1},{3,0},{4,7},{5,6},{6,5},{7,4},{8,11},{9,10},{10,... | collective-permute-start | bytes 36872 | tf_op jit(solution)/shard_map/ppermute | solution.py:412
  73.5 0.5 shard_map.145.gates
  74.1 3.1 %collective-permute-done.9.p3 = bf16[48,128]{1,0:T(8,128)(2,1)S(1)} collective-permute-done((bf16[48,128]{1,0:T(8,128)(2,1)S(1)}, bf16[48,128]{1,0:T(8,128)(2,1)S(1)}, u32[]{:S(2)}, u32[]{:S(2)}) %collective-permute-start.9) | collective-permute-done | bytes 12320 | tf_op jit(solution)/shard_map/ppermute | solution.py:412
  77.3 0.1 collective-permute-start.13
  77.4 1.2 %collective-permute-done.13.other = bf16[128,128]{1,0:T(8,128)(2,1)S(1)} collective-permute-done((bf16[128,128]{1,0:T(8,128)(2,1)S(1)}, bf16[128,128]{1,0:T(8,128)(2,1)S(1)}, u32[]{:S(2)}, u32[]{:S(2)}) %collective-permute-start.13) | collective-permute-done | bytes 32800 | tf_op jit(solution)/shard_map/ppermute | solution.py:439
  78.6 0.4 shard_map.148
  79.0 18.0 %all_to_all.11 = bf16[64,32,128]{2,1,0:T(8,128)(2,1)S(1)} all-to-all(bf16[64,32,128]{2,1,0:T(8,128)(2,1)S(1)} %bitcast.17), channel_id=1, replica_groups=mesh['zy'=16,'core'=2,'tp'=4] {'zy','tp'}, dimensions={0} | all-to-all | bytes 1048576 | tf_op jit(solution)/shard_map/all_to_all | solution.py:440
  97.0 0.7 shard_map.149
  (35 shorter events, 0.1 us)
Async XLA Ops:
  27.1 6.8 %copy-start = (bf16[4096,128]{1,0:T(8,128)(2,1)S(1)}, bf16[4096,128]{1,0:T(8,128)(2,1)}, u32[]{:S(2)}) copy-start(bf16[4096,128]{1,0:T(8,128)(2,1)} %w_query.1) | copy-start | bytes 3145732
  27.1 6.8 %copy-start.1 = (bf16[4096,128]{1,0:T(8,128)(2,1)S(1)}, bf16[4096,128]{1,0:T(8,128)(2,1)}, u32[]{:S(2)}) copy-start(bf16[4096,128]{1,0:T(8,128)(2,1)} %w_forget.1) | copy-start | bytes 3145732
  27.1 6.8 %copy-start.2 = (f32[4096]{0:T(1024)S(1)}, f32[4096]{0:T(1024)}, u32[]{:S(2)}) copy-start(f32[4096]{0:T(1024)} %param.14) | copy-start | bytes 49156
  27.1 17.9 %collective-permute-start = (bf16[16,128,128]{2,1,0:T(8,128)(2,1)S(1)}, bf16[16,128,128]{2,1,0:T(8,128)(2,1)S(1)}, u32[]{:S(2)}, u32[]{:S(2)}) collective-permute-start(bf16[16,128,128]{2,1,0:T(8,128)(2,1)S(1)} %bitcast.19), channel_id=1, source_target_pairs={{0,4},{4,0},{1,5},{5,1},{2,6},{6,2},{3,7},{7,3},{8,12},{12,8},{9,1... | collective-permute-start | bytes 1572872 | tf_op jit(solution)/shard_map/ppermute | solution.py:419
  27.2 9.5 %collective-permute-start.1 = (bf16[1,32,4096]{2,1,0:T(8,128)(2,1)}, bf16[1,32,4096]{2,1,0:T(8,128)(2,1)S(1)}, u32[]{:S(2)}, u32[]{:S(2)}) collective-permute-start(bf16[1,32,4096]{2,1,0:T(8,128)(2,1)} %w0.2), channel_id=1, source_target_pairs={{0,1},{1,0},{2,3},{3,2},{4,5},{5,4},{6,7},{7,6},{8,9},{9,8},{10,11... | collective-permute-start | bytes 786440 | tf_op jit(solution)/shard_map/ppermute | solution.py:412
  27.8 14.3 %collective-permute-start.2 = (bf16[1,32,4096]{2,1,0:T(8,128)(2,1)}, bf16[1,32,4096]{2,1,0:T(8,128)(2,1)S(1)}, u32[]{:S(2)}, u32[]{:S(2)}) collective-permute-start(bf16[1,32,4096]{2,1,0:T(8,128)(2,1)} %w0.2), channel_id=1, source_target_pairs={{0,2},{1,3},{2,0},{3,1},{4,6},{5,7},{6,4},{7,5},{8,10},{9,11},{10,... | collective-permute-start | bytes 786440 | tf_op jit(solution)/shard_map/ppermute | solution.py:412
  29.6 15.1 %collective-permute-start.3 = (bf16[1,32,4096]{2,1,0:T(8,128)(2,1)}, bf16[1,32,4096]{2,1,0:T(8,128)(2,1)S(1)}, u32[]{:S(2)}, u32[]{:S(2)}) collective-permute-start(bf16[1,32,4096]{2,1,0:T(8,128)(2,1)} %w0.2), channel_id=1, source_target_pairs={{0,3},{1,2},{2,1},{3,0},{4,7},{5,6},{6,5},{7,4},{8,11},{9,10},{10,... | collective-permute-start | bytes 786440 | tf_op jit(solution)/shard_map/ppermute | solution.py:412
  31.9 1.2 %copy-start.4 = (bf16[128,4096]{1,0:T(8,128)(2,1)S(1)}, bf16[128,4096]{1,0:T(8,128)(2,1)}, u32[]{:S(2)}) copy-start(bf16[128,4096]{1,0:T(8,128)(2,1)} %w_out.1) | copy-start | bytes 3145732
  33.8 43.5 %collective-permute-start.14 = (bf16[16,128,128]{2,1,0:T(8,128)(2,1)S(1)}, bf16[16,128,128]{2,1,0:T(8,128)(2,1)S(1)}, u32[]{:S(2)}, u32[]{:S(2)}) collective-permute-start(bf16[16,128,128]{2,1,0:T(8,128)(2,1)S(1)} %get-tuple-element.28), channel_id=1, source_target_pairs={{0,4},{4,0},{1,5},{5,1},{2,6},{6,2},{3,7},{7,3},{8,12},{12,8},{9,1... | collective-permute-start | bytes 1572872 | tf_op jit(solution)/shard_map/ppermute | solution.py:434
  34.0 10.7 %copy-start.5 = (bf16[1,32,4096]{2,1,0:T(8,128)(2,1)S(1)}, bf16[1,32,4096]{2,1,0:T(8,128)(2,1)}, u32[]{:S(2)}) copy-start(bf16[1,32,4096]{2,1,0:T(8,128)(2,1)} %w0.2) | copy-start | bytes 786436
  45.0 5.1 %copy-start.7 = (bf16[1,32,4096]{2,1,0:T(8,128)(2,1)S(1)}, bf16[1,32,4096]{2,1,0:T(8,128)(2,1)}, u32[]{:S(2)}) copy-start(bf16[1,32,4096]{2,1,0:T(8,128)(2,1)} %w0.3) | copy-start | bytes 786436
  45.0 10.7 %copy-start.3 = (f32[128,1,32,128]{3,2,1,0:T(8,128)S(1)}, f32[128,1,32,128]{3,2,1,0:T(8,128)}, u32[]{:S(2)}) copy-start(f32[128,1,32,128]{3,2,1,0:T(8,128)} %param.22) | copy-start | bytes 6291460
  45.0 10.7 %copy-start.6 = (f32[128,4,128]{2,1,0:T(4,128)S(1)}, f32[128,4,128]{2,1,0:T(4,128)}, u32[]{:S(2)}) copy-start(f32[128,4,128]{2,1,0:T(4,128)} %prev_forget.1) | copy-start | bytes 786436
  45.0 10.7 %copy-start.8 = (bf16[128,4,1,32]{0,3,2,1:T(8,128)(2,1)S(1)}, bf16[128,4,1,32]{0,3,2,1:T(8,128)(2,1)}, u32[]{:S(2)}) copy-start(bf16[128,4,1,32]{0,3,2,1:T(8,128)(2,1)} %param.24) | copy-start | bytes 98308
  45.0 10.7 %copy-start.9 = (s32[128]{0:T(128)S(1)}, s32[128]{0:T(128)}, u32[]{:S(2)}) copy-start(s32[128]{0:T(128)} %param.25) | copy-start | bytes 1540
  46.2 21.1 %copy-start.10 = (f32[128]{0:T(128)S(1)}, f32[128]{0:T(128)}, u32[]{:S(2)}) copy-start(f32[128]{0:T(128)} %param.19) | copy-start | bytes 1540
  46.2 21.1 %copy-start.11 = (f32[32]{0:T(128)S(1)}, f32[32]{0:T(128)}, u32[]{:S(2)}) copy-start(f32[32]{0:T(128)} %param.20) | copy-start | bytes 388
  46.2 6.2 %collective-permute-start.4 = (bf16[288,128]{1,0:T(8,128)(2,1)S(1)}, bf16[288,128]{1,0:T(8,128)(2,1)S(1)}, u32[]{:S(2)}, u32[]{:S(2)}) collective-permute-start(bf16[288,128]{1,0:T(8,128)(2,1)S(1)} %get-tuple-element.17), channel_id=1, source_target_pairs={{0,1},{1,0},{2,3},{3,2},{4,5},{5,4},{6,7},{7,6},{8,9},{9,8},{10,11... | collective-permute-start | bytes 221192 | tf_op jit(solution)/shard_map/ppermute | solution.py:412
  46.3 8.5 %collective-permute-start.5 = (bf16[288,128]{1,0:T(8,128)(2,1)S(1)}, bf16[288,128]{1,0:T(8,128)(2,1)S(1)}, u32[]{:S(2)}, u32[]{:S(2)}) collective-permute-start(bf16[288,128]{1,0:T(8,128)(2,1)S(1)} %get-tuple-element.18), channel_id=1, source_target_pairs={{0,2},{1,3},{2,0},{3,1},{4,6},{5,7},{6,4},{7,5},{8,10},{9,11},{10,... | collective-permute-start | bytes 221192 | tf_op jit(solution)/shard_map/ppermute | solution.py:412
  50.1 18.7 %collective-permute-start.10 = (bf16[1,32,4096]{2,1,0:T(8,128)(2,1)S(1)}, bf16[1,32,4096]{2,1,0:T(8,128)(2,1)S(1)}, u32[]{:S(2)}, u32[]{:S(2)}) collective-permute-start(bf16[1,32,4096]{2,1,0:T(8,128)(2,1)S(1)} %copy-done.7), channel_id=1, source_target_pairs={{0,1},{1,0},{2,3},{3,2},{4,5},{5,4},{6,7},{7,6},{8,9},{9,8},{10,11... | collective-permute-start | bytes 786440 | tf_op jit(solution)/shard_map/ppermute | solution.py:412
  50.1 22.2 %collective-permute-start.11 = (bf16[1,32,4096]{2,1,0:T(8,128)(2,1)S(1)}, bf16[1,32,4096]{2,1,0:T(8,128)(2,1)S(1)}, u32[]{:S(2)}, u32[]{:S(2)}) collective-permute-start(bf16[1,32,4096]{2,1,0:T(8,128)(2,1)S(1)} %copy-done.7), channel_id=1, source_target_pairs={{0,2},{1,3},{2,0},{3,1},{4,6},{5,7},{6,4},{7,5},{8,10},{9,11},{10,... | collective-permute-start | bytes 786440 | tf_op jit(solution)/shard_map/ppermute | solution.py:412
  52.5 21.1 %collective-permute-start.12 = (bf16[1,32,4096]{2,1,0:T(8,128)(2,1)S(1)}, bf16[1,32,4096]{2,1,0:T(8,128)(2,1)S(1)}, u32[]{:S(2)}, u32[]{:S(2)}) collective-permute-start(bf16[1,32,4096]{2,1,0:T(8,128)(2,1)S(1)} %copy-done.7), channel_id=1, source_target_pairs={{0,3},{1,2},{2,1},{3,0},{4,7},{5,6},{6,5},{7,4},{8,11},{9,10},{10,... | collective-permute-start | bytes 786440 | tf_op jit(solution)/shard_map/ppermute | solution.py:412
  54.8 12.5 %collective-permute-start.6 = (bf16[288,128]{1,0:T(8,128)(2,1)S(1)}, bf16[288,128]{1,0:T(8,128)(2,1)S(1)}, u32[]{:S(2)}, u32[]{:S(2)}) collective-permute-start(bf16[288,128]{1,0:T(8,128)(2,1)S(1)} %get-tuple-element.19), channel_id=1, source_target_pairs={{0,3},{1,2},{2,1},{3,0},{4,7},{5,6},{6,5},{7,4},{8,11},{9,10},{10,... | collective-permute-start | bytes 221192 | tf_op jit(solution)/shard_map/ppermute | solution.py:412
  68.8 5.3 %collective-permute-start.7 = (bf16[48,128]{1,0:T(8,128)(2,1)S(1)}, bf16[48,128]{1,0:T(8,128)(2,1)S(1)}, u32[]{:S(2)}, u32[]{:S(2)}) collective-permute-start(bf16[48,128]{1,0:T(8,128)(2,1)S(1)} %get-tuple-element.22), channel_id=1, source_target_pairs={{0,1},{1,0},{2,3},{3,2},{4,5},{5,4},{6,7},{7,6},{8,9},{9,8},{10,11... | collective-permute-start | bytes 36872 | tf_op jit(solution)/shard_map/ppermute | solution.py:412
  68.9 5.3 %collective-permute-start.8 = (bf16[48,128]{1,0:T(8,128)(2,1)S(1)}, bf16[48,128]{1,0:T(8,128)(2,1)S(1)}, u32[]{:S(2)}, u32[]{:S(2)}) collective-permute-start(bf16[48,128]{1,0:T(8,128)(2,1)S(1)} %get-tuple-element.23), channel_id=1, source_target_pairs={{0,2},{1,3},{2,0},{3,1},{4,6},{5,7},{6,4},{7,5},{8,10},{9,11},{10,... | collective-permute-start | bytes 36872 | tf_op jit(solution)/shard_map/ppermute | solution.py:412
  72.3 4.9 %collective-permute-start.9 = (bf16[48,128]{1,0:T(8,128)(2,1)S(1)}, bf16[48,128]{1,0:T(8,128)(2,1)S(1)}, u32[]{:S(2)}, u32[]{:S(2)}) collective-permute-start(bf16[48,128]{1,0:T(8,128)(2,1)S(1)} %get-tuple-element.24), channel_id=1, source_target_pairs={{0,3},{1,2},{2,1},{3,0},{4,7},{5,6},{6,5},{7,4},{8,11},{9,10},{10,... | collective-permute-start | bytes 36872 | tf_op jit(solution)/shard_map/ppermute | solution.py:412
  77.3 1.3 %collective-permute-start.13 = (bf16[128,128]{1,0:T(8,128)(2,1)S(1)}, bf16[128,128]{1,0:T(8,128)(2,1)S(1)}, u32[]{:S(2)}, u32[]{:S(2)}) collective-permute-start(bf16[128,128]{1,0:T(8,128)(2,1)S(1)} %shard_map.146.hidden), channel_id=1, source_target_pairs={{0,4},{4,0},{1,5},{5,1},{2,6},{6,2},{3,7},{7,3},{8,12},{12,8},{9,1... | collective-permute-start | bytes 98312 | tf_op jit(solution)/shard_map/ppermute | solution.py:439

commit v4 on v3

--- a/solution.py
+++ b/solution.py
@@ -29,7 +29,7 @@
     )
 
 
-def advance_kernel(accepted, prev_forget, prev_input, state, new_state, rounded, live):
+def advance_kernel(accepted, prev_forget, prev_input, state, new_state, live):
     block = pl.program_id(0)
     count, proposals, size = prev_forget.shape
     lanes = prev_input.shape[2]
@@ -54,7 +54,6 @@
         for p in range(proposals):
             fresh = fresh + terms[p][s : s + 1] * values[p][:, s : s + 1]
         new_state[s] = fresh
-        rounded[s] = fresh.astype(jnp.bfloat16)
 
 
 def advance(accepted, prev_forget, prev_input, state):
@@ -71,8 +70,8 @@
             pl.BlockSpec((proposals, values, seqs), lambda i: (0, 0, 0)),
             span,
         ],
-        out_specs=[span, span],
-        out_shape=[shaped(state.shape, jnp.float32), shaped(state.shape, jnp.bfloat16)],
+        out_specs=span,
+        out_shape=shaped(state.shape, jnp.float32),
         scratch_shapes=[pltpu.VMEM((keys, seqs), jnp.float32)],
         name="advance",
         cost_estimate=pl.CostEstimate(
@@ -93,23 +92,31 @@
     return jnp.concatenate([*parts, rest], axis=0).astype(jnp.bfloat16)
 
 
-def source_kernel(tokens, out):
+def source_kernel(tokens, gain, weight, out, folded):
     steps = tokens.shape[0]
     for z in range(out.shape[0] // steps):
         out[pl.ds(z * steps, steps)] = tokens[...]
-
-
-def source(tokens, planes):
+    size = gain.shape[1]
+    for b in range(gain.shape[0]):
+        at = pl.ds(b * size, size)
+        value = weight[0, :, at].astype(jnp.float32) * gain[pl.ds(b, 1), :]
+        folded[:, at] = value.astype(jnp.bfloat16)
+
+
+def source(tokens, gain, weight, planes):
     steps, features, seqs = tokens.shape
     return call(
         source_kernel,
-        shaped((planes * steps, features, seqs), jnp.bfloat16),
+        [
+            shaped((planes * steps, features, seqs), jnp.bfloat16),
+            shaped(weight.shape[1:], jnp.bfloat16),
+        ],
         [],
         (1_000_000, 1 << 20),
         60 << 20,
-        [whole()],
-        whole(),
-    )(tokens)
+        [whole()] * 3,
+        [whole()] * 2,
+    )(tokens, gain, weight)
 
 
 def turn_kernel(gain, w_query, w_forget, keyed):
@@ -135,29 +142,10 @@
     )(gain, w_query, w_forget)
 
 
-def fold_kernel(gain, w0, w1, w2, w3, out):
-    values, size = w0.shape[1], gain.shape[1]
-    for b in range(gain.shape[0]):
-        at = pl.ds(b * size, size)
-        for d, weight in enumerate((w0, w1, w2, w3)):
-            value = weight[0, :, at].astype(jnp.float32) * gain[pl.ds(b, 1), :]
-            out[pl.ds(d * values, values), at] = value.astype(jnp.bfloat16)
-
-
-def fold(gain, weights):
-    _, values, width = weights[0].shape
-    return call(
-        fold_kernel,
-        shaped((4 * values, width), jnp.bfloat16),
-        [],
-        (1_000_000_000, 2 << 20),
-        16 << 20,
-        [whole()] * 5,
-        whole(),
-    )(gain, *weights)
-
-
-def project_kernel(own, other, keyed, mixing, o0, o1, o2, o3, held, scale):
+def project_kernel(own, other, keyed, w0, w1, w2, w3, o0, o1, o2, o3, held, scale, mixing):
+    values = w0.shape[0]
+    for d, weight in enumerate((w0, w1, w2, w3)):
+        mixing[pl.ds(d * values, values), :] = weight[...]
     core = lax.axis_index("core")
     blocks, size, seqs = own.shape
     squares = jnp.zeros((8, seqs), jnp.float32)
@@ -175,25 +163,26 @@
     first = first.astype(jnp.bfloat16)
     second = jnp.dot(mixing[...], rows, preferred_element_type=jnp.float32) * factor
     second = second.astype(jnp.bfloat16)
-    keys, values = first.shape[0], second.shape[0] // 4
+    keys = first.shape[0]
     for d, out in enumerate((o0, o1, o2, o3)):
         out[pl.ds(0, keys), :] = first
         out[pl.ds(keys, values), :] = second[d * values : (d + 1) * values]
 
 
-def project(own, other, keyed, mixing):
+def project(own, other, keyed, weights):
     blocks, size, seqs = own.shape
-    rows = keyed.shape[0] + mixing.shape[0] // 4
+    values, width = weights[0].shape
+    rows = keyed.shape[0] + values
     outs = call(
         project_kernel,
         [shaped((rows, seqs), jnp.bfloat16)] * 4
         + [shaped((2 * blocks * size, seqs), jnp.bfloat16), shaped((8, seqs), jnp.float32)],
-        [],
+        [pltpu.VMEM((4 * values, width), jnp.bfloat16)],
         (1_000_000_000, 3 << 20),
         16 << 20,
-        [whole()] * 4,
+        [whole()] * 7,
         [whole()] * 6,
-    )(own, other, keyed, mixing)
+    )(own, other, keyed, *weights)
     return outs[:4], outs[4], outs[5]
 
 
@@ -285,7 +274,7 @@
     group = 8
     for b in range(count // group):
         read = jnp.dot(
-            before[pl.ds(b * group * values, group * values), :],
+            before[pl.ds(b * group * values, group * values), :].astype(jnp.bfloat16),
             asked,
             preferred_element_type=jnp.float32,
         )
@@ -412,27 +401,25 @@
         return [parts[0]] + [lax.ppermute(parts[d], "tp", hops[d]) for d in (1, 2, 3)]
 
     gain = input_norm_gain.reshape(-1, size)
-    own = lax.all_to_all(
-        source(tokens.transpose(1, 2, 0), planes), ("zy", "tp"), 0, 0, tiled=True
-    )
+    spread, folded = source(tokens.transpose(1, 2, 0), gain, w_input, planes)
+    own = lax.all_to_all(spread, ("zy", "tp"), 0, 0, tiled=True)
     own = own.reshape(planes, group * features, seqs)
     other = lax.ppermute(own, "core", swap)
-    inputs = passed([w_input] * group)
+    inputs = passed([folded] * group)
     gates = passed([w_gate] * group)
     keyed = turn(gain, w_query, w_forget)
-    mixing = fold(gain, inputs)
-    new_state, rounded = advance(
+    new_state = advance(
         accepted,
         prev_forget,
         prev_input.reshape(seqs, proposals, -1).transpose(1, 2, 0),
         state[:, 0],
     )
 
-    sends, rows, scale = project(own, other, keyed, mixing)
+    sends, rows, scale = project(own, other, keyed, inputs)
     received = passed(sends)
     ours, theirs = turn_outward(w_out)
     theirs = lax.ppermute(theirs, "core", swap)
-    shown = recur(received, rounded.reshape(-1, size), forget_floor[None], head_gain[None])
+    shown = recur(received, new_state.reshape(-1, size), forget_floor[None], head_gain[None])
     parts = passed(shown)
     opened = gate(gain, gates, rows, scale)
     hidden = hide(parts, opened)

time: 98 us -> 100 us (1.020)
  local copies, waits for them, and re-layouts: 1.29 us -> 2.88 us
  waiting for transfers between devices: 22.8 us -> 24.3 us
    unnamed x24 -> x26, local copies, waits for them, and re-layouts: 1.29 us -> 2.88 us
    ppermute x12, waiting for transfers between devices: 21.6 us -> 23.1 us  [passed(): lax.ppermute(parts[d], 'tp', hops[d])]
  transfers between devices with their start and end apart: 15 -> 15, of which waited for: 6 -> 8; matrix products, arithmetic and copies ran while one was open for 0% -> 0% of each run, Pallas kernels for 8% -> 8%
where the time goes in v4:
time: 100 us
  blocking collectives  42.9 us (43%)
  waiting for transfers between devices  24.3 us (24%)
  starting transfers between devices  18.6 us (19%)
  Pallas kernels  10.7 us (11%)
  local copies, waits for them, and re-layouts  2.88 us (3%)
    all_to_all x1, blocking collectives, body(): own = lax.all_to_all(spread, ('zy', 'tp'), 0, 0, tiled=True)  24.9 us
    ppermute x12, waiting for transfers between devices, passed(): lax.ppermute(parts[d], 'tp', hops[d])  23.1 us
    ppermute x12, starting transfers between devices, passed(): lax.ppermute(parts[d], 'tp', hops[d])  18.4 us
    all_to_all x1, blocking collectives, body(): lax.all_to_all(kept.reshape(planes * group, features, seqs), ('zy', 'tp')...  18 us
    pallas_call x1, Pallas kernels, advance(): pl.pallas_call(advance_kernel, grid=(seqs // count,), in_specs=[pl.BlockS...  3.12 us
    unnamed x26, local copies, waits for them, and re-layouts  2.88 us
  transfers between devices with their start and end apart: 15, of which 8 were waited for; matrix products, arithmetic and copies ran while one was open for 0% of the time, Pallas kernels for 8%

profile of v4, /device:TPU:0, one launch (start us, length us, event | category | flops | bytes accessed | tf_op | source)
XLA Modules:
  0.0 100.2 jit_solution(6789803953851377281)
XLA Ops:
  0.6 1.9 %shard_map.140 = (bf16[64,32,128]{2,1,0:T(8,128)(2,1)}, bf16[32,4096]{1,0:T(8,128)(2,1)}) custom-call(bf16[4,32,128]{2,1,0:T(8,128)(2,1)} %bitcast.31, f32[32,128]{1,0:T(8,128)} %bitcast.24, bf16[1,32,4096]{2,1,0:T(8,128)(2,1)} %weight.1), custom_call_target="tpu_custom_call" | custom-call | flops 1000000 | bytes 1048576 | tf_op jit(solution)/shard_map/pallas_call | solution.py:108
  2.6 24.9 %all_to_all.10 = bf16[64,32,128]{2,1,0:T(8,128)(2,1)S(1)} all-to-all(bf16[64,32,128]{2,1,0:T(8,128)(2,1)} %get-tuple-element.16), channel_id=1, replica_groups=mesh['zy'=16,'core'=2,'tp'=4] {'zy','tp'}, dimensions={0} | all-to-all | bytes 1048576 | tf_op jit(solution)/shard_map/all_to_all | solution.py:405
  27.5 0.6 collective-permute-start.1
  28.1 1.8 %collective-permute-start.2 = (bf16[32,4096]{1,0:T(8,128)(2,1)}, bf16[32,4096]{1,0:T(8,128)(2,1)S(1)}, u32[]{:S(2)}, u32[]{:S(2)}) collective-permute-start(bf16[32,4096]{1,0:T(8,128)(2,1)} %get-tuple-element.17.w0), channel_id=1, source_target_pairs={{0,2},{1,3},{2,0},{3,1},{4,6},{5,7},{6,4},{7,5},{8,10},{9,11},{10,... | collective-permute-start | bytes 786440 | tf_op jit(solution)/shard_map/ppermute | solution.py:401
  29.9 2.3 %collective-permute-start.3 = (bf16[32,4096]{1,0:T(8,128)(2,1)}, bf16[32,4096]{1,0:T(8,128)(2,1)S(1)}, u32[]{:S(2)}, u32[]{:S(2)}) collective-permute-start(bf16[32,4096]{1,0:T(8,128)(2,1)} %get-tuple-element.17.w0), channel_id=1, source_target_pairs={{0,3},{1,2},{2,1},{3,0},{4,7},{5,6},{6,5},{7,4},{8,11},{9,10},{10,... | collective-permute-start | bytes 786440 | tf_op jit(solution)/shard_map/ppermute | solution.py:401
  32.2 1.2 %copy-done.9 = bf16[128,4096]{1,0:T(8,128)(2,1)S(1)} copy-done((bf16[128,4096]{1,0:T(8,128)(2,1)S(1)}, bf16[128,4096]{1,0:T(8,128)(2,1)}, u32[]{:S(2)}) %copy-start.9) | copy-done | bytes 1048600
  33.5 0.7 shard_map.146
  34.3 0.7 shard_map.141.keyed
  35.0 1.9 %collective-permute-done.1.w1 = bf16[32,4096]{1,0:T(8,128)(2,1)S(1)} collective-permute-done((bf16[32,4096]{1,0:T(8,128)(2,1)}, bf16[32,4096]{1,0:T(8,128)(2,1)S(1)}, u32[]{:S(2)}, u32[]{:S(2)}) %collective-permute-start.1) | collective-permute-done | bytes 262176 | tf_op jit(solution)/shard_map/ppermute | solution.py:401
  36.9 5.5 %collective-permute-done.2.w2 = bf16[32,4096]{1,0:T(8,128)(2,1)S(1)} collective-permute-done((bf16[32,4096]{1,0:T(8,128)(2,1)}, bf16[32,4096]{1,0:T(8,128)(2,1)S(1)}, u32[]{:S(2)}, u32[]{:S(2)}) %collective-permute-start.2) | collective-permute-done | bytes 262176 | tf_op jit(solution)/shard_map/ppermute | solution.py:401
  42.4 2.6 %collective-permute-done.3.w3 = bf16[32,4096]{1,0:T(8,128)(2,1)S(1)} collective-permute-done((bf16[32,4096]{1,0:T(8,128)(2,1)}, bf16[32,4096]{1,0:T(8,128)(2,1)S(1)}, u32[]{:S(2)}, u32[]{:S(2)}) %collective-permute-start.3) | collective-permute-done | bytes 262176 | tf_op jit(solution)/shard_map/ppermute | solution.py:401
  45.0 1.1 %shard_map.142 = (bf16[288,128]{1,0:T(8,128)(2,1)S(1)}, bf16[288,128]{1,0:T(8,128)(2,1)S(1)}, bf16[288,128]{1,0:T(8,128)(2,1)S(1)}, bf16[288,128]{1,0:T(8,128)(2...) custom-call(bf16[16,128,128]{2,1,0:T(8,128)(2,1)S(1)} %bitcast.23, ...), custom_call_target="tpu_custom_call" | custom-call | flops 1000000000 | bytes 3145728 | tf_op jit(solution)/shard_map/pallas_call | solution.py:176
  46.2 0.1 collective-permute-start.4
  46.3 2.0 %collective-permute-start.10 = (bf16[1,32,4096]{2,1,0:T(8,128)(2,1)S(1)}, bf16[1,32,4096]{2,1,0:T(8,128)(2,1)S(1)}, u32[]{:S(2)}, u32[]{:S(2)}) collective-permute-start(bf16[1,32,4096]{2,1,0:T(8,128)(2,1)S(1)} %copy-done.10), channel_id=1, source_target_pairs={{0,1},{1,0},{2,3},{3,2},{4,5},{5,4},{6,7},{7,6},{8,9},{9,8},{10,11... | collective-permute-start | bytes 786440 | tf_op jit(solution)/shard_map/ppermute | solution.py:401
  48.3 1.9 %collective-permute-start.5 = (bf16[288,128]{1,0:T(8,128)(2,1)S(1)}, bf16[288,128]{1,0:T(8,128)(2,1)S(1)}, u32[]{:S(2)}, u32[]{:S(2)}) collective-permute-start(bf16[288,128]{1,0:T(8,128)(2,1)S(1)} %get-tuple-element.20), channel_id=1, source_target_pairs={{0,2},{1,3},{2,0},{3,1},{4,6},{5,7},{6,4},{7,5},{8,10},{9,11},{10,... | collective-permute-start | bytes 221192 | tf_op jit(solution)/shard_map/ppermute | solution.py:401
  50.2 1.7 %collective-permute-start.11 = (bf16[1,32,4096]{2,1,0:T(8,128)(2,1)S(1)}, bf16[1,32,4096]{2,1,0:T(8,128)(2,1)S(1)}, u32[]{:S(2)}, u32[]{:S(2)}) collective-permute-start(bf16[1,32,4096]{2,1,0:T(8,128)(2,1)S(1)} %copy-done.10), channel_id=1, source_target_pairs={{0,2},{1,3},{2,0},{3,1},{4,6},{5,7},{6,4},{7,5},{8,10},{9,11},{10,... | collective-permute-start | bytes 786440 | tf_op jit(solution)/shard_map/ppermute | solution.py:401
  51.8 2.3 %collective-permute-start.12 = (bf16[1,32,4096]{2,1,0:T(8,128)(2,1)S(1)}, bf16[1,32,4096]{2,1,0:T(8,128)(2,1)S(1)}, u32[]{:S(2)}, u32[]{:S(2)}) collective-permute-start(bf16[1,32,4096]{2,1,0:T(8,128)(2,1)S(1)} %copy-done.10), channel_id=1, source_target_pairs={{0,3},{1,2},{2,1},{3,0},{4,7},{5,6},{6,5},{7,4},{8,11},{9,10},{10,... | collective-permute-start | bytes 786440 | tf_op jit(solution)/shard_map/ppermute | solution.py:401
  54.2 6.3 %collective-permute-done.5.r2 = bf16[288,128]{1,0:T(8,128)(2,1)S(1)} collective-permute-done((bf16[288,128]{1,0:T(8,128)(2,1)S(1)}, bf16[288,128]{1,0:T(8,128)(2,1)S(1)}, u32[]{:S(2)}, u32[]{:S(2)}) %collective-permute-start.5) | collective-permute-done | bytes 73760 | tf_op jit(solution)/shard_map/ppermute | solution.py:401
  60.5 0.9 collective-permute-start.6
  61.4 3.1 %advance.1 = f32[128,32,128]{2,1,0:T(8,128)} custom-call(s32[1,128]{1,0:T(1,128)S(1)} %bitcast.28, f32[128,4,128]{2,1,0:T(4,128)S(1)} %copy-done.4, bf16[4,32,128]{2,1,0:T(8,128)(2,1)S(1)} %bitcast.27, f32[128,32,128]{2,1,0:T(8,128)S(1)} %bitcast.17), custom_call_target="tpu_custom_call" | custom-call | flops 1000000000 | bytes 5242880 | tf_op jit(solution)/shard_map/advance/pallas_call | solution.py:64
  64.5 3.4 %collective-permute-done.6.r3 = bf16[288,128]{1,0:T(8,128)(2,1)S(1)} collective-permute-done((bf16[288,128]{1,0:T(8,128)(2,1)S(1)}, bf16[288,128]{1,0:T(8,128)(2,1)S(1)}, u32[]{:S(2)}, u32[]{:S(2)}) %collective-permute-start.6) | collective-permute-done | bytes 73760 | tf_op jit(solution)/shard_map/ppermute | solution.py:401
  67.9 1.6 %copy-done.1 = f32[128,32,128]{2,1,0:T(8,128)S(1)} copy-done((f32[128,32,128]{2,1,0:T(8,128)S(1)}, f32[128,32,128]{2,1,0:T(8,128)}, u32[]{:S(2)}) %copy-start.1) | copy-done | bytes 2097176
  69.5 1.4 %shard_map.143 = (bf16[48,128]{1,0:T(8,128)(2,1)S(1)}, bf16[48,128]{1,0:T(8,128)(2,1)S(1)}, bf16[48,128]{1,0:T(8,128)(2,1)S(1)}, bf16[48,128]{1,0:T(8,128)(2,1)S(1)}) custom-call(bf16[288,128]{1,0:T(8,128)(2,1)S(1)} %get-tuple-element.18.r0, bf16[288,128]{1,0:T(8,128)(2,1)S(1)} %collective-permute-done.4.r1, bf16[288,128]{1,0:T(8,128)(2,1)S(1)} %collective-permute-done.5.r2, ...), custom_call_target="tpu_custom_call" | custom-call | flops 1000000000 | bytes 2097152 | tf_op jit(solution)/shard_map/pallas_call | solution.py:298
  71.0 3.7 %collective-permute-start.8 = (bf16[48,128]{1,0:T(8,128)(2,1)S(1)}, bf16[48,128]{1,0:T(8,128)(2,1)S(1)}, u32[]{:S(2)}, u32[]{:S(2)}) collective-permute-start(bf16[48,128]{1,0:T(8,128)(2,1)S(1)} %get-tuple-element.24), channel_id=1, source_target_pairs={{0,2},{1,3},{2,0},{3,1},{4,6},{5,7},{6,4},{7,5},{8,10},{9,11},{10,... | collective-permute-start | bytes 36872 | tf_op jit(solution)/shard_map/ppermute | solution.py:401
  74.8 0.9 collective-permute-start.9
  75.7 0.5 shard_map.144.gates
  76.3 0.3 collective-permute-done.8.p2
  76.6 3.1 %collective-permute-done.9.p3 = bf16[48,128]{1,0:T(8,128)(2,1)S(1)} collective-permute-done((bf16[48,128]{1,0:T(8,128)(2,1)S(1)}, bf16[48,128]{1,0:T(8,128)(2,1)S(1)}, u32[]{:S(2)}, u32[]{:S(2)}) %collective-permute-start.9) | collective-permute-done | bytes 12320 | tf_op jit(solution)/shard_map/ppermute | solution.py:401
  79.8 1.2 %collective-permute-done.13.other = bf16[128,128]{1,0:T(8,128)(2,1)S(1)} collective-permute-done((bf16[128,128]{1,0:T(8,128)(2,1)S(1)}, bf16[128,128]{1,0:T(8,128)(2,1)S(1)}, u32[]{:S(2)}, u32[]{:S(2)}) %collective-permute-start.13) | collective-permute-done | bytes 32800 | tf_op jit(solution)/shard_map/ppermute | solution.py:426
  81.0 0.4 shard_map.147
  81.4 18.0 %all_to_all.11 = bf16[64,32,128]{2,1,0:T(8,128)(2,1)S(1)} all-to-all(bf16[64,32,128]{2,1,0:T(8,128)(2,1)S(1)} %bitcast.20), channel_id=1, replica_groups=mesh['zy'=16,'core'=2,'tp'=4] {'zy','tp'}, dimensions={0} | all-to-all | bytes 1048576 | tf_op jit(solution)/shard_map/all_to_all | solution.py:427
  99.5 0.7 shard_map.148
  (36 shorter events, 0.4 us)
Async XLA Ops:
  27.4 6.8 %copy-start.2 = (bf16[4096,128]{1,0:T(8,128)(2,1)S(1)}, bf16[4096,128]{1,0:T(8,128)(2,1)}, u32[]{:S(2)}) copy-start(bf16[4096,128]{1,0:T(8,128)(2,1)} %w_query.1) | copy-start | bytes 3145732
  27.5 6.8 %copy-start.3 = (bf16[4096,128]{1,0:T(8,128)(2,1)S(1)}, bf16[4096,128]{1,0:T(8,128)(2,1)}, u32[]{:S(2)}) copy-start(bf16[4096,128]{1,0:T(8,128)(2,1)} %w_forget.1) | copy-start | bytes 3145732
  27.5 6.8 %copy-start.6 = (f32[4096]{0:T(1024)S(1)}, f32[4096]{0:T(1024)}, u32[]{:S(2)}) copy-start(f32[4096]{0:T(1024)} %param.14) | copy-start | bytes 49156
  27.5 17.6 %collective-permute-start = (bf16[16,128,128]{2,1,0:T(8,128)(2,1)S(1)}, bf16[16,128,128]{2,1,0:T(8,128)(2,1)S(1)}, u32[]{:S(2)}, u32[]{:S(2)}) collective-permute-start(bf16[16,128,128]{2,1,0:T(8,128)(2,1)S(1)} %bitcast.22), channel_id=1, source_target_pairs={{0,4},{4,0},{1,5},{5,1},{2,6},{6,2},{3,7},{7,3},{8,12},{12,8},{9,1... | collective-permute-start | bytes 1572872 | tf_op jit(solution)/shard_map/ppermute | solution.py:407
  27.5 9.5 %collective-permute-start.1 = (bf16[32,4096]{1,0:T(8,128)(2,1)}, bf16[32,4096]{1,0:T(8,128)(2,1)S(1)}, u32[]{:S(2)}, u32[]{:S(2)}) collective-permute-start(bf16[32,4096]{1,0:T(8,128)(2,1)} %get-tuple-element.17.w0), channel_id=1, source_target_pairs={{0,1},{1,0},{2,3},{3,2},{4,5},{5,4},{6,7},{7,6},{8,9},{9,8},{10,11... | collective-permute-start | bytes 786440 | tf_op jit(solution)/shard_map/ppermute | solution.py:401
  28.1 14.3 %collective-permute-start.2 = (bf16[32,4096]{1,0:T(8,128)(2,1)}, bf16[32,4096]{1,0:T(8,128)(2,1)S(1)}, u32[]{:S(2)}, u32[]{:S(2)}) collective-permute-start(bf16[32,4096]{1,0:T(8,128)(2,1)} %get-tuple-element.17.w0), channel_id=1, source_target_pairs={{0,2},{1,3},{2,0},{3,1},{4,6},{5,7},{6,4},{7,5},{8,10},{9,11},{10,... | collective-permute-start | bytes 786440 | tf_op jit(solution)/shard_map/ppermute | solution.py:401
  29.9 15.1 %collective-permute-start.3 = (bf16[32,4096]{1,0:T(8,128)(2,1)}, bf16[32,4096]{1,0:T(8,128)(2,1)S(1)}, u32[]{:S(2)}, u32[]{:S(2)}) collective-permute-start(bf16[32,4096]{1,0:T(8,128)(2,1)} %get-tuple-element.17.w0), channel_id=1, source_target_pairs={{0,3},{1,2},{2,1},{3,0},{4,7},{5,6},{6,5},{7,4},{8,11},{9,10},{10,... | collective-permute-start | bytes 786440 | tf_op jit(solution)/shard_map/ppermute | solution.py:401
  32.2 1.2 %copy-start.9 = (bf16[128,4096]{1,0:T(8,128)(2,1)S(1)}, bf16[128,4096]{1,0:T(8,128)(2,1)}, u32[]{:S(2)}) copy-start(bf16[128,4096]{1,0:T(8,128)(2,1)} %w_out.1) | copy-start | bytes 3145732
  34.1 10.9 %copy-start.5 = (bf16[32,4096]{1,0:T(8,128)(2,1)S(1)}, bf16[32,4096]{1,0:T(8,128)(2,1)}, u32[]{:S(2)}) copy-start(bf16[32,4096]{1,0:T(8,128)(2,1)} %get-tuple-element.17.w0) | copy-start | bytes 786436
  34.2 45.7 %collective-permute-start.14 = (bf16[16,128,128]{2,1,0:T(8,128)(2,1)S(1)}, bf16[16,128,128]{2,1,0:T(8,128)(2,1)S(1)}, u32[]{:S(2)}, u32[]{:S(2)}) collective-permute-start(bf16[16,128,128]{2,1,0:T(8,128)(2,1)S(1)} %get-tuple-element.29), channel_id=1, source_target_pairs={{0,4},{4,0},{1,5},{5,1},{2,6},{6,2},{3,7},{7,3},{8,12},{12,8},{9,1... | collective-permute-start | bytes 1572872 | tf_op jit(solution)/shard_map/ppermute | solution.py:421
  35.0 11.3 %copy-start.10 = (bf16[1,32,4096]{2,1,0:T(8,128)(2,1)S(1)}, bf16[1,32,4096]{2,1,0:T(8,128)(2,1)}, u32[]{:S(2)}) copy-start(bf16[1,32,4096]{2,1,0:T(8,128)(2,1)} %w0.1) | copy-start | bytes 786436
  35.0 26.4 %copy-start = (f32[128,1,32,128]{3,2,1,0:T(8,128)S(1)}, f32[128,1,32,128]{3,2,1,0:T(8,128)}, u32[]{:S(2)}) copy-start(f32[128,1,32,128]{3,2,1,0:T(8,128)} %param.22) | copy-start | bytes 6291460
  35.0 26.4 %copy-start.4 = (f32[128,4,128]{2,1,0:T(4,128)S(1)}, f32[128,4,128]{2,1,0:T(4,128)}, u32[]{:S(2)}) copy-start(f32[128,4,128]{2,1,0:T(4,128)} %prev_forget.1) | copy-start | bytes 786436
  35.0 26.4 %copy-start.7 = (bf16[128,4,1,32]{0,3,2,1:T(8,128)(2,1)S(1)}, bf16[128,4,1,32]{0,3,2,1:T(8,128)(2,1)}, u32[]{:S(2)}) copy-start(bf16[128,4,1,32]{0,3,2,1:T(8,128)(2,1)} %param.24) | copy-start | bytes 98308
  35.0 26.4 %copy-start.8 = (s32[128]{0:T(128)S(1)}, s32[128]{0:T(128)}, u32[]{:S(2)}) copy-start(s32[128]{0:T(128)} %param.25) | copy-start | bytes 1540
  46.2 5.6 %collective-permute-start.4 = (bf16[288,128]{1,0:T(8,128)(2,1)S(1)}, bf16[288,128]{1,0:T(8,128)(2,1)S(1)}, u32[]{:S(2)}, u32[]{:S(2)}) collective-permute-start(bf16[288,128]{1,0:T(8,128)(2,1)S(1)} %get-tuple-element.19), channel_id=1, source_target_pairs={{0,1},{1,0},{2,3},{3,2},{4,5},{5,4},{6,7},{7,6},{8,9},{9,8},{10,11... | collective-permute-start | bytes 221192 | tf_op jit(solution)/shard_map/ppermute | solution.py:401
  46.3 24.8 %collective-permute-start.10 = (bf16[1,32,4096]{2,1,0:T(8,128)(2,1)S(1)}, bf16[1,32,4096]{2,1,0:T(8,128)(2,1)S(1)}, u32[]{:S(2)}, u32[]{:S(2)}) collective-permute-start(bf16[1,32,4096]{2,1,0:T(8,128)(2,1)S(1)} %copy-done.10), channel_id=1, source_target_pairs={{0,1},{1,0},{2,3},{3,2},{4,5},{5,4},{6,7},{7,6},{8,9},{9,8},{10,11... | collective-permute-start | bytes 786440 | tf_op jit(solution)/shard_map/ppermute | solution.py:401
  48.3 12.2 %collective-permute-start.5 = (bf16[288,128]{1,0:T(8,128)(2,1)S(1)}, bf16[288,128]{1,0:T(8,128)(2,1)S(1)}, u32[]{:S(2)}, u32[]{:S(2)}) collective-permute-start(bf16[288,128]{1,0:T(8,128)(2,1)S(1)} %get-tuple-element.20), channel_id=1, source_target_pairs={{0,2},{1,3},{2,0},{3,1},{4,6},{5,7},{6,4},{7,5},{8,10},{9,11},{10,... | collective-permute-start | bytes 221192 | tf_op jit(solution)/shard_map/ppermute | solution.py:401
  50.2 24.6 %collective-permute-start.11 = (bf16[1,32,4096]{2,1,0:T(8,128)(2,1)S(1)}, bf16[1,32,4096]{2,1,0:T(8,128)(2,1)S(1)}, u32[]{:S(2)}, u32[]{:S(2)}) collective-permute-start(bf16[1,32,4096]{2,1,0:T(8,128)(2,1)S(1)} %copy-done.10), channel_id=1, source_target_pairs={{0,2},{1,3},{2,0},{3,1},{4,6},{5,7},{6,4},{7,5},{8,10},{9,11},{10,... | collective-permute-start | bytes 786440 | tf_op jit(solution)/shard_map/ppermute | solution.py:401
  51.8 23.9 %collective-permute-start.12 = (bf16[1,32,4096]{2,1,0:T(8,128)(2,1)S(1)}, bf16[1,32,4096]{2,1,0:T(8,128)(2,1)S(1)}, u32[]{:S(2)}, u32[]{:S(2)}) collective-permute-start(bf16[1,32,4096]{2,1,0:T(8,128)(2,1)S(1)} %copy-done.10), channel_id=1, source_target_pairs={{0,3},{1,2},{2,1},{3,0},{4,7},{5,6},{6,5},{7,4},{8,11},{9,10},{10,... | collective-permute-start | bytes 786440 | tf_op jit(solution)/shard_map/ppermute | solution.py:401
  60.5 7.4 %collective-permute-start.6 = (bf16[288,128]{1,0:T(8,128)(2,1)S(1)}, bf16[288,128]{1,0:T(8,128)(2,1)S(1)}, u32[]{:S(2)}, u32[]{:S(2)}) collective-permute-start(bf16[288,128]{1,0:T(8,128)(2,1)S(1)} %get-tuple-element.21), channel_id=1, source_target_pairs={{0,3},{1,2},{2,1},{3,0},{4,7},{5,6},{6,5},{7,4},{8,11},{9,10},{10,... | collective-permute-start | bytes 221192 | tf_op jit(solution)/shard_map/ppermute | solution.py:401
  61.4 6.5 %copy-start.11 = (f32[128]{0:T(128)S(1)}, f32[128]{0:T(128)}, u32[]{:S(2)}) copy-start(f32[128]{0:T(128)} %param.19) | copy-start | bytes 1540
  61.4 6.5 %copy-start.12 = (f32[32]{0:T(128)S(1)}, f32[32]{0:T(128)}, u32[]{:S(2)}) copy-start(f32[32]{0:T(128)} %param.20) | copy-start | bytes 388
  67.9 1.6 %copy-start.1 = (f32[128,32,128]{2,1,0:T(8,128)S(1)}, f32[128,32,128]{2,1,0:T(8,128)}, u32[]{:S(2)}) copy-start(f32[128,32,128]{2,1,0:T(8,128)} %advance.1) | copy-start | bytes 6291460
  70.9 5.3 %collective-permute-start.7 = (bf16[48,128]{1,0:T(8,128)(2,1)S(1)}, bf16[48,128]{1,0:T(8,128)(2,1)S(1)}, u32[]{:S(2)}, u32[]{:S(2)}) collective-permute-start(bf16[48,128]{1,0:T(8,128)(2,1)S(1)} %get-tuple-element.23), channel_id=1, source_target_pairs={{0,1},{1,0},{2,3},{3,2},{4,5},{5,4},{6,7},{7,6},{8,9},{9,8},{10,11... | collective-permute-start | bytes 36872 | tf_op jit(solution)/shard_map/ppermute | solution.py:401
  71.0 5.5 %collective-permute-start.8 = (bf16[48,128]{1,0:T(8,128)(2,1)S(1)}, bf16[48,128]{1,0:T(8,128)(2,1)S(1)}, u32[]{:S(2)}, u32[]{:S(2)}) collective-permute-start(bf16[48,128]{1,0:T(8,128)(2,1)S(1)} %get-tuple-element.24), channel_id=1, source_target_pairs={{0,2},{1,3},{2,0},{3,1},{4,6},{5,7},{6,4},{7,5},{8,10},{9,11},{10,... | collective-permute-start | bytes 36872 | tf_op jit(solution)/shard_map/ppermute | solution.py:401
  74.8 4.9 %collective-permute-start.9 = (bf16[48,128]{1,0:T(8,128)(2,1)S(1)}, bf16[48,128]{1,0:T(8,128)(2,1)S(1)}, u32[]{:S(2)}, u32[]{:S(2)}) collective-permute-start(bf16[48,128]{1,0:T(8,128)(2,1)S(1)} %get-tuple-element.25), channel_id=1, source_target_pairs={{0,3},{1,2},{2,1},{3,0},{4,7},{5,6},{6,5},{7,4},{8,11},{9,10},{10,... | collective-permute-start | bytes 36872 | tf_op jit(solution)/shard_map/ppermute | solution.py:401
  79.7 1.3 %collective-permute-start.13 = (bf16[128,128]{1,0:T(8,128)(2,1)S(1)}, bf16[128,128]{1,0:T(8,128)(2,1)S(1)}, u32[]{:S(2)}, u32[]{:S(2)}) collective-permute-start(bf16[128,128]{1,0:T(8,128)(2,1)S(1)} %shard_map.145.hidden), channel_id=1, source_target_pairs={{0,4},{4,0},{1,5},{5,1},{2,6},{6,2},{3,7},{7,3},{8,12},{12,8},{9,1... | collective-permute-start | bytes 98312 | tf_op jit(solution)/shard_map/ppermute | solution.py:426

commit v5 on v1

--- a/solution.py
+++ b/solution.py
@@ -93,23 +93,32 @@
     return jnp.concatenate([*parts, rest], axis=0).astype(jnp.bfloat16)
 
 
-def source_kernel(tokens, out):
+def source_kernel(tokens, gain, w_input, w_gate, out, folded):
     steps = tokens.shape[0]
     for z in range(out.shape[0] // steps):
         out[pl.ds(z * steps, steps)] = tokens[...]
-
-
-def source(tokens, planes):
+    size = gain.shape[1]
+    for b in range(gain.shape[0]):
+        at = pl.ds(b * size, size)
+        for i, weight in enumerate((w_input, w_gate)):
+            value = weight[0, :, at].astype(jnp.float32) * gain[pl.ds(b, 1), :]
+            folded[i, :, at] = value.astype(jnp.bfloat16)
+
+
+def source(tokens, gain, w_input, w_gate, planes):
     steps, features, seqs = tokens.shape
     return call(
         source_kernel,
-        shaped((planes * steps, features, seqs), jnp.bfloat16),
+        [
+            shaped((planes * steps, features, seqs), jnp.bfloat16),
+            shaped((2, *w_input.shape[1:]), jnp.bfloat16),
+        ],
         [],
         (1_000_000, 1 << 20),
         60 << 20,
-        [whole()],
-        whole(),
-    )(tokens)
+        [whole()] * 4,
+        [whole()] * 2,
+    )(tokens, gain, w_input, w_gate)
 
 
 def turn_kernel(gain, w_query, w_forget, keyed):
@@ -135,29 +144,20 @@
     )(gain, w_query, w_forget)
 
 
-def fold_kernel(gain, w0, w1, w2, w3, out):
-    values, size = w0.shape[1], gain.shape[1]
-    for b in range(gain.shape[0]):
-        at = pl.ds(b * size, size)
-        for d, weight in enumerate((w0, w1, w2, w3)):
-            value = weight[0, :, at].astype(jnp.float32) * gain[pl.ds(b, 1), :]
-            out[pl.ds(d * values, values), at] = value.astype(jnp.bfloat16)
-
-
-def fold(gain, weights):
-    _, values, width = weights[0].shape
-    return call(
-        fold_kernel,
-        shaped((4 * values, width), jnp.bfloat16),
-        [],
-        (1_000_000_000, 2 << 20),
-        16 << 20,
-        [whole()] * 5,
-        whole(),
-    )(gain, *weights)
-
-
-def project_kernel(own, other, keyed, mixing, o0, o1, o2, o3, held, scale):
+def bring(which, weights, held, sems):
+    copies = [
+        pltpu.make_async_copy(ref.at[which if ref.shape[0] > 1 else 0], held.at[d], sems.at[d])
+        for d, ref in enumerate(weights)
+    ]
+    for copy in copies:
+        copy.start()
+    return copies
+
+
+def project_kernel(
+    own, other, keyed, w0, w1, w2, w3, o0, o1, o2, o3, held, scale, mixing, sems
+):
+    copies = bring(0, (w0, w1, w2, w3), mixing, sems)
     core = lax.axis_index("core")
     blocks, size, seqs = own.shape
     squares = jnp.zeros((8, seqs), jnp.float32)
@@ -173,53 +173,56 @@
     rows = held[...]
     first = jnp.dot(keyed[...], rows, preferred_element_type=jnp.float32) * factor
     first = first.astype(jnp.bfloat16)
-    second = jnp.dot(mixing[...], rows, preferred_element_type=jnp.float32) * factor
+    for copy in copies:
+        copy.wait()
+    group, values, width = mixing.shape
+    mixed = mixing[...].reshape(group * values, width)
+    second = jnp.dot(mixed, rows, preferred_element_type=jnp.float32) * factor
     second = second.astype(jnp.bfloat16)
-    keys, values = first.shape[0], second.shape[0] // 4
+    keys = first.shape[0]
     for d, out in enumerate((o0, o1, o2, o3)):
         out[pl.ds(0, keys), :] = first
         out[pl.ds(keys, values), :] = second[d * values : (d + 1) * values]
 
 
-def project(own, other, keyed, mixing):
+def project(own, other, keyed, weights):
     blocks, size, seqs = own.shape
-    rows = keyed.shape[0] + mixing.shape[0] // 4
+    _, values, width = weights[0].shape
+    rows = keyed.shape[0] + values
     outs = call(
         project_kernel,
         [shaped((rows, seqs), jnp.bfloat16)] * 4
         + [shaped((2 * blocks * size, seqs), jnp.bfloat16), shaped((8, seqs), jnp.float32)],
-        [],
+        [pltpu.VMEM((4, values, width), jnp.bfloat16), pltpu.SemaphoreType.DMA((4,))],
         (1_000_000_000, 3 << 20),
         16 << 20,
-        [whole()] * 4,
+        [whole()] * 3 + [pl.BlockSpec(memory_space=pltpu.HBM)] * 4,
         [whole()] * 6,
-    )(own, other, keyed, mixing)
+    )(own, other, keyed, *weights)
     return outs[:4], outs[4], outs[5]
 
 
-def gate_kernel(gain, w0, w1, w2, w3, rows, scale, out, held):
-    values, size = w0.shape[1], gain.shape[1]
-    for b in range(gain.shape[0]):
-        at = pl.ds(b * size, size)
-        for d, weight in enumerate((w0, w1, w2, w3)):
-            value = weight[0, :, at].astype(jnp.float32) * gain[pl.ds(b, 1), :]
-            held[pl.ds(d * values, values), at] = value.astype(jnp.bfloat16)
-    raw = jnp.dot(held[...], rows[...], preferred_element_type=jnp.float32) * scale[0:1]
+def gate_kernel(w0, w1, w2, w3, rows, scale, out, mixing, sems):
+    for copy in bring(1, (w0, w1, w2, w3), mixing, sems):
+        copy.wait()
+    group, values, width = mixing.shape
+    mixed = mixing[...].reshape(group * values, width)
+    raw = jnp.dot(mixed, rows[...], preferred_element_type=jnp.float32) * scale[0:1]
     raw = raw.astype(jnp.bfloat16).astype(jnp.float32)
     out[...] = raw * jax.nn.sigmoid(raw)
 
 
-def gate(gain, weights, rows, scale):
+def gate(weights, rows, scale):
     _, values, width = weights[0].shape
     return call(
         gate_kernel,
         shaped((4 * values, rows.shape[1]), jnp.float32),
-        [pltpu.VMEM((4 * values, width), jnp.bfloat16)],
+        [pltpu.VMEM((4, values, width), jnp.bfloat16), pltpu.SemaphoreType.DMA((4,))],
         (1_000_000_000, 3 << 20),
         16 << 20,
-        [whole()] * 7,
+        [pl.BlockSpec(memory_space=pltpu.HBM)] * 4 + [whole()] * 2,
         whole(),
-    )(gain, *weights, rows, scale)
+    )(*weights, rows, scale)
 
 
 def outward_kernel(w_out, outward, held, sems):
@@ -402,13 +405,16 @@
         return [parts[0]] + [lax.ppermute(parts[d], "tp", hops[d]) for d in (1, 2, 3)]
 
     gain = input_norm_gain.reshape(-1, size)
-    inputs = passed([w_input] * group)
-    own = lax.all_to_all(source(tokens.transpose(1, 2, 0), planes), ("zy", "tp"), 0, 0, tiled=True)
+    spread, folded = source(tokens.transpose(1, 2, 0), gain, w_input, w_gate, planes)
+    far = lax.ppermute(folded, "tp", hops[2])
+    own = lax.all_to_all(spread, ("zy", "tp"), 0, 0, tiled=True)
     own = own.reshape(planes, group * features, seqs)
     other = lax.ppermute(own, "core", swap)
-    gates = passed([w_gate] * group)
+    near = [lax.ppermute(folded[:1], "tp", hops[d]) for d in (1, 3)]
+    inputs = [folded, near[0], far, near[1]]
+    near = [lax.ppermute(folded[1:], "tp", hops[d]) for d in (1, 3)]
+    gates = [folded, near[0], far, near[1]]
     keyed = turn(gain, w_query, w_forget)
-    mixing = fold(gain, inputs)
     new_state, rounded = advance(
         accepted,
         prev_forget,
@@ -416,12 +422,12 @@
         state[:, 0],
     )
 
-    sends, rows, scale = project(own, other, keyed, mixing)
+    sends, rows, scale = project(own, other, keyed, inputs)
     received = passed(sends)
     shown = recur(received, rounded.reshape(-1, size), forget_floor[None], head_gain[None])
     parts = passed(shown)
     outward = turn_outward(w_out)
-    opened = gate(gain, gates, rows, scale)
+    opened = gate(gates, rows, scale)
     sent = outward_half(away_kernel, parts, opened, outward)
     came = lax.ppermute(sent, "core", swap)
     kept = outward_half(keep_kernel, parts, opened, outward, came)

time: 92.3 us -> 90.2 us (0.977)
  blocking collectives: 43.3 us -> 25.8 us
  starting transfers between devices: 17.8 us -> 28.3 us
  waiting for transfers between devices: 17.2 us -> 22.4 us
    all_to_all x1 -> x0, blocking collectives: 24.9 us -> none  [body(): lax.all_to_all(source(tokens.transpose(1, 2, 0), planes), ('zy', 'tp'), 0...]
    ppermute x12 -> x6, waiting for transfers between devices: 15.3 us -> 3.52 us  [passed(): lax.ppermute(parts[d], 'tp', hops[d])]
    all_to_all x0 -> x1, waiting for transfers between devices: none -> 11.5 us  [body(): own = lax.all_to_all(spread, ('zy', 'tp'), 0, 0, tiled=True)]
    all_to_all x0 -> x1, starting transfers between devices: none -> 11.5 us  [body(): own = lax.all_to_all(spread, ('zy', 'tp'), 0, 0, tiled=True)]
    ppermute x12 -> x6, starting transfers between devices: 17.7 us -> 9.55 us  [passed(): lax.ppermute(parts[d], 'tp', hops[d])]
    all_to_all x1, blocking collectives: 18.5 us -> 25.8 us  [body(): lax.all_to_all(kept.reshape(planes * group, features, seqs), ('zy', 'tp')...]
    ppermute x0 -> x5, starting transfers between devices: none -> 7.16 us  [the longest x1 3.15 us: body(): far = lax.ppermute(folded, 'tp', hops[2])]
    ppermute x0 -> x5, waiting for transfers between devices: none -> 5.44 us  [the longest x2 5.43 us: body(): near = [lax.ppermute(folded[:1], 'tp', hops[d]) for d in (1, 3)]]
  transfers between devices with their start and end apart: 14 -> 14, of which waited for: 6 -> 5; matrix products, arithmetic and copies ran while one was open for 0% -> 1% of each run, Pallas kernels for 9% -> 9%
where the time goes in v5:
time: 90.2 us; the launch traced here: 89.9 us
  starting transfers between devices  28.3 us (31%)
  blocking collectives  25.8 us (29%)
  waiting for transfers between devices  22.4 us (25%)
  Pallas kernels  11.4 us (13%)
  local copies, waits for them, and re-layouts  1.13 us (1%)
    all_to_all x1, blocking collectives, body(): lax.all_to_all(kept.reshape(planes * group, features, seqs), ('zy', 'tp')...  25.8 us
    all_to_all x1, waiting for transfers between devices, body(): own = lax.all_to_all(spread, ('zy', 'tp'), 0, 0, tiled=True)  11.5 us
    all_to_all x1, starting transfers between devices, body(): own = lax.all_to_all(spread, ('zy', 'tp'), 0, 0, tiled=True)  11.5 us
    ppermute x6, starting transfers between devices, passed(): lax.ppermute(parts[d], 'tp', hops[d])  9.55 us
    ppermute x2, waiting for transfers between devices, body(): near = [lax.ppermute(folded[:1], 'tp', hops[d]) for d in (1, 3)]  5.43 us
    ppermute x6, waiting for transfers between devices, passed(): lax.ppermute(parts[d], 'tp', hops[d])  3.52 us
    ppermute x1, starting transfers between devices, body(): far = lax.ppermute(folded, 'tp', hops[2])  3.15 us
    pallas_call x1, Pallas kernels, advance(): pl.pallas_call(advance_kernel, grid=(seqs // count,), in_specs=[pl.BlockS...  3.12 us
  transfers between devices with their start and end apart: 14, of which 5 were waited for; matrix products, arithmetic and copies ran while one was open for 1% of the time, Pallas kernels for 9%

profile of v5, /device:TPU:0, one launch (start us, length us, event | category | flops | bytes accessed | tf_op | source)
XLA Modules:
  0.0 89.9 jit_solution(2573778232286395981)
XLA Ops:
  0.6 2.2 %shard_map.140 = (bf16[64,32,128]{2,1,0:T(8,128)(2,1)}, bf16[2,32,4096]{2,1,0:T(8,128)(2,1)}) custom-call(bf16[4,32,128]{2,1,0:T(8,128)(2,1)} %bitcast.29, f32[32,128]{1,0:T(8,128)} %bitcast.21, bf16[1,32,4096]{2,1,0:T(8,128)(2,1)} %w_input.1, bf16[1,32,4096]{2,1,0:T(8,128)(2,1)} %w_gate.1), custom_call_target="tpu_custom_call" | custom-call | flops 1000000 | bytes 1048576 | tf_op jit(solution)/shard_map/pallas_call | solution.py:110
  2.9 11.5 %all-to-all-start = ((bf16[64,32,128]{2,1,0:T(8,128)(2,1)}), bf16[64,32,128]{2,1,0:T(8,128)(2,1)S(1)}, u32[]{:S(2)}, u32[]{:S(2)}) async-start(bf16[64,32,128]{2,1,0:T(8,128)(2,1)} %get-tuple-element.16), calls=%async_computation | async-start | bytes 1048576 | tf_op jit(solution)/shard_map/all_to_all | solution.py:410
  14.4 3.2 %collective-permute-start.2 = (bf16[2,32,4096]{2,1,0:T(8,128)(2,1)}, bf16[2,32,4096]{2,1,0:T(8,128)(2,1)S(1)}, u32[]{:S(2)}, u32[]{:S(2)}) collective-permute-start(bf16[2,32,4096]{2,1,0:T(8,128)(2,1)} %get-tuple-element.17.w0), channel_id=1, source_target_pairs={{0,2},{1,3},{2,0},{3,1},{4,6},{5,7},{6,4},{7,5},{8,10},{9,11},{10,... | collective-permute-start | bytes 1572872 | tf_op jit(solution)/shard_map/ppermute | solution.py:409
  17.6 11.5 %all-to-all-done = bf16[64,32,128]{2,1,0:T(8,128)(2,1)S(1)} async-done(((bf16[64,32,128]{2,1,0:T(8,128)(2,1)}), bf16[64,32,128]{2,1,0:T(8,128)(2,1)S(1)}, u32[]{:S(2)}, u32[]{:S(2)}) %all-to-all-start) | async-done | bytes 524320 | tf_op jit(solution)/shard_map/all_to_all | solution.py:410
  29.1 1.1 %fusion = (bf16[1,32,4096]{2,1,0:T(8,128)(2,1)S(1)}, bf16[1,32,4096]{2,1,0:T(8,128)(2,1)S(1)}) fusion(bf16[2,32,4096]{2,1,0:T(8,128)(2,1)} %get-tuple-element.17.w0), kind=kLoop, calls=%fused_computation | loop fusion | bytes 1048576 | tf_op jit(solution)/shard_map/slice | solution.py:415
  30.2 0.0 copy-start.1
  30.2 0.6 collective-permute-start.1
  30.8 1.3 %collective-permute-start.3 = (bf16[1,32,4096]{2,1,0:T(8,128)(2,1)S(1)}, bf16[1,32,4096]{2,1,0:T(8,128)(2,1)S(1)}, u32[]{:S(2)}, u32[]{:S(2)}) collective-permute-start(bf16[1,32,4096]{2,1,0:T(8,128)(2,1)S(1)} %get-tuple-element.33), channel_id=1, source_target_pairs={{0,3},{1,2},{2,1},{3,0},{4,7},{5,6},{6,5},{7,4},{8,11},{9,10},{10,... | collective-permute-start | bytes 786440 | tf_op jit(solution)/shard_map/ppermute | solution.py:413
  32.1 0.5 collective-permute-start.10
  32.6 0.7 shard_map.145.outward
  33.3 0.7 shard_map.141.keyed
  34.0 5.4 %collective-permute-done.1.w1 = bf16[1,32,4096]{2,1,0:T(8,128)(2,1)S(1)} collective-permute-done((bf16[1,32,4096]{2,1,0:T(8,128)(2,1)S(1)}, bf16[1,32,4096]{2,1,0:T(8,128)(2,1)S(1)}, u32[]{:S(2)}, u32[]{:S(2)}) %collective-permute-start.1) | collective-permute-done | bytes 262176 | tf_op jit(solution)/shard_map/ppermute | solution.py:413
  39.4 1.6 %collective-permute-start.11 = (bf16[1,32,4096]{2,1,0:T(8,128)(2,1)S(1)}, bf16[1,32,4096]{2,1,0:T(8,128)(2,1)S(1)}, u32[]{:S(2)}, u32[]{:S(2)}) collective-permute-start(bf16[1,32,4096]{2,1,0:T(8,128)(2,1)S(1)} %get-tuple-element.32), channel_id=1, source_target_pairs={{0,3},{1,2},{2,1},{3,0},{4,7},{5,6},{6,5},{7,4},{8,11},{9,10},{10,... | collective-permute-start | bytes 786440 | tf_op jit(solution)/shard_map/ppermute | solution.py:415
  41.1 1.4 %shard_map.142 = (bf16[288,128]{1,0:T(8,128)(2,1)S(1)}, bf16[288,128]{1,0:T(8,128)(2,1)S(1)}, bf16[288,128]{1,0:T(8,128)(2,1)S(1)}, bf16[288,128]{1,0:T(8,128)(2...) custom-call(bf16[16,128,128]{2,1,0:T(8,128)(2,1)S(1)} %bitcast.18, ...), custom_call_target="tpu_custom_call" | custom-call | flops 1000000000 | bytes 3145728 | tf_op jit(solution)/shard_map/pallas_call | solution.py:192
  42.6 0.9 collective-permute-start.4
  43.4 2.3 %collective-permute-start.5 = (bf16[288,128]{1,0:T(8,128)(2,1)S(1)}, bf16[288,128]{1,0:T(8,128)(2,1)S(1)}, u32[]{:S(2)}, u32[]{:S(2)}) collective-permute-start(bf16[288,128]{1,0:T(8,128)(2,1)S(1)} %get-tuple-element.20), channel_id=1, source_target_pairs={{0,2},{1,3},{2,0},{3,1},{4,6},{5,7},{6,4},{7,5},{8,10},{9,11},{10,... | collective-permute-start | bytes 221192 | tf_op jit(solution)/shard_map/ppermute | solution.py:405
  45.7 1.6 %collective-permute-start.6 = (bf16[288,128]{1,0:T(8,128)(2,1)S(1)}, bf16[288,128]{1,0:T(8,128)(2,1)S(1)}, u32[]{:S(2)}, u32[]{:S(2)}) collective-permute-start(bf16[288,128]{1,0:T(8,128)(2,1)S(1)} %get-tuple-element.21), channel_id=1, source_target_pairs={{0,3},{1,2},{2,1},{3,0},{4,7},{5,6},{6,5},{7,4},{8,11},{9,10},{10,... | collective-permute-start | bytes 221192 | tf_op jit(solution)/shard_map/ppermute | solution.py:405
  47.4 3.1 %advance.1 = (f32[128,32,128]{2,1,0:T(8,128)}, bf16[128,32,128]{2,1,0:T(8,128)(2,1)S(1)}) custom-call(s32[1,128]{1,0:T(1,128)S(1)} %bitcast.25, f32[128,4,128]{2,1,0:T(4,128)S(1)} %copy-done.6, bf16[4,32,128]{2,1,0:T(8,128)(2,1)S(1)} %bitcast.24, f32[128,32,128]{2,1,0:T(8,128)S(1)} %bitcast.23), custom_call_target="tpu_custom_call" | custom-call | flops 1000000000 | bytes 5242880 | tf_op jit(solution)/shard_map/advance/pallas_call | solution.py:65
  50.5 0.8 collective-permute-done.6.r3
  51.3 1.4 %shard_map.143 = (bf16[48,128]{1,0:T(8,128)(2,1)S(1)}, bf16[48,128]{1,0:T(8,128)(2,1)S(1)}, bf16[48,128]{1,0:T(8,128)(2,1)S(1)}, bf16[48,128]{1,0:T(8,128)(2,1)S(1)}) custom-call(bf16[288,128]{1,0:T(8,128)(2,1)S(1)} %get-tuple-element.18.r0, bf16[288,128]{1,0:T(8,128)(2,1)S(1)} %collective-permute-done.4.r1, bf16[288,128]{1,0:T(8,128)(2,1)S(1)} %collective-permute-done.5.r2, ...), custom_call_target="tpu_custom_call" | custom-call | flops 1000000000 | bytes 2097152 | tf_op jit(solution)/shard_map/pallas_call | solution.py:308
  52.7 0.1 collective-permute-start.7
  52.8 3.1 %collective-permute-start.8 = (bf16[48,128]{1,0:T(8,128)(2,1)S(1)}, bf16[48,128]{1,0:T(8,128)(2,1)S(1)}, u32[]{:S(2)}, u32[]{:S(2)}) collective-permute-start(bf16[48,128]{1,0:T(8,128)(2,1)S(1)} %get-tuple-element.25), channel_id=1, source_target_pairs={{0,2},{1,3},{2,0},{3,1},{4,6},{5,7},{6,4},{7,5},{8,10},{9,11},{10,... | collective-permute-start | bytes 36872 | tf_op jit(solution)/shard_map/ppermute | solution.py:405
  55.9 1.6 %collective-permute-start.9 = (bf16[48,128]{1,0:T(8,128)(2,1)S(1)}, bf16[48,128]{1,0:T(8,128)(2,1)S(1)}, u32[]{:S(2)}, u32[]{:S(2)}) collective-permute-start(bf16[48,128]{1,0:T(8,128)(2,1)S(1)} %get-tuple-element.26), channel_id=1, source_target_pairs={{0,3},{1,2},{2,1},{3,0},{4,7},{5,6},{6,5},{7,4},{8,11},{9,10},{10,... | collective-permute-start | bytes 36872 | tf_op jit(solution)/shard_map/ppermute | solution.py:405
  57.5 0.6 shard_map.144.gates
  58.1 0.0 collective-permute-done.8.p2
  58.1 2.7 %collective-permute-done.9.p3 = bf16[48,128]{1,0:T(8,128)(2,1)S(1)} collective-permute-done((bf16[48,128]{1,0:T(8,128)(2,1)S(1)}, bf16[48,128]{1,0:T(8,128)(2,1)S(1)}, u32[]{:S(2)}, u32[]{:S(2)}) %collective-permute-start.9) | collective-permute-done | bytes 12320 | tf_op jit(solution)/shard_map/ppermute | solution.py:405
  60.8 0.3 shard_map.146
  61.1 0.1 collective-permute-start.12
  61.2 1.9 %collective-permute-done.12.came = bf16[16,128,128]{2,1,0:T(8,128)(2,1)S(1)} collective-permute-done((bf16[16,128,128]{2,1,0:T(8,128)(2,1)S(1)}, bf16[16,128,128]{2,1,0:T(8,128)(2,1)S(1)}, u32[]{:S(2)}, u32[]{:S(2)}) %collective-permute-start.12) | collective-permute-done | bytes 524320 | tf_op jit(solution)/shard_map/ppermute | solution.py:432
  63.1 0.3 shard_map.147
  63.4 25.8 %all_to_all.10 = bf16[64,32,128]{2,1,0:T(8,128)(2,1)S(1)} all-to-all(bf16[64,32,128]{2,1,0:T(8,128)(2,1)S(1)} %bitcast.20), channel_id=1, replica_groups=mesh['zy'=16,'core'=2,'tp'=4] {'zy','tp'}, dimensions={0} | all-to-all | bytes 1048576 | tf_op jit(solution)/shard_map/all_to_all | solution.py:434
  89.2 0.7 shard_map.148
  (30 shorter events, 0.1 us)
Async XLA Ops:
  0.6 32.0 %copy-start.5 = (bf16[128,4096]{1,0:T(8,128)(2,1)S(1)}, bf16[128,4096]{1,0:T(8,128)(2,1)}, u32[]{:S(2)}) copy-start(bf16[128,4096]{1,0:T(8,128)(2,1)} %w_out.1) | copy-start | bytes 3145732
  2.9 26.2 %all-to-all-start = ((bf16[64,32,128]{2,1,0:T(8,128)(2,1)}), bf16[64,32,128]{2,1,0:T(8,128)(2,1)S(1)}, u32[]{:S(2)}, u32[]{:S(2)}) async-start(bf16[64,32,128]{2,1,0:T(8,128)(2,1)} %get-tuple-element.16), calls=%async_computation | async-start | bytes 1048576 | tf_op jit(solution)/shard_map/all_to_all | solution.py:410
  14.4 26.7 %collective-permute-start.2 = (bf16[2,32,4096]{2,1,0:T(8,128)(2,1)}, bf16[2,32,4096]{2,1,0:T(8,128)(2,1)S(1)}, u32[]{:S(2)}, u32[]{:S(2)}) collective-permute-start(bf16[2,32,4096]{2,1,0:T(8,128)(2,1)} %get-tuple-element.17.w0), channel_id=1, source_target_pairs={{0,2},{1,3},{2,0},{3,1},{4,6},{5,7},{6,4},{7,5},{8,10},{9,11},{10,... | collective-permute-start | bytes 1572872 | tf_op jit(solution)/shard_map/ppermute | solution.py:409
  29.1 12.0 %collective-permute-start = (bf16[16,128,128]{2,1,0:T(8,128)(2,1)S(1)}, bf16[16,128,128]{2,1,0:T(8,128)(2,1)S(1)}, u32[]{:S(2)}, u32[]{:S(2)}) collective-permute-start(bf16[16,128,128]{2,1,0:T(8,128)(2,1)S(1)} %bitcast.17), channel_id=1, source_target_pairs={{0,4},{4,0},{1,5},{5,1},{2,6},{6,2},{3,7},{7,3},{8,12},{12,8},{9,1... | collective-permute-start | bytes 1572872 | tf_op jit(solution)/shard_map/ppermute | solution.py:412
  30.2 3.1 %copy-start.1 = (bf16[4096,128]{1,0:T(8,128)(2,1)S(1)}, bf16[4096,128]{1,0:T(8,128)(2,1)}, u32[]{:S(2)}) copy-start(bf16[4096,128]{1,0:T(8,128)(2,1)} %w_query.1) | copy-start | bytes 3145732
  30.2 3.1 %copy-start.2 = (bf16[4096,128]{1,0:T(8,128)(2,1)S(1)}, bf16[4096,128]{1,0:T(8,128)(2,1)}, u32[]{:S(2)}) copy-start(bf16[4096,128]{1,0:T(8,128)(2,1)} %w_forget.1) | copy-start | bytes 3145732
  30.2 3.1 %copy-start.3 = (f32[4096]{0:T(1024)S(1)}, f32[4096]{0:T(1024)}, u32[]{:S(2)}) copy-start(f32[4096]{0:T(1024)} %param.14) | copy-start | bytes 49156
  30.2 9.3 %collective-permute-start.1 = (bf16[1,32,4096]{2,1,0:T(8,128)(2,1)S(1)}, bf16[1,32,4096]{2,1,0:T(8,128)(2,1)S(1)}, u32[]{:S(2)}, u32[]{:S(2)}) collective-permute-start(bf16[1,32,4096]{2,1,0:T(8,128)(2,1)S(1)} %get-tuple-element.33), channel_id=1, source_target_pairs={{0,1},{1,0},{2,3},{3,2},{4,5},{5,4},{6,7},{7,6},{8,9},{9,8},{10,11... | collective-permute-start | bytes 786440 | tf_op jit(solution)/shard_map/ppermute | solution.py:413
  30.8 10.2 %collective-permute-start.3 = (bf16[1,32,4096]{2,1,0:T(8,128)(2,1)S(1)}, bf16[1,32,4096]{2,1,0:T(8,128)(2,1)S(1)}, u32[]{:S(2)}, u32[]{:S(2)}) collective-permute-start(bf16[1,32,4096]{2,1,0:T(8,128)(2,1)S(1)} %get-tuple-element.33), channel_id=1, source_target_pairs={{0,3},{1,2},{2,1},{3,0},{4,7},{5,6},{6,5},{7,4},{8,11},{9,10},{10,... | collective-permute-start | bytes 786440 | tf_op jit(solution)/shard_map/ppermute | solution.py:413
  32.1 25.4 %collective-permute-start.10 = (bf16[1,32,4096]{2,1,0:T(8,128)(2,1)S(1)}, bf16[1,32,4096]{2,1,0:T(8,128)(2,1)S(1)}, u32[]{:S(2)}, u32[]{:S(2)}) collective-permute-start(bf16[1,32,4096]{2,1,0:T(8,128)(2,1)S(1)} %get-tuple-element.32), channel_id=1, source_target_pairs={{0,1},{1,0},{2,3},{3,2},{4,5},{5,4},{6,7},{7,6},{8,9},{9,8},{10,11... | collective-permute-start | bytes 786440 | tf_op jit(solution)/shard_map/ppermute | solution.py:415
  33.3 7.8 %copy-start = (bf16[2,32,4096]{2,1,0:T(8,128)(2,1)S(1)}, bf16[2,32,4096]{2,1,0:T(8,128)(2,1)}, u32[]{:S(2)}) copy-start(bf16[2,32,4096]{2,1,0:T(8,128)(2,1)} %get-tuple-element.17.w0) | copy-start | bytes 1572868
  34.0 13.4 %copy-start.4 = (f32[128,1,32,128]{3,2,1,0:T(8,128)S(1)}, f32[128,1,32,128]{3,2,1,0:T(8,128)}, u32[]{:S(2)}) copy-start(f32[128,1,32,128]{3,2,1,0:T(8,128)} %param.22) | copy-start | bytes 6291460
  34.0 13.4 %copy-start.6 = (f32[128,4,128]{2,1,0:T(4,128)S(1)}, f32[128,4,128]{2,1,0:T(4,128)}, u32[]{:S(2)}) copy-start(f32[128,4,128]{2,1,0:T(4,128)} %prev_forget.1) | copy-start | bytes 786436
  34.0 13.3 %copy-start.7 = (bf16[128,4,1,32]{0,3,2,1:T(8,128)(2,1)S(1)}, bf16[128,4,1,32]{0,3,2,1:T(8,128)(2,1)}, u32[]{:S(2)}) copy-start(bf16[128,4,1,32]{0,3,2,1:T(8,128)(2,1)} %param.24) | copy-start | bytes 98308
  34.0 13.3 %copy-start.8 = (s32[128]{0:T(128)S(1)}, s32[128]{0:T(128)}, u32[]{:S(2)}) copy-start(s32[128]{0:T(128)} %param.25) | copy-start | bytes 1540
  39.4 18.1 %collective-permute-start.11 = (bf16[1,32,4096]{2,1,0:T(8,128)(2,1)S(1)}, bf16[1,32,4096]{2,1,0:T(8,128)(2,1)S(1)}, u32[]{:S(2)}, u32[]{:S(2)}) collective-permute-start(bf16[1,32,4096]{2,1,0:T(8,128)(2,1)S(1)} %get-tuple-element.32), channel_id=1, source_target_pairs={{0,3},{1,2},{2,1},{3,0},{4,7},{5,6},{6,5},{7,4},{8,11},{9,10},{10,... | collective-permute-start | bytes 786440 | tf_op jit(solution)/shard_map/ppermute | solution.py:415
  42.5 8.8 %copy-start.9 = (f32[128]{0:T(128)S(1)}, f32[128]{0:T(128)}, u32[]{:S(2)}) copy-start(f32[128]{0:T(128)} %param.19) | copy-start | bytes 1540
  42.5 8.7 %copy-start.10 = (f32[32]{0:T(128)S(1)}, f32[32]{0:T(128)}, u32[]{:S(2)}) copy-start(f32[32]{0:T(128)} %param.20) | copy-start | bytes 388
  42.6 7.9 %collective-permute-start.4 = (bf16[288,128]{1,0:T(8,128)(2,1)S(1)}, bf16[288,128]{1,0:T(8,128)(2,1)S(1)}, u32[]{:S(2)}, u32[]{:S(2)}) collective-permute-start(bf16[288,128]{1,0:T(8,128)(2,1)S(1)} %get-tuple-element.19), channel_id=1, source_target_pairs={{0,1},{1,0},{2,3},{3,2},{4,5},{5,4},{6,7},{7,6},{8,9},{9,8},{10,11... | collective-permute-start | bytes 221192 | tf_op jit(solution)/shard_map/ppermute | solution.py:405
  43.4 7.0 %collective-permute-start.5 = (bf16[288,128]{1,0:T(8,128)(2,1)S(1)}, bf16[288,128]{1,0:T(8,128)(2,1)S(1)}, u32[]{:S(2)}, u32[]{:S(2)}) collective-permute-start(bf16[288,128]{1,0:T(8,128)(2,1)S(1)} %get-tuple-element.20), channel_id=1, source_target_pairs={{0,2},{1,3},{2,0},{3,1},{4,6},{5,7},{6,4},{7,5},{8,10},{9,11},{10,... | collective-permute-start | bytes 221192 | tf_op jit(solution)/shard_map/ppermute | solution.py:405
  45.7 5.6 %collective-permute-start.6 = (bf16[288,128]{1,0:T(8,128)(2,1)S(1)}, bf16[288,128]{1,0:T(8,128)(2,1)S(1)}, u32[]{:S(2)}, u32[]{:S(2)}) collective-permute-start(bf16[288,128]{1,0:T(8,128)(2,1)S(1)} %get-tuple-element.21), channel_id=1, source_target_pairs={{0,3},{1,2},{2,1},{3,0},{4,7},{5,6},{6,5},{7,4},{8,11},{9,10},{10,... | collective-permute-start | bytes 221192 | tf_op jit(solution)/shard_map/ppermute | solution.py:405
  52.7 5.3 %collective-permute-start.7 = (bf16[48,128]{1,0:T(8,128)(2,1)S(1)}, bf16[48,128]{1,0:T(8,128)(2,1)S(1)}, u32[]{:S(2)}, u32[]{:S(2)}) collective-permute-start(bf16[48,128]{1,0:T(8,128)(2,1)S(1)} %get-tuple-element.24), channel_id=1, source_target_pairs={{0,1},{1,0},{2,3},{3,2},{4,5},{5,4},{6,7},{7,6},{8,9},{9,8},{10,11... | collective-permute-start | bytes 36872 | tf_op jit(solution)/shard_map/ppermute | solution.py:405
  52.8 5.3 %collective-permute-start.8 = (bf16[48,128]{1,0:T(8,128)(2,1)S(1)}, bf16[48,128]{1,0:T(8,128)(2,1)S(1)}, u32[]{:S(2)}, u32[]{:S(2)}) collective-permute-start(bf16[48,128]{1,0:T(8,128)(2,1)S(1)} %get-tuple-element.25), channel_id=1, source_target_pairs={{0,2},{1,3},{2,0},{3,1},{4,6},{5,7},{6,4},{7,5},{8,10},{9,11},{10,... | collective-permute-start | bytes 36872 | tf_op jit(solution)/shard_map/ppermute | solution.py:405
  55.9 4.9 %collective-permute-start.9 = (bf16[48,128]{1,0:T(8,128)(2,1)S(1)}, bf16[48,128]{1,0:T(8,128)(2,1)S(1)}, u32[]{:S(2)}, u32[]{:S(2)}) collective-permute-start(bf16[48,128]{1,0:T(8,128)(2,1)S(1)} %get-tuple-element.26), channel_id=1, source_target_pairs={{0,3},{1,2},{2,1},{3,0},{4,7},{5,6},{6,5},{7,4},{8,11},{9,10},{10,... | collective-permute-start | bytes 36872 | tf_op jit(solution)/shard_map/ppermute | solution.py:405
  61.1 2.0 %collective-permute-start.12 = (bf16[16,128,128]{2,1,0:T(8,128)(2,1)S(1)}, bf16[16,128,128]{2,1,0:T(8,128)(2,1)S(1)}, u32[]{:S(2)}, u32[]{:S(2)}) collective-permute-start(bf16[16,128,128]{2,1,0:T(8,128)(2,1)S(1)} %shard_map.146), channel_id=1, source_target_pairs={{0,4},{4,0},{1,5},{5,1},{2,6},{6,2},{3,7},{7,3},{8,12},{12,8},{9,1... | collective-permute-start | bytes 1572872 | tf_op jit(solution)/shard_map/ppermute | solution.py:432

commit v6 on v0

--- a/solution.py
+++ b/solution.py
@@ -80,7 +80,7 @@
         cost_estimate=pl.CostEstimate(
             flops=1_000_000_000, bytes_accessed=5 << 20, transcendentals=0
         ),
-        compiler_params=pltpu.CompilerParams(vmem_limit_bytes=60 << 20),
+        compiler_params=pltpu.CompilerParams(vmem_limit_bytes=16 << 20),
     )(accepted[None], prev_forget, prev_input, state)
 
 
@@ -179,7 +179,7 @@
             pltpu.SemaphoreType.DMA((4,)),
         ],
         (1_000_000_000, 2 << 20),
-        16 << 20,
+        60 << 20,
         [far] * 4,
         [whole()] * 5,
     )(
@@ -219,10 +219,18 @@
     )(w_out)
 
 
-def project_kernel(own, other, keyed, w0, w1, w2, w3, o0, o1, o2, o3, held, ready):
+def project_kernel(
+    own, other, keyed, w0, w1, w2, w3, o0, o1, o2, o3, held, ready, weights, sems
+):
     core, mine = lax.axis_index("core"), lax.axis_index("tp")
     blocks, _, seqs = own.shape
-    group, keys = 4, keyed.shape[0]
+    group, keys, more = 4, keyed.shape[0], w0.shape[0]
+    copies = [pltpu.make_async_copy(keyed, weights.at[pl.ds(0, keys), :], sems.at[4])]
+    for d, ref in enumerate((w0, w1, w2, w3)):
+        at = pl.multiple_of(keys + (mine ^ d) * more, more)
+        copies.append(pltpu.make_async_copy(ref, weights.at[pl.ds(at, more), :], sems.at[d]))
+    for copy in copies:
+        copy.start()
     part = held.shape[0] // (2 * blocks)
     squares = jnp.zeros((16, seqs), jnp.float32)
     for half, ref in ((core, own), (1 - core, other)):
@@ -232,64 +240,73 @@
                 held[pl.ds(at, part), pl.ds(t * seqs, seqs)] = ref[b, pl.ds(t * part, part), :]
             squares = squares + ref[b, pl.ds(group * part, 16), :].astype(jnp.float32)
     totals = squares[0:4] + squares[4:8] + squares[8:12]
-    rows = held[...]
-    first = jnp.dot(keyed[...], rows, preferred_element_type=jnp.float32).astype(jnp.bfloat16)
+    height = weights.shape[0]
     for t in range(group):
-        ready[t, pl.ds(0, keys), :] = first[:, t * seqs : (t + 1) * seqs]
-        tail = three_rows(split_in_three(totals[t : t + 1]), seqs)
-        ready[t, pl.ds(ready.shape[1] - 16, 16), :] = tail
-    for d, weight in enumerate((w0, w1, w2, w3)):
-        more = weight.shape[0]
-        at = pl.multiple_of(keys + (mine ^ d) * more, more)
-        second = jnp.dot(weight[...], rows, preferred_element_type=jnp.float32).astype(jnp.bfloat16)
-        for t in range(group):
-            ready[t, pl.ds(at, more), :] = second[:, t * seqs : (t + 1) * seqs]
+        ready[t, pl.ds(height, 16), :] = three_rows(split_in_three(totals[t : t + 1]), seqs)
+    for copy in copies:
+        copy.wait()
+    both = jnp.dot(weights[...], held[...], preferred_element_type=jnp.float32)
+    both = both.astype(jnp.bfloat16)
+    for t in range(group):
+        ready[t, pl.ds(0, height), :] = both[:, t * seqs : (t + 1) * seqs]
     for d, out in enumerate((o0, o1, o2, o3)):
-        out[...] = ready[(mine ^ d)]
+        out[...] = ready[mine ^ d]
 
 
 def project(own, other, keyed, weights):
     _, _, seqs = own.shape
     keys, width = keyed.shape
-    rows = keys + 4 * weights[0].shape[0] + 16
+    height = keys + 4 * weights[0].shape[0]
+    far = pl.BlockSpec(memory_space=pltpu.HBM)
     return call(
         project_kernel,
-        [shaped((rows, seqs), jnp.bfloat16)] * 4,
-        [pltpu.VMEM((width, 4 * seqs), jnp.bfloat16), pltpu.VMEM((4, rows, seqs), jnp.bfloat16)],
+        [shaped((height + 16, seqs), jnp.bfloat16)] * 4,
+        [
+            pltpu.VMEM((width, 4 * seqs), jnp.bfloat16),
+            pltpu.VMEM((4, height + 16, seqs), jnp.bfloat16),
+            pltpu.VMEM((height, width), jnp.bfloat16),
+            pltpu.SemaphoreType.DMA((5,)),
+        ],
         (1_000_000_000, 3 << 20),
         16 << 20,
-        [whole()] * 7,
+        [whole()] * 2 + [far] * 5,
         [whole()] * 4,
     )(own, other, keyed, *weights)
 
 
-def finish_kernel(width, p0, p1, p2, p3, o0, o1, o2, o3, held):
+def finish_kernel(width, p0, p1, p2, p3, o0, o1, o2, o3, gates, held):
     mine = lax.axis_index("tp")
     group = 4
-    rows, keys = held.shape[0], o0.shape[0] * 4 // 5
+    values = gates.shape[0] // group
+    rows, keys = held.shape[0], o0.shape[0] - values
     total = sum(ref[pl.ds(rows, 16), :].astype(jnp.float32) for ref in (p0, p1, p2, p3))
     factor = lax.rsqrt(jnp.sum(total, axis=0, keepdims=True) / width + NORM_EPSILON)
     value = sum(ref[pl.ds(0, rows), :].astype(jnp.float32) for ref in (p0, p1, p2, p3))
     held[...] = (value * factor).astype(jnp.bfloat16)
-    more = (rows - keys) // group
     for d, out in enumerate((o0, o1, o2, o3)):
-        at = pl.multiple_of(keys + (mine ^ d) * more, more)
+        at = pl.multiple_of(keys + (mine ^ d) * 2 * values, 2 * values)
         out[pl.ds(0, keys), :] = held[pl.ds(0, keys), :]
-        out[pl.ds(keys, more), :] = held[pl.ds(at, more), :]
+        out[pl.ds(keys, values), :] = held[pl.ds(at, values), :]
+    for c in range(group):
+        raw = held[pl.ds(keys + c * 2 * values + values, values), :].astype(jnp.float32)
+        gates[pl.ds(c * values, values), :] = raw * jax.nn.sigmoid(raw)
 
 
 def finish(parts, keys, width):
     rows, seqs = parts[0].shape
     rows = rows - 16
-    return call(
+    values = (rows - keys) // 8
+    outs = call(
         functools.partial(finish_kernel, width),
-        [shaped((keys + (rows - keys) // 4, seqs), jnp.bfloat16)] * 4,
+        [shaped((keys + values, seqs), jnp.bfloat16)] * 4
+        + [shaped((4 * values, seqs), jnp.float32)],
         [pltpu.VMEM((rows, seqs), jnp.bfloat16)],
         (100_000_000, 1 << 20),
         16 << 20,
         [whole()] * 4,
-        [whole()] * 4,
+        [whole()] * 5,
     )(*parts)
+    return outs[:4], outs[4]
 
 
 def recur_kernel(r0, r1, r2, r3, before, floor, head_gain, o0, o1, o2, o3, seen, ready):
@@ -335,9 +352,7 @@
     for t in range(steps):
         out = sums[t]
         square = jnp.sum(out * out, axis=0, keepdims=True)
-        gate = seen[t, pl.ds(2 * size + values, values), :].astype(jnp.float32)
-        shown = out * scale * (gate * jax.nn.sigmoid(gate))
-        ready[t, pl.ds(0, values), :] = shown.astype(jnp.bfloat16)
+        ready[t, pl.ds(0, values), :] = (out * scale).astype(jnp.bfloat16)
         ready[t, pl.ds(values, 16), :] = three_rows(split_in_three(square), count)
     for d, ref in enumerate((o0, o1, o2, o3)):
         ref[...] = ready[mine ^ d]
@@ -360,35 +375,36 @@
     )(*received, before, floor, head_gain)
 
 
-def gathered(parts, joined):
+def gathered(parts, gates, joined):
     mine = lax.axis_index("tp")
     values = joined.shape[0] // 4
     total = None
     for d, ref in enumerate(parts):
         at = pl.multiple_of((mine ^ d) * values, values)
-        joined[pl.ds(at, values), :] = ref[pl.ds(0, values), :]
+        value = ref[pl.ds(0, values), :].astype(jnp.float32) * gates[pl.ds(at, values), :]
+        joined[pl.ds(at, values), :] = value.astype(jnp.bfloat16)
         square = jnp.sum(ref[pl.ds(values, 16), :].astype(jnp.float32), axis=0, keepdims=True)
         total = square if total is None else total + square
     return lax.rsqrt(total / joined.shape[0] + NORM_EPSILON)
 
 
-def away_kernel(p0, p1, p2, p3, outward, sent, joined):
+def away_kernel(p0, p1, p2, p3, gates, outward, sent, joined):
     core = lax.axis_index("core")
-    factor = gathered((p0, p1, p2, p3), joined)
+    factor = gathered((p0, p1, p2, p3), gates, joined)
     for b in range(sent.shape[0]):
         part = jnp.dot(outward[2 * b + 1 - core], joined[...], preferred_element_type=jnp.float32)
         sent[b] = (part * factor).astype(jnp.bfloat16)
 
 
-def keep_kernel(p0, p1, p2, p3, outward, came, kept, joined):
+def keep_kernel(p0, p1, p2, p3, gates, outward, came, kept, joined):
     core = lax.axis_index("core")
-    factor = gathered((p0, p1, p2, p3), joined)
+    factor = gathered((p0, p1, p2, p3), gates, joined)
     for b in range(kept.shape[0]):
         part = jnp.dot(outward[2 * b + core], joined[...], preferred_element_type=jnp.float32)
         kept[b] = (part * factor + came[b].astype(jnp.float32)).astype(jnp.bfloat16)
 
 
-def outward_half(kernel, parts, outward, *more):
+def outward_half(kernel, parts, gates, outward, *more):
     blocks, size, _ = outward.shape
     return call(
         kernel,
@@ -396,9 +412,9 @@
         [pltpu.VMEM((size, parts[0].shape[1]), jnp.bfloat16)],
         (100_000_000, 2 << 20),
         16 << 20,
-        [whole()] * (5 + len(more)),
+        [whole()] * (6 + len(more)),
         whole(),
-    )(*parts, outward, *more)
+    )(*parts, gates, outward, *more)
 
 
 def sum_kernel(parts, out):
@@ -457,14 +473,14 @@
     )
 
     partial = passed(project(own, other, keyed, weights))
-    received = passed(finish(partial, 2 * size, width))
+    sends, opened = finish(partial, 2 * size, width)
+    received = passed(sends)
+    outward = turn_outward(w_out)
     shown = recur(received, rounded.reshape(-1, size), forget_floor[None], head_gain[None])
     parts = passed(shown)
-    parts[0], w_out = lax.optimization_barrier((parts[0], w_out))
-    outward = turn_outward(w_out)
-    sent = outward_half(away_kernel, parts, outward)
+    sent = outward_half(away_kernel, parts, opened, outward)
     came = lax.ppermute(sent, "core", swap)
-    kept = outward_half(keep_kernel, parts, outward, came)
+    kept = outward_half(keep_kernel, parts, opened, outward, came)
     terms = lax.all_to_all(
         kept.reshape(planes * group, features, seqs), ("zy", "tp"), 0, 0, tiled=True
     )

time: 96.8 us -> 95.2 us (0.983)
  local copies, waits for them, and re-layouts: 5.69 us -> 1.97 us
  blocking collectives: 38.2 us -> 39.9 us
    unnamed x16 -> x18, local copies, waits for them, and re-layouts: 5.69 us -> 1.97 us
    pallas_call x1, Pallas kernels: 4.98 us -> 3.12 us  [advance(): pl.pallas_call(advance_kernel, grid=(seqs // count,), in_specs=[pl.BlockS...]
    pallas_call x1, Pallas kernels: 0.94 us -> 2.68 us  [turn(): call(turn_kernel, [shaped((2 * size, width // 4), jnp.bfloat16)] + [shape...]
    all_to_all x1, blocking collectives: 17.8 us -> 19.5 us  [body(): lax.all_to_all(kept.reshape(planes * group, features, seqs), ('zy', 'tp')...]
  transfers between devices with their start and end apart: 14 -> 14, of which waited for: 10 -> 9; matrix products, arithmetic and copies ran while one was open for 0% -> 0% of each run, Pallas kernels for 7% -> 7%
where the time goes in v6:
time: 95.2 us; the launch traced here: 94.8 us
  blocking collectives  39.9 us (42%)
  waiting for transfers between devices  20.1 us (21%)
  starting transfers between devices  19.2 us (20%)
  Pallas kernels  12.9 us (14%)
  local copies, waits for them, and re-layouts  1.97 us (2%)
    all_to_all x1, blocking collectives, body(): own = lax.all_to_all(spread, 'zy', 0, 0, tiled=True)  20.4 us
    all_to_all x1, blocking collectives, body(): lax.all_to_all(kept.reshape(planes * group, features, seqs), ('zy', 'tp')...  19.5 us
    ppermute x12, starting transfers between devices, passed(): lax.ppermute(parts[d], 'tp', hops[d])  19.1 us
    ppermute x12, waiting for transfers between devices, passed(): lax.ppermute(parts[d], 'tp', hops[d])  18.2 us
    pallas_call x1, Pallas kernels, advance(): pl.pallas_call(advance_kernel, grid=(seqs // count,), in_specs=[pl.BlockS...  3.12 us
    pallas_call x1, Pallas kernels, turn(): call(turn_kernel, [shaped((2 * size, width // 4), jnp.bfloat16)] + [shape...  2.68 us
    unnamed x18, local copies, waits for them, and re-layouts  1.97 us
  transfers between devices with their start and end apart: 14, of which 9 were waited for; matrix products, arithmetic and copies ran while one was open for 0% of the time, Pallas kernels for 7%

profile of v6, /device:TPU:0, one launch (start us, length us, event | category | flops | bytes accessed | tf_op | source)
XLA Modules:
  0.0 94.8 jit_solution(14493617617870926476)
XLA Ops:
  0.6 1.7 %shard_map.140 = bf16[16,144,128]{2,1,0:T(8,128)(2,1)} custom-call(bf16[4,32,128]{2,1,0:T(8,128)(2,1)} %bitcast.26, f32[32,128]{1,0:T(8,128)} %bitcast.28), custom_call_target="tpu_custom_call" | custom-call | flops 1000000 | bytes 1048576 | tf_op jit(solution)/shard_map/pallas_call | solution.py:120
  2.4 20.4 %all_to_all.10.own = bf16[16,144,128]{2,1,0:T(8,128)(2,1)S(1)} all-to-all(bf16[16,144,128]{2,1,0:T(8,128)(2,1)} %shard_map.140), channel_id=1, replica_groups=mesh['zy'=16,'core'=2,'tp'=4] {'zy'}, dimensions={0} | all-to-all | bytes 1179648 | tf_op jit(solution)/shard_map/all_to_all | solution.py:464
  22.8 2.7 %shard_map.141 = (bf16[256,1024]{1,0:T(8,128)(2,1)}, bf16[64,1024]{1,0:T(8,128)(2,1)}, bf16[64,1024]{1,0:T(8,128)(2,1)}, bf16[64,1024]{1,0:T(8,128)(2,1)}, bf16[64,1024]{1,0:T(8,128)(2,1)}) custom-call(bf16[32,128,128]{2,1,0:T(8,128)(2,1)} %bitcast.29, bf16[32,128,128]{2,1,0:T(8,128)(2,1)} %bitcast.30, bf16[1,32,4096]{2,1,0:T(8,128)(2,1)} %w_input.1, ...), custom_call_target="tpu_custom_call" | custom-call | flops 1000000000 | bytes 2097152 | tf_op jit(solution)/shard_map/pallas_call | solution.py:172
  25.5 1.6 %collective-permute-start.1 = (bf16[64,1024]{1,0:T(8,128)(2,1)}, bf16[64,1024]{1,0:T(8,128)(2,1)S(1)}, u32[]{:S(2)}, u32[]{:S(2)}) collective-permute-start(bf16[64,1024]{1,0:T(8,128)(2,1)} %get-tuple-element.24), channel_id=1, source_target_pairs={{0,1},{1,0},{2,3},{3,2},{4,5},{5,4},{6,7},{7,6},{8,9},{9,8},{10,11... | collective-permute-start | bytes 393224 | tf_op jit(solution)/shard_map/ppermute | solution.py:461
  27.0 2.7 %collective-permute-start.2 = (bf16[64,1024]{1,0:T(8,128)(2,1)}, bf16[64,1024]{1,0:T(8,128)(2,1)S(1)}, u32[]{:S(2)}, u32[]{:S(2)}) collective-permute-start(bf16[64,1024]{1,0:T(8,128)(2,1)} %get-tuple-element.25), channel_id=1, source_target_pairs={{0,2},{1,3},{2,0},{3,1},{4,6},{5,7},{6,4},{7,5},{8,10},{9,11},{10,... | collective-permute-start | bytes 393224 | tf_op jit(solution)/shard_map/ppermute | solution.py:461
  29.8 0.5 collective-permute-start.3
  30.2 1.9 %collective-permute-done.1.w1 = bf16[64,1024]{1,0:T(8,128)(2,1)S(1)} collective-permute-done((bf16[64,1024]{1,0:T(8,128)(2,1)}, bf16[64,1024]{1,0:T(8,128)(2,1)S(1)}, u32[]{:S(2)}, u32[]{:S(2)}) %collective-permute-start.1) | collective-permute-done | bytes 131104 | tf_op jit(solution)/shard_map/ppermute | solution.py:461
  32.1 4.6 %collective-permute-done.2.w2 = bf16[64,1024]{1,0:T(8,128)(2,1)S(1)} collective-permute-done((bf16[64,1024]{1,0:T(8,128)(2,1)}, bf16[64,1024]{1,0:T(8,128)(2,1)S(1)}, u32[]{:S(2)}, u32[]{:S(2)}) %collective-permute-start.2) | collective-permute-done | bytes 131104 | tf_op jit(solution)/shard_map/ppermute | solution.py:461
  36.8 2.4 %collective-permute-done.3.w3 = bf16[64,1024]{1,0:T(8,128)(2,1)S(1)} collective-permute-done((bf16[64,1024]{1,0:T(8,128)(2,1)}, bf16[64,1024]{1,0:T(8,128)(2,1)S(1)}, u32[]{:S(2)}, u32[]{:S(2)}) %collective-permute-start.3) | collective-permute-done | bytes 131104 | tf_op jit(solution)/shard_map/ppermute | solution.py:461
  39.2 1.0 %copy-done.7 = bf16[256,1024]{1,0:T(8,128)(2,1)S(1)} copy-done((bf16[256,1024]{1,0:T(8,128)(2,1)S(1)}, bf16[256,1024]{1,0:T(8,128)(2,1)}, u32[]{:S(2)}) %copy-start.7) | copy-done | bytes 524312
  40.2 0.9 copy-done.8
  41.1 1.8 %shard_map.142 = (bf16[528,128]{1,0:T(8,128)(2,1)S(1)}, bf16[528,128]{1,0:T(8,128)(2,1)S(1)}, bf16[528,128]{1,0:T(8,128)(2,1)S(1)}, bf16[528,128]{1,0:T(8,128)(2,1)S(1)}) custom-call(bf16[16,144,128]{2,1,0:T(8,128)(2,1)S(1)} %all_to_all.10.own, bf16[16,144,128]{2,1,0:T(8,128)(2,1)S(1)} %collective-permute-done.other, bf16[256,1024]{1,0:T(8,128)(2,1)S(1)} %copy-done.7, ...), custom_call_target="tpu_custom_call" | custom-call | flops 1000000000 | bytes 3145728 | tf_op jit(solution)/shard_map/pallas_call | solution.py:261
  43.0 2.0 %collective-permute-start.5 = (bf16[528,128]{1,0:T(8,128)(2,1)S(1)}, bf16[528,128]{1,0:T(8,128)(2,1)S(1)}, u32[]{:S(2)}, u32[]{:S(2)}) collective-permute-start(bf16[528,128]{1,0:T(8,128)(2,1)S(1)} %get-tuple-element.29), channel_id=1, source_target_pairs={{0,2},{1,3},{2,0},{3,1},{4,6},{5,7},{6,4},{7,5},{8,10},{9,11},{10,... | collective-permute-start | bytes 405512 | tf_op jit(solution)/shard_map/ppermute | solution.py:461
  45.0 2.7 %collective-permute-start.6 = (bf16[528,128]{1,0:T(8,128)(2,1)S(1)}, bf16[528,128]{1,0:T(8,128)(2,1)S(1)}, u32[]{:S(2)}, u32[]{:S(2)}) collective-permute-start(bf16[528,128]{1,0:T(8,128)(2,1)S(1)} %get-tuple-element.30), channel_id=1, source_target_pairs={{0,3},{1,2},{2,1},{3,0},{4,7},{5,6},{6,5},{7,4},{8,11},{9,10},{10,... | collective-permute-start | bytes 405512 | tf_op jit(solution)/shard_map/ppermute | solution.py:461
  47.7 1.8 %collective-permute-done.4.p1 = bf16[528,128]{1,0:T(8,128)(2,1)S(1)} collective-permute-done((bf16[528,128]{1,0:T(8,128)(2,1)S(1)}, bf16[528,128]{1,0:T(8,128)(2,1)S(1)}, u32[]{:S(2)}, u32[]{:S(2)}) %collective-permute-start.4) | collective-permute-done | bytes 135200 | tf_op jit(solution)/shard_map/ppermute | solution.py:461
  49.5 1.7 %collective-permute-done.5.p2 = bf16[528,128]{1,0:T(8,128)(2,1)S(1)} collective-permute-done((bf16[528,128]{1,0:T(8,128)(2,1)S(1)}, bf16[528,128]{1,0:T(8,128)(2,1)S(1)}, u32[]{:S(2)}, u32[]{:S(2)}) %collective-permute-start.5) | collective-permute-done | bytes 135200 | tf_op jit(solution)/shard_map/ppermute | solution.py:461
  51.2 2.1 %collective-permute-done.6.p3 = bf16[528,128]{1,0:T(8,128)(2,1)S(1)} collective-permute-done((bf16[528,128]{1,0:T(8,128)(2,1)S(1)}, bf16[528,128]{1,0:T(8,128)(2,1)S(1)}, u32[]{:S(2)}, u32[]{:S(2)}) %collective-permute-start.6) | collective-permute-done | bytes 135200 | tf_op jit(solution)/shard_map/ppermute | solution.py:461
  53.2 0.2 shard_map.143
  53.5 4.2 %collective-permute-start.8 = (bf16[288,128]{1,0:T(8,128)(2,1)S(1)}, bf16[288,128]{1,0:T(8,128)(2,1)S(1)}, u32[]{:S(2)}, u32[]{:S(2)}) collective-permute-start(bf16[288,128]{1,0:T(8,128)(2,1)S(1)} %get-tuple-element.33), channel_id=1, source_target_pairs={{0,2},{1,3},{2,0},{3,1},{4,6},{5,7},{6,4},{7,5},{8,10},{9,11},{10,... | collective-permute-start | bytes 221192 | tf_op jit(solution)/shard_map/ppermute | solution.py:461
  57.6 0.5 collective-permute-start.9
  58.2 3.1 %advance.1 = (f32[128,32,128]{2,1,0:T(8,128)}, bf16[128,32,128]{2,1,0:T(8,128)(2,1)S(1)}) custom-call(s32[1,128]{1,0:T(1,128)S(1)} %bitcast.22, f32[128,4,128]{2,1,0:T(4,128)S(1)} %copy-done.2, bf16[4,32,128]{2,1,0:T(8,128)(2,1)S(1)} %bitcast.21, f32[128,32,128]{2,1,0:T(8,128)S(1)} %bitcast.20), custom_call_target="tpu_custom_call" | custom-call | flops 1000000000 | bytes 5242880 | tf_op jit(solution)/shard_map/advance/pallas_call | solution.py:67
  61.3 1.9 %collective-permute-done.9.r3 = bf16[288,128]{1,0:T(8,128)(2,1)S(1)} collective-permute-done((bf16[288,128]{1,0:T(8,128)(2,1)S(1)}, bf16[288,128]{1,0:T(8,128)(2,1)S(1)}, u32[]{:S(2)}, u32[]{:S(2)}) %collective-permute-start.9) | collective-permute-done | bytes 73760 | tf_op jit(solution)/shard_map/ppermute | solution.py:461
  63.2 1.4 %shard_map.144 = (bf16[48,128]{1,0:T(8,128)(2,1)S(1)}, bf16[48,128]{1,0:T(8,128)(2,1)S(1)}, bf16[48,128]{1,0:T(8,128)(2,1)S(1)}, bf16[48,128]{1,0:T(8,128)(2,1)S(1)}) custom-call(bf16[288,128]{1,0:T(8,128)(2,1)S(1)} %get-tuple-element.31.r0, bf16[288,128]{1,0:T(8,128)(2,1)S(1)} %collective-permute-done.7.r1, bf16[288,128]{1,0:T(8,128)(2,1)S(1)} %collective-permute-done.8.r2, ...), custom_call_target="tpu_custom_call" | custom-call | flops 1000000000 | bytes 2097152 | tf_op jit(solution)/shard_map/pallas_call | solution.py:364
  64.7 2.3 %collective-permute-start.11 = (bf16[48,128]{1,0:T(8,128)(2,1)S(1)}, bf16[48,128]{1,0:T(8,128)(2,1)S(1)}, u32[]{:S(2)}, u32[]{:S(2)}) collective-permute-start(bf16[48,128]{1,0:T(8,128)(2,1)S(1)} %get-tuple-element.38), channel_id=1, source_target_pairs={{0,2},{1,3},{2,0},{3,1},{4,6},{5,7},{6,4},{7,5},{8,10},{9,11},{10,... | collective-permute-start | bytes 36872 | tf_op jit(solution)/shard_map/ppermute | solution.py:461
  67.0 2.4 %collective-permute-start.12 = (bf16[48,128]{1,0:T(8,128)(2,1)S(1)}, bf16[48,128]{1,0:T(8,128)(2,1)S(1)}, u32[]{:S(2)}, u32[]{:S(2)}) collective-permute-start(bf16[48,128]{1,0:T(8,128)(2,1)S(1)} %get-tuple-element.39), channel_id=1, source_target_pairs={{0,3},{1,2},{2,1},{3,0},{4,7},{5,6},{6,5},{7,4},{8,11},{9,10},{10,... | collective-permute-start | bytes 36872 | tf_op jit(solution)/shard_map/ppermute | solution.py:461
  69.4 0.7 shard_map.145.outward
  70.1 1.8 %collective-permute-done.12.p3 = bf16[48,128]{1,0:T(8,128)(2,1)S(1)} collective-permute-done((bf16[48,128]{1,0:T(8,128)(2,1)S(1)}, bf16[48,128]{1,0:T(8,128)(2,1)S(1)}, u32[]{:S(2)}, u32[]{:S(2)}) %collective-permute-start.12) | collective-permute-done | bytes 12320 | tf_op jit(solution)/shard_map/ppermute | solution.py:461
  71.9 0.3 shard_map.146
  72.4 1.9 %collective-permute-done.13.came = bf16[16,128,128]{2,1,0:T(8,128)(2,1)S(1)} collective-permute-done((bf16[16,128,128]{2,1,0:T(8,128)(2,1)S(1)}, bf16[16,128,128]{2,1,0:T(8,128)(2,1)S(1)}, u32[]{:S(2)}, u32[]{:S(2)}) %collective-permute-start.13) | collective-permute-done | bytes 524320 | tf_op jit(solution)/shard_map/ppermute | solution.py:482
  74.3 0.3 shard_map.147
  74.6 19.5 %all_to_all.11 = bf16[64,32,128]{2,1,0:T(8,128)(2,1)S(1)} all-to-all(bf16[64,32,128]{2,1,0:T(8,128)(2,1)S(1)} %bitcast.19), channel_id=1, replica_groups=mesh['zy'=16,'core'=2,'tp'=4] {'zy','tp'}, dimensions={0} | all-to-all | bytes 1048576 | tf_op jit(solution)/shard_map/all_to_all | solution.py:484
  94.1 0.7 shard_map.148
  (26 shorter events, 0.4 us)
Async XLA Ops:
  22.8 16.4 %collective-permute-start = (bf16[16,144,128]{2,1,0:T(8,128)(2,1)S(1)}, bf16[16,144,128]{2,1,0:T(8,128)(2,1)S(1)}, u32[]{:S(2)}, u32[]{:S(2)}) collective-permute-start(bf16[16,144,128]{2,1,0:T(8,128)(2,1)S(1)} %all_to_all.10.own), channel_id=1, source_target_pairs={{0,4},{4,0},{1,5},{5,1},{2,6},{6,2},{3,7},{7,3},{8,12},{12,8},{9,1... | collective-permute-start | bytes 1769480 | tf_op jit(solution)/shard_map/ppermute | solution.py:465
  25.5 6.7 %collective-permute-start.1 = (bf16[64,1024]{1,0:T(8,128)(2,1)}, bf16[64,1024]{1,0:T(8,128)(2,1)S(1)}, u32[]{:S(2)}, u32[]{:S(2)}) collective-permute-start(bf16[64,1024]{1,0:T(8,128)(2,1)} %get-tuple-element.24), channel_id=1, source_target_pairs={{0,1},{1,0},{2,3},{3,2},{4,5},{5,4},{6,7},{7,6},{8,9},{9,8},{10,11... | collective-permute-start | bytes 393224 | tf_op jit(solution)/shard_map/ppermute | solution.py:461
  27.0 9.7 %collective-permute-start.2 = (bf16[64,1024]{1,0:T(8,128)(2,1)}, bf16[64,1024]{1,0:T(8,128)(2,1)S(1)}, u32[]{:S(2)}, u32[]{:S(2)}) collective-permute-start(bf16[64,1024]{1,0:T(8,128)(2,1)} %get-tuple-element.25), channel_id=1, source_target_pairs={{0,2},{1,3},{2,0},{3,1},{4,6},{5,7},{6,4},{7,5},{8,10},{9,11},{10,... | collective-permute-start | bytes 393224 | tf_op jit(solution)/shard_map/ppermute | solution.py:461
  29.8 9.4 %collective-permute-start.3 = (bf16[64,1024]{1,0:T(8,128)(2,1)}, bf16[64,1024]{1,0:T(8,128)(2,1)S(1)}, u32[]{:S(2)}, u32[]{:S(2)}) collective-permute-start(bf16[64,1024]{1,0:T(8,128)(2,1)} %get-tuple-element.26), channel_id=1, source_target_pairs={{0,3},{1,2},{2,1},{3,0},{4,7},{5,6},{6,5},{7,4},{8,11},{9,10},{10,... | collective-permute-start | bytes 393224 | tf_op jit(solution)/shard_map/ppermute | solution.py:461
  39.2 1.0 %copy-start.7 = (bf16[256,1024]{1,0:T(8,128)(2,1)S(1)}, bf16[256,1024]{1,0:T(8,128)(2,1)}, u32[]{:S(2)}) copy-start(bf16[256,1024]{1,0:T(8,128)(2,1)} %get-tuple-element.22.keyed) | copy-start | bytes 1572868
  40.2 0.9 copy-start.8
  41.1 17.0 %copy-start = (f32[128,1,32,128]{3,2,1,0:T(8,128)S(1)}, f32[128,1,32,128]{3,2,1,0:T(8,128)}, u32[]{:S(2)}) copy-start(f32[128,1,32,128]{3,2,1,0:T(8,128)} %param.22) | copy-start | bytes 6291460
  41.1 17.0 %copy-start.2 = (f32[128,4,128]{2,1,0:T(4,128)S(1)}, f32[128,4,128]{2,1,0:T(4,128)}, u32[]{:S(2)}) copy-start(f32[128,4,128]{2,1,0:T(4,128)} %prev_forget.1) | copy-start | bytes 786436
  41.1 17.0 %copy-start.3 = (bf16[128,4,1,32]{0,3,2,1:T(8,128)(2,1)S(1)}, bf16[128,4,1,32]{0,3,2,1:T(8,128)(2,1)}, u32[]{:S(2)}) copy-start(bf16[128,4,1,32]{0,3,2,1:T(8,128)(2,1)} %param.24) | copy-start | bytes 98308
  41.1 17.0 %copy-start.4 = (s32[128]{0:T(128)S(1)}, s32[128]{0:T(128)}, u32[]{:S(2)}) copy-start(s32[128]{0:T(128)} %param.25) | copy-start | bytes 1540
  42.9 6.5 %collective-permute-start.4 = (bf16[528,128]{1,0:T(8,128)(2,1)S(1)}, bf16[528,128]{1,0:T(8,128)(2,1)S(1)}, u32[]{:S(2)}, u32[]{:S(2)}) collective-permute-start(bf16[528,128]{1,0:T(8,128)(2,1)S(1)} %get-tuple-element.28), channel_id=1, source_target_pairs={{0,1},{1,0},{2,3},{3,2},{4,5},{5,4},{6,7},{7,6},{8,9},{9,8},{10,11... | collective-permute-start | bytes 405512 | tf_op jit(solution)/shard_map/ppermute | solution.py:461
  43.0 8.2 %collective-permute-start.5 = (bf16[528,128]{1,0:T(8,128)(2,1)S(1)}, bf16[528,128]{1,0:T(8,128)(2,1)S(1)}, u32[]{:S(2)}, u32[]{:S(2)}) collective-permute-start(bf16[528,128]{1,0:T(8,128)(2,1)S(1)} %get-tuple-element.29), channel_id=1, source_target_pairs={{0,2},{1,3},{2,0},{3,1},{4,6},{5,7},{6,4},{7,5},{8,10},{9,11},{10,... | collective-permute-start | bytes 405512 | tf_op jit(solution)/shard_map/ppermute | solution.py:461
  45.0 8.2 %collective-permute-start.6 = (bf16[528,128]{1,0:T(8,128)(2,1)S(1)}, bf16[528,128]{1,0:T(8,128)(2,1)S(1)}, u32[]{:S(2)}, u32[]{:S(2)}) collective-permute-start(bf16[528,128]{1,0:T(8,128)(2,1)S(1)} %get-tuple-element.30), channel_id=1, source_target_pairs={{0,3},{1,2},{2,1},{3,0},{4,7},{5,6},{6,5},{7,4},{8,11},{9,10},{10,... | collective-permute-start | bytes 405512 | tf_op jit(solution)/shard_map/ppermute | solution.py:461
  53.2 10.0 %copy-start.5 = (f32[128]{0:T(128)S(1)}, f32[128]{0:T(128)}, u32[]{:S(2)}) copy-start(f32[128]{0:T(128)} %param.19) | copy-start | bytes 1540
  53.2 10.0 %copy-start.6 = (f32[32]{0:T(128)S(1)}, f32[32]{0:T(128)}, u32[]{:S(2)}) copy-start(f32[32]{0:T(128)} %param.20) | copy-start | bytes 388
  53.4 7.9 %collective-permute-start.7 = (bf16[288,128]{1,0:T(8,128)(2,1)S(1)}, bf16[288,128]{1,0:T(8,128)(2,1)S(1)}, u32[]{:S(2)}, u32[]{:S(2)}) collective-permute-start(bf16[288,128]{1,0:T(8,128)(2,1)S(1)} %get-tuple-element.32), channel_id=1, source_target_pairs={{0,1},{1,0},{2,3},{3,2},{4,5},{5,4},{6,7},{7,6},{8,9},{9,8},{10,11... | collective-permute-start | bytes 221192 | tf_op jit(solution)/shard_map/ppermute | solution.py:461
  53.5 7.8 %collective-permute-start.8 = (bf16[288,128]{1,0:T(8,128)(2,1)S(1)}, bf16[288,128]{1,0:T(8,128)(2,1)S(1)}, u32[]{:S(2)}, u32[]{:S(2)}) collective-permute-start(bf16[288,128]{1,0:T(8,128)(2,1)S(1)} %get-tuple-element.33), channel_id=1, source_target_pairs={{0,2},{1,3},{2,0},{3,1},{4,6},{5,7},{6,4},{7,5},{8,10},{9,11},{10,... | collective-permute-start | bytes 221192 | tf_op jit(solution)/shard_map/ppermute | solution.py:461
  57.6 5.6 %collective-permute-start.9 = (bf16[288,128]{1,0:T(8,128)(2,1)S(1)}, bf16[288,128]{1,0:T(8,128)(2,1)S(1)}, u32[]{:S(2)}, u32[]{:S(2)}) collective-permute-start(bf16[288,128]{1,0:T(8,128)(2,1)S(1)} %get-tuple-element.34), channel_id=1, source_target_pairs={{0,3},{1,2},{2,1},{3,0},{4,7},{5,6},{6,5},{7,4},{8,11},{9,10},{10,... | collective-permute-start | bytes 221192 | tf_op jit(solution)/shard_map/ppermute | solution.py:461
  61.3 8.1 %copy-start.1 = (bf16[128,4096]{1,0:T(8,128)(2,1)S(1)}, bf16[128,4096]{1,0:T(8,128)(2,1)}, u32[]{:S(2)}) copy-start(bf16[128,4096]{1,0:T(8,128)(2,1)} %w_out.1) | copy-start | bytes 3145732
  64.7 5.5 %collective-permute-start.10 = (bf16[48,128]{1,0:T(8,128)(2,1)S(1)}, bf16[48,128]{1,0:T(8,128)(2,1)S(1)}, u32[]{:S(2)}, u32[]{:S(2)}) collective-permute-start(bf16[48,128]{1,0:T(8,128)(2,1)S(1)} %get-tuple-element.37), channel_id=1, source_target_pairs={{0,1},{1,0},{2,3},{3,2},{4,5},{5,4},{6,7},{7,6},{8,9},{9,8},{10,11... | collective-permute-start | bytes 36872 | tf_op jit(solution)/shard_map/ppermute | solution.py:461
  64.7 5.4 %collective-permute-start.11 = (bf16[48,128]{1,0:T(8,128)(2,1)S(1)}, bf16[48,128]{1,0:T(8,128)(2,1)S(1)}, u32[]{:S(2)}, u32[]{:S(2)}) collective-permute-start(bf16[48,128]{1,0:T(8,128)(2,1)S(1)} %get-tuple-element.38), channel_id=1, source_target_pairs={{0,2},{1,3},{2,0},{3,1},{4,6},{5,7},{6,4},{7,5},{8,10},{9,11},{10,... | collective-permute-start | bytes 36872 | tf_op jit(solution)/shard_map/ppermute | solution.py:461
  67.0 4.9 %collective-permute-start.12 = (bf16[48,128]{1,0:T(8,128)(2,1)S(1)}, bf16[48,128]{1,0:T(8,128)(2,1)S(1)}, u32[]{:S(2)}, u32[]{:S(2)}) collective-permute-start(bf16[48,128]{1,0:T(8,128)(2,1)S(1)} %get-tuple-element.39), channel_id=1, source_target_pairs={{0,3},{1,2},{2,1},{3,0},{4,7},{5,6},{6,5},{7,4},{8,11},{9,10},{10,... | collective-permute-start | bytes 36872 | tf_op jit(solution)/shard_map/ppermute | solution.py:461
  72.3 2.0 %collective-permute-start.13 = (bf16[16,128,128]{2,1,0:T(8,128)(2,1)S(1)}, bf16[16,128,128]{2,1,0:T(8,128)(2,1)S(1)}, u32[]{:S(2)}, u32[]{:S(2)}) collective-permute-start(bf16[16,128,128]{2,1,0:T(8,128)(2,1)S(1)} %shard_map.146), channel_id=1, source_target_pairs={{0,4},{4,0},{1,5},{5,1},{2,6},{6,2},{3,7},{7,3},{8,12},{12,8},{9,1... | collective-permute-start | bytes 1572872 | tf_op jit(solution)/shard_map/ppermute | solution.py:482

commit v7 on v5

--- a/solution.py
+++ b/solution.py
@@ -93,7 +93,7 @@
     return jnp.concatenate([*parts, rest], axis=0).astype(jnp.bfloat16)
 
 
-def source_kernel(tokens, gain, w_input, w_gate, out, folded):
+def source_kernel(tokens, gain, w_input, w_gate, out, both, inputs, gates):
     steps = tokens.shape[0]
     for z in range(out.shape[0] // steps):
         out[pl.ds(z * steps, steps)] = tokens[...]
@@ -102,7 +102,9 @@
         at = pl.ds(b * size, size)
         for i, weight in enumerate((w_input, w_gate)):
             value = weight[0, :, at].astype(jnp.float32) * gain[pl.ds(b, 1), :]
-            folded[i, :, at] = value.astype(jnp.bfloat16)
+            value = value.astype(jnp.bfloat16)
+            both[i, :, at] = value
+            (inputs, gates)[i][0, :, at] = value
 
 
 def source(tokens, gain, w_input, w_gate, planes):
@@ -112,12 +114,14 @@
         [
             shaped((planes * steps, features, seqs), jnp.bfloat16),
             shaped((2, *w_input.shape[1:]), jnp.bfloat16),
+            shaped(w_input.shape, jnp.bfloat16),
+            shaped(w_gate.shape, jnp.bfloat16),
         ],
         [],
         (1_000_000, 1 << 20),
         60 << 20,
         [whole()] * 4,
-        [whole()] * 2,
+        [whole()] * 4,
     )(tokens, gain, w_input, w_gate)
 
 
@@ -154,10 +158,32 @@
     return copies
 
 
-def project_kernel(
-    own, other, keyed, w0, w1, w2, w3, o0, o1, o2, o3, held, scale, mixing, sems
-):
-    copies = bring(0, (w0, w1, w2, w3), mixing, sems)
+def collect_kernel(w0, w1, w2, w3, out, sems):
+    values = w0.shape[1]
+    copies = [
+        pltpu.make_async_copy(ref.at[0], out.at[pl.ds(d * values, values), :], sems.at[d])
+        for d, ref in enumerate((w0, w1, w2, w3))
+    ]
+    for copy in copies:
+        copy.start()
+    for copy in copies:
+        copy.wait()
+
+
+def collect(weights):
+    _, values, width = weights[0].shape
+    return call(
+        collect_kernel,
+        shaped((4 * values, width), jnp.bfloat16),
+        [pltpu.SemaphoreType.DMA((4,))],
+        (1_000_000_000, 2 << 20),
+        16 << 20,
+        [pl.BlockSpec(memory_space=pltpu.HBM)] * 4,
+        whole(),
+    )(*weights)
+
+
+def project_kernel(own, other, keyed, mixing, o0, o1, o2, o3, held, scale):
     core = lax.axis_index("core")
     blocks, size, seqs = own.shape
     squares = jnp.zeros((8, seqs), jnp.float32)
@@ -173,32 +199,27 @@
     rows = held[...]
     first = jnp.dot(keyed[...], rows, preferred_element_type=jnp.float32) * factor
     first = first.astype(jnp.bfloat16)
-    for copy in copies:
-        copy.wait()
-    group, values, width = mixing.shape
-    mixed = mixing[...].reshape(group * values, width)
-    second = jnp.dot(mixed, rows, preferred_element_type=jnp.float32) * factor
+    second = jnp.dot(mixing[...], rows, preferred_element_type=jnp.float32) * factor
     second = second.astype(jnp.bfloat16)
-    keys = first.shape[0]
+    keys, values = first.shape[0], second.shape[0] // 4
     for d, out in enumerate((o0, o1, o2, o3)):
         out[pl.ds(0, keys), :] = first
         out[pl.ds(keys, values), :] = second[d * values : (d + 1) * values]
 
 
-def project(own, other, keyed, weights):
+def project(own, other, keyed, mixing):
     blocks, size, seqs = own.shape
-    _, values, width = weights[0].shape
-    rows = keyed.shape[0] + values
+    rows = keyed.shape[0] + mixing.shape[0] // 4
     outs = call(
         project_kernel,
         [shaped((rows, seqs), jnp.bfloat16)] * 4
         + [shaped((2 * blocks * size, seqs), jnp.bfloat16), shaped((8, seqs), jnp.float32)],
-        [pltpu.VMEM((4, values, width), jnp.bfloat16), pltpu.SemaphoreType.DMA((4,))],
+        [],
         (1_000_000_000, 3 << 20),
         16 << 20,
-        [whole()] * 3 + [pl.BlockSpec(memory_space=pltpu.HBM)] * 4,
+        [whole()] * 4,
         [whole()] * 6,
-    )(own, other, keyed, *weights)
+    )(own, other, keyed, mixing)
     return outs[:4], outs[4], outs[5]
 
 
@@ -247,7 +268,7 @@
         shaped((width // size, size, size), jnp.bfloat16),
         [pltpu.VMEM((4, size, width // 4), jnp.bfloat16), pltpu.SemaphoreType.DMA((4,))],
         (1_000_000_000, 2 << 20),
-        16 << 20,
+        60 << 20,
         [pl.BlockSpec(memory_space=pltpu.HBM)],
         whole(),
     )(w_out)
@@ -405,16 +426,17 @@
         return [parts[0]] + [lax.ppermute(parts[d], "tp", hops[d]) for d in (1, 2, 3)]
 
     gain = input_norm_gain.reshape(-1, size)
-    spread, folded = source(tokens.transpose(1, 2, 0), gain, w_input, w_gate, planes)
-    far = lax.ppermute(folded, "tp", hops[2])
+    spread, both, own_input, own_gate = source(tokens.transpose(1, 2, 0), gain, w_input, w_gate, planes)
+    far = lax.ppermute(both, "tp", hops[2])
     own = lax.all_to_all(spread, ("zy", "tp"), 0, 0, tiled=True)
     own = own.reshape(planes, group * features, seqs)
     other = lax.ppermute(own, "core", swap)
-    near = [lax.ppermute(folded[:1], "tp", hops[d]) for d in (1, 3)]
-    inputs = [folded, near[0], far, near[1]]
-    near = [lax.ppermute(folded[1:], "tp", hops[d]) for d in (1, 3)]
-    gates = [folded, near[0], far, near[1]]
+    near = [lax.ppermute(own_input, "tp", hops[d]) for d in (1, 3)]
+    inputs = [own_input, near[0], far, near[1]]
+    near = [lax.ppermute(own_gate, "tp", hops[d]) for d in (1, 3)]
+    gates = [own_gate, near[0], far, near[1]]
     keyed = turn(gain, w_query, w_forget)
+    mixing = collect(inputs)
     new_state, rounded = advance(
         accepted,
         prev_forget,
@@ -422,7 +444,7 @@
         state[:, 0],
     )
 
-    sends, rows, scale = project(own, other, keyed, inputs)
+    sends, rows, scale = project(own, other, keyed, mixing)
     received = passed(sends)
     shown = recur(received, rounded.reshape(-1, size), forget_floor[None], head_gain[None])
     parts = passed(shown)

time: 90.2 us -> 90.3 us (level)
  Pallas kernels: 11.4 us -> 14.2 us
  blocking collectives: 25.8 us -> 24 us
  starting transfers between devices: 28.3 us -> 29.7 us
  waiting for transfers between devices: 22.4 us -> 21.1 us
  local copies, waits for them, and re-layouts: 1.13 us -> 0.07 us
    pallas_call x1, Pallas kernels: 0.67 us -> 2.53 us  [turn_outward(): call(outward_kernel, shaped((width // size, size, size), jnp.bfloat16), [...]
    all_to_all x1, blocking collectives: 25.8 us -> 24 us  [body(): lax.all_to_all(kept.reshape(planes * group, features, seqs), ('zy', 'tp')...]
    ppermute x5, starting transfers between devices: 7.16 us -> 8.56 us  [the longest x2 3.57 us: body(): near = [lax.ppermute(own_gate, 'tp', hops[d]) for d in (1, 3)]]
    ppermute x5, waiting for transfers between devices: 5.44 us -> 4.25 us  [the longest x2 4.25 us: body(): near = [lax.ppermute(own_input, 'tp', hops[d]) for d in (1, 3)]]
    pallas_call x0 -> x1, Pallas kernels: none -> 1.09 us  [collect(): call(collect_kernel, shaped((4 * values, width), jnp.bfloat16), [pltpu.Se...]
    slice x1 -> x0, local copies, waits for them, and re-layouts: 1.06 us -> none  [body(): near = [lax.ppermute(folded[1:], 'tp', hops[d]) for d in (1, 3)]]
  transfers between devices with their start and end apart: 14 -> 14, of which waited for: 5 -> 5; matrix products, arithmetic and copies ran while one was open for 1% -> 0% of each run, Pallas kernels for 9% -> 12%
where the time goes in v7:
time: 90.3 us; the launch traced here: 90 us
  starting transfers between devices  29.7 us (33%)
  blocking collectives  24 us (27%)
  waiting for transfers between devices  21.1 us (23%)
  Pallas kernels  14.2 us (16%)
    all_to_all x1, blocking collectives, body(): lax.all_to_all(kept.reshape(planes * group, features, seqs), ('zy', 'tp')...  24 us
    all_to_all x1, starting transfers between devices, body(): own = lax.all_to_all(spread, ('zy', 'tp'), 0, 0, tiled=True)  11.5 us
    all_to_all x1, waiting for transfers between devices, body(): own = lax.all_to_all(spread, ('zy', 'tp'), 0, 0, tiled=True)  11.5 us
    ppermute x6, starting transfers between devices, passed(): lax.ppermute(parts[d], 'tp', hops[d])  9.56 us
    ppermute x2, waiting for transfers between devices, body(): near = [lax.ppermute(own_input, 'tp', hops[d]) for d in (1, 3)]  4.25 us
    ppermute x2, starting transfers between devices, body(): near = [lax.ppermute(own_gate, 'tp', hops[d]) for d in (1, 3)]  3.57 us
    ppermute x6, waiting for transfers between devices, passed(): lax.ppermute(parts[d], 'tp', hops[d])  3.5 us
    ppermute x1, starting transfers between devices, body(): far = lax.ppermute(both, 'tp', hops[2])  3.15 us
  transfers between devices with their start and end apart: 14, of which 5 were waited for; matrix products, arithmetic and copies ran while one was open for 0% of the time, Pallas kernels for 12%

profile of v7, /device:TPU:0, one launch (start us, length us, event | category | flops | bytes accessed | tf_op | source)
XLA Modules:
  0.0 90.0 jit_solution(18434364929534294022)
XLA Ops:
  0.6 2.4 %shard_map.140 = (bf16[64,32,128]{2,1,0:T(8,128)(2,1)}, bf16[2,32,4096]{2,1,0:T(8,128)(2,1)}, bf16[1,32,4096]{2,1,0:T(8,128)(2,1)}, bf16[1,32,4096]{2,1,0:T(8,128)(2,1)}) custom-call(bf16[4,32,128]{2,1,0:T(8,128)(2,1)} %bitcast.29, f32[32,128]{1,0:T(8,128)} %bitcast.21, bf16[1,32,4096]{2,1,0:T(8,128)(2,1)} %w_input.1, bf16[1,32,4096]{2,1,0:T(8,128)(2,1)} %w_gate.1), custom_call_target="tpu_custom_call" | custom-call | flops 1000000 | bytes 1048576 | tf_op jit(solution)/shard_map/pallas_call | solution.py:112
  3.0 11.5 %all-to-all-start = ((bf16[64,32,128]{2,1,0:T(8,128)(2,1)}), bf16[64,32,128]{2,1,0:T(8,128)(2,1)S(1)}, u32[]{:S(2)}, u32[]{:S(2)}) async-start(bf16[64,32,128]{2,1,0:T(8,128)(2,1)} %get-tuple-element.18), calls=%async_computation | async-start | bytes 1048576 | tf_op jit(solution)/shard_map/all_to_all | solution.py:431
  14.5 0.0 copy-start.2
  14.6 0.0 copy-start.3
  14.6 3.2 %collective-permute-start.2 = (bf16[2,32,4096]{2,1,0:T(8,128)(2,1)}, bf16[2,32,4096]{2,1,0:T(8,128)(2,1)S(1)}, u32[]{:S(2)}, u32[]{:S(2)}) collective-permute-start(bf16[2,32,4096]{2,1,0:T(8,128)(2,1)} %get-tuple-element.20), channel_id=1, source_target_pairs={{0,2},{1,3},{2,0},{3,1},{4,6},{5,7},{6,4},{7,5},{8,10},{9,11},{10,... | collective-permute-start | bytes 1572872 | tf_op jit(solution)/shard_map/ppermute | solution.py:430
  17.7 11.5 %all-to-all-done = bf16[64,32,128]{2,1,0:T(8,128)(2,1)S(1)} async-done(((bf16[64,32,128]{2,1,0:T(8,128)(2,1)}), bf16[64,32,128]{2,1,0:T(8,128)(2,1)S(1)}, u32[]{:S(2)}, u32[]{:S(2)}) %all-to-all-start) | async-done | bytes 524320 | tf_op jit(solution)/shard_map/all_to_all | solution.py:431
  29.2 0.6 collective-permute-start.1
  29.8 1.3 %collective-permute-start.3 = (bf16[1,32,4096]{2,1,0:T(8,128)(2,1)}, bf16[1,32,4096]{2,1,0:T(8,128)(2,1)}, u32[]{:S(2)}, u32[]{:S(2)}) collective-permute-start(bf16[1,32,4096]{2,1,0:T(8,128)(2,1)} %get-tuple-element.19.w0), channel_id=1, source_target_pairs={{0,3},{1,2},{2,1},{3,0},{4,7},{5,6},{6,5},{7,4},{8,11},{9,10},{10,... | collective-permute-start | bytes 786440 | tf_op jit(solution)/shard_map/ppermute | solution.py:434
  31.1 0.5 collective-permute-start.10
  31.5 2.5 %shard_map.146.outward = bf16[32,128,128]{2,1,0:T(8,128)(2,1)} custom-call(bf16[128,4096]{1,0:T(8,128)(2,1)} %w_out.1), custom_call_target="tpu_custom_call" | custom-call | flops 1000000000 | bytes 2097152 | tf_op jit(solution)/shard_map/pallas_call | solution.py:266
  34.1 0.7 shard_map.141.keyed
  34.8 4.2 %collective-permute-done.1.w1 = bf16[1,32,4096]{2,1,0:T(8,128)(2,1)} collective-permute-done((bf16[1,32,4096]{2,1,0:T(8,128)(2,1)}, bf16[1,32,4096]{2,1,0:T(8,128)(2,1)}, u32[]{:S(2)}, u32[]{:S(2)}) %collective-permute-start.1) | collective-permute-done | bytes 262176 | tf_op jit(solution)/shard_map/ppermute | solution.py:434
  39.0 3.1 %collective-permute-start.11 = (bf16[1,32,4096]{2,1,0:T(8,128)(2,1)S(1)}, bf16[1,32,4096]{2,1,0:T(8,128)(2,1)S(1)}, u32[]{:S(2)}, u32[]{:S(2)}) collective-permute-start(bf16[1,32,4096]{2,1,0:T(8,128)(2,1)S(1)} %copy-done.6), channel_id=1, source_target_pairs={{0,3},{1,2},{2,1},{3,0},{4,7},{5,6},{6,5},{7,4},{8,11},{9,10},{10,... | collective-permute-start | bytes 786440 | tf_op jit(solution)/shard_map/ppermute | solution.py:436
  42.1 1.1 %shard_map.142.mixing = bf16[128,4096]{1,0:T(8,128)(2,1)S(1)} custom-call(bf16[1,32,4096]{2,1,0:T(8,128)(2,1)S(1)} %copy-done.7, bf16[1,32,4096]{2,1,0:T(8,128)(2,1)} %collective-permute-done.1.w1, bf16[2,32,4096]{2,1,0:T(8,128)(2,1)S(1)} %collective-permute-done.2.w2, bf16[1,32,4096]{2,1,0:T(8,128)(2,1)} %collective-permute-done.3.w3), custom_call_target="tpu_custom_call" | custom-call | flops 1000000000 | bytes 2097152 | tf_op jit(solution)/shard_map/pallas_call | solution.py:175
  43.3 1.2 %shard_map.143 = (bf16[288,128]{1,0:T(8,128)(2,1)S(1)}, bf16[288,128]{1,0:T(8,128)(2,1)S(1)}, bf16[288,128]{1,0:T(8,128)(2,1)S(1)}, bf16[288,128]{1,0:T(8,128)(2...) custom-call(bf16[16,128,128]{2,1,0:T(8,128)(2,1)S(1)} %bitcast.20, ...), custom_call_target="tpu_custom_call" | custom-call | flops 1000000000 | bytes 3145728 | tf_op jit(solution)/shard_map/pallas_call | solution.py:213
  44.5 0.6 collective-permute-start.4
  45.1 1.1 %collective-permute-start.5 = (bf16[288,128]{1,0:T(8,128)(2,1)S(1)}, bf16[288,128]{1,0:T(8,128)(2,1)S(1)}, u32[]{:S(2)}, u32[]{:S(2)}) collective-permute-start(bf16[288,128]{1,0:T(8,128)(2,1)S(1)} %get-tuple-element.23), channel_id=1, source_target_pairs={{0,2},{1,3},{2,0},{3,1},{4,6},{5,7},{6,4},{7,5},{8,10},{9,11},{10,... | collective-permute-start | bytes 221192 | tf_op jit(solution)/shard_map/ppermute | solution.py:426
  46.2 3.1 %collective-permute-start.6 = (bf16[288,128]{1,0:T(8,128)(2,1)S(1)}, bf16[288,128]{1,0:T(8,128)(2,1)S(1)}, u32[]{:S(2)}, u32[]{:S(2)}) collective-permute-start(bf16[288,128]{1,0:T(8,128)(2,1)S(1)} %get-tuple-element.24), channel_id=1, source_target_pairs={{0,3},{1,2},{2,1},{3,0},{4,7},{5,6},{6,5},{7,4},{8,11},{9,10},{10,... | collective-permute-start | bytes 221192 | tf_op jit(solution)/shard_map/ppermute | solution.py:426
  49.3 3.1 %advance.1 = (f32[128,32,128]{2,1,0:T(8,128)}, bf16[128,32,128]{2,1,0:T(8,128)(2,1)S(1)}) custom-call(s32[1,128]{1,0:T(1,128)S(1)} %bitcast.25, f32[128,4,128]{2,1,0:T(4,128)S(1)} %copy-done.5, bf16[4,32,128]{2,1,0:T(8,128)(2,1)S(1)} %bitcast.24, f32[128,32,128]{2,1,0:T(8,128)S(1)} %bitcast.23), custom_call_target="tpu_custom_call" | custom-call | flops 1000000000 | bytes 5242880 | tf_op jit(solution)/shard_map/advance/pallas_call | solution.py:65
  52.4 1.4 %shard_map.144 = (bf16[48,128]{1,0:T(8,128)(2,1)S(1)}, bf16[48,128]{1,0:T(8,128)(2,1)S(1)}, bf16[48,128]{1,0:T(8,128)(2,1)S(1)}, bf16[48,128]{1,0:T(8,128)(2,1)S(1)}) custom-call(bf16[288,128]{1,0:T(8,128)(2,1)S(1)} %get-tuple-element.21.r0, bf16[288,128]{1,0:T(8,128)(2,1)S(1)} %collective-permute-done.4.r1, bf16[288,128]{1,0:T(8,128)(2,1)S(1)} %collective-permute-done.5.r2, ...), custom_call_target="tpu_custom_call" | custom-call | flops 1000000000 | bytes 2097152 | tf_op jit(solution)/shard_map/pallas_call | solution.py:329
  53.9 0.1 collective-permute-start.7
  54.0 3.8 %collective-permute-start.8 = (bf16[48,128]{1,0:T(8,128)(2,1)S(1)}, bf16[48,128]{1,0:T(8,128)(2,1)S(1)}, u32[]{:S(2)}, u32[]{:S(2)}) collective-permute-start(bf16[48,128]{1,0:T(8,128)(2,1)S(1)} %get-tuple-element.28), channel_id=1, source_target_pairs={{0,2},{1,3},{2,0},{3,1},{4,6},{5,7},{6,4},{7,5},{8,10},{9,11},{10,... | collective-permute-start | bytes 36872 | tf_op jit(solution)/shard_map/ppermute | solution.py:426
  57.8 0.8 collective-permute-start.9
  58.7 0.6 shard_map.145.gates
  59.2 0.4 collective-permute-done.8.p2
  59.6 3.1 %collective-permute-done.9.p3 = bf16[48,128]{1,0:T(8,128)(2,1)S(1)} collective-permute-done((bf16[48,128]{1,0:T(8,128)(2,1)S(1)}, bf16[48,128]{1,0:T(8,128)(2,1)S(1)}, u32[]{:S(2)}, u32[]{:S(2)}) %collective-permute-start.9) | collective-permute-done | bytes 12320 | tf_op jit(solution)/shard_map/ppermute | solution.py:426
  62.7 0.3 shard_map.147
  63.0 0.1 collective-permute-start.12
  63.1 1.9 %collective-permute-done.12.came = bf16[16,128,128]{2,1,0:T(8,128)(2,1)S(1)} collective-permute-done((bf16[16,128,128]{2,1,0:T(8,128)(2,1)S(1)}, bf16[16,128,128]{2,1,0:T(8,128)(2,1)S(1)}, u32[]{:S(2)}, u32[]{:S(2)}) %collective-permute-start.12) | collective-permute-done | bytes 524320 | tf_op jit(solution)/shard_map/ppermute | solution.py:454
  65.0 0.3 shard_map.148
  65.4 24.0 %all_to_all.10 = bf16[64,32,128]{2,1,0:T(8,128)(2,1)S(1)} all-to-all(bf16[64,32,128]{2,1,0:T(8,128)(2,1)S(1)} %bitcast.18), channel_id=1, replica_groups=mesh['zy'=16,'core'=2,'tp'=4] {'zy','tp'}, dimensions={0} | all-to-all | bytes 1048576 | tf_op jit(solution)/shard_map/all_to_all | solution.py:456
  89.3 0.7 shard_map.149
  (32 shorter events, 0.1 us)
Async XLA Ops:
  3.0 26.2 %all-to-all-start = ((bf16[64,32,128]{2,1,0:T(8,128)(2,1)}), bf16[64,32,128]{2,1,0:T(8,128)(2,1)S(1)}, u32[]{:S(2)}, u32[]{:S(2)}) async-start(bf16[64,32,128]{2,1,0:T(8,128)(2,1)} %get-tuple-element.18), calls=%async_computation | async-start | bytes 1048576 | tf_op jit(solution)/shard_map/all_to_all | solution.py:431
  14.5 19.5 %copy-start.1 = (bf16[4096,128]{1,0:T(8,128)(2,1)S(1)}, bf16[4096,128]{1,0:T(8,128)(2,1)}, u32[]{:S(2)}) copy-start(bf16[4096,128]{1,0:T(8,128)(2,1)} %w_query.1) | copy-start | bytes 3145732
  14.5 19.5 %copy-start.2 = (bf16[4096,128]{1,0:T(8,128)(2,1)S(1)}, bf16[4096,128]{1,0:T(8,128)(2,1)}, u32[]{:S(2)}) copy-start(bf16[4096,128]{1,0:T(8,128)(2,1)} %w_forget.1) | copy-start | bytes 3145732
  14.6 19.5 %copy-start.3 = (f32[4096]{0:T(1024)S(1)}, f32[4096]{0:T(1024)}, u32[]{:S(2)}) copy-start(f32[4096]{0:T(1024)} %param.14) | copy-start | bytes 49156
  14.6 27.6 %collective-permute-start.2 = (bf16[2,32,4096]{2,1,0:T(8,128)(2,1)}, bf16[2,32,4096]{2,1,0:T(8,128)(2,1)S(1)}, u32[]{:S(2)}, u32[]{:S(2)}) collective-permute-start(bf16[2,32,4096]{2,1,0:T(8,128)(2,1)} %get-tuple-element.20), channel_id=1, source_target_pairs={{0,2},{1,3},{2,0},{3,1},{4,6},{5,7},{6,4},{7,5},{8,10},{9,11},{10,... | collective-permute-start | bytes 1572872 | tf_op jit(solution)/shard_map/ppermute | solution.py:430
  29.2 14.1 %collective-permute-start = (bf16[16,128,128]{2,1,0:T(8,128)(2,1)S(1)}, bf16[16,128,128]{2,1,0:T(8,128)(2,1)S(1)}, u32[]{:S(2)}, u32[]{:S(2)}) collective-permute-start(bf16[16,128,128]{2,1,0:T(8,128)(2,1)S(1)} %bitcast.19), channel_id=1, source_target_pairs={{0,4},{4,0},{1,5},{5,1},{2,6},{6,2},{3,7},{7,3},{8,12},{12,8},{9,1... | collective-permute-start | bytes 1572872 | tf_op jit(solution)/shard_map/ppermute | solution.py:433
  29.2 9.8 %collective-permute-start.1 = (bf16[1,32,4096]{2,1,0:T(8,128)(2,1)}, bf16[1,32,4096]{2,1,0:T(8,128)(2,1)}, u32[]{:S(2)}, u32[]{:S(2)}) collective-permute-start(bf16[1,32,4096]{2,1,0:T(8,128)(2,1)} %get-tuple-element.19.w0), channel_id=1, source_target_pairs={{0,1},{1,0},{2,3},{3,2},{4,5},{5,4},{6,7},{7,6},{8,9},{9,8},{10,11... | collective-permute-start | bytes 786440 | tf_op jit(solution)/shard_map/ppermute | solution.py:434
  29.8 12.3 %collective-permute-start.3 = (bf16[1,32,4096]{2,1,0:T(8,128)(2,1)}, bf16[1,32,4096]{2,1,0:T(8,128)(2,1)}, u32[]{:S(2)}, u32[]{:S(2)}) collective-permute-start(bf16[1,32,4096]{2,1,0:T(8,128)(2,1)} %get-tuple-element.19.w0), channel_id=1, source_target_pairs={{0,3},{1,2},{2,1},{3,0},{4,7},{5,6},{6,5},{7,4},{8,11},{9,10},{10,... | collective-permute-start | bytes 786440 | tf_op jit(solution)/shard_map/ppermute | solution.py:434
  31.1 27.6 %collective-permute-start.10 = (bf16[1,32,4096]{2,1,0:T(8,128)(2,1)}, bf16[1,32,4096]{2,1,0:T(8,128)(2,1)S(1)}, u32[]{:S(2)}, u32[]{:S(2)}) collective-permute-start(bf16[1,32,4096]{2,1,0:T(8,128)(2,1)} %get-tuple-element.30.w0), channel_id=1, source_target_pairs={{0,1},{1,0},{2,3},{3,2},{4,5},{5,4},{6,7},{7,6},{8,9},{9,8},{10,11... | collective-permute-start | bytes 786440 | tf_op jit(solution)/shard_map/ppermute | solution.py:436
  34.1 4.9 %copy-start.6 = (bf16[1,32,4096]{2,1,0:T(8,128)(2,1)S(1)}, bf16[1,32,4096]{2,1,0:T(8,128)(2,1)}, u32[]{:S(2)}) copy-start(bf16[1,32,4096]{2,1,0:T(8,128)(2,1)} %get-tuple-element.30.w0) | copy-start | bytes 786436
  34.1 8.0 %copy-start.7 = (bf16[1,32,4096]{2,1,0:T(8,128)(2,1)S(1)}, bf16[1,32,4096]{2,1,0:T(8,128)(2,1)}, u32[]{:S(2)}) copy-start(bf16[1,32,4096]{2,1,0:T(8,128)(2,1)} %get-tuple-element.19.w0) | copy-start | bytes 786436
  39.0 19.6 %collective-permute-start.11 = (bf16[1,32,4096]{2,1,0:T(8,128)(2,1)S(1)}, bf16[1,32,4096]{2,1,0:T(8,128)(2,1)S(1)}, u32[]{:S(2)}, u32[]{:S(2)}) collective-permute-start(bf16[1,32,4096]{2,1,0:T(8,128)(2,1)S(1)} %copy-done.6), channel_id=1, source_target_pairs={{0,3},{1,2},{2,1},{3,0},{4,7},{5,6},{6,5},{7,4},{8,11},{9,10},{10,... | collective-permute-start | bytes 786440 | tf_op jit(solution)/shard_map/ppermute | solution.py:436
  43.2 6.0 %copy-start.4 = (f32[128,1,32,128]{3,2,1,0:T(8,128)S(1)}, f32[128,1,32,128]{3,2,1,0:T(8,128)}, u32[]{:S(2)}) copy-start(f32[128,1,32,128]{3,2,1,0:T(8,128)} %param.22) | copy-start | bytes 6291460
  43.2 6.0 %copy-start.5 = (f32[128,4,128]{2,1,0:T(4,128)S(1)}, f32[128,4,128]{2,1,0:T(4,128)}, u32[]{:S(2)}) copy-start(f32[128,4,128]{2,1,0:T(4,128)} %prev_forget.1) | copy-start | bytes 786436
  43.3 6.0 %copy-start.8 = (bf16[128,4,1,32]{0,3,2,1:T(8,128)(2,1)S(1)}, bf16[128,4,1,32]{0,3,2,1:T(8,128)(2,1)}, u32[]{:S(2)}) copy-start(bf16[128,4,1,32]{0,3,2,1:T(8,128)(2,1)} %param.24) | copy-start | bytes 98308
  43.3 6.0 %copy-start.9 = (s32[128]{0:T(128)S(1)}, s32[128]{0:T(128)}, u32[]{:S(2)}) copy-start(s32[128]{0:T(128)} %param.25) | copy-start | bytes 1540
  44.5 8.0 %copy-start.10 = (f32[128]{0:T(128)S(1)}, f32[128]{0:T(128)}, u32[]{:S(2)}) copy-start(f32[128]{0:T(128)} %param.19) | copy-start | bytes 1540
  44.5 8.0 %copy-start.11 = (f32[32]{0:T(128)S(1)}, f32[32]{0:T(128)}, u32[]{:S(2)}) copy-start(f32[32]{0:T(128)} %param.20) | copy-start | bytes 388
  44.5 7.9 %collective-permute-start.4 = (bf16[288,128]{1,0:T(8,128)(2,1)S(1)}, bf16[288,128]{1,0:T(8,128)(2,1)S(1)}, u32[]{:S(2)}, u32[]{:S(2)}) collective-permute-start(bf16[288,128]{1,0:T(8,128)(2,1)S(1)} %get-tuple-element.22), channel_id=1, source_target_pairs={{0,1},{1,0},{2,3},{3,2},{4,5},{5,4},{6,7},{7,6},{8,9},{9,8},{10,11... | collective-permute-start | bytes 221192 | tf_op jit(solution)/shard_map/ppermute | solution.py:426
  45.1 7.3 %collective-permute-start.5 = (bf16[288,128]{1,0:T(8,128)(2,1)S(1)}, bf16[288,128]{1,0:T(8,128)(2,1)S(1)}, u32[]{:S(2)}, u32[]{:S(2)}) collective-permute-start(bf16[288,128]{1,0:T(8,128)(2,1)S(1)} %get-tuple-element.23), channel_id=1, source_target_pairs={{0,2},{1,3},{2,0},{3,1},{4,6},{5,7},{6,4},{7,5},{8,10},{9,11},{10,... | collective-permute-start | bytes 221192 | tf_op jit(solution)/shard_map/ppermute | solution.py:426
  46.2 6.2 %collective-permute-start.6 = (bf16[288,128]{1,0:T(8,128)(2,1)S(1)}, bf16[288,128]{1,0:T(8,128)(2,1)S(1)}, u32[]{:S(2)}, u32[]{:S(2)}) collective-permute-start(bf16[288,128]{1,0:T(8,128)(2,1)S(1)} %get-tuple-element.24), channel_id=1, source_target_pairs={{0,3},{1,2},{2,1},{3,0},{4,7},{5,6},{6,5},{7,4},{8,11},{9,10},{10,... | collective-permute-start | bytes 221192 | tf_op jit(solution)/shard_map/ppermute | solution.py:426
  53.9 8.9 %copy-start = (bf16[32,128,128]{2,1,0:T(8,128)(2,1)S(1)}, bf16[32,128,128]{2,1,0:T(8,128)(2,1)}, u32[]{:S(2)}) copy-start(bf16[32,128,128]{2,1,0:T(8,128)(2,1)} %shard_map.146.outward) | copy-start | bytes 3145732
  53.9 5.3 %collective-permute-start.7 = (bf16[48,128]{1,0:T(8,128)(2,1)S(1)}, bf16[48,128]{1,0:T(8,128)(2,1)S(1)}, u32[]{:S(2)}, u32[]{:S(2)}) collective-permute-start(bf16[48,128]{1,0:T(8,128)(2,1)S(1)} %get-tuple-element.27), channel_id=1, source_target_pairs={{0,1},{1,0},{2,3},{3,2},{4,5},{5,4},{6,7},{7,6},{8,9},{9,8},{10,11... | collective-permute-start | bytes 36872 | tf_op jit(solution)/shard_map/ppermute | solution.py:426
  54.0 5.6 %collective-permute-start.8 = (bf16[48,128]{1,0:T(8,128)(2,1)S(1)}, bf16[48,128]{1,0:T(8,128)(2,1)S(1)}, u32[]{:S(2)}, u32[]{:S(2)}) collective-permute-start(bf16[48,128]{1,0:T(8,128)(2,1)S(1)} %get-tuple-element.28), channel_id=1, source_target_pairs={{0,2},{1,3},{2,0},{3,1},{4,6},{5,7},{6,4},{7,5},{8,10},{9,11},{10,... | collective-permute-start | bytes 36872 | tf_op jit(solution)/shard_map/ppermute | solution.py:426
  57.8 4.9 %collective-permute-start.9 = (bf16[48,128]{1,0:T(8,128)(2,1)S(1)}, bf16[48,128]{1,0:T(8,128)(2,1)S(1)}, u32[]{:S(2)}, u32[]{:S(2)}) collective-permute-start(bf16[48,128]{1,0:T(8,128)(2,1)S(1)} %get-tuple-element.29), channel_id=1, source_target_pairs={{0,3},{1,2},{2,1},{3,0},{4,7},{5,6},{6,5},{7,4},{8,11},{9,10},{10,... | collective-permute-start | bytes 36872 | tf_op jit(solution)/shard_map/ppermute | solution.py:426
  63.0 2.0 %collective-permute-start.12 = (bf16[16,128,128]{2,1,0:T(8,128)(2,1)S(1)}, bf16[16,128,128]{2,1,0:T(8,128)(2,1)S(1)}, u32[]{:S(2)}, u32[]{:S(2)}) collective-permute-start(bf16[16,128,128]{2,1,0:T(8,128)(2,1)S(1)} %shard_map.147), channel_id=1, source_target_pairs={{0,4},{4,0},{1,5},{5,1},{2,6},{6,2},{3,7},{7,3},{8,12},{12,8},{9,1... | collective-permute-start | bytes 1572872 | tf_op jit(solution)/shard_map/ppermute | solution.py:454

commit v8 on v3

--- a/solution.py
+++ b/solution.py
@@ -93,22 +93,33 @@
     return jnp.concatenate([*parts, rest], axis=0).astype(jnp.bfloat16)
 
 
-def source_kernel(tokens, out):
+def source_kernel(tokens, out, held, sems):
     steps = tokens.shape[0]
-    for z in range(out.shape[0] // steps):
-        out[pl.ds(z * steps, steps)] = tokens[...]
+    planes = out.shape[0] // steps
+    copy = pltpu.make_async_copy(tokens, held, sems.at[planes])
+    copy.start()
+    copy.wait()
+    copies = [
+        pltpu.make_async_copy(held, out.at[pl.ds(z * steps, steps)], sems.at[z])
+        for z in range(planes)
+    ]
+    for copy in copies:
+        copy.start()
+    for copy in copies:
+        copy.wait()
 
 
 def source(tokens, planes):
     steps, features, seqs = tokens.shape
+    far = pl.BlockSpec(memory_space=pltpu.HBM)
     return call(
         source_kernel,
         shaped((planes * steps, features, seqs), jnp.bfloat16),
-        [],
+        [pltpu.VMEM(tokens.shape, jnp.bfloat16), pltpu.SemaphoreType.DMA((planes + 1,))],
         (1_000_000, 1 << 20),
         60 << 20,
-        [whole()],
-        whole(),
+        [far],
+        far,
     )(tokens)
 
 
@@ -280,20 +291,27 @@
             moved = moved * forget[u]
         sums.append(out)
         asked.append(moved.astype(jnp.bfloat16))
-    lane = lax.broadcasted_iota(jnp.int32, (values, count), 1)
-    asked = jnp.concatenate(asked, axis=1)
+    half = count // 2
+    lane = lax.rem(lax.broadcasted_iota(jnp.int32, (values, steps * half), 1), half)
     group = 8
-    for b in range(count // group):
-        read = jnp.dot(
-            before[pl.ds(b * group * values, group * values), :],
-            asked,
-            preferred_element_type=jnp.float32,
-        )
-        for s in range(group):
-            hit = lane == b * group + s
-            for t in range(steps):
-                part = read[s * values : (s + 1) * values, t * count : (t + 1) * count]
-                sums[t] = sums[t] + jnp.where(hit, part, 0.0)
+    halves = []
+    for h in range(2):
+        wanted = jnp.concatenate([a[:, h * half : (h + 1) * half] for a in asked], axis=1)
+        total = jnp.zeros((values, steps * half), jnp.float32)
+        for b in range(half // group):
+            first = h * half + b * group
+            read = jnp.dot(
+                before[pl.ds(first * values, group * values), :],
+                wanted,
+                preferred_element_type=jnp.float32,
+            )
+            for s in range(group):
+                part = read[s * values : (s + 1) * values]
+                total = total + jnp.where(lane == b * group + s, part, 0.0)
+        halves.append(total)
+    for t in range(steps):
+        cut = [total[:, t * half : (t + 1) * half] for total in halves]
+        sums[t] = sums[t] + jnp.concatenate(cut, axis=1)
     for t in range(steps):
         out = sums[t]
         square = jnp.sum(out * out, axis=0, keepdims=True)
@@ -409,15 +427,15 @@
     hops = [[(i, i ^ d) for i in range(group)] for d in range(group)]
 
     def passed(parts):
-        return [parts[0]] + [lax.ppermute(parts[d], "tp", hops[d]) for d in (1, 2, 3)]
+        far = lax.ppermute(parts[2], "tp", hops[2])
+        near = [lax.ppermute(parts[d], "tp", hops[d]) for d in (1, 3)]
+        return [parts[0], near[0], far, near[1]]
 
     gain = input_norm_gain.reshape(-1, size)
-    own = lax.all_to_all(
-        source(tokens.transpose(1, 2, 0), planes), ("zy", "tp"), 0, 0, tiled=True
-    )
+    inputs = passed([w_input] * group)
+    own = lax.all_to_all(source(tokens.transpose(1, 2, 0), planes), ("zy", "tp"), 0, 0, tiled=True)
     own = own.reshape(planes, group * features, seqs)
     other = lax.ppermute(own, "core", swap)
-    inputs = passed([w_input] * group)
     gates = passed([w_gate] * group)
     keyed = turn(gain, w_query, w_forget)
     mixing = fold(gain, inputs)

time: 98 us -> 97.7 us (level)
  no operation moved by 1% of the time
where the time goes in v8:
time: 97.7 us; the launch traced here: 97.3 us
  blocking collectives  42.9 us (44%)
  waiting for transfers between devices  22.8 us (23%)
  starting transfers between devices  19.2 us (20%)
  Pallas kernels  10.3 us (11%)
  local copies, waits for them, and re-layouts  1.29 us (1%)
    all_to_all x1, blocking collectives, body(): lax.all_to_all(source(tokens.transpose(1, 2, 0), planes), ('zy', 'tp'), 0...  24.9 us
    all_to_all x1, blocking collectives, body(): lax.all_to_all(kept.reshape(planes * group, features, seqs), ('zy', 'tp')...  18 us
    ppermute x8, waiting for transfers between devices, passed(): near = [lax.ppermute(parts[d], 'tp', hops[d]) for d in (1, 3)]  16.1 us
    ppermute x4, starting transfers between devices, passed(): far = lax.ppermute(parts[2], 'tp', hops[2])  11.4 us
    ppermute x8, starting transfers between devices, passed(): near = [lax.ppermute(parts[d], 'tp', hops[d]) for d in (1, 3)]  7.62 us
    ppermute x4, waiting for transfers between devices, passed(): far = lax.ppermute(parts[2], 'tp', hops[2])  5.54 us
    pallas_call x1, Pallas kernels, advance(): pl.pallas_call(advance_kernel, grid=(seqs // count,), in_specs=[pl.BlockS...  3.12 us
  transfers between devices with their start and end apart: 15, of which 6 were waited for; matrix products, arithmetic and copies ran while one was open for 0% of the time, Pallas kernels for 8%

profile of v8, /device:TPU:0, one launch (start us, length us, event | category | flops | bytes accessed | tf_op | source)
XLA Modules:
  0.0 97.3 jit_solution(7756738938892414761)
XLA Ops:
  0.6 1.7 %shard_map.140 = bf16[64,32,128]{2,1,0:T(8,128)(2,1)} custom-call(bf16[4,32,128]{2,1,0:T(8,128)(2,1)} %bitcast.30), custom_call_target="tpu_custom_call" | custom-call | flops 1000000 | bytes 1048576 | tf_op jit(solution)/shard_map/pallas_call | solution.py:115
  2.3 24.9 %all_to_all.10 = bf16[64,32,128]{2,1,0:T(8,128)(2,1)S(1)} all-to-all(bf16[64,32,128]{2,1,0:T(8,128)(2,1)} %shard_map.140), channel_id=1, replica_groups=mesh['zy'=16,'core'=2,'tp'=4] {'zy','tp'}, dimensions={0} | all-to-all | bytes 1048576 | tf_op jit(solution)/shard_map/all_to_all | solution.py:436
  27.2 0.6 collective-permute-start.1
  27.9 1.8 %collective-permute-start.2 = (bf16[1,32,4096]{2,1,0:T(8,128)(2,1)}, bf16[1,32,4096]{2,1,0:T(8,128)(2,1)S(1)}, u32[]{:S(2)}, u32[]{:S(2)}) collective-permute-start(bf16[1,32,4096]{2,1,0:T(8,128)(2,1)} %w0.2), channel_id=1, source_target_pairs={{0,2},{1,3},{2,0},{3,1},{4,6},{5,7},{6,4},{7,5},{8,10},{9,11},{10,... | collective-permute-start | bytes 786440 | tf_op jit(solution)/shard_map/ppermute | solution.py:430
  29.7 2.3 %collective-permute-start.3 = (bf16[1,32,4096]{2,1,0:T(8,128)(2,1)}, bf16[1,32,4096]{2,1,0:T(8,128)(2,1)S(1)}, u32[]{:S(2)}, u32[]{:S(2)}) collective-permute-start(bf16[1,32,4096]{2,1,0:T(8,128)(2,1)} %w0.2), channel_id=1, source_target_pairs={{0,3},{1,2},{2,1},{3,0},{4,7},{5,6},{6,5},{7,4},{8,11},{9,10},{10,... | collective-permute-start | bytes 786440 | tf_op jit(solution)/shard_map/ppermute | solution.py:431
  32.0 1.2 %copy-done.4 = bf16[128,4096]{1,0:T(8,128)(2,1)S(1)} copy-done((bf16[128,4096]{1,0:T(8,128)(2,1)S(1)}, bf16[128,4096]{1,0:T(8,128)(2,1)}, u32[]{:S(2)}) %copy-start.4) | copy-done | bytes 1048600
  33.2 0.7 shard_map.147
  33.9 0.1 collective-permute-start.14
  34.1 0.7 shard_map.141.keyed
  34.7 2.0 %collective-permute-done.1.w1 = bf16[1,32,4096]{2,1,0:T(8,128)(2,1)S(1)} collective-permute-done((bf16[1,32,4096]{2,1,0:T(8,128)(2,1)}, bf16[1,32,4096]{2,1,0:T(8,128)(2,1)S(1)}, u32[]{:S(2)}, u32[]{:S(2)}) %collective-permute-start.1) | collective-permute-done | bytes 262176 | tf_op jit(solution)/shard_map/ppermute | solution.py:431
  36.7 5.5 %collective-permute-done.2.w2 = bf16[1,32,4096]{2,1,0:T(8,128)(2,1)S(1)} collective-permute-done((bf16[1,32,4096]{2,1,0:T(8,128)(2,1)}, bf16[1,32,4096]{2,1,0:T(8,128)(2,1)S(1)}, u32[]{:S(2)}, u32[]{:S(2)}) %collective-permute-start.2) | collective-permute-done | bytes 262176 | tf_op jit(solution)/shard_map/ppermute | solution.py:430
  42.2 2.6 %collective-permute-done.3.w3 = bf16[1,32,4096]{2,1,0:T(8,128)(2,1)S(1)} collective-permute-done((bf16[1,32,4096]{2,1,0:T(8,128)(2,1)}, bf16[1,32,4096]{2,1,0:T(8,128)(2,1)S(1)}, u32[]{:S(2)}, u32[]{:S(2)}) %collective-permute-start.3) | collective-permute-done | bytes 262176 | tf_op jit(solution)/shard_map/ppermute | solution.py:431
  44.8 0.3 shard_map.142.mixing
  45.1 1.2 %shard_map.143 = (bf16[288,128]{1,0:T(8,128)(2,1)S(1)}, bf16[288,128]{1,0:T(8,128)(2,1)S(1)}, bf16[288,128]{1,0:T(8,128)(2,1)S(1)}, bf16[288,128]{1,0:T(8,128)(2...) custom-call(bf16[16,128,128]{2,1,0:T(8,128)(2,1)S(1)} %bitcast.20, ...), custom_call_target="tpu_custom_call" | custom-call | flops 1000000000 | bytes 3145728 | tf_op jit(solution)/shard_map/pallas_call | solution.py:198
  46.3 0.1 collective-permute-start.4
  46.4 3.8 %collective-permute-start.5 = (bf16[288,128]{1,0:T(8,128)(2,1)S(1)}, bf16[288,128]{1,0:T(8,128)(2,1)S(1)}, u32[]{:S(2)}, u32[]{:S(2)}) collective-permute-start(bf16[288,128]{1,0:T(8,128)(2,1)S(1)} %get-tuple-element.18), channel_id=1, source_target_pairs={{0,2},{1,3},{2,0},{3,1},{4,6},{5,7},{6,4},{7,5},{8,10},{9,11},{10,... | collective-permute-start | bytes 221192 | tf_op jit(solution)/shard_map/ppermute | solution.py:430
  50.2 2.4 %collective-permute-start.11 = (bf16[1,32,4096]{2,1,0:T(8,128)(2,1)S(1)}, bf16[1,32,4096]{2,1,0:T(8,128)(2,1)S(1)}, u32[]{:S(2)}, u32[]{:S(2)}) collective-permute-start(bf16[1,32,4096]{2,1,0:T(8,128)(2,1)S(1)} %copy-done.7), channel_id=1, source_target_pairs={{0,2},{1,3},{2,0},{3,1},{4,6},{5,7},{6,4},{7,5},{8,10},{9,11},{10,... | collective-permute-start | bytes 786440 | tf_op jit(solution)/shard_map/ppermute | solution.py:430
  52.6 2.3 %collective-permute-start.12 = (bf16[1,32,4096]{2,1,0:T(8,128)(2,1)S(1)}, bf16[1,32,4096]{2,1,0:T(8,128)(2,1)S(1)}, u32[]{:S(2)}, u32[]{:S(2)}) collective-permute-start(bf16[1,32,4096]{2,1,0:T(8,128)(2,1)S(1)} %copy-done.7), channel_id=1, source_target_pairs={{0,3},{1,2},{2,1},{3,0},{4,7},{5,6},{6,5},{7,4},{8,11},{9,10},{10,... | collective-permute-start | bytes 786440 | tf_op jit(solution)/shard_map/ppermute | solution.py:431
  54.9 0.9 collective-permute-start.6
  55.8 3.1 %advance.1 = (f32[128,32,128]{2,1,0:T(8,128)}, bf16[128,32,128]{2,1,0:T(8,128)(2,1)S(1)}) custom-call(s32[1,128]{1,0:T(1,128)S(1)} %bitcast.26, f32[128,4,128]{2,1,0:T(4,128)S(1)} %copy-done.6, bf16[4,32,128]{2,1,0:T(8,128)(2,1)S(1)} %bitcast.25, f32[128,32,128]{2,1,0:T(8,128)S(1)} %bitcast.24), custom_call_target="tpu_custom_call" | custom-call | flops 1000000000 | bytes 5242880 | tf_op jit(solution)/shard_map/advance/pallas_call | solution.py:65
  59.0 8.4 %collective-permute-done.6.r3 = bf16[288,128]{1,0:T(8,128)(2,1)S(1)} collective-permute-done((bf16[288,128]{1,0:T(8,128)(2,1)S(1)}, bf16[288,128]{1,0:T(8,128)(2,1)S(1)}, u32[]{:S(2)}, u32[]{:S(2)}) %collective-permute-start.6) | collective-permute-done | bytes 73760 | tf_op jit(solution)/shard_map/ppermute | solution.py:431
  67.4 1.0 %shard_map.144 = (bf16[48,128]{1,0:T(8,128)(2,1)S(1)}, bf16[48,128]{1,0:T(8,128)(2,1)S(1)}, bf16[48,128]{1,0:T(8,128)(2,1)S(1)}, bf16[48,128]{1,0:T(8,128)(2,1)S(1)}) custom-call(bf16[288,128]{1,0:T(8,128)(2,1)S(1)} %get-tuple-element.16.r0, bf16[288,128]{1,0:T(8,128)(2,1)S(1)} %collective-permute-done.4.r1, bf16[288,128]{1,0:T(8,128)(2,1)S(1)} %collective-permute-done.5.r2, ...), custom_call_target="tpu_custom_call" | custom-call | flops 1000000000 | bytes 2097152 | tf_op jit(solution)/shard_map/pallas_call | solution.py:327
  68.4 0.1 collective-permute-start.7
  68.5 3.5 %collective-permute-start.8 = (bf16[48,128]{1,0:T(8,128)(2,1)S(1)}, bf16[48,128]{1,0:T(8,128)(2,1)S(1)}, u32[]{:S(2)}, u32[]{:S(2)}) collective-permute-start(bf16[48,128]{1,0:T(8,128)(2,1)S(1)} %get-tuple-element.23), channel_id=1, source_target_pairs={{0,2},{1,3},{2,0},{3,1},{4,6},{5,7},{6,4},{7,5},{8,10},{9,11},{10,... | collective-permute-start | bytes 36872 | tf_op jit(solution)/shard_map/ppermute | solution.py:430
  72.0 1.2 %collective-permute-start.9 = (bf16[48,128]{1,0:T(8,128)(2,1)S(1)}, bf16[48,128]{1,0:T(8,128)(2,1)S(1)}, u32[]{:S(2)}, u32[]{:S(2)}) collective-permute-start(bf16[48,128]{1,0:T(8,128)(2,1)S(1)} %get-tuple-element.24), channel_id=1, source_target_pairs={{0,3},{1,2},{2,1},{3,0},{4,7},{5,6},{6,5},{7,4},{8,11},{9,10},{10,... | collective-permute-start | bytes 36872 | tf_op jit(solution)/shard_map/ppermute | solution.py:431
  73.2 0.5 shard_map.145.gates
  73.8 3.1 %collective-permute-done.9.p3 = bf16[48,128]{1,0:T(8,128)(2,1)S(1)} collective-permute-done((bf16[48,128]{1,0:T(8,128)(2,1)S(1)}, bf16[48,128]{1,0:T(8,128)(2,1)S(1)}, u32[]{:S(2)}, u32[]{:S(2)}) %collective-permute-start.9) | collective-permute-done | bytes 12320 | tf_op jit(solution)/shard_map/ppermute | solution.py:431
  76.9 0.1 collective-permute-start.13
  77.0 1.2 %collective-permute-done.13.other = bf16[128,128]{1,0:T(8,128)(2,1)S(1)} collective-permute-done((bf16[128,128]{1,0:T(8,128)(2,1)S(1)}, bf16[128,128]{1,0:T(8,128)(2,1)S(1)}, u32[]{:S(2)}, u32[]{:S(2)}) %collective-permute-start.13) | collective-permute-done | bytes 32800 | tf_op jit(solution)/shard_map/ppermute | solution.py:457
  78.2 0.4 shard_map.148
  78.7 18.0 %all_to_all.11 = bf16[64,32,128]{2,1,0:T(8,128)(2,1)S(1)} all-to-all(bf16[64,32,128]{2,1,0:T(8,128)(2,1)S(1)} %bitcast.17), channel_id=1, replica_groups=mesh['zy'=16,'core'=2,'tp'=4] {'zy','tp'}, dimensions={0} | all-to-all | bytes 1048576 | tf_op jit(solution)/shard_map/all_to_all | solution.py:458
  96.6 0.7 shard_map.149
  (35 shorter events, 0.1 us)
Async XLA Ops:
  27.2 6.8 %copy-start = (bf16[4096,128]{1,0:T(8,128)(2,1)S(1)}, bf16[4096,128]{1,0:T(8,128)(2,1)}, u32[]{:S(2)}) copy-start(bf16[4096,128]{1,0:T(8,128)(2,1)} %w_query.1) | copy-start | bytes 3145732
  27.2 6.8 %copy-start.1 = (bf16[4096,128]{1,0:T(8,128)(2,1)S(1)}, bf16[4096,128]{1,0:T(8,128)(2,1)}, u32[]{:S(2)}) copy-start(bf16[4096,128]{1,0:T(8,128)(2,1)} %w_forget.1) | copy-start | bytes 3145732
  27.2 6.8 %copy-start.2 = (f32[4096]{0:T(1024)S(1)}, f32[4096]{0:T(1024)}, u32[]{:S(2)}) copy-start(f32[4096]{0:T(1024)} %param.14) | copy-start | bytes 49156
  27.2 17.9 %collective-permute-start = (bf16[16,128,128]{2,1,0:T(8,128)(2,1)S(1)}, bf16[16,128,128]{2,1,0:T(8,128)(2,1)S(1)}, u32[]{:S(2)}, u32[]{:S(2)}) collective-permute-start(bf16[16,128,128]{2,1,0:T(8,128)(2,1)S(1)} %bitcast.19), channel_id=1, source_target_pairs={{0,4},{4,0},{1,5},{5,1},{2,6},{6,2},{3,7},{7,3},{8,12},{12,8},{9,1... | collective-permute-start | bytes 1572872 | tf_op jit(solution)/shard_map/ppermute | solution.py:438
  27.2 9.5 %collective-permute-start.1 = (bf16[1,32,4096]{2,1,0:T(8,128)(2,1)}, bf16[1,32,4096]{2,1,0:T(8,128)(2,1)S(1)}, u32[]{:S(2)}, u32[]{:S(2)}) collective-permute-start(bf16[1,32,4096]{2,1,0:T(8,128)(2,1)} %w0.2), channel_id=1, source_target_pairs={{0,1},{1,0},{2,3},{3,2},{4,5},{5,4},{6,7},{7,6},{8,9},{9,8},{10,11... | collective-permute-start | bytes 786440 | tf_op jit(solution)/shard_map/ppermute | solution.py:431
  27.9 14.3 %collective-permute-start.2 = (bf16[1,32,4096]{2,1,0:T(8,128)(2,1)}, bf16[1,32,4096]{2,1,0:T(8,128)(2,1)S(1)}, u32[]{:S(2)}, u32[]{:S(2)}) collective-permute-start(bf16[1,32,4096]{2,1,0:T(8,128)(2,1)} %w0.2), channel_id=1, source_target_pairs={{0,2},{1,3},{2,0},{3,1},{4,6},{5,7},{6,4},{7,5},{8,10},{9,11},{10,... | collective-permute-start | bytes 786440 | tf_op jit(solution)/shard_map/ppermute | solution.py:430
  29.7 15.1 %collective-permute-start.3 = (bf16[1,32,4096]{2,1,0:T(8,128)(2,1)}, bf16[1,32,4096]{2,1,0:T(8,128)(2,1)S(1)}, u32[]{:S(2)}, u32[]{:S(2)}) collective-permute-start(bf16[1,32,4096]{2,1,0:T(8,128)(2,1)} %w0.2), channel_id=1, source_target_pairs={{0,3},{1,2},{2,1},{3,0},{4,7},{5,6},{6,5},{7,4},{8,11},{9,10},{10,... | collective-permute-start | bytes 786440 | tf_op jit(solution)/shard_map/ppermute | solution.py:431
  32.0 1.2 %copy-start.4 = (bf16[128,4096]{1,0:T(8,128)(2,1)S(1)}, bf16[128,4096]{1,0:T(8,128)(2,1)}, u32[]{:S(2)}) copy-start(bf16[128,4096]{1,0:T(8,128)(2,1)} %w_out.1) | copy-start | bytes 3145732
  33.9 43.1 %collective-permute-start.14 = (bf16[16,128,128]{2,1,0:T(8,128)(2,1)S(1)}, bf16[16,128,128]{2,1,0:T(8,128)(2,1)S(1)}, u32[]{:S(2)}, u32[]{:S(2)}) collective-permute-start(bf16[16,128,128]{2,1,0:T(8,128)(2,1)S(1)} %get-tuple-element.28), channel_id=1, source_target_pairs={{0,4},{4,0},{1,5},{5,1},{2,6},{6,2},{3,7},{7,3},{8,12},{12,8},{9,1... | collective-permute-start | bytes 1572872 | tf_op jit(solution)/shard_map/ppermute | solution.py:452
  34.0 10.7 %copy-start.5 = (bf16[1,32,4096]{2,1,0:T(8,128)(2,1)S(1)}, bf16[1,32,4096]{2,1,0:T(8,128)(2,1)}, u32[]{:S(2)}) copy-start(bf16[1,32,4096]{2,1,0:T(8,128)(2,1)} %w0.2) | copy-start | bytes 786436
  45.1 5.1 %copy-start.7 = (bf16[1,32,4096]{2,1,0:T(8,128)(2,1)S(1)}, bf16[1,32,4096]{2,1,0:T(8,128)(2,1)}, u32[]{:S(2)}) copy-start(bf16[1,32,4096]{2,1,0:T(8,128)(2,1)} %w0.3) | copy-start | bytes 786436
  45.1 10.7 %copy-start.3 = (f32[128,1,32,128]{3,2,1,0:T(8,128)S(1)}, f32[128,1,32,128]{3,2,1,0:T(8,128)}, u32[]{:S(2)}) copy-start(f32[128,1,32,128]{3,2,1,0:T(8,128)} %param.22) | copy-start | bytes 6291460
  45.1 10.7 %copy-start.6 = (f32[128,4,128]{2,1,0:T(4,128)S(1)}, f32[128,4,128]{2,1,0:T(4,128)}, u32[]{:S(2)}) copy-start(f32[128,4,128]{2,1,0:T(4,128)} %prev_forget.1) | copy-start | bytes 786436
  45.1 10.7 %copy-start.8 = (bf16[128,4,1,32]{0,3,2,1:T(8,128)(2,1)S(1)}, bf16[128,4,1,32]{0,3,2,1:T(8,128)(2,1)}, u32[]{:S(2)}) copy-start(bf16[128,4,1,32]{0,3,2,1:T(8,128)(2,1)} %param.24) | copy-start | bytes 98308
  45.1 10.7 %copy-start.9 = (s32[128]{0:T(128)S(1)}, s32[128]{0:T(128)}, u32[]{:S(2)}) copy-start(s32[128]{0:T(128)} %param.25) | copy-start | bytes 1540
  46.3 21.1 %copy-start.10 = (f32[128]{0:T(128)S(1)}, f32[128]{0:T(128)}, u32[]{:S(2)}) copy-start(f32[128]{0:T(128)} %param.19) | copy-start | bytes 1540
  46.3 21.1 %copy-start.11 = (f32[32]{0:T(128)S(1)}, f32[32]{0:T(128)}, u32[]{:S(2)}) copy-start(f32[32]{0:T(128)} %param.20) | copy-start | bytes 388
  46.3 6.2 %collective-permute-start.4 = (bf16[288,128]{1,0:T(8,128)(2,1)S(1)}, bf16[288,128]{1,0:T(8,128)(2,1)S(1)}, u32[]{:S(2)}, u32[]{:S(2)}) collective-permute-start(bf16[288,128]{1,0:T(8,128)(2,1)S(1)} %get-tuple-element.17), channel_id=1, source_target_pairs={{0,1},{1,0},{2,3},{3,2},{4,5},{5,4},{6,7},{7,6},{8,9},{9,8},{10,11... | collective-permute-start | bytes 221192 | tf_op jit(solution)/shard_map/ppermute | solution.py:431
  46.4 8.5 %collective-permute-start.5 = (bf16[288,128]{1,0:T(8,128)(2,1)S(1)}, bf16[288,128]{1,0:T(8,128)(2,1)S(1)}, u32[]{:S(2)}, u32[]{:S(2)}) collective-permute-start(bf16[288,128]{1,0:T(8,128)(2,1)S(1)} %get-tuple-element.18), channel_id=1, source_target_pairs={{0,2},{1,3},{2,0},{3,1},{4,6},{5,7},{6,4},{7,5},{8,10},{9,11},{10,... | collective-permute-start | bytes 221192 | tf_op jit(solution)/shard_map/ppermute | solution.py:430
  50.2 18.3 %collective-permute-start.10 = (bf16[1,32,4096]{2,1,0:T(8,128)(2,1)S(1)}, bf16[1,32,4096]{2,1,0:T(8,128)(2,1)S(1)}, u32[]{:S(2)}, u32[]{:S(2)}) collective-permute-start(bf16[1,32,4096]{2,1,0:T(8,128)(2,1)S(1)} %copy-done.7), channel_id=1, source_target_pairs={{0,1},{1,0},{2,3},{3,2},{4,5},{5,4},{6,7},{7,6},{8,9},{9,8},{10,11... | collective-permute-start | bytes 786440 | tf_op jit(solution)/shard_map/ppermute | solution.py:431
  50.2 21.8 %collective-permute-start.11 = (bf16[1,32,4096]{2,1,0:T(8,128)(2,1)S(1)}, bf16[1,32,4096]{2,1,0:T(8,128)(2,1)S(1)}, u32[]{:S(2)}, u32[]{:S(2)}) collective-permute-start(bf16[1,32,4096]{2,1,0:T(8,128)(2,1)S(1)} %copy-done.7), channel_id=1, source_target_pairs={{0,2},{1,3},{2,0},{3,1},{4,6},{5,7},{6,4},{7,5},{8,10},{9,11},{10,... | collective-permute-start | bytes 786440 | tf_op jit(solution)/shard_map/ppermute | solution.py:430
  52.6 20.6 %collective-permute-start.12 = (bf16[1,32,4096]{2,1,0:T(8,128)(2,1)S(1)}, bf16[1,32,4096]{2,1,0:T(8,128)(2,1)S(1)}, u32[]{:S(2)}, u32[]{:S(2)}) collective-permute-start(bf16[1,32,4096]{2,1,0:T(8,128)(2,1)S(1)} %copy-done.7), channel_id=1, source_target_pairs={{0,3},{1,2},{2,1},{3,0},{4,7},{5,6},{6,5},{7,4},{8,11},{9,10},{10,... | collective-permute-start | bytes 786440 | tf_op jit(solution)/shard_map/ppermute | solution.py:431
  54.9 12.5 %collective-permute-start.6 = (bf16[288,128]{1,0:T(8,128)(2,1)S(1)}, bf16[288,128]{1,0:T(8,128)(2,1)S(1)}, u32[]{:S(2)}, u32[]{:S(2)}) collective-permute-start(bf16[288,128]{1,0:T(8,128)(2,1)S(1)} %get-tuple-element.19), channel_id=1, source_target_pairs={{0,3},{1,2},{2,1},{3,0},{4,7},{5,6},{6,5},{7,4},{8,11},{9,10},{10,... | collective-permute-start | bytes 221192 | tf_op jit(solution)/shard_map/ppermute | solution.py:431
  68.4 5.3 %collective-permute-start.7 = (bf16[48,128]{1,0:T(8,128)(2,1)S(1)}, bf16[48,128]{1,0:T(8,128)(2,1)S(1)}, u32[]{:S(2)}, u32[]{:S(2)}) collective-permute-start(bf16[48,128]{1,0:T(8,128)(2,1)S(1)} %get-tuple-element.22), channel_id=1, source_target_pairs={{0,1},{1,0},{2,3},{3,2},{4,5},{5,4},{6,7},{7,6},{8,9},{9,8},{10,11... | collective-permute-start | bytes 36872 | tf_op jit(solution)/shard_map/ppermute | solution.py:431
  68.5 5.3 %collective-permute-start.8 = (bf16[48,128]{1,0:T(8,128)(2,1)S(1)}, bf16[48,128]{1,0:T(8,128)(2,1)S(1)}, u32[]{:S(2)}, u32[]{:S(2)}) collective-permute-start(bf16[48,128]{1,0:T(8,128)(2,1)S(1)} %get-tuple-element.23), channel_id=1, source_target_pairs={{0,2},{1,3},{2,0},{3,1},{4,6},{5,7},{6,4},{7,5},{8,10},{9,11},{10,... | collective-permute-start | bytes 36872 | tf_op jit(solution)/shard_map/ppermute | solution.py:430
  72.0 4.9 %collective-permute-start.9 = (bf16[48,128]{1,0:T(8,128)(2,1)S(1)}, bf16[48,128]{1,0:T(8,128)(2,1)S(1)}, u32[]{:S(2)}, u32[]{:S(2)}) collective-permute-start(bf16[48,128]{1,0:T(8,128)(2,1)S(1)} %get-tuple-element.24), channel_id=1, source_target_pairs={{0,3},{1,2},{2,1},{3,0},{4,7},{5,6},{6,5},{7,4},{8,11},{9,10},{10,... | collective-permute-start | bytes 36872 | tf_op jit(solution)/shard_map/ppermute | solution.py:431
  76.9 1.3 %collective-permute-start.13 = (bf16[128,128]{1,0:T(8,128)(2,1)S(1)}, bf16[128,128]{1,0:T(8,128)(2,1)S(1)}, u32[]{:S(2)}, u32[]{:S(2)}) collective-permute-start(bf16[128,128]{1,0:T(8,128)(2,1)S(1)} %shard_map.146.hidden), channel_id=1, source_target_pairs={{0,4},{4,0},{1,5},{5,1},{2,6},{6,2},{3,7},{7,3},{8,12},{12,8},{9,1... | collective-permute-start | bytes 98312 | tf_op jit(solution)/shard_map/ppermute | solution.py:457

commit v9 on v8

--- a/solution.py
+++ b/solution.py
@@ -123,14 +123,21 @@
     )(tokens)
 
 
+def ordered(blocks, size):
+    core = lax.axis_index("core")
+    for half in range(2):
+        for b in range(blocks // 2):
+            row = 2 * b + (core if half == 0 else 1 - core)
+            yield row, pl.ds(pl.multiple_of(row * size, size), size), half * (blocks // 2) + b
+
+
 def turn_kernel(gain, w_query, w_forget, keyed):
-    size = gain.shape[1]
-    for b in range(w_query.shape[0] // size):
-        at = pl.ds(b * size, size)
-        row = gain[pl.ds(b, 1), :]
+    blocks, size = gain.shape
+    for row, at, to in ordered(blocks, size):
+        scale = gain[pl.ds(row, 1), :]
         for i, weight in enumerate((w_query, w_forget)):
             block = weight[at, :].astype(jnp.float32).T
-            keyed[pl.ds(i * size, size), at] = (block * row).astype(jnp.bfloat16)
+            keyed[pl.ds(i * size, size), pl.ds(to * size, size)] = (block * scale).astype(jnp.bfloat16)
 
 
 def turn(gain, w_query, w_forget):
@@ -147,12 +154,17 @@
 
 
 def fold_kernel(gain, w0, w1, w2, w3, out):
-    values, size = w0.shape[1], gain.shape[1]
-    for b in range(gain.shape[0]):
-        at = pl.ds(b * size, size)
-        for d, weight in enumerate((w0, w1, w2, w3)):
-            value = weight[0, :, at].astype(jnp.float32) * gain[pl.ds(b, 1), :]
-            out[pl.ds(d * values, values), at] = value.astype(jnp.bfloat16)
+    fold_into(out, gain, (w0, w1, w2, w3))
+
+
+def fold_into(out, gain, weights):
+    blocks, size = gain.shape
+    values = weights[0].shape[1]
+    for row, at, to in ordered(blocks, size):
+        scale = gain[pl.ds(row, 1), :]
+        for d, weight in enumerate(weights):
+            value = weight[0, :, at].astype(jnp.float32) * scale
+            out[pl.ds(d * values, values), pl.ds(to * size, size)] = value.astype(jnp.bfloat16)
 
 
 def fold(gain, weights):
@@ -168,69 +180,92 @@
     )(gain, *weights)
 
 
-def project_kernel(own, other, keyed, mixing, o0, o1, o2, o3, held, scale):
-    core = lax.axis_index("core")
-    blocks, size, seqs = own.shape
-    squares = jnp.zeros((8, seqs), jnp.float32)
-    for half, ref in ((core, own), (1 - core, other)):
-        for b in range(blocks):
-            part = ref[b]
-            held[pl.ds(pl.multiple_of((2 * b + half) * size, size), size), :] = part
-            wide = part.astype(jnp.float32)
-            squares = squares + jnp.sum((wide * wide).reshape(size // 8, 8, seqs), axis=0)
-    total = jnp.sum(squares, axis=0, keepdims=True)
-    factor = lax.rsqrt(total / (2 * blocks * size) + NORM_EPSILON)
+def squared(rows):
+    wide = rows[...].astype(jnp.float32)
+    return jnp.sum((wide * wide).reshape(rows.shape[0] // 8, 8, rows.shape[1]), axis=0)
+
+
+def begin_kernel(own, keyed, mixing, out, squares):
+    cut, keys = pl.ds(0, own.shape[0]), keyed.shape[0]
+    squares[...] = squared(own)
+    rows = own[...]
+    out[pl.ds(0, keys), :] = jnp.dot(keyed[:, cut], rows, preferred_element_type=jnp.float32)
+    out[pl.ds(keys, mixing.shape[0]), :] = jnp.dot(
+        mixing[:, cut], rows, preferred_element_type=jnp.float32
+    )
+
+
+def begin(own, keyed, mixing):
+    seqs = own.shape[1]
+    return call(
+        begin_kernel,
+        [
+            shaped((keyed.shape[0] + mixing.shape[0], seqs), jnp.float32),
+            shaped((8, seqs), jnp.float32),
+        ],
+        [],
+        (1_000_000_000, 2 << 20),
+        16 << 20,
+        [whole()] * 3,
+        [whole()] * 2,
+    )(own, keyed, mixing)
+
+
+def project_kernel(other, keyed, mixing, started, squares, o0, o1, o2, o3, scale):
+    half, keys = other.shape[0], keyed.shape[0]
+    cut = pl.ds(half, half)
+    total = jnp.sum(squares[...] + squared(other), axis=0, keepdims=True)
+    factor = lax.rsqrt(total / (2 * half) + NORM_EPSILON)
     scale[...] = jnp.broadcast_to(factor, scale.shape)
-    rows = held[...]
-    first = jnp.dot(keyed[...], rows, preferred_element_type=jnp.float32) * factor
-    first = first.astype(jnp.bfloat16)
-    second = jnp.dot(mixing[...], rows, preferred_element_type=jnp.float32) * factor
-    second = second.astype(jnp.bfloat16)
-    keys, values = first.shape[0], second.shape[0] // 4
+    rows = other[...]
+    first = jnp.dot(keyed[:, cut], rows, preferred_element_type=jnp.float32)
+    first = ((first + started[pl.ds(0, keys), :]) * factor).astype(jnp.bfloat16)
+    second = jnp.dot(mixing[:, cut], rows, preferred_element_type=jnp.float32)
+    second = second + started[pl.ds(keys, second.shape[0]), :]
+    second = (second * factor).astype(jnp.bfloat16)
+    values = second.shape[0] // 4
     for d, out in enumerate((o0, o1, o2, o3)):
         out[pl.ds(0, keys), :] = first
         out[pl.ds(keys, values), :] = second[d * values : (d + 1) * values]
 
 
-def project(own, other, keyed, mixing):
-    blocks, size, seqs = own.shape
+def project(other, keyed, mixing, started, squares):
+    seqs = other.shape[1]
     rows = keyed.shape[0] + mixing.shape[0] // 4
     outs = call(
         project_kernel,
-        [shaped((rows, seqs), jnp.bfloat16)] * 4
-        + [shaped((2 * blocks * size, seqs), jnp.bfloat16), shaped((8, seqs), jnp.float32)],
-        [],
-        (1_000_000_000, 3 << 20),
-        16 << 20,
-        [whole()] * 4,
-        [whole()] * 6,
-    )(own, other, keyed, mixing)
-    return outs[:4], outs[4], outs[5]
-
-
-def gate_kernel(gain, w0, w1, w2, w3, rows, scale, out, held):
-    values, size = w0.shape[1], gain.shape[1]
-    for b in range(gain.shape[0]):
-        at = pl.ds(b * size, size)
-        for d, weight in enumerate((w0, w1, w2, w3)):
-            value = weight[0, :, at].astype(jnp.float32) * gain[pl.ds(b, 1), :]
-            held[pl.ds(d * values, values), at] = value.astype(jnp.bfloat16)
-    raw = jnp.dot(held[...], rows[...], preferred_element_type=jnp.float32) * scale[0:1]
-    raw = raw.astype(jnp.bfloat16).astype(jnp.float32)
+        [shaped((rows, seqs), jnp.bfloat16)] * 4 + [shaped((8, seqs), jnp.float32)],
+        [],
+        (1_000_000_000, 2 << 20),
+        16 << 20,
+        [whole()] * 5,
+        [whole()] * 5,
+    )(other, keyed, mixing, started, squares)
+    return outs[:4], outs[4]
+
+
+def gate_kernel(gain, w0, w1, w2, w3, own, other, scale, out, held):
+    fold_into(held, gain, (w0, w1, w2, w3))
+    half = own.shape[0]
+    raw = jnp.dot(held[:, pl.ds(0, half)], own[...], preferred_element_type=jnp.float32)
+    raw = raw + jnp.dot(
+        held[:, pl.ds(half, half)], other[...], preferred_element_type=jnp.float32
+    )
+    raw = (raw * scale[0:1]).astype(jnp.bfloat16).astype(jnp.float32)
     out[...] = raw * jax.nn.sigmoid(raw)
 
 
-def gate(gain, weights, rows, scale):
+def gate(gain, weights, own, other, scale):
     _, values, width = weights[0].shape
     return call(
         gate_kernel,
-        shaped((4 * values, rows.shape[1]), jnp.float32),
+        shaped((4 * values, own.shape[1]), jnp.float32),
         [pltpu.VMEM((4 * values, width), jnp.bfloat16)],
         (1_000_000_000, 3 << 20),
         16 << 20,
-        [whole()] * 7,
+        [whole()] * 8,
         whole(),
-    )(gain, *weights, rows, scale)
+    )(gain, *weights, own, other, scale)
 
 
 def outward_kernel(w_out, mine, theirs, held, sems):
@@ -428,13 +463,14 @@
 
     def passed(parts):
         far = lax.ppermute(parts[2], "tp", hops[2])
-        near = [lax.ppermute(parts[d], "tp", hops[d]) for d in (1, 3)]
-        return [parts[0], near[0], far, near[1]]
+        wrap = lax.ppermute(parts[3], "tp", hops[3])
+        near = lax.ppermute(parts[1], "tp", hops[1])
+        return [parts[0], near, far, wrap]
 
     gain = input_norm_gain.reshape(-1, size)
     inputs = passed([w_input] * group)
     own = lax.all_to_all(source(tokens.transpose(1, 2, 0), planes), ("zy", "tp"), 0, 0, tiled=True)
-    own = own.reshape(planes, group * features, seqs)
+    own = own.reshape(planes * group * features, seqs)
     other = lax.ppermute(own, "core", swap)
     gates = passed([w_gate] * group)
     keyed = turn(gain, w_query, w_forget)
@@ -446,13 +482,14 @@
         state[:, 0],
     )
 
-    sends, rows, scale = project(own, other, keyed, mixing)
+    started, squares = begin(own, keyed, mixing)
+    sends, scale = project(other, keyed, mixing, started, squares)
     received = passed(sends)
     ours, theirs = turn_outward(w_out)
     theirs = lax.ppermute(theirs, "core", swap)
     shown = recur(received, rounded.reshape(-1, size), forget_floor[None], head_gain[None])
     parts = passed(shown)
-    opened = gate(gain, gates, rows, scale)
+    opened = gate(gain, gates, own, other, scale)
     hidden = hide(parts, opened)
     kept = emit(hidden, lax.ppermute(hidden, "core", swap), ours, theirs)
     terms = lax.all_to_all(

time: 97.7 us -> 97.7 us (level)
  no operation moved by 1% of the time
where the time goes in v9:
time: 97.7 us; the launch traced here: 97.4 us
  blocking collectives  42.9 us (44%)
  waiting for transfers between devices  22.7 us (23%)
  starting transfers between devices  19.2 us (20%)
  Pallas kernels  10.5 us (11%)
  local copies, waits for them, and re-layouts  1.29 us (1%)
    all_to_all x1, blocking collectives, body(): lax.all_to_all(source(tokens.transpose(1, 2, 0), planes), ('zy', 'tp'), 0...  24.9 us
    all_to_all x1, blocking collectives, body(): lax.all_to_all(kept.reshape(planes * group, features, seqs), ('zy', 'tp')...  18 us
    ppermute x4, waiting for transfers between devices, passed(): wrap = lax.ppermute(parts[3], 'tp', hops[3])  14.1 us
    ppermute x4, starting transfers between devices, passed(): far = lax.ppermute(parts[2], 'tp', hops[2])  11.4 us
    ppermute x4, starting transfers between devices, passed(): wrap = lax.ppermute(parts[3], 'tp', hops[3])  6.8 us
    ppermute x4, waiting for transfers between devices, passed(): far = lax.ppermute(parts[2], 'tp', hops[2])  5.51 us
    pallas_call x1, Pallas kernels, advance(): pl.pallas_call(advance_kernel, grid=(seqs // count,), in_specs=[pl.BlockS...  3.12 us
    ppermute x4, waiting for transfers between devices, passed(): near = lax.ppermute(parts[1], 'tp', hops[1])  1.97 us
  transfers between devices with their start and end apart: 15, of which 6 were waited for; matrix products, arithmetic and copies ran while one was open for 0% of the time, Pallas kernels for 8%

profile of v9, /device:TPU:0, one launch (start us, length us, event | category | flops | bytes accessed | tf_op | source)
XLA Modules:
  0.0 97.4 jit_solution(14677425844708072879)
XLA Ops:
  0.6 1.7 %shard_map.140 = bf16[64,32,128]{2,1,0:T(8,128)(2,1)} custom-call(bf16[4,32,128]{2,1,0:T(8,128)(2,1)} %bitcast.31), custom_call_target="tpu_custom_call" | custom-call | flops 1000000 | bytes 1048576 | tf_op jit(solution)/shard_map/pallas_call | solution.py:115
  2.3 24.9 %all_to_all.10 = bf16[64,32,128]{2,1,0:T(8,128)(2,1)S(1)} all-to-all(bf16[64,32,128]{2,1,0:T(8,128)(2,1)} %shard_map.140), channel_id=1, replica_groups=mesh['zy'=16,'core'=2,'tp'=4] {'zy','tp'}, dimensions={0} | all-to-all | bytes 1048576 | tf_op jit(solution)/shard_map/all_to_all | solution.py:472
  27.2 0.6 collective-permute-start.1
  27.9 1.8 %collective-permute-start.2 = (bf16[1,32,4096]{2,1,0:T(8,128)(2,1)}, bf16[1,32,4096]{2,1,0:T(8,128)(2,1)S(1)}, u32[]{:S(2)}, u32[]{:S(2)}) collective-permute-start(bf16[1,32,4096]{2,1,0:T(8,128)(2,1)} %w0.2), channel_id=1, source_target_pairs={{0,2},{1,3},{2,0},{3,1},{4,6},{5,7},{6,4},{7,5},{8,10},{9,11},{10,... | collective-permute-start | bytes 786440 | tf_op jit(solution)/shard_map/ppermute | solution.py:465
  29.7 2.3 %collective-permute-start.3 = (bf16[1,32,4096]{2,1,0:T(8,128)(2,1)}, bf16[1,32,4096]{2,1,0:T(8,128)(2,1)S(1)}, u32[]{:S(2)}, u32[]{:S(2)}) collective-permute-start(bf16[1,32,4096]{2,1,0:T(8,128)(2,1)} %w0.2), channel_id=1, source_target_pairs={{0,3},{1,2},{2,1},{3,0},{4,7},{5,6},{6,5},{7,4},{8,11},{9,10},{10,... | collective-permute-start | bytes 786440 | tf_op jit(solution)/shard_map/ppermute | solution.py:466
  32.0 1.2 %copy-done.4 = bf16[128,4096]{1,0:T(8,128)(2,1)S(1)} copy-done((bf16[128,4096]{1,0:T(8,128)(2,1)S(1)}, bf16[128,4096]{1,0:T(8,128)(2,1)}, u32[]{:S(2)}) %copy-start.4) | copy-done | bytes 1048600
  33.2 0.7 shard_map.148
  33.9 0.1 collective-permute-start.14
  34.1 0.7 shard_map.141.keyed
  34.7 2.0 %collective-permute-done.1.w1 = bf16[1,32,4096]{2,1,0:T(8,128)(2,1)S(1)} collective-permute-done((bf16[1,32,4096]{2,1,0:T(8,128)(2,1)}, bf16[1,32,4096]{2,1,0:T(8,128)(2,1)S(1)}, u32[]{:S(2)}, u32[]{:S(2)}) %collective-permute-start.1) | collective-permute-done | bytes 262176 | tf_op jit(solution)/shard_map/ppermute | solution.py:467
  36.7 5.5 %collective-permute-done.2.w2 = bf16[1,32,4096]{2,1,0:T(8,128)(2,1)S(1)} collective-permute-done((bf16[1,32,4096]{2,1,0:T(8,128)(2,1)}, bf16[1,32,4096]{2,1,0:T(8,128)(2,1)S(1)}, u32[]{:S(2)}, u32[]{:S(2)}) %collective-permute-start.2) | collective-permute-done | bytes 262176 | tf_op jit(solution)/shard_map/ppermute | solution.py:465
  42.2 2.6 %collective-permute-done.3.w3 = bf16[1,32,4096]{2,1,0:T(8,128)(2,1)S(1)} collective-permute-done((bf16[1,32,4096]{2,1,0:T(8,128)(2,1)}, bf16[1,32,4096]{2,1,0:T(8,128)(2,1)S(1)}, u32[]{:S(2)}, u32[]{:S(2)}) %collective-permute-start.3) | collective-permute-done | bytes 262176 | tf_op jit(solution)/shard_map/ppermute | solution.py:466
  44.8 0.3 shard_map.142.mixing
  45.1 0.6 shard_map.143
  45.7 0.6 shard_map.144
  46.4 0.1 collective-permute-start.4
  46.5 3.8 %collective-permute-start.5 = (bf16[288,128]{1,0:T(8,128)(2,1)S(1)}, bf16[288,128]{1,0:T(8,128)(2,1)S(1)}, u32[]{:S(2)}, u32[]{:S(2)}) collective-permute-start(bf16[288,128]{1,0:T(8,128)(2,1)S(1)} %get-tuple-element.21), channel_id=1, source_target_pairs={{0,2},{1,3},{2,0},{3,1},{4,6},{5,7},{6,4},{7,5},{8,10},{9,11},{10,... | collective-permute-start | bytes 221192 | tf_op jit(solution)/shard_map/ppermute | solution.py:465
  50.3 2.4 %collective-permute-start.11 = (bf16[1,32,4096]{2,1,0:T(8,128)(2,1)S(1)}, bf16[1,32,4096]{2,1,0:T(8,128)(2,1)S(1)}, u32[]{:S(2)}, u32[]{:S(2)}) collective-permute-start(bf16[1,32,4096]{2,1,0:T(8,128)(2,1)S(1)} %copy-done.7), channel_id=1, source_target_pairs={{0,2},{1,3},{2,0},{3,1},{4,6},{5,7},{6,4},{7,5},{8,10},{9,11},{10,... | collective-permute-start | bytes 786440 | tf_op jit(solution)/shard_map/ppermute | solution.py:465
  52.6 2.3 %collective-permute-start.12 = (bf16[1,32,4096]{2,1,0:T(8,128)(2,1)S(1)}, bf16[1,32,4096]{2,1,0:T(8,128)(2,1)S(1)}, u32[]{:S(2)}, u32[]{:S(2)}) collective-permute-start(bf16[1,32,4096]{2,1,0:T(8,128)(2,1)S(1)} %copy-done.7), channel_id=1, source_target_pairs={{0,3},{1,2},{2,1},{3,0},{4,7},{5,6},{6,5},{7,4},{8,11},{9,10},{10,... | collective-permute-start | bytes 786440 | tf_op jit(solution)/shard_map/ppermute | solution.py:466
  55.0 0.9 collective-permute-start.6
  55.9 3.1 %advance.1 = (f32[128,32,128]{2,1,0:T(8,128)}, bf16[128,32,128]{2,1,0:T(8,128)(2,1)S(1)}) custom-call(s32[1,128]{1,0:T(1,128)S(1)} %bitcast.27, f32[128,4,128]{2,1,0:T(4,128)S(1)} %copy-done.6, bf16[4,32,128]{2,1,0:T(8,128)(2,1)S(1)} %bitcast.26, f32[128,32,128]{2,1,0:T(8,128)S(1)} %bitcast.25), custom_call_target="tpu_custom_call" | custom-call | flops 1000000000 | bytes 5242880 | tf_op jit(solution)/shard_map/advance/pallas_call | solution.py:65
  59.0 8.5 %collective-permute-done.6.r3 = bf16[288,128]{1,0:T(8,128)(2,1)S(1)} collective-permute-done((bf16[288,128]{1,0:T(8,128)(2,1)S(1)}, bf16[288,128]{1,0:T(8,128)(2,1)S(1)}, u32[]{:S(2)}, u32[]{:S(2)}) %collective-permute-start.6) | collective-permute-done | bytes 73760 | tf_op jit(solution)/shard_map/ppermute | solution.py:466
  67.5 1.0 %shard_map.145 = (bf16[48,128]{1,0:T(8,128)(2,1)S(1)}, bf16[48,128]{1,0:T(8,128)(2,1)S(1)}, bf16[48,128]{1,0:T(8,128)(2,1)S(1)}, bf16[48,128]{1,0:T(8,128)(2,1)S(1)}) custom-call(bf16[288,128]{1,0:T(8,128)(2,1)S(1)} %get-tuple-element.19.r0, bf16[288,128]{1,0:T(8,128)(2,1)S(1)} %collective-permute-done.4.r1, bf16[288,128]{1,0:T(8,128)(2,1)S(1)} %collective-permute-done.5.r2, ...), custom_call_target="tpu_custom_call" | custom-call | flops 1000000000 | bytes 2097152 | tf_op jit(solution)/shard_map/pallas_call | solution.py:362
  68.5 0.1 collective-permute-start.7
  68.6 3.5 %collective-permute-start.8 = (bf16[48,128]{1,0:T(8,128)(2,1)S(1)}, bf16[48,128]{1,0:T(8,128)(2,1)S(1)}, u32[]{:S(2)}, u32[]{:S(2)}) collective-permute-start(bf16[48,128]{1,0:T(8,128)(2,1)S(1)} %get-tuple-element.26), channel_id=1, source_target_pairs={{0,2},{1,3},{2,0},{3,1},{4,6},{5,7},{6,4},{7,5},{8,10},{9,11},{10,... | collective-permute-start | bytes 36872 | tf_op jit(solution)/shard_map/ppermute | solution.py:465
  72.1 1.2 %collective-permute-start.9 = (bf16[48,128]{1,0:T(8,128)(2,1)S(1)}, bf16[48,128]{1,0:T(8,128)(2,1)S(1)}, u32[]{:S(2)}, u32[]{:S(2)}) collective-permute-start(bf16[48,128]{1,0:T(8,128)(2,1)S(1)} %get-tuple-element.27), channel_id=1, source_target_pairs={{0,3},{1,2},{2,1},{3,0},{4,7},{5,6},{6,5},{7,4},{8,11},{9,10},{10,... | collective-permute-start | bytes 36872 | tf_op jit(solution)/shard_map/ppermute | solution.py:466
  73.3 0.6 shard_map.146.gates
  74.0 3.0 %collective-permute-done.9.p3 = bf16[48,128]{1,0:T(8,128)(2,1)S(1)} collective-permute-done((bf16[48,128]{1,0:T(8,128)(2,1)S(1)}, bf16[48,128]{1,0:T(8,128)(2,1)S(1)}, u32[]{:S(2)}, u32[]{:S(2)}) %collective-permute-start.9) | collective-permute-done | bytes 12320 | tf_op jit(solution)/shard_map/ppermute | solution.py:466
  77.1 1.2 %collective-permute-done.13.other = bf16[128,128]{1,0:T(8,128)(2,1)S(1)} collective-permute-done((bf16[128,128]{1,0:T(8,128)(2,1)S(1)}, bf16[128,128]{1,0:T(8,128)(2,1)S(1)}, u32[]{:S(2)}, u32[]{:S(2)}) %collective-permute-start.13) | collective-permute-done | bytes 32800 | tf_op jit(solution)/shard_map/ppermute | solution.py:494
  78.3 0.4 shard_map.149
  78.7 18.0 %all_to_all.11 = bf16[64,32,128]{2,1,0:T(8,128)(2,1)S(1)} all-to-all(bf16[64,32,128]{2,1,0:T(8,128)(2,1)S(1)} %bitcast.17), channel_id=1, replica_groups=mesh['zy'=16,'core'=2,'tp'=4] {'zy','tp'}, dimensions={0} | all-to-all | bytes 1048576 | tf_op jit(solution)/shard_map/all_to_all | solution.py:495
  96.7 0.7 shard_map.150
  (36 shorter events, 0.2 us)
Async XLA Ops:
  27.2 6.8 %copy-start = (bf16[4096,128]{1,0:T(8,128)(2,1)S(1)}, bf16[4096,128]{1,0:T(8,128)(2,1)}, u32[]{:S(2)}) copy-start(bf16[4096,128]{1,0:T(8,128)(2,1)} %w_query.1) | copy-start | bytes 3145732
  27.2 6.8 %copy-start.1 = (bf16[4096,128]{1,0:T(8,128)(2,1)S(1)}, bf16[4096,128]{1,0:T(8,128)(2,1)}, u32[]{:S(2)}) copy-start(bf16[4096,128]{1,0:T(8,128)(2,1)} %w_forget.1) | copy-start | bytes 3145732
  27.2 6.8 %copy-start.2 = (f32[4096]{0:T(1024)S(1)}, f32[4096]{0:T(1024)}, u32[]{:S(2)}) copy-start(f32[4096]{0:T(1024)} %param.14) | copy-start | bytes 49156
  27.2 18.5 %collective-permute-start = (bf16[2048,128]{1,0:T(8,128)(2,1)S(1)}, bf16[2048,128]{1,0:T(8,128)(2,1)S(1)}, u32[]{:S(2)}, u32[]{:S(2)}) collective-permute-start(bf16[2048,128]{1,0:T(8,128)(2,1)S(1)} %bitcast.19), channel_id=1, source_target_pairs={{0,4},{4,0},{1,5},{5,1},{2,6},{6,2},{3,7},{7,3},{8,12},{12,8},{9,1... | collective-permute-start | bytes 1572872 | tf_op jit(solution)/shard_map/ppermute | solution.py:474
  27.2 9.5 %collective-permute-start.1 = (bf16[1,32,4096]{2,1,0:T(8,128)(2,1)}, bf16[1,32,4096]{2,1,0:T(8,128)(2,1)S(1)}, u32[]{:S(2)}, u32[]{:S(2)}) collective-permute-start(bf16[1,32,4096]{2,1,0:T(8,128)(2,1)} %w0.2), channel_id=1, source_target_pairs={{0,1},{1,0},{2,3},{3,2},{4,5},{5,4},{6,7},{7,6},{8,9},{9,8},{10,11... | collective-permute-start | bytes 786440 | tf_op jit(solution)/shard_map/ppermute | solution.py:467
  27.9 14.3 %collective-permute-start.2 = (bf16[1,32,4096]{2,1,0:T(8,128)(2,1)}, bf16[1,32,4096]{2,1,0:T(8,128)(2,1)S(1)}, u32[]{:S(2)}, u32[]{:S(2)}) collective-permute-start(bf16[1,32,4096]{2,1,0:T(8,128)(2,1)} %w0.2), channel_id=1, source_target_pairs={{0,2},{1,3},{2,0},{3,1},{4,6},{5,7},{6,4},{7,5},{8,10},{9,11},{10,... | collective-permute-start | bytes 786440 | tf_op jit(solution)/shard_map/ppermute | solution.py:465
  29.7 15.1 %collective-permute-start.3 = (bf16[1,32,4096]{2,1,0:T(8,128)(2,1)}, bf16[1,32,4096]{2,1,0:T(8,128)(2,1)S(1)}, u32[]{:S(2)}, u32[]{:S(2)}) collective-permute-start(bf16[1,32,4096]{2,1,0:T(8,128)(2,1)} %w0.2), channel_id=1, source_target_pairs={{0,3},{1,2},{2,1},{3,0},{4,7},{5,6},{6,5},{7,4},{8,11},{9,10},{10,... | collective-permute-start | bytes 786440 | tf_op jit(solution)/shard_map/ppermute | solution.py:466
  32.0 1.2 %copy-start.4 = (bf16[128,4096]{1,0:T(8,128)(2,1)S(1)}, bf16[128,4096]{1,0:T(8,128)(2,1)}, u32[]{:S(2)}) copy-start(bf16[128,4096]{1,0:T(8,128)(2,1)} %w_out.1) | copy-start | bytes 3145732
  33.9 43.2 %collective-permute-start.14 = (bf16[16,128,128]{2,1,0:T(8,128)(2,1)S(1)}, bf16[16,128,128]{2,1,0:T(8,128)(2,1)S(1)}, u32[]{:S(2)}, u32[]{:S(2)}) collective-permute-start(bf16[16,128,128]{2,1,0:T(8,128)(2,1)S(1)} %get-tuple-element.30), channel_id=1, source_target_pairs={{0,4},{4,0},{1,5},{5,1},{2,6},{6,2},{3,7},{7,3},{8,12},{12,8},{9,1... | collective-permute-start | bytes 1572872 | tf_op jit(solution)/shard_map/ppermute | solution.py:489
  34.0 10.7 %copy-start.5 = (bf16[1,32,4096]{2,1,0:T(8,128)(2,1)S(1)}, bf16[1,32,4096]{2,1,0:T(8,128)(2,1)}, u32[]{:S(2)}) copy-start(bf16[1,32,4096]{2,1,0:T(8,128)(2,1)} %w0.2) | copy-start | bytes 786436
  45.7 4.6 %copy-start.7 = (bf16[1,32,4096]{2,1,0:T(8,128)(2,1)S(1)}, bf16[1,32,4096]{2,1,0:T(8,128)(2,1)}, u32[]{:S(2)}) copy-start(bf16[1,32,4096]{2,1,0:T(8,128)(2,1)} %w0.3) | copy-start | bytes 786436
  45.7 10.2 %copy-start.3 = (f32[128,1,32,128]{3,2,1,0:T(8,128)S(1)}, f32[128,1,32,128]{3,2,1,0:T(8,128)}, u32[]{:S(2)}) copy-start(f32[128,1,32,128]{3,2,1,0:T(8,128)} %param.22) | copy-start | bytes 6291460
  45.7 10.2 %copy-start.6 = (f32[128,4,128]{2,1,0:T(4,128)S(1)}, f32[128,4,128]{2,1,0:T(4,128)}, u32[]{:S(2)}) copy-start(f32[128,4,128]{2,1,0:T(4,128)} %prev_forget.1) | copy-start | bytes 786436
  45.7 10.2 %copy-start.8 = (bf16[128,4,1,32]{0,3,2,1:T(8,128)(2,1)S(1)}, bf16[128,4,1,32]{0,3,2,1:T(8,128)(2,1)}, u32[]{:S(2)}) copy-start(bf16[128,4,1,32]{0,3,2,1:T(8,128)(2,1)} %param.24) | copy-start | bytes 98308
  45.7 10.2 %copy-start.9 = (s32[128]{0:T(128)S(1)}, s32[128]{0:T(128)}, u32[]{:S(2)}) copy-start(s32[128]{0:T(128)} %param.25) | copy-start | bytes 1540
  46.4 21.1 %copy-start.10 = (f32[128]{0:T(128)S(1)}, f32[128]{0:T(128)}, u32[]{:S(2)}) copy-start(f32[128]{0:T(128)} %param.19) | copy-start | bytes 1540
  46.4 21.1 %copy-start.11 = (f32[32]{0:T(128)S(1)}, f32[32]{0:T(128)}, u32[]{:S(2)}) copy-start(f32[32]{0:T(128)} %param.20) | copy-start | bytes 388
  46.4 6.2 %collective-permute-start.4 = (bf16[288,128]{1,0:T(8,128)(2,1)S(1)}, bf16[288,128]{1,0:T(8,128)(2,1)S(1)}, u32[]{:S(2)}, u32[]{:S(2)}) collective-permute-start(bf16[288,128]{1,0:T(8,128)(2,1)S(1)} %get-tuple-element.20), channel_id=1, source_target_pairs={{0,1},{1,0},{2,3},{3,2},{4,5},{5,4},{6,7},{7,6},{8,9},{9,8},{10,11... | collective-permute-start | bytes 221192 | tf_op jit(solution)/shard_map/ppermute | solution.py:467
  46.5 8.5 %collective-permute-start.5 = (bf16[288,128]{1,0:T(8,128)(2,1)S(1)}, bf16[288,128]{1,0:T(8,128)(2,1)S(1)}, u32[]{:S(2)}, u32[]{:S(2)}) collective-permute-start(bf16[288,128]{1,0:T(8,128)(2,1)S(1)} %get-tuple-element.21), channel_id=1, source_target_pairs={{0,2},{1,3},{2,0},{3,1},{4,6},{5,7},{6,4},{7,5},{8,10},{9,11},{10,... | collective-permute-start | bytes 221192 | tf_op jit(solution)/shard_map/ppermute | solution.py:465
  50.3 18.3 %collective-permute-start.10 = (bf16[1,32,4096]{2,1,0:T(8,128)(2,1)S(1)}, bf16[1,32,4096]{2,1,0:T(8,128)(2,1)S(1)}, u32[]{:S(2)}, u32[]{:S(2)}) collective-permute-start(bf16[1,32,4096]{2,1,0:T(8,128)(2,1)S(1)} %copy-done.7), channel_id=1, source_target_pairs={{0,1},{1,0},{2,3},{3,2},{4,5},{5,4},{6,7},{7,6},{8,9},{9,8},{10,11... | collective-permute-start | bytes 786440 | tf_op jit(solution)/shard_map/ppermute | solution.py:467
  50.3 21.8 %collective-permute-start.11 = (bf16[1,32,4096]{2,1,0:T(8,128)(2,1)S(1)}, bf16[1,32,4096]{2,1,0:T(8,128)(2,1)S(1)}, u32[]{:S(2)}, u32[]{:S(2)}) collective-permute-start(bf16[1,32,4096]{2,1,0:T(8,128)(2,1)S(1)} %copy-done.7), channel_id=1, source_target_pairs={{0,2},{1,3},{2,0},{3,1},{4,6},{5,7},{6,4},{7,5},{8,10},{9,11},{10,... | collective-permute-start | bytes 786440 | tf_op jit(solution)/shard_map/ppermute | solution.py:465
  52.6 20.6 %collective-permute-start.12 = (bf16[1,32,4096]{2,1,0:T(8,128)(2,1)S(1)}, bf16[1,32,4096]{2,1,0:T(8,128)(2,1)S(1)}, u32[]{:S(2)}, u32[]{:S(2)}) collective-permute-start(bf16[1,32,4096]{2,1,0:T(8,128)(2,1)S(1)} %copy-done.7), channel_id=1, source_target_pairs={{0,3},{1,2},{2,1},{3,0},{4,7},{5,6},{6,5},{7,4},{8,11},{9,10},{10,... | collective-permute-start | bytes 786440 | tf_op jit(solution)/shard_map/ppermute | solution.py:466
  55.0 12.5 %collective-permute-start.6 = (bf16[288,128]{1,0:T(8,128)(2,1)S(1)}, bf16[288,128]{1,0:T(8,128)(2,1)S(1)}, u32[]{:S(2)}, u32[]{:S(2)}) collective-permute-start(bf16[288,128]{1,0:T(8,128)(2,1)S(1)} %get-tuple-element.22), channel_id=1, source_target_pairs={{0,3},{1,2},{2,1},{3,0},{4,7},{5,6},{6,5},{7,4},{8,11},{9,10},{10,... | collective-permute-start | bytes 221192 | tf_op jit(solution)/shard_map/ppermute | solution.py:466
  68.5 5.4 %collective-permute-start.7 = (bf16[48,128]{1,0:T(8,128)(2,1)S(1)}, bf16[48,128]{1,0:T(8,128)(2,1)S(1)}, u32[]{:S(2)}, u32[]{:S(2)}) collective-permute-start(bf16[48,128]{1,0:T(8,128)(2,1)S(1)} %get-tuple-element.25), channel_id=1, source_target_pairs={{0,1},{1,0},{2,3},{3,2},{4,5},{5,4},{6,7},{7,6},{8,9},{9,8},{10,11... | collective-permute-start | bytes 36872 | tf_op jit(solution)/shard_map/ppermute | solution.py:467
  68.6 5.3 %collective-permute-start.8 = (bf16[48,128]{1,0:T(8,128)(2,1)S(1)}, bf16[48,128]{1,0:T(8,128)(2,1)S(1)}, u32[]{:S(2)}, u32[]{:S(2)}) collective-permute-start(bf16[48,128]{1,0:T(8,128)(2,1)S(1)} %get-tuple-element.26), channel_id=1, source_target_pairs={{0,2},{1,3},{2,0},{3,1},{4,6},{5,7},{6,4},{7,5},{8,10},{9,11},{10,... | collective-permute-start | bytes 36872 | tf_op jit(solution)/shard_map/ppermute | solution.py:465
  72.1 4.9 %collective-permute-start.9 = (bf16[48,128]{1,0:T(8,128)(2,1)S(1)}, bf16[48,128]{1,0:T(8,128)(2,1)S(1)}, u32[]{:S(2)}, u32[]{:S(2)}) collective-permute-start(bf16[48,128]{1,0:T(8,128)(2,1)S(1)} %get-tuple-element.27), channel_id=1, source_target_pairs={{0,3},{1,2},{2,1},{3,0},{4,7},{5,6},{6,5},{7,4},{8,11},{9,10},{10,... | collective-permute-start | bytes 36872 | tf_op jit(solution)/shard_map/ppermute | solution.py:466
  77.0 1.3 %collective-permute-start.13 = (bf16[128,128]{1,0:T(8,128)(2,1)S(1)}, bf16[128,128]{1,0:T(8,128)(2,1)S(1)}, u32[]{:S(2)}, u32[]{:S(2)}) collective-permute-start(bf16[128,128]{1,0:T(8,128)(2,1)S(1)} %shard_map.147.hidden), channel_id=1, source_target_pairs={{0,4},{4,0},{1,5},{5,1},{2,6},{6,2},{3,7},{7,3},{8,12},{12,8},{9,1... | collective-permute-start | bytes 98312 | tf_op jit(solution)/shard_map/ppermute | solution.py:494

commit v10 on v8

--- a/solution.py
+++ b/solution.py
@@ -428,8 +428,9 @@
 
     def passed(parts):
         far = lax.ppermute(parts[2], "tp", hops[2])
-        near = [lax.ppermute(parts[d], "tp", hops[d]) for d in (1, 3)]
-        return [parts[0], near[0], far, near[1]]
+        wrap = lax.ppermute(parts[3], "tp", hops[3])
+        near = lax.ppermute(parts[1], "tp", hops[1])
+        return [parts[0], near, far, wrap]
 
     gain = input_norm_gain.reshape(-1, size)
     inputs = passed([w_input] * group)

time: 97.7 us -> 97.7 us (level)
  no operation moved by 1% of the time
where the time goes in v10:
time: 97.7 us; the launch traced here: 97.3 us
  blocking collectives  42.9 us (44%)
  waiting for transfers between devices  22.8 us (23%)
  starting transfers between devices  19.2 us (20%)
  Pallas kernels  10.3 us (11%)
  local copies, waits for them, and re-layouts  1.29 us (1%)
    all_to_all x1, blocking collectives, body(): lax.all_to_all(source(tokens.transpose(1, 2, 0), planes), ('zy', 'tp'), 0...  24.9 us
    all_to_all x1, blocking collectives, body(): lax.all_to_all(kept.reshape(planes * group, features, seqs), ('zy', 'tp')...  18 us
    ppermute x4, waiting for transfers between devices, passed(): wrap = lax.ppermute(parts[3], 'tp', hops[3])  14.1 us
    ppermute x4, starting transfers between devices, passed(): far = lax.ppermute(parts[2], 'tp', hops[2])  11.4 us
    ppermute x4, starting transfers between devices, passed(): wrap = lax.ppermute(parts[3], 'tp', hops[3])  6.8 us
    ppermute x4, waiting for transfers between devices, passed(): far = lax.ppermute(parts[2], 'tp', hops[2])  5.54 us
    pallas_call x1, Pallas kernels, advance(): pl.pallas_call(advance_kernel, grid=(seqs // count,), in_specs=[pl.BlockS...  3.12 us
    ppermute x4, waiting for transfers between devices, passed(): near = lax.ppermute(parts[1], 'tp', hops[1])  1.99 us
  transfers between devices with their start and end apart: 15, of which 6 were waited for; matrix products, arithmetic and copies ran while one was open for 0% of the time, Pallas kernels for 8%

profile of v10, /device:TPU:0, one launch (start us, length us, event | category | flops | bytes accessed | tf_op | source)
XLA Modules:
  0.0 97.3 jit_solution(7756738938892414761)
XLA Ops:
  0.6 1.7 %shard_map.140 = bf16[64,32,128]{2,1,0:T(8,128)(2,1)} custom-call(bf16[4,32,128]{2,1,0:T(8,128)(2,1)} %bitcast.30), custom_call_target="tpu_custom_call" | custom-call | flops 1000000 | bytes 1048576 | tf_op jit(solution)/shard_map/pallas_call | solution.py:115
  2.3 24.9 %all_to_all.10 = bf16[64,32,128]{2,1,0:T(8,128)(2,1)S(1)} all-to-all(bf16[64,32,128]{2,1,0:T(8,128)(2,1)} %shard_map.140), channel_id=1, replica_groups=mesh['zy'=16,'core'=2,'tp'=4] {'zy','tp'}, dimensions={0} | all-to-all | bytes 1048576 | tf_op jit(solution)/shard_map/all_to_all | solution.py:437
  27.2 0.6 collective-permute-start.1
  27.9 1.8 %collective-permute-start.2 = (bf16[1,32,4096]{2,1,0:T(8,128)(2,1)}, bf16[1,32,4096]{2,1,0:T(8,128)(2,1)S(1)}, u32[]{:S(2)}, u32[]{:S(2)}) collective-permute-start(bf16[1,32,4096]{2,1,0:T(8,128)(2,1)} %w0.2), channel_id=1, source_target_pairs={{0,2},{1,3},{2,0},{3,1},{4,6},{5,7},{6,4},{7,5},{8,10},{9,11},{10,... | collective-permute-start | bytes 786440 | tf_op jit(solution)/shard_map/ppermute | solution.py:430
  29.7 2.3 %collective-permute-start.3 = (bf16[1,32,4096]{2,1,0:T(8,128)(2,1)}, bf16[1,32,4096]{2,1,0:T(8,128)(2,1)S(1)}, u32[]{:S(2)}, u32[]{:S(2)}) collective-permute-start(bf16[1,32,4096]{2,1,0:T(8,128)(2,1)} %w0.2), channel_id=1, source_target_pairs={{0,3},{1,2},{2,1},{3,0},{4,7},{5,6},{6,5},{7,4},{8,11},{9,10},{10,... | collective-permute-start | bytes 786440 | tf_op jit(solution)/shard_map/ppermute | solution.py:431
  32.0 1.2 %copy-done.4 = bf16[128,4096]{1,0:T(8,128)(2,1)S(1)} copy-done((bf16[128,4096]{1,0:T(8,128)(2,1)S(1)}, bf16[128,4096]{1,0:T(8,128)(2,1)}, u32[]{:S(2)}) %copy-start.4) | copy-done | bytes 1048600
  33.2 0.7 shard_map.147
  33.9 0.1 collective-permute-start.14
  34.1 0.7 shard_map.141.keyed
  34.7 2.0 %collective-permute-done.1.w1 = bf16[1,32,4096]{2,1,0:T(8,128)(2,1)S(1)} collective-permute-done((bf16[1,32,4096]{2,1,0:T(8,128)(2,1)}, bf16[1,32,4096]{2,1,0:T(8,128)(2,1)S(1)}, u32[]{:S(2)}, u32[]{:S(2)}) %collective-permute-start.1) | collective-permute-done | bytes 262176 | tf_op jit(solution)/shard_map/ppermute | solution.py:432
  36.7 5.5 %collective-permute-done.2.w2 = bf16[1,32,4096]{2,1,0:T(8,128)(2,1)S(1)} collective-permute-done((bf16[1,32,4096]{2,1,0:T(8,128)(2,1)}, bf16[1,32,4096]{2,1,0:T(8,128)(2,1)S(1)}, u32[]{:S(2)}, u32[]{:S(2)}) %collective-permute-start.2) | collective-permute-done | bytes 262176 | tf_op jit(solution)/shard_map/ppermute | solution.py:430
  42.2 2.6 %collective-permute-done.3.w3 = bf16[1,32,4096]{2,1,0:T(8,128)(2,1)S(1)} collective-permute-done((bf16[1,32,4096]{2,1,0:T(8,128)(2,1)}, bf16[1,32,4096]{2,1,0:T(8,128)(2,1)S(1)}, u32[]{:S(2)}, u32[]{:S(2)}) %collective-permute-start.3) | collective-permute-done | bytes 262176 | tf_op jit(solution)/shard_map/ppermute | solution.py:431
  44.8 0.3 shard_map.142.mixing
  45.1 1.2 %shard_map.143 = (bf16[288,128]{1,0:T(8,128)(2,1)S(1)}, bf16[288,128]{1,0:T(8,128)(2,1)S(1)}, bf16[288,128]{1,0:T(8,128)(2,1)S(1)}, bf16[288,128]{1,0:T(8,128)(2...) custom-call(bf16[16,128,128]{2,1,0:T(8,128)(2,1)S(1)} %bitcast.20, ...), custom_call_target="tpu_custom_call" | custom-call | flops 1000000000 | bytes 3145728 | tf_op jit(solution)/shard_map/pallas_call | solution.py:198
  46.3 0.1 collective-permute-start.4
  46.4 3.8 %collective-permute-start.5 = (bf16[288,128]{1,0:T(8,128)(2,1)S(1)}, bf16[288,128]{1,0:T(8,128)(2,1)S(1)}, u32[]{:S(2)}, u32[]{:S(2)}) collective-permute-start(bf16[288,128]{1,0:T(8,128)(2,1)S(1)} %get-tuple-element.18), channel_id=1, source_target_pairs={{0,2},{1,3},{2,0},{3,1},{4,6},{5,7},{6,4},{7,5},{8,10},{9,11},{10,... | collective-permute-start | bytes 221192 | tf_op jit(solution)/shard_map/ppermute | solution.py:430
  50.2 2.4 %collective-permute-start.11 = (bf16[1,32,4096]{2,1,0:T(8,128)(2,1)S(1)}, bf16[1,32,4096]{2,1,0:T(8,128)(2,1)S(1)}, u32[]{:S(2)}, u32[]{:S(2)}) collective-permute-start(bf16[1,32,4096]{2,1,0:T(8,128)(2,1)S(1)} %copy-done.7), channel_id=1, source_target_pairs={{0,2},{1,3},{2,0},{3,1},{4,6},{5,7},{6,4},{7,5},{8,10},{9,11},{10,... | collective-permute-start | bytes 786440 | tf_op jit(solution)/shard_map/ppermute | solution.py:430
  52.6 2.3 %collective-permute-start.12 = (bf16[1,32,4096]{2,1,0:T(8,128)(2,1)S(1)}, bf16[1,32,4096]{2,1,0:T(8,128)(2,1)S(1)}, u32[]{:S(2)}, u32[]{:S(2)}) collective-permute-start(bf16[1,32,4096]{2,1,0:T(8,128)(2,1)S(1)} %copy-done.7), channel_id=1, source_target_pairs={{0,3},{1,2},{2,1},{3,0},{4,7},{5,6},{6,5},{7,4},{8,11},{9,10},{10,... | collective-permute-start | bytes 786440 | tf_op jit(solution)/shard_map/ppermute | solution.py:431
  54.9 0.9 collective-permute-start.6
  55.8 3.1 %advance.1 = (f32[128,32,128]{2,1,0:T(8,128)}, bf16[128,32,128]{2,1,0:T(8,128)(2,1)S(1)}) custom-call(s32[1,128]{1,0:T(1,128)S(1)} %bitcast.26, f32[128,4,128]{2,1,0:T(4,128)S(1)} %copy-done.6, bf16[4,32,128]{2,1,0:T(8,128)(2,1)S(1)} %bitcast.25, f32[128,32,128]{2,1,0:T(8,128)S(1)} %bitcast.24), custom_call_target="tpu_custom_call" | custom-call | flops 1000000000 | bytes 5242880 | tf_op jit(solution)/shard_map/advance/pallas_call | solution.py:65
  59.0 8.4 %collective-permute-done.6.r3 = bf16[288,128]{1,0:T(8,128)(2,1)S(1)} collective-permute-done((bf16[288,128]{1,0:T(8,128)(2,1)S(1)}, bf16[288,128]{1,0:T(8,128)(2,1)S(1)}, u32[]{:S(2)}, u32[]{:S(2)}) %collective-permute-start.6) | collective-permute-done | bytes 73760 | tf_op jit(solution)/shard_map/ppermute | solution.py:431
  67.4 1.0 %shard_map.144 = (bf16[48,128]{1,0:T(8,128)(2,1)S(1)}, bf16[48,128]{1,0:T(8,128)(2,1)S(1)}, bf16[48,128]{1,0:T(8,128)(2,1)S(1)}, bf16[48,128]{1,0:T(8,128)(2,1)S(1)}) custom-call(bf16[288,128]{1,0:T(8,128)(2,1)S(1)} %get-tuple-element.16.r0, bf16[288,128]{1,0:T(8,128)(2,1)S(1)} %collective-permute-done.4.r1, bf16[288,128]{1,0:T(8,128)(2,1)S(1)} %collective-permute-done.5.r2, ...), custom_call_target="tpu_custom_call" | custom-call | flops 1000000000 | bytes 2097152 | tf_op jit(solution)/shard_map/pallas_call | solution.py:327
  68.4 0.1 collective-permute-start.7
  68.5 3.5 %collective-permute-start.8 = (bf16[48,128]{1,0:T(8,128)(2,1)S(1)}, bf16[48,128]{1,0:T(8,128)(2,1)S(1)}, u32[]{:S(2)}, u32[]{:S(2)}) collective-permute-start(bf16[48,128]{1,0:T(8,128)(2,1)S(1)} %get-tuple-element.23), channel_id=1, source_target_pairs={{0,2},{1,3},{2,0},{3,1},{4,6},{5,7},{6,4},{7,5},{8,10},{9,11},{10,... | collective-permute-start | bytes 36872 | tf_op jit(solution)/shard_map/ppermute | solution.py:430
  72.0 1.2 %collective-permute-start.9 = (bf16[48,128]{1,0:T(8,128)(2,1)S(1)}, bf16[48,128]{1,0:T(8,128)(2,1)S(1)}, u32[]{:S(2)}, u32[]{:S(2)}) collective-permute-start(bf16[48,128]{1,0:T(8,128)(2,1)S(1)} %get-tuple-element.24), channel_id=1, source_target_pairs={{0,3},{1,2},{2,1},{3,0},{4,7},{5,6},{6,5},{7,4},{8,11},{9,10},{10,... | collective-permute-start | bytes 36872 | tf_op jit(solution)/shard_map/ppermute | solution.py:431
  73.2 0.5 shard_map.145.gates
  73.8 3.1 %collective-permute-done.9.p3 = bf16[48,128]{1,0:T(8,128)(2,1)S(1)} collective-permute-done((bf16[48,128]{1,0:T(8,128)(2,1)S(1)}, bf16[48,128]{1,0:T(8,128)(2,1)S(1)}, u32[]{:S(2)}, u32[]{:S(2)}) %collective-permute-start.9) | collective-permute-done | bytes 12320 | tf_op jit(solution)/shard_map/ppermute | solution.py:431
  76.9 0.1 collective-permute-start.13
  77.0 1.2 %collective-permute-done.13.other = bf16[128,128]{1,0:T(8,128)(2,1)S(1)} collective-permute-done((bf16[128,128]{1,0:T(8,128)(2,1)S(1)}, bf16[128,128]{1,0:T(8,128)(2,1)S(1)}, u32[]{:S(2)}, u32[]{:S(2)}) %collective-permute-start.13) | collective-permute-done | bytes 32800 | tf_op jit(solution)/shard_map/ppermute | solution.py:458
  78.2 0.4 shard_map.148
  78.7 18.0 %all_to_all.11 = bf16[64,32,128]{2,1,0:T(8,128)(2,1)S(1)} all-to-all(bf16[64,32,128]{2,1,0:T(8,128)(2,1)S(1)} %bitcast.17), channel_id=1, replica_groups=mesh['zy'=16,'core'=2,'tp'=4] {'zy','tp'}, dimensions={0} | all-to-all | bytes 1048576 | tf_op jit(solution)/shard_map/all_to_all | solution.py:459
  96.6 0.7 shard_map.149
  (35 shorter events, 0.1 us)
Async XLA Ops:
  27.2 6.8 %copy-start = (bf16[4096,128]{1,0:T(8,128)(2,1)S(1)}, bf16[4096,128]{1,0:T(8,128)(2,1)}, u32[]{:S(2)}) copy-start(bf16[4096,128]{1,0:T(8,128)(2,1)} %w_query.1) | copy-start | bytes 3145732
  27.2 6.8 %copy-start.1 = (bf16[4096,128]{1,0:T(8,128)(2,1)S(1)}, bf16[4096,128]{1,0:T(8,128)(2,1)}, u32[]{:S(2)}) copy-start(bf16[4096,128]{1,0:T(8,128)(2,1)} %w_forget.1) | copy-start | bytes 3145732
  27.2 6.8 %copy-start.2 = (f32[4096]{0:T(1024)S(1)}, f32[4096]{0:T(1024)}, u32[]{:S(2)}) copy-start(f32[4096]{0:T(1024)} %param.14) | copy-start | bytes 49156
  27.2 17.9 %collective-permute-start = (bf16[16,128,128]{2,1,0:T(8,128)(2,1)S(1)}, bf16[16,128,128]{2,1,0:T(8,128)(2,1)S(1)}, u32[]{:S(2)}, u32[]{:S(2)}) collective-permute-start(bf16[16,128,128]{2,1,0:T(8,128)(2,1)S(1)} %bitcast.19), channel_id=1, source_target_pairs={{0,4},{4,0},{1,5},{5,1},{2,6},{6,2},{3,7},{7,3},{8,12},{12,8},{9,1... | collective-permute-start | bytes 1572872 | tf_op jit(solution)/shard_map/ppermute | solution.py:439
  27.2 9.5 %collective-permute-start.1 = (bf16[1,32,4096]{2,1,0:T(8,128)(2,1)}, bf16[1,32,4096]{2,1,0:T(8,128)(2,1)S(1)}, u32[]{:S(2)}, u32[]{:S(2)}) collective-permute-start(bf16[1,32,4096]{2,1,0:T(8,128)(2,1)} %w0.2), channel_id=1, source_target_pairs={{0,1},{1,0},{2,3},{3,2},{4,5},{5,4},{6,7},{7,6},{8,9},{9,8},{10,11... | collective-permute-start | bytes 786440 | tf_op jit(solution)/shard_map/ppermute | solution.py:432
  27.9 14.3 %collective-permute-start.2 = (bf16[1,32,4096]{2,1,0:T(8,128)(2,1)}, bf16[1,32,4096]{2,1,0:T(8,128)(2,1)S(1)}, u32[]{:S(2)}, u32[]{:S(2)}) collective-permute-start(bf16[1,32,4096]{2,1,0:T(8,128)(2,1)} %w0.2), channel_id=1, source_target_pairs={{0,2},{1,3},{2,0},{3,1},{4,6},{5,7},{6,4},{7,5},{8,10},{9,11},{10,... | collective-permute-start | bytes 786440 | tf_op jit(solution)/shard_map/ppermute | solution.py:430
  29.7 15.1 %collective-permute-start.3 = (bf16[1,32,4096]{2,1,0:T(8,128)(2,1)}, bf16[1,32,4096]{2,1,0:T(8,128)(2,1)S(1)}, u32[]{:S(2)}, u32[]{:S(2)}) collective-permute-start(bf16[1,32,4096]{2,1,0:T(8,128)(2,1)} %w0.2), channel_id=1, source_target_pairs={{0,3},{1,2},{2,1},{3,0},{4,7},{5,6},{6,5},{7,4},{8,11},{9,10},{10,... | collective-permute-start | bytes 786440 | tf_op jit(solution)/shard_map/ppermute | solution.py:431
  32.0 1.2 %copy-start.4 = (bf16[128,4096]{1,0:T(8,128)(2,1)S(1)}, bf16[128,4096]{1,0:T(8,128)(2,1)}, u32[]{:S(2)}) copy-start(bf16[128,4096]{1,0:T(8,128)(2,1)} %w_out.1) | copy-start | bytes 3145732
  33.9 43.1 %collective-permute-start.14 = (bf16[16,128,128]{2,1,0:T(8,128)(2,1)S(1)}, bf16[16,128,128]{2,1,0:T(8,128)(2,1)S(1)}, u32[]{:S(2)}, u32[]{:S(2)}) collective-permute-start(bf16[16,128,128]{2,1,0:T(8,128)(2,1)S(1)} %get-tuple-element.28), channel_id=1, source_target_pairs={{0,4},{4,0},{1,5},{5,1},{2,6},{6,2},{3,7},{7,3},{8,12},{12,8},{9,1... | collective-permute-start | bytes 1572872 | tf_op jit(solution)/shard_map/ppermute | solution.py:453
  34.0 10.7 %copy-start.5 = (bf16[1,32,4096]{2,1,0:T(8,128)(2,1)S(1)}, bf16[1,32,4096]{2,1,0:T(8,128)(2,1)}, u32[]{:S(2)}) copy-start(bf16[1,32,4096]{2,1,0:T(8,128)(2,1)} %w0.2) | copy-start | bytes 786436
  45.1 5.1 %copy-start.7 = (bf16[1,32,4096]{2,1,0:T(8,128)(2,1)S(1)}, bf16[1,32,4096]{2,1,0:T(8,128)(2,1)}, u32[]{:S(2)}) copy-start(bf16[1,32,4096]{2,1,0:T(8,128)(2,1)} %w0.3) | copy-start | bytes 786436
  45.1 10.7 %copy-start.3 = (f32[128,1,32,128]{3,2,1,0:T(8,128)S(1)}, f32[128,1,32,128]{3,2,1,0:T(8,128)}, u32[]{:S(2)}) copy-start(f32[128,1,32,128]{3,2,1,0:T(8,128)} %param.22) | copy-start | bytes 6291460
  45.1 10.7 %copy-start.6 = (f32[128,4,128]{2,1,0:T(4,128)S(1)}, f32[128,4,128]{2,1,0:T(4,128)}, u32[]{:S(2)}) copy-start(f32[128,4,128]{2,1,0:T(4,128)} %prev_forget.1) | copy-start | bytes 786436
  45.1 10.7 %copy-start.8 = (bf16[128,4,1,32]{0,3,2,1:T(8,128)(2,1)S(1)}, bf16[128,4,1,32]{0,3,2,1:T(8,128)(2,1)}, u32[]{:S(2)}) copy-start(bf16[128,4,1,32]{0,3,2,1:T(8,128)(2,1)} %param.24) | copy-start | bytes 98308
  45.1 10.7 %copy-start.9 = (s32[128]{0:T(128)S(1)}, s32[128]{0:T(128)}, u32[]{:S(2)}) copy-start(s32[128]{0:T(128)} %param.25) | copy-start | bytes 1540
  46.3 21.1 %copy-start.10 = (f32[128]{0:T(128)S(1)}, f32[128]{0:T(128)}, u32[]{:S(2)}) copy-start(f32[128]{0:T(128)} %param.19) | copy-start | bytes 1540
  46.3 21.1 %copy-start.11 = (f32[32]{0:T(128)S(1)}, f32[32]{0:T(128)}, u32[]{:S(2)}) copy-start(f32[32]{0:T(128)} %param.20) | copy-start | bytes 388
  46.3 6.2 %collective-permute-start.4 = (bf16[288,128]{1,0:T(8,128)(2,1)S(1)}, bf16[288,128]{1,0:T(8,128)(2,1)S(1)}, u32[]{:S(2)}, u32[]{:S(2)}) collective-permute-start(bf16[288,128]{1,0:T(8,128)(2,1)S(1)} %get-tuple-element.17), channel_id=1, source_target_pairs={{0,1},{1,0},{2,3},{3,2},{4,5},{5,4},{6,7},{7,6},{8,9},{9,8},{10,11... | collective-permute-start | bytes 221192 | tf_op jit(solution)/shard_map/ppermute | solution.py:432
  46.4 8.5 %collective-permute-start.5 = (bf16[288,128]{1,0:T(8,128)(2,1)S(1)}, bf16[288,128]{1,0:T(8,128)(2,1)S(1)}, u32[]{:S(2)}, u32[]{:S(2)}) collective-permute-start(bf16[288,128]{1,0:T(8,128)(2,1)S(1)} %get-tuple-element.18), channel_id=1, source_target_pairs={{0,2},{1,3},{2,0},{3,1},{4,6},{5,7},{6,4},{7,5},{8,10},{9,11},{10,... | collective-permute-start | bytes 221192 | tf_op jit(solution)/shard_map/ppermute | solution.py:430
  50.2 18.3 %collective-permute-start.10 = (bf16[1,32,4096]{2,1,0:T(8,128)(2,1)S(1)}, bf16[1,32,4096]{2,1,0:T(8,128)(2,1)S(1)}, u32[]{:S(2)}, u32[]{:S(2)}) collective-permute-start(bf16[1,32,4096]{2,1,0:T(8,128)(2,1)S(1)} %copy-done.7), channel_id=1, source_target_pairs={{0,1},{1,0},{2,3},{3,2},{4,5},{5,4},{6,7},{7,6},{8,9},{9,8},{10,11... | collective-permute-start | bytes 786440 | tf_op jit(solution)/shard_map/ppermute | solution.py:432
  50.2 21.8 %collective-permute-start.11 = (bf16[1,32,4096]{2,1,0:T(8,128)(2,1)S(1)}, bf16[1,32,4096]{2,1,0:T(8,128)(2,1)S(1)}, u32[]{:S(2)}, u32[]{:S(2)}) collective-permute-start(bf16[1,32,4096]{2,1,0:T(8,128)(2,1)S(1)} %copy-done.7), channel_id=1, source_target_pairs={{0,2},{1,3},{2,0},{3,1},{4,6},{5,7},{6,4},{7,5},{8,10},{9,11},{10,... | collective-permute-start | bytes 786440 | tf_op jit(solution)/shard_map/ppermute | solution.py:430
  52.6 20.6 %collective-permute-start.12 = (bf16[1,32,4096]{2,1,0:T(8,128)(2,1)S(1)}, bf16[1,32,4096]{2,1,0:T(8,128)(2,1)S(1)}, u32[]{:S(2)}, u32[]{:S(2)}) collective-permute-start(bf16[1,32,4096]{2,1,0:T(8,128)(2,1)S(1)} %copy-done.7), channel_id=1, source_target_pairs={{0,3},{1,2},{2,1},{3,0},{4,7},{5,6},{6,5},{7,4},{8,11},{9,10},{10,... | collective-permute-start | bytes 786440 | tf_op jit(solution)/shard_map/ppermute | solution.py:431
  54.9 12.5 %collective-permute-start.6 = (bf16[288,128]{1,0:T(8,128)(2,1)S(1)}, bf16[288,128]{1,0:T(8,128)(2,1)S(1)}, u32[]{:S(2)}, u32[]{:S(2)}) collective-permute-start(bf16[288,128]{1,0:T(8,128)(2,1)S(1)} %get-tuple-element.19), channel_id=1, source_target_pairs={{0,3},{1,2},{2,1},{3,0},{4,7},{5,6},{6,5},{7,4},{8,11},{9,10},{10,... | collective-permute-start | bytes 221192 | tf_op jit(solution)/shard_map/ppermute | solution.py:431
  68.4 5.3 %collective-permute-start.7 = (bf16[48,128]{1,0:T(8,128)(2,1)S(1)}, bf16[48,128]{1,0:T(8,128)(2,1)S(1)}, u32[]{:S(2)}, u32[]{:S(2)}) collective-permute-start(bf16[48,128]{1,0:T(8,128)(2,1)S(1)} %get-tuple-element.22), channel_id=1, source_target_pairs={{0,1},{1,0},{2,3},{3,2},{4,5},{5,4},{6,7},{7,6},{8,9},{9,8},{10,11... | collective-permute-start | bytes 36872 | tf_op jit(solution)/shard_map/ppermute | solution.py:432
  68.5 5.3 %collective-permute-start.8 = (bf16[48,128]{1,0:T(8,128)(2,1)S(1)}, bf16[48,128]{1,0:T(8,128)(2,1)S(1)}, u32[]{:S(2)}, u32[]{:S(2)}) collective-permute-start(bf16[48,128]{1,0:T(8,128)(2,1)S(1)} %get-tuple-element.23), channel_id=1, source_target_pairs={{0,2},{1,3},{2,0},{3,1},{4,6},{5,7},{6,4},{7,5},{8,10},{9,11},{10,... | collective-permute-start | bytes 36872 | tf_op jit(solution)/shard_map/ppermute | solution.py:430
  72.0 4.9 %collective-permute-start.9 = (bf16[48,128]{1,0:T(8,128)(2,1)S(1)}, bf16[48,128]{1,0:T(8,128)(2,1)S(1)}, u32[]{:S(2)}, u32[]{:S(2)}) collective-permute-start(bf16[48,128]{1,0:T(8,128)(2,1)S(1)} %get-tuple-element.24), channel_id=1, source_target_pairs={{0,3},{1,2},{2,1},{3,0},{4,7},{5,6},{6,5},{7,4},{8,11},{9,10},{10,... | collective-permute-start | bytes 36872 | tf_op jit(solution)/shard_map/ppermute | solution.py:431
  76.9 1.3 %collective-permute-start.13 = (bf16[128,128]{1,0:T(8,128)(2,1)S(1)}, bf16[128,128]{1,0:T(8,128)(2,1)S(1)}, u32[]{:S(2)}, u32[]{:S(2)}) collective-permute-start(bf16[128,128]{1,0:T(8,128)(2,1)S(1)} %shard_map.146.hidden), channel_id=1, source_target_pairs={{0,4},{4,0},{1,5},{5,1},{2,6},{6,2},{3,7},{7,3},{8,12},{12,8},{9,1... | collective-permute-start | bytes 98312 | tf_op jit(solution)/shard_map/ppermute | solution.py:458

commit v11 on v10

--- a/solution.py
+++ b/solution.py
@@ -29,7 +29,7 @@
     )
 
 
-def advance_kernel(accepted, prev_forget, prev_input, state, new_state, rounded, live):
+def advance_kernel(accepted, prev_forget, prev_input, state, new_state, live):
     block = pl.program_id(0)
     count, proposals, size = prev_forget.shape
     lanes = prev_input.shape[2]
@@ -54,13 +54,12 @@
         for p in range(proposals):
             fresh = fresh + terms[p][s : s + 1] * values[p][:, s : s + 1]
         new_state[s] = fresh
-        rounded[s] = fresh.astype(jnp.bfloat16)
 
 
 def advance(accepted, prev_forget, prev_input, state):
     seqs, values, keys = state.shape
     proposals = prev_forget.shape[1]
-    count = 32
+    count = 16
     span = pl.BlockSpec((count, values, keys), lambda i: (i, 0, 0))
     return pl.pallas_call(
         advance_kernel,
@@ -71,14 +70,14 @@
             pl.BlockSpec((proposals, values, seqs), lambda i: (0, 0, 0)),
             span,
         ],
-        out_specs=[span, span],
-        out_shape=[shaped(state.shape, jnp.float32), shaped(state.shape, jnp.bfloat16)],
+        out_specs=span,
+        out_shape=shaped(state.shape, jnp.float32),
         scratch_shapes=[pltpu.VMEM((keys, seqs), jnp.float32)],
         name="advance",
         cost_estimate=pl.CostEstimate(
             flops=1_000_000_000, bytes_accessed=5 << 20, transcendentals=0
         ),
-        compiler_params=pltpu.CompilerParams(vmem_limit_bytes=16 << 20),
+        compiler_params=pltpu.CompilerParams(vmem_limit_bytes=60 << 20),
     )(accepted[None], prev_forget, prev_input, state)
 
 
@@ -301,7 +300,7 @@
         for b in range(half // group):
             first = h * half + b * group
             read = jnp.dot(
-                before[pl.ds(first * values, group * values), :],
+                before[pl.ds(first * values, group * values), :].astype(jnp.bfloat16),
                 wanted,
                 preferred_element_type=jnp.float32,
             )
@@ -437,10 +436,13 @@
     own = lax.all_to_all(source(tokens.transpose(1, 2, 0), planes), ("zy", "tp"), 0, 0, tiled=True)
     own = own.reshape(planes, group * features, seqs)
     other = lax.ppermute(own, "core", swap)
-    gates = passed([w_gate] * group)
+    wrap = lax.ppermute(w_gate, "tp", hops[3])
+    far = lax.ppermute(w_gate, "tp", hops[2])
+    near = lax.ppermute(w_gate, "tp", hops[1])
+    gates = [w_gate, near, far, wrap]
     keyed = turn(gain, w_query, w_forget)
     mixing = fold(gain, inputs)
-    new_state, rounded = advance(
+    new_state = advance(
         accepted,
         prev_forget,
         prev_input.reshape(seqs, proposals, -1).transpose(1, 2, 0),
@@ -451,7 +453,7 @@
     received = passed(sends)
     ours, theirs = turn_outward(w_out)
     theirs = lax.ppermute(theirs, "core", swap)
-    shown = recur(received, rounded.reshape(-1, size), forget_floor[None], head_gain[None])
+    shown = recur(received, new_state.reshape(-1, size), forget_floor[None], head_gain[None])
     parts = passed(shown)
     opened = gate(gain, gates, rows, scale)
     hidden = hide(parts, opened)

time: 97.7 us -> 101 us (1.034)
  Pallas kernels: 10.3 us -> 14.1 us
  waiting for transfers between devices: 22.8 us -> 21 us
  local copies, waits for them, and re-layouts: 1.29 us -> 2.84 us
    ppermute x4 -> x3, waiting for transfers between devices: 14.1 us -> 5.69 us  [passed(): wrap = lax.ppermute(parts[3], 'tp', hops[3])]
    ppermute x4 -> x3, waiting for transfers between devices: 5.54 us -> 12.2 us  [passed(): far = lax.ppermute(parts[2], 'tp', hops[2])]
    ppermute x0 -> x3, starting transfers between devices: none -> 6 us  [the longest x1 2.35 us: body(): wrap = lax.ppermute(w_gate, 'tp', hops[3])]
    ppermute x4 -> x3, starting transfers between devices: 11.4 us -> 7.47 us  [passed(): far = lax.ppermute(parts[2], 'tp', hops[2])]
    pallas_call x1, Pallas kernels: 3.12 us -> 6.91 us  [advance(): pl.pallas_call(advance_kernel, grid=(seqs // count,), in_specs=[pl.BlockS...]
    ppermute x4 -> x3, starting transfers between devices: 6.8 us -> 4.11 us  [passed(): wrap = lax.ppermute(parts[3], 'tp', hops[3])]
    unnamed x24 -> x18, local copies, waits for them, and re-layouts: 1.29 us -> 2.84 us
  transfers between devices with their start and end apart: 15 -> 15, of which waited for: 6 -> 7; matrix products, arithmetic and copies ran while one was open for 0% -> 0% of each run, Pallas kernels for 8% -> 11%
where the time goes in v11:
time: 101 us; the launch traced here: 100 us
  blocking collectives  42.9 us (42%)
  waiting for transfers between devices  21 us (21%)
  starting transfers between devices  18.6 us (18%)
  Pallas kernels  14.1 us (14%)
  local copies, waits for them, and re-layouts  2.84 us (3%)
    all_to_all x1, blocking collectives, body(): lax.all_to_all(source(tokens.transpose(1, 2, 0), planes), ('zy', 'tp'), 0...  24.9 us
    all_to_all x1, blocking collectives, body(): lax.all_to_all(kept.reshape(planes * group, features, seqs), ('zy', 'tp')...  18 us
    ppermute x3, waiting for transfers between devices, passed(): far = lax.ppermute(parts[2], 'tp', hops[2])  12.2 us
    ppermute x3, starting transfers between devices, passed(): far = lax.ppermute(parts[2], 'tp', hops[2])  7.47 us
    pallas_call x1, Pallas kernels, advance(): pl.pallas_call(advance_kernel, grid=(seqs // count,), in_specs=[pl.BlockS...  6.91 us
    ppermute x3, waiting for transfers between devices, passed(): wrap = lax.ppermute(parts[3], 'tp', hops[3])  5.69 us
    ppermute x3, starting transfers between devices, passed(): wrap = lax.ppermute(parts[3], 'tp', hops[3])  4.11 us
    unnamed x18, local copies, waits for them, and re-layouts  2.84 us
  transfers between devices with their start and end apart: 15, of which 7 were waited for; matrix products, arithmetic and copies ran while one was open for 0% of the time, Pallas kernels for 11%

profile of v11, /device:TPU:0, one launch (start us, length us, event | category | flops | bytes accessed | tf_op | source)
XLA Modules:
  0.0 100.2 jit_solution(15870761162287436963)
XLA Ops:
  0.6 1.7 %shard_map.140 = bf16[64,32,128]{2,1,0:T(8,128)(2,1)} custom-call(bf16[4,32,128]{2,1,0:T(8,128)(2,1)} %bitcast.30), custom_call_target="tpu_custom_call" | custom-call | flops 1000000 | bytes 1048576 | tf_op jit(solution)/shard_map/pallas_call | solution.py:114
  2.3 24.9 %all_to_all.10 = bf16[64,32,128]{2,1,0:T(8,128)(2,1)S(1)} all-to-all(bf16[64,32,128]{2,1,0:T(8,128)(2,1)} %shard_map.140), channel_id=1, replica_groups=mesh['zy'=16,'core'=2,'tp'=4] {'zy','tp'}, dimensions={0} | all-to-all | bytes 1048576 | tf_op jit(solution)/shard_map/all_to_all | solution.py:436
  27.2 0.6 collective-permute-start.1
  27.9 1.8 %collective-permute-start.2 = (bf16[1,32,4096]{2,1,0:T(8,128)(2,1)}, bf16[1,32,4096]{2,1,0:T(8,128)(2,1)S(1)}, u32[]{:S(2)}, u32[]{:S(2)}) collective-permute-start(bf16[1,32,4096]{2,1,0:T(8,128)(2,1)} %w0.2), channel_id=1, source_target_pairs={{0,2},{1,3},{2,0},{3,1},{4,6},{5,7},{6,4},{7,5},{8,10},{9,11},{10,... | collective-permute-start | bytes 786440 | tf_op jit(solution)/shard_map/ppermute | solution.py:429
  29.7 2.3 %collective-permute-start.3 = (bf16[1,32,4096]{2,1,0:T(8,128)(2,1)}, bf16[1,32,4096]{2,1,0:T(8,128)(2,1)S(1)}, u32[]{:S(2)}, u32[]{:S(2)}) collective-permute-start(bf16[1,32,4096]{2,1,0:T(8,128)(2,1)} %w0.2), channel_id=1, source_target_pairs={{0,3},{1,2},{2,1},{3,0},{4,7},{5,6},{6,5},{7,4},{8,11},{9,10},{10,... | collective-permute-start | bytes 786440 | tf_op jit(solution)/shard_map/ppermute | solution.py:430
  32.0 1.2 %copy-done.4 = bf16[128,4096]{1,0:T(8,128)(2,1)S(1)} copy-done((bf16[128,4096]{1,0:T(8,128)(2,1)S(1)}, bf16[128,4096]{1,0:T(8,128)(2,1)}, u32[]{:S(2)}) %copy-start.4) | copy-done | bytes 1048600
  33.2 0.7 shard_map.147
  33.9 0.1 collective-permute-start.14
  34.1 0.7 shard_map.141.keyed
  34.7 2.0 %collective-permute-done.1.w1 = bf16[1,32,4096]{2,1,0:T(8,128)(2,1)S(1)} collective-permute-done((bf16[1,32,4096]{2,1,0:T(8,128)(2,1)}, bf16[1,32,4096]{2,1,0:T(8,128)(2,1)S(1)}, u32[]{:S(2)}, u32[]{:S(2)}) %collective-permute-start.1) | collective-permute-done | bytes 262176 | tf_op jit(solution)/shard_map/ppermute | solution.py:431
  36.7 5.5 %collective-permute-done.2.w2 = bf16[1,32,4096]{2,1,0:T(8,128)(2,1)S(1)} collective-permute-done((bf16[1,32,4096]{2,1,0:T(8,128)(2,1)}, bf16[1,32,4096]{2,1,0:T(8,128)(2,1)S(1)}, u32[]{:S(2)}, u32[]{:S(2)}) %collective-permute-start.2) | collective-permute-done | bytes 262176 | tf_op jit(solution)/shard_map/ppermute | solution.py:429
  42.2 2.6 %collective-permute-done.3.w3 = bf16[1,32,4096]{2,1,0:T(8,128)(2,1)S(1)} collective-permute-done((bf16[1,32,4096]{2,1,0:T(8,128)(2,1)}, bf16[1,32,4096]{2,1,0:T(8,128)(2,1)S(1)}, u32[]{:S(2)}, u32[]{:S(2)}) %collective-permute-start.3) | collective-permute-done | bytes 262176 | tf_op jit(solution)/shard_map/ppermute | solution.py:430
  44.8 0.3 shard_map.142.mixing
  45.1 1.1 %shard_map.143 = (bf16[288,128]{1,0:T(8,128)(2,1)S(1)}, bf16[288,128]{1,0:T(8,128)(2,1)S(1)}, bf16[288,128]{1,0:T(8,128)(2,1)S(1)}, bf16[288,128]{1,0:T(8,128)(2...) custom-call(bf16[16,128,128]{2,1,0:T(8,128)(2,1)S(1)} %bitcast.22, ...), custom_call_target="tpu_custom_call" | custom-call | flops 1000000000 | bytes 3145728 | tf_op jit(solution)/shard_map/pallas_call | solution.py:197
  46.4 2.0 %collective-permute-start.10 = (bf16[1,32,4096]{2,1,0:T(8,128)(2,1)S(1)}, bf16[1,32,4096]{2,1,0:T(8,128)(2,1)S(1)}, u32[]{:S(2)}, u32[]{:S(2)}) collective-permute-start(bf16[1,32,4096]{2,1,0:T(8,128)(2,1)S(1)} %copy-done.6), channel_id=1, source_target_pairs={{0,1},{1,0},{2,3},{3,2},{4,5},{5,4},{6,7},{7,6},{8,9},{9,8},{10,11... | collective-permute-start | bytes 786440 | tf_op jit(solution)/shard_map/ppermute | solution.py:441
  48.4 1.9 %collective-permute-start.5 = (bf16[288,128]{1,0:T(8,128)(2,1)S(1)}, bf16[288,128]{1,0:T(8,128)(2,1)S(1)}, u32[]{:S(2)}, u32[]{:S(2)}) collective-permute-start(bf16[288,128]{1,0:T(8,128)(2,1)S(1)} %get-tuple-element.16), channel_id=1, source_target_pairs={{0,2},{1,3},{2,0},{3,1},{4,6},{5,7},{6,4},{7,5},{8,10},{9,11},{10,... | collective-permute-start | bytes 221192 | tf_op jit(solution)/shard_map/ppermute | solution.py:429
  50.2 1.6 %collective-permute-start.11 = (bf16[1,32,4096]{2,1,0:T(8,128)(2,1)S(1)}, bf16[1,32,4096]{2,1,0:T(8,128)(2,1)S(1)}, u32[]{:S(2)}, u32[]{:S(2)}) collective-permute-start(bf16[1,32,4096]{2,1,0:T(8,128)(2,1)S(1)} %copy-done.6), channel_id=1, source_target_pairs={{0,2},{1,3},{2,0},{3,1},{4,6},{5,7},{6,4},{7,5},{8,10},{9,11},{10,... | collective-permute-start | bytes 786440 | tf_op jit(solution)/shard_map/ppermute | solution.py:440
  51.9 2.3 %collective-permute-start.12 = (bf16[1,32,4096]{2,1,0:T(8,128)(2,1)S(1)}, bf16[1,32,4096]{2,1,0:T(8,128)(2,1)S(1)}, u32[]{:S(2)}, u32[]{:S(2)}) collective-permute-start(bf16[1,32,4096]{2,1,0:T(8,128)(2,1)S(1)} %copy-done.6), channel_id=1, source_target_pairs={{0,3},{1,2},{2,1},{3,0},{4,7},{5,6},{6,5},{7,4},{8,11},{9,10},{10,... | collective-permute-start | bytes 786440 | tf_op jit(solution)/shard_map/ppermute | solution.py:439
  54.2 6.3 %collective-permute-done.5.r2 = bf16[288,128]{1,0:T(8,128)(2,1)S(1)} collective-permute-done((bf16[288,128]{1,0:T(8,128)(2,1)S(1)}, bf16[288,128]{1,0:T(8,128)(2,1)S(1)}, u32[]{:S(2)}, u32[]{:S(2)}) %collective-permute-start.5) | collective-permute-done | bytes 73760 | tf_op jit(solution)/shard_map/ppermute | solution.py:429
  60.6 0.9 collective-permute-start.6
  61.4 6.9 %advance.1 = f32[128,32,128]{2,1,0:T(8,128)} custom-call(s32[1,128]{1,0:T(1,128)} %bitcast.32, f32[128,4,128]{2,1,0:T(4,128)} %prev_forget.1, bf16[4,32,128]{2,1,0:T(8,128)(2,1)} %bitcast.29, f32[128,32,128]{2,1,0:T(8,128)} %bitcast.28), custom_call_target="tpu_custom_call" | custom-call | flops 1000000000 | bytes 5242880 | tf_op jit(solution)/shard_map/advance/pallas_call | solution.py:64
  68.4 1.6 %copy-done = f32[128,32,128]{2,1,0:T(8,128)S(1)} copy-done((f32[128,32,128]{2,1,0:T(8,128)S(1)}, f32[128,32,128]{2,1,0:T(8,128)}, u32[]{:S(2)}) %copy-start) | copy-done | bytes 2097176
  70.0 1.0 %shard_map.144 = (bf16[48,128]{1,0:T(8,128)(2,1)S(1)}, bf16[48,128]{1,0:T(8,128)(2,1)S(1)}, bf16[48,128]{1,0:T(8,128)(2,1)S(1)}, bf16[48,128]{1,0:T(8,128)(2,1)S(1)}) custom-call(bf16[288,128]{1,0:T(8,128)(2,1)S(1)} %get-tuple-element.14.r0, bf16[288,128]{1,0:T(8,128)(2,1)S(1)} %collective-permute-done.4.r1, bf16[288,128]{1,0:T(8,128)(2,1)S(1)} %collective-permute-done.5.r2, ...), custom_call_target="tpu_custom_call" | custom-call | flops 1000000000 | bytes 2097152 | tf_op jit(solution)/shard_map/pallas_call | solution.py:326
  71.1 3.8 %collective-permute-start.8 = (bf16[48,128]{1,0:T(8,128)(2,1)S(1)}, bf16[48,128]{1,0:T(8,128)(2,1)S(1)}, u32[]{:S(2)}, u32[]{:S(2)}) collective-permute-start(bf16[48,128]{1,0:T(8,128)(2,1)S(1)} %get-tuple-element.20), channel_id=1, source_target_pairs={{0,2},{1,3},{2,0},{3,1},{4,6},{5,7},{6,4},{7,5},{8,10},{9,11},{10,... | collective-permute-start | bytes 36872 | tf_op jit(solution)/shard_map/ppermute | solution.py:429
  74.9 0.9 collective-permute-start.9
  75.8 0.5 shard_map.145.gates
  76.4 0.3 collective-permute-done.8.p2
  76.7 3.1 %collective-permute-done.9.p3 = bf16[48,128]{1,0:T(8,128)(2,1)S(1)} collective-permute-done((bf16[48,128]{1,0:T(8,128)(2,1)S(1)}, bf16[48,128]{1,0:T(8,128)(2,1)S(1)}, u32[]{:S(2)}, u32[]{:S(2)}) %collective-permute-start.9) | collective-permute-done | bytes 12320 | tf_op jit(solution)/shard_map/ppermute | solution.py:430
  80.0 1.2 %collective-permute-done.13.other = bf16[128,128]{1,0:T(8,128)(2,1)S(1)} collective-permute-done((bf16[128,128]{1,0:T(8,128)(2,1)S(1)}, bf16[128,128]{1,0:T(8,128)(2,1)S(1)}, u32[]{:S(2)}, u32[]{:S(2)}) %collective-permute-start.13) | collective-permute-done | bytes 32800 | tf_op jit(solution)/shard_map/ppermute | solution.py:460
  81.1 0.4 shard_map.148
  81.6 18.0 %all_to_all.11 = bf16[64,32,128]{2,1,0:T(8,128)(2,1)S(1)} all-to-all(bf16[64,32,128]{2,1,0:T(8,128)(2,1)S(1)} %bitcast.19), channel_id=1, replica_groups=mesh['zy'=16,'core'=2,'tp'=4] {'zy','tp'}, dimensions={0} | all-to-all | bytes 1048576 | tf_op jit(solution)/shard_map/all_to_all | solution.py:461
  99.5 0.7 shard_map.149
  (29 shorter events, 0.3 us)
Async XLA Ops:
  27.2 6.8 %copy-start.1 = (bf16[4096,128]{1,0:T(8,128)(2,1)S(1)}, bf16[4096,128]{1,0:T(8,128)(2,1)}, u32[]{:S(2)}) copy-start(bf16[4096,128]{1,0:T(8,128)(2,1)} %w_query.1) | copy-start | bytes 3145732
  27.2 6.8 %copy-start.2 = (bf16[4096,128]{1,0:T(8,128)(2,1)S(1)}, bf16[4096,128]{1,0:T(8,128)(2,1)}, u32[]{:S(2)}) copy-start(bf16[4096,128]{1,0:T(8,128)(2,1)} %w_forget.1) | copy-start | bytes 3145732
  27.2 6.8 %copy-start.3 = (f32[4096]{0:T(1024)S(1)}, f32[4096]{0:T(1024)}, u32[]{:S(2)}) copy-start(f32[4096]{0:T(1024)} %param.14) | copy-start | bytes 49156
  27.2 17.9 %collective-permute-start = (bf16[16,128,128]{2,1,0:T(8,128)(2,1)S(1)}, bf16[16,128,128]{2,1,0:T(8,128)(2,1)S(1)}, u32[]{:S(2)}, u32[]{:S(2)}) collective-permute-start(bf16[16,128,128]{2,1,0:T(8,128)(2,1)S(1)} %bitcast.21), channel_id=1, source_target_pairs={{0,4},{4,0},{1,5},{5,1},{2,6},{6,2},{3,7},{7,3},{8,12},{12,8},{9,1... | collective-permute-start | bytes 1572872 | tf_op jit(solution)/shard_map/ppermute | solution.py:438
  27.2 9.5 %collective-permute-start.1 = (bf16[1,32,4096]{2,1,0:T(8,128)(2,1)}, bf16[1,32,4096]{2,1,0:T(8,128)(2,1)S(1)}, u32[]{:S(2)}, u32[]{:S(2)}) collective-permute-start(bf16[1,32,4096]{2,1,0:T(8,128)(2,1)} %w0.2), channel_id=1, source_target_pairs={{0,1},{1,0},{2,3},{3,2},{4,5},{5,4},{6,7},{7,6},{8,9},{9,8},{10,11... | collective-permute-start | bytes 786440 | tf_op jit(solution)/shard_map/ppermute | solution.py:431
  27.9 14.3 %collective-permute-start.2 = (bf16[1,32,4096]{2,1,0:T(8,128)(2,1)}, bf16[1,32,4096]{2,1,0:T(8,128)(2,1)S(1)}, u32[]{:S(2)}, u32[]{:S(2)}) collective-permute-start(bf16[1,32,4096]{2,1,0:T(8,128)(2,1)} %w0.2), channel_id=1, source_target_pairs={{0,2},{1,3},{2,0},{3,1},{4,6},{5,7},{6,4},{7,5},{8,10},{9,11},{10,... | collective-permute-start | bytes 786440 | tf_op jit(solution)/shard_map/ppermute | solution.py:429
  29.7 15.1 %collective-permute-start.3 = (bf16[1,32,4096]{2,1,0:T(8,128)(2,1)}, bf16[1,32,4096]{2,1,0:T(8,128)(2,1)S(1)}, u32[]{:S(2)}, u32[]{:S(2)}) collective-permute-start(bf16[1,32,4096]{2,1,0:T(8,128)(2,1)} %w0.2), channel_id=1, source_target_pairs={{0,3},{1,2},{2,1},{3,0},{4,7},{5,6},{6,5},{7,4},{8,11},{9,10},{10,... | collective-permute-start | bytes 786440 | tf_op jit(solution)/shard_map/ppermute | solution.py:430
  32.0 1.2 %copy-start.4 = (bf16[128,4096]{1,0:T(8,128)(2,1)S(1)}, bf16[128,4096]{1,0:T(8,128)(2,1)}, u32[]{:S(2)}) copy-start(bf16[128,4096]{1,0:T(8,128)(2,1)} %w_out.1) | copy-start | bytes 3145732
  33.9 46.0 %collective-permute-start.14 = (bf16[16,128,128]{2,1,0:T(8,128)(2,1)S(1)}, bf16[16,128,128]{2,1,0:T(8,128)(2,1)S(1)}, u32[]{:S(2)}, u32[]{:S(2)}) collective-permute-start(bf16[16,128,128]{2,1,0:T(8,128)(2,1)S(1)} %get-tuple-element.25), channel_id=1, source_target_pairs={{0,4},{4,0},{1,5},{5,1},{2,6},{6,2},{3,7},{7,3},{8,12},{12,8},{9,1... | collective-permute-start | bytes 1572872 | tf_op jit(solution)/shard_map/ppermute | solution.py:455
  34.0 10.7 %copy-start.5 = (bf16[1,32,4096]{2,1,0:T(8,128)(2,1)S(1)}, bf16[1,32,4096]{2,1,0:T(8,128)(2,1)}, u32[]{:S(2)}) copy-start(bf16[1,32,4096]{2,1,0:T(8,128)(2,1)} %w0.2) | copy-start | bytes 786436
  45.1 1.3 %copy-start.6 = (bf16[1,32,4096]{2,1,0:T(8,128)(2,1)S(1)}, bf16[1,32,4096]{2,1,0:T(8,128)(2,1)}, u32[]{:S(2)}) copy-start(bf16[1,32,4096]{2,1,0:T(8,128)(2,1)} %w0.3) | copy-start | bytes 786436
  46.2 5.6 %collective-permute-start.4 = (bf16[288,128]{1,0:T(8,128)(2,1)S(1)}, bf16[288,128]{1,0:T(8,128)(2,1)S(1)}, u32[]{:S(2)}, u32[]{:S(2)}) collective-permute-start(bf16[288,128]{1,0:T(8,128)(2,1)S(1)} %get-tuple-element.15), channel_id=1, source_target_pairs={{0,1},{1,0},{2,3},{3,2},{4,5},{5,4},{6,7},{7,6},{8,9},{9,8},{10,11... | collective-permute-start | bytes 221192 | tf_op jit(solution)/shard_map/ppermute | solution.py:431
  46.4 24.8 %collective-permute-start.10 = (bf16[1,32,4096]{2,1,0:T(8,128)(2,1)S(1)}, bf16[1,32,4096]{2,1,0:T(8,128)(2,1)S(1)}, u32[]{:S(2)}, u32[]{:S(2)}) collective-permute-start(bf16[1,32,4096]{2,1,0:T(8,128)(2,1)S(1)} %copy-done.6), channel_id=1, source_target_pairs={{0,1},{1,0},{2,3},{3,2},{4,5},{5,4},{6,7},{7,6},{8,9},{9,8},{10,11... | collective-permute-start | bytes 786440 | tf_op jit(solution)/shard_map/ppermute | solution.py:441
  48.4 12.2 %collective-permute-start.5 = (bf16[288,128]{1,0:T(8,128)(2,1)S(1)}, bf16[288,128]{1,0:T(8,128)(2,1)S(1)}, u32[]{:S(2)}, u32[]{:S(2)}) collective-permute-start(bf16[288,128]{1,0:T(8,128)(2,1)S(1)} %get-tuple-element.16), channel_id=1, source_target_pairs={{0,2},{1,3},{2,0},{3,1},{4,6},{5,7},{6,4},{7,5},{8,10},{9,11},{10,... | collective-permute-start | bytes 221192 | tf_op jit(solution)/shard_map/ppermute | solution.py:429
  50.2 24.7 %collective-permute-start.11 = (bf16[1,32,4096]{2,1,0:T(8,128)(2,1)S(1)}, bf16[1,32,4096]{2,1,0:T(8,128)(2,1)S(1)}, u32[]{:S(2)}, u32[]{:S(2)}) collective-permute-start(bf16[1,32,4096]{2,1,0:T(8,128)(2,1)S(1)} %copy-done.6), channel_id=1, source_target_pairs={{0,2},{1,3},{2,0},{3,1},{4,6},{5,7},{6,4},{7,5},{8,10},{9,11},{10,... | collective-permute-start | bytes 786440 | tf_op jit(solution)/shard_map/ppermute | solution.py:440
  51.9 23.9 %collective-permute-start.12 = (bf16[1,32,4096]{2,1,0:T(8,128)(2,1)S(1)}, bf16[1,32,4096]{2,1,0:T(8,128)(2,1)S(1)}, u32[]{:S(2)}, u32[]{:S(2)}) collective-permute-start(bf16[1,32,4096]{2,1,0:T(8,128)(2,1)S(1)} %copy-done.6), channel_id=1, source_target_pairs={{0,3},{1,2},{2,1},{3,0},{4,7},{5,6},{6,5},{7,4},{8,11},{9,10},{10,... | collective-permute-start | bytes 786440 | tf_op jit(solution)/shard_map/ppermute | solution.py:439
  60.6 7.8 %collective-permute-start.6 = (bf16[288,128]{1,0:T(8,128)(2,1)S(1)}, bf16[288,128]{1,0:T(8,128)(2,1)S(1)}, u32[]{:S(2)}, u32[]{:S(2)}) collective-permute-start(bf16[288,128]{1,0:T(8,128)(2,1)S(1)} %get-tuple-element.17), channel_id=1, source_target_pairs={{0,3},{1,2},{2,1},{3,0},{4,7},{5,6},{6,5},{7,4},{8,11},{9,10},{10,... | collective-permute-start | bytes 221192 | tf_op jit(solution)/shard_map/ppermute | solution.py:430
  61.4 6.9 %copy-start.7 = (f32[128]{0:T(128)S(1)}, f32[128]{0:T(128)}, u32[]{:S(2)}) copy-start(f32[128]{0:T(128)} %param.19) | copy-start | bytes 1540
  61.4 6.9 %copy-start.8 = (f32[32]{0:T(128)S(1)}, f32[32]{0:T(128)}, u32[]{:S(2)}) copy-start(f32[32]{0:T(128)} %param.20) | copy-start | bytes 388
  68.4 1.6 %copy-start = (f32[128,32,128]{2,1,0:T(8,128)S(1)}, f32[128,32,128]{2,1,0:T(8,128)}, u32[]{:S(2)}) copy-start(f32[128,32,128]{2,1,0:T(8,128)} %advance.1) | copy-start | bytes 6291460
  71.0 5.3 %collective-permute-start.7 = (bf16[48,128]{1,0:T(8,128)(2,1)S(1)}, bf16[48,128]{1,0:T(8,128)(2,1)S(1)}, u32[]{:S(2)}, u32[]{:S(2)}) collective-permute-start(bf16[48,128]{1,0:T(8,128)(2,1)S(1)} %get-tuple-element.19), channel_id=1, source_target_pairs={{0,1},{1,0},{2,3},{3,2},{4,5},{5,4},{6,7},{7,6},{8,9},{9,8},{10,11... | collective-permute-start | bytes 36872 | tf_op jit(solution)/shard_map/ppermute | solution.py:431
  71.1 5.6 %collective-permute-start.8 = (bf16[48,128]{1,0:T(8,128)(2,1)S(1)}, bf16[48,128]{1,0:T(8,128)(2,1)S(1)}, u32[]{:S(2)}, u32[]{:S(2)}) collective-permute-start(bf16[48,128]{1,0:T(8,128)(2,1)S(1)} %get-tuple-element.20), channel_id=1, source_target_pairs={{0,2},{1,3},{2,0},{3,1},{4,6},{5,7},{6,4},{7,5},{8,10},{9,11},{10,... | collective-permute-start | bytes 36872 | tf_op jit(solution)/shard_map/ppermute | solution.py:429
  74.9 4.9 %collective-permute-start.9 = (bf16[48,128]{1,0:T(8,128)(2,1)S(1)}, bf16[48,128]{1,0:T(8,128)(2,1)S(1)}, u32[]{:S(2)}, u32[]{:S(2)}) collective-permute-start(bf16[48,128]{1,0:T(8,128)(2,1)S(1)} %get-tuple-element.21), channel_id=1, source_target_pairs={{0,3},{1,2},{2,1},{3,0},{4,7},{5,6},{6,5},{7,4},{8,11},{9,10},{10,... | collective-permute-start | bytes 36872 | tf_op jit(solution)/shard_map/ppermute | solution.py:430
  79.9 1.3 %collective-permute-start.13 = (bf16[128,128]{1,0:T(8,128)(2,1)S(1)}, bf16[128,128]{1,0:T(8,128)(2,1)S(1)}, u32[]{:S(2)}, u32[]{:S(2)}) collective-permute-start(bf16[128,128]{1,0:T(8,128)(2,1)S(1)} %shard_map.146.hidden), channel_id=1, source_target_pairs={{0,4},{4,0},{1,5},{5,1},{2,6},{6,2},{3,7},{7,3},{8,12},{12,8},{9,1... | collective-permute-start | bytes 98312 | tf_op jit(solution)/shard_map/ppermute | solution.py:460
